TPU v7x, 512 devices: a whole 4x4x16 slice. The times are simulated.
512 devices in a mesh: sp: 64 (over z, y), tp: 8 (over x, core).
Axes of the slice: x: 4, y: 4, z: 16, core: 2. Of those that a mesh axis runs over, the one named last changes fastest.
Arguments:
- tokens: bfloat16 [49152, 2048], P(('sp', 'tp')), may hold values from -6 to 6
- input_gain: float32 [2048], replicated, may hold values from 0.1 to 1.9
- branch_value: bfloat16 [2048, 1024], P('sp', 'tp'), may hold values from -0.125 to 0.125
- branch_gate: bfloat16 [2048, 1024], P('sp', 'tp'), may hold values from -0.125 to 0.125
- query_weight: bfloat16 [2048, 1024], P('sp', 'tp'), may hold values from -0.125 to 0.125
- key_weight: bfloat16 [2048, 1024], P('sp', 'tp'), may hold values from -0.125 to 0.125
- value_weight: bfloat16 [2048, 1024], P('sp', 'tp'), may hold values from -0.125 to 0.125
- swish_weight: bfloat16 [2048, 1024], P('sp', 'tp'), may hold values from -0.125 to 0.125
- kernel_taps: float32 [31, 1024], P(None, 'tp'), may hold values from -8 to 8
- channel_gain: float32 [1024], P('tp'), may hold values from 0.1 to 1.9
- decay_logs: float32 [16, 49152], P('tp', 'sp'), may hold values from -1.5 to 0
- start_state: float32 [2, 16, 64, 64], P(None, 'tp')
- head_gain: float32 [1024], P('tp'), may hold values from 0.1 to 1.9
- output_conv: bfloat16 [1024, 2048], P('tp', 'sp'), may hold values from -0.125 to 0.125
- output_heads: bfloat16 [1024, 2048], P('tp', 'sp'), may hold values from -0.125 to 0.125
Outputs:
- mixed: bfloat16 [49152, 2048], P(('sp', 'tp'))
All inputs are finite; a program needn't handle non-finite values.
Results may differ from a plain program's by a relative error of at most 0.018.
Values may be sent and summed in bfloat16 or wider, within the bound.
No kernel may reach another device: no remote copies, remote signals or barrier semaphores. Data moves between devices by JAX's collectives and lax.ppermute only.
A program may use at most 64 MiB of HBM per device.

v0:
```python
import jax
import jax.numpy as jnp
from jax import lax
from jax.experimental import pallas as pl
from jax.experimental.pallas import tpu as pltpu
from jax.sharding import Mesh
from jax.sharding import PartitionSpec as P

DC = 1024
EPSILON = 1e-06
F32 = jnp.float32
BF16 = jnp.bfloat16
SP = ("zh", "zl", "y")
ALL = ("zh", "zl", "y", "x", "c")
NT = (((1,), (1,)), ((), ()))
TN = (((0,), (0,)), ((), ()))
VMEM = pl.BlockSpec(memory_space=pltpu.VMEM)
SMEM = pl.BlockSpec(memory_space=pltpu.SMEM)


def call(kernel, out_shape, scalars, arrays, scratch=()):
    return pl.pallas_call(
        kernel,
        out_shape=out_shape,
        in_specs=[SMEM] * len(scalars) + [VMEM] * len(arrays),
        out_specs=jax.tree.map(lambda _: VMEM, out_shape),
        scratch_shapes=scratch,
        compiler_params=pltpu.CompilerParams(vmem_limit_bytes=56 * 1024 * 1024),
    )(*scalars, *arrays)


def shape(dims, dtype):
    return jax.ShapeDtypeStruct(dims, dtype)


def swap_groups(read, write, rows):
    group = lax.broadcasted_iota(jnp.int32, (rows, 128), 1) // 32
    for outer in range(4):
        for inner in range(4):
            made = None
            for k in range(4):
                moved = read(outer, k)
                turn = ((k - inner) * 32) % 128
                if turn:
                    moved = pltpu.roll(moved, turn, 1)
                made = moved if made is None else jnp.where(group == k, moved, made)
            write(outer, inner, made)


def shard_kernel(k, v, bv, bg, q, s, oc, oh, out):
    for i, part in enumerate((k, v, bv, bg, q, s)):
        out[:, i * 128 : i * 128 + 128] = part[...]
    for i, part in ((6, oc), (7, oh)):
        out[:, i * 128 : i * 128 + 128] = jnp.transpose(part[...].astype(F32)).astype(BF16)


def norm_kernel(tokens, edge, gain, out):
    rows = 16

    def block(source, at, to):
        x = source[at, :].astype(F32)
        inverse = lax.rsqrt(jnp.mean(x * x, axis=1, keepdims=True) + EPSILON)
        normed = x * inverse * gain[...]

        def read(zl, zh):
            z = zh * 4 + zl
            return normed[:, z * 128 : z * 128 + 128]

        def write(zl, y, made):
            where = (y * 4 + zl) * 128
            made = made.astype(BF16)
            for copy in range(4):
                out[copy, to, where : where + 128] = made

        swap_groups(read, write, rows)

    def step(i, carry):
        at = pl.ds(pl.multiple_of(i * rows, rows), rows)
        block(tokens, at, at)
        return carry

    lax.fori_loop(0, 6, step, 0)
    block(edge, slice(0, 16), slice(96, 112))


def last_kernel(parts, out):
    rows = 16

    def step(i, carry):
        at = pl.ds(pl.multiple_of(i * rows, rows), rows)
        total = parts[0, at, :].astype(F32)
        for k in range(1, 4):
            total = total + parts[k, at, :].astype(F32)

        def read(zl, y):
            where = (y * 4 + zl) * 128
            return total[:, where : where + 128]

        def write(zl, zh, made):
            where = (zh * 4 + zl) * 128
            out[at, where : where + 128] = made.astype(BF16)

        swap_groups(read, write, rows)
        return carry

    lax.fori_loop(0, 6, step, 0)


def lane_is_second(rows):
    return lax.broadcasted_iota(jnp.int32, (rows, 128), 1) >= 64


def by_lane(running):
    turned = jnp.transpose(running)
    return jnp.where(lane_is_second(turned.shape[0]), turned[:, 1:2], turned[:, 0:1])


def put_rows(core, own, other, targets):
    for k in range(4):
        mine = pl.ds(pl.multiple_of(k * 192 + core * 96, 32), 96)
        theirs = pl.ds(pl.multiple_of(k * 192 + (1 - core) * 96, 32), 96)
        part = slice(k * 112, k * 112 + 96)
        for n, target in enumerate(targets):
            lanes = slice(n * 128, n * 128 + 128)
            target[mine, :] = own[part, lanes].astype(BF16)
            target[theirs, :] = other[part, lanes].astype(BF16)


def states_kernel(core, own, other, weight, running, tail, keys, values, message):
    w = weight[...]
    put_rows(
        core[0],
        jnp.dot(own[...], w, preferred_element_type=F32),
        jnp.dot(other[...], w, preferred_element_type=F32),
        (keys, values),
    )
    logs = by_lane(running[...])
    closing = logs[767:768, :]
    k = keys[...].astype(F32) * 0.125
    v = values[...]
    second = lane_is_second(64)
    ahead = lax.dot_general(
        (k * jnp.exp(closing - logs)).astype(BF16), v, TN, preferred_element_type=F32
    )
    back = lax.dot_general((k * jnp.exp(logs)).astype(BF16), v, TN, preferred_element_type=F32)
    parts = (
        (slice(0, 64), jnp.where(second, ahead[64:, :], ahead[:64, :]).astype(BF16)),
        (slice(64, 128), jnp.where(second, back[64:, :], back[:64, :]).astype(BF16)),
        (slice(128, 144), log_rows(closing)),
        (slice(144, 160), jnp.transpose(tail[...].astype(F32))[112:128, :].astype(BF16)),
    )
    for at, part in parts:
        for copy in range(16):
            message[copy, at, :] = part


def log_rows(log):
    high = log.astype(BF16)
    low = (log - high.astype(F32)).astype(BF16)
    first = lax.broadcasted_iota(jnp.int32, (16, 128), 0) < 8
    return jnp.where(first, high.astype(F32), low.astype(F32)).astype(BF16)


def scan_states(gathered, count, position):
    def log_of(m):
        return gathered[m, 128:129, :].astype(F32) + gathered[m, 136:137, :].astype(F32)

    def one_way(order, rows):
        state = jnp.zeros((64, 128), F32)
        log = jnp.zeros((1, 128), F32)
        held, held_log = state, log
        for m in order:
            here = position == m
            held = jnp.where(here, state, held)
            held_log = jnp.where(here, log, held_log)
            own = log_of(m)
            state = jnp.exp(own) * state + gathered[m, rows, :].astype(F32)
            log = log + own
        return held, held_log, state, log

    ahead = one_way(range(count), slice(0, 64))
    back = one_way(reversed(range(count)), slice(64, 128))
    return ahead, back


def level_kernel(position, gathered, inside, message, spare):
    ahead, back = scan_states(gathered, 16, position[0])
    inside[0:64, :] = ahead[0]
    inside[64:128, :] = back[0]
    inside[128:136, :] = jnp.broadcast_to(ahead[1], (8, 128))
    inside[136:144, :] = jnp.broadcast_to(back[1], (8, 128))
    parts = (
        (slice(0, 64), ahead[2].astype(BF16)),
        (slice(64, 128), back[2].astype(BF16)),
        (slice(128, 144), log_rows(ahead[3])),
    )
    for at, part in parts:
        for copy in range(4):
            message[copy, at, :] = part

    for y in range(4):
        for zl in range(4):
            where = y * 512 + zl * 128
            spare[:, where : where + 128] = gathered[zl * 4 + y, 144:160, :]


def column_block(position, shift):
    return pl.ds(pl.multiple_of(((position + 4 - shift) % 4) * 512, 512), 512)


def by_piece(y, rows, pieces, lanes):
    total = None
    for shift, piece in enumerate(pieces):
        part = jnp.dot(
            rows[:, column_block(y, shift)], piece[:, lanes], preferred_element_type=F32
        )
        total = part if total is None else total + part
    return total


def conv_kernel(core, y, own, other, p0, p1, p2, p3, taps, convolved, moments, padded):
    pieces = (p0, p1, p2, p3)

    def rows_of(rows):
        both = by_piece(y[0], rows, pieces, slice(0, 256))
        return (both[:, :128] * jax.nn.sigmoid(both[:, 128:])).astype(BF16).astype(F32)

    first, second = rows_of(own), rows_of(other)
    for k in range(4):
        mine = pl.ds(pl.multiple_of(16 + k * 192 + core[0] * 96, 16), 96)
        theirs = pl.ds(pl.multiple_of(16 + k * 192 + (1 - core[0]) * 96, 16), 96)
        padded[mine, :] = first[k * 112 : k * 112 + 96, :]
        padded[theirs, :] = second[k * 112 : k * 112 + 96, :]
    is_second = jnp.full((16, 128), core[0], jnp.int32) == 1
    padded[0:16, :] = jnp.where(is_second, first[432:448, :], second[432:448, :])
    padded[784:800, :] = jnp.where(is_second, second[96:112, :], first[96:112, :])
    ones = jnp.ones((8, 128), F32)
    rows = 128
    for i in range(6):
        total = None
        for j in range(31):
            start = i * rows + j + 1
            term = taps[j : j + 1, :] * padded[start : start + rows, :]
            total = term if total is None else total + term
        convolved[i * rows : (i + 1) * rows, :] = total
        highest = lax.Precision.HIGHEST
        s1 = lax.dot_general(ones, total, NT, precision=highest, preferred_element_type=F32)
        s2 = lax.dot_general(ones, total * total, NT, precision=highest, preferred_element_type=F32)
        moments[0:1, i * rows : (i + 1) * rows] = s1[0:1]
        moments[1:2, i * rows : (i + 1) * rows] = s2[0:1]


def within_kernel(
    core, y, own, other, p0, p1, p2, p3, keys, values, running, queries, gates, within
):
    pieces = (p0, p1, p2, p3)
    put_rows(
        core[0],
        by_piece(y[0], own, pieces, slice(0, 256)),
        by_piece(y[0], other, pieces, slice(0, 256)),
        (queries, gates),
    )
    logs = running[...]
    turned = jnp.transpose(logs)
    k = (keys[...].astype(F32) * 0.125).astype(BF16)
    v = values[...]
    rows = 128
    zero = jnp.zeros((), BF16)
    masks = [lane_is_second(768) == bool(h) for h in range(2)]
    head_values = [jnp.where(mask, v, zero) for mask in masks]
    for i in range(6):
        at = slice(i * rows, (i + 1) * rows)
        q = queries[at, :]
        diagonal = lax.broadcasted_iota(jnp.int32, (rows, 768), 1) == (
            lax.broadcasted_iota(jnp.int32, (rows, 768), 0) + i * rows
        )
        total = None
        for h in range(2):
            scores = lax.dot_general(
                jnp.where(masks[h][:rows], q, zero), k, NT, preferred_element_type=F32
            )
            distance = jnp.abs(turned[at, h : h + 1] - logs[h : h + 1, :])
            weights = jnp.exp(-distance) + jnp.where(diagonal, 1.0, 0.0)
            part = jnp.dot(
                (scores * weights).astype(BF16), head_values[h], preferred_element_type=F32
            )
            total = part if total is None else total + part
        within[at, :] = total


def out_rows(y, rows, pieces, spare, write):
    for shift, piece in enumerate(pieces):
        lanes = column_block(y, shift)
        part = lax.dot_general(rows[:, :240], piece[:, 256:496], NT, preferred_element_type=F32)
        part = part + jnp.dot(rows[:, 240:], spare[:, lanes], preferred_element_type=F32)
        write(lanes, part)


def mixers_kernel(
    core,
    y,
    position,
    queries,
    gates,
    within,
    running,
    gathered,
    inside,
    start,
    head_gain,
    convolved,
    moments,
    channel_gain,
    p0,
    p1,
    p2,
    p3,
    spare,
    mine,
    sent,
    rows_in,
):
    ahead, back = scan_states(gathered, 4, position[0])
    forward = inside[0:64, :] + jnp.exp(inside[128:129, :]) * (
        ahead[0] + jnp.exp(ahead[1]) * start[0:64, :]
    )
    backward = inside[64:128, :] + jnp.exp(inside[136:137, :]) * (
        back[0] + jnp.exp(back[1]) * start[64:128, :]
    )
    second = lane_is_second(64)

    def diagonal_blocks(state):
        return jnp.concatenate(
            [jnp.where(second, 0.0, state), jnp.where(second, state, 0.0)], axis=0
        ).astype(BF16)

    forward, backward = diagonal_blocks(forward), diagonal_blocks(backward)
    logs = by_lane(running[...])
    closing = logs[767:768, :]
    sums = moments[0]
    for k in range(1, 8):
        sums = sums + moments[k]
    sums = jnp.transpose(jnp.concatenate([sums, jnp.zeros((6, 768), F32)], axis=0)) / DC
    rows = 128
    half = lane_is_second(rows)

    def head_mean(x):
        low = jnp.sum(jnp.where(half, 0.0, x), axis=1, keepdims=True)
        high = jnp.sum(jnp.where(half, x, 0.0), axis=1, keepdims=True)
        return jnp.where(half, high, low) / 64

    for i in range(6):
        at = slice(i * rows, (i + 1) * rows)
        average, squares = sums[at, 0:1], sums[at, 1:2]
        scaled = (convolved[at, :] - average) * lax.rsqrt(squares - average * average + EPSILON)
        rows_in[at, 0:128] = jax.nn.silu(scaled * channel_gain[...]).astype(BF16)
        q = queries[at, :]
        log = logs[at, :]
        retained = (
            within[at, :]
            + jnp.exp(log) * jnp.dot(q, forward, preferred_element_type=F32)
            + jnp.exp(closing - log) * jnp.dot(q, backward, preferred_element_type=F32)
        )
        centred = retained - head_mean(retained)
        normed = centred * lax.rsqrt(head_mean(centred * centred) + EPSILON)
        gate = jax.nn.silu(gates[at, :].astype(F32))
        rows_in[at, 128:256] = (normed * head_gain[...] * gate).astype(BF16)

    def half_of(which):
        return jnp.concatenate(
            [
                rows_in[pl.ds(pl.multiple_of(k * 192 + which * 96, 32), 96), :]
                for k in range(4)
            ],
            axis=0,
        )

    mine[...] = half_of(core[0])

    def write(lanes, part):
        sent[:, lanes] = part.astype(BF16)

    out_rows(y[0], half_of(1 - core[0]), (p0, p1, p2, p3), spare, write)


def join_kernel(y, mine, arrived, p0, p1, p2, p3, spare, out):
    def write(lanes, part):
        out[:, lanes] = (part + arrived[:, lanes].astype(F32)).astype(BF16)

    out_rows(y[0], mine[...], (p0, p1, p2, p3), spare, write)


def ring(x, axis, shift):
    count = lax.axis_size(axis)
    return lax.ppermute(x, axis, [(i, (i + shift) % count) for i in range(count)])


def copies(x, axes, count):
    return lax.all_to_all(
        jnp.broadcast_to(x[None], (count, *x.shape)), axes, 0, 0, tiled=True
    )


def body(
    tokens,
    input_gain,
    branch_value,
    branch_gate,
    query_weight,
    key_weight,
    value_weight,
    swish_weight,
    kernel_taps,
    channel_gain,
    decay_logs,
    start_state,
    head_gain,
    output_conv,
    output_heads,
):
    core = lax.axis_index("c").astype(jnp.int32)[None]
    y = lax.axis_index("y").astype(jnp.int32)[None]
    high = lax.axis_index("zh").astype(jnp.int32)[None]
    low = lax.axis_index(("zl", "y")).astype(jnp.int32)[None]

    place = lax.axis_index(("x", "c"))
    count = lax.axis_size(SP)
    edge = lax.ppermute(
        jnp.where(place == 7, tokens[80:96], tokens[0:16]),
        ALL,
        [(i * 8 + 7, i * 8 + 15) for i in range(count - 1)]
        + [(i * 8 + 8, i * 8) for i in range(count - 1)],
    )
    shard = call(
        shard_kernel,
        shape((32, 1024), BF16),
        (),
        (
            key_weight,
            value_weight,
            branch_value,
            branch_gate,
            query_weight,
            swish_weight,
            output_conv,
            output_heads,
        ),
    )
    normed = call(
        norm_kernel, shape((4, 112, 2048), BF16), (), (tokens, edge, input_gain[None])
    )
    shard, normed = lax.optimization_barrier((shard, normed))
    own = lax.all_to_all(normed, "x", 0, 0, tiled=True).reshape(448, 2048)
    rows = lax.all_gather(shard, "zh", axis=0, tiled=True)
    tail = rows[:, 896:]
    rows = lax.all_gather(rows[:, :1008], "zl", axis=0, tiled=True)
    own, rows = lax.optimization_barrier((own, rows))
    other = ring(own, "c", 1)
    state_weight = copies(rows[:, :256], "y", 4).reshape(2048, 256)
    gate_piece, rest_piece = rows[:, 256:512], rows[:, 512:]
    gate_pieces = (gate_piece,) + tuple(ring(gate_piece, "y", d) for d in (1, 2, 3))
    rest_pieces = (rest_piece,) + tuple(ring(rest_piece, "y", d) for d in (1, 2, 3))

    running = jnp.cumsum(decay_logs, axis=1)
    running = jnp.concatenate([running, jnp.zeros((6, 768), F32)], axis=0)
    start = start_state.transpose(0, 2, 1, 3).reshape(128, 128)

    half = shape((768, 128), BF16)
    full = shape((768, 128), F32)
    keys, values, sent = call(
        states_kernel,
        (half, half, shape((16, 160, 128), BF16)),
        (core,),
        (own, other, state_weight, running, tail),
    )
    inside, sent, spare = call(
        level_kernel,
        (shape((144, 128), F32), shape((4, 144, 128), BF16), shape((16, 2048), BF16)),
        (low,),
        (lax.all_to_all(sent, ("zl", "y"), 0, 0, tiled=True),),
    )
    gathered = lax.all_to_all(sent, "zh", 0, 0, tiled=True)

    convolved, moments = call(
        conv_kernel,
        (full, shape((2, 768), F32)),
        (core, y),
        (own, other, *gate_pieces, kernel_taps),
        scratch=(pltpu.VMEM((800, 128), F32),),
    )
    moments = lax.all_gather(moments, ("x", "c"))
    queries, gates, within = call(
        within_kernel,
        (half, half, full),
        (core, y),
        (own, other, *rest_pieces, keys, values, running),
    )
    mine, sent = call(
        mixers_kernel,
        (shape((384, 256), BF16), shape((384, 2048), BF16)),
        (core, y, high),
        (
            queries,
            gates,
            within,
            running,
            gathered,
            inside,
            start,
            head_gain[None],
            convolved,
            moments,
            channel_gain[None],
            *rest_pieces,
            spare,
        ),
        scratch=(pltpu.VMEM((768, 256), BF16),),
    )
    arrived = ring(sent, "c", 1)
    joined = call(
        join_kernel,
        shape((384, 2048), BF16),
        (y,),
        (mine, arrived, *rest_pieces, spare),
    )
    parts = lax.all_to_all(joined.reshape(4, 96, 2048), "x", 0, 0, tiled=True)
    return call(last_kernel, shape((96, 2048), BF16), (), (parts,))


def solution(mesh):
    split = Mesh(mesh.devices.reshape(4, 4, 4, 4, 2), ALL)
    in_specs = (
        P(ALL, None),
        P(),
        P(SP, ("x", "c")),
        P(SP, ("x", "c")),
        P(SP, ("x", "c")),
        P(SP, ("x", "c")),
        P(SP, ("x", "c")),
        P(SP, ("x", "c")),
        P(None, ("x", "c")),
        P(("x", "c")),
        P(("x", "c"), SP),
        P(None, ("x", "c"), None, None),
        P(("x", "c")),
        P(("x", "c"), SP),
        P(("x", "c"), SP),
    )

    return jax.shard_map(
        body, mesh=split, in_specs=in_specs, out_specs=P(ALL, None), check_vma=False
    )
```

profile of v0, /device:TPU:1, one launch (start us, length us, event | category | flops | bytes accessed | tf_op | source)
XLA Modules:
  0.0 221.0 jit_solution(6134985271755916792)
XLA Ops:
  0.0 0.9 slice_select_fusion
  0.9 0.7 collective-permute-start
  1.6 1.4 copy.22.oc
  3.0 1.4 copy.23.oh
  4.4 1.6 shard_map.145
  5.9 0.0 collective-permute-done.edge
  5.9 0.6 copy-done.17
  6.6 3.9 %shard_map.146 = bf16[4,112,2048]{2,1,0:T(8,128)(2,1)} custom-call(bf16[96,2048]{1,0:T(8,128)(2,1)} %tokens.1, bf16[16,2048]{1,0:T(8,128)(2,1)} %copy-done.17, f32[1,2048]{1,0:T(1,128)} %bitcast.28), custom_call_target="tpu_custom_call" | custom-call | tf_op jit(solution)/shard_map/pallas_call | solution.py:22
  10.5 7.2 %all-to-all-start = ((bf16[4,112,2048]{2,1,0:T(8,128)(2,1)}), bf16[4,112,2048]{2,1,0:T(8,128)(2,1)S(1)}, u32[]{:S(2)}, u32[]{:S(2)}) async-start(bf16[4,112,2048]{2,1,0:T(8,128)(2,1)} %shard_map.146), calls=%async_computation | async-start | bytes 3670016 | tf_op jit(solution)/shard_map/all_to_all | solution.py:453
  17.7 26.6 %all_gather.12 = bf16[128,1024]{1,0:T(8,128)(2,1)S(1)} all-gather(bf16[32,1024]{1,0:T(8,128)(2,1)S(1)} %copy-done.12), channel_id=1, replica_groups=mesh['zh'=4,'zl'=4,'y'=4,'x'=4,'c'=2] {'zh'}, dimensions={0}, use_global_device_ids=true | all-gather | bytes 327680 | tf_op jit(solution)/shard_map/all_gather | solution.py:454
  44.3 17.1 %all_gather.13 = bf16[512,1008]{1,0:T(8,128)(2,1)S(1)} all-gather(bf16[128,1008]{1,0:T(8,128)(2,1)S(1)} %bitcast.25), channel_id=1, replica_groups=mesh['zh'=4,'zl'=4,'y'=4,'x'=4,'c'=2] {'zl'}, dimensions={0}, use_global_device_ids=true | all-gather | bytes 1290240 | tf_op jit(solution)/shard_map/all_gather | solution.py:456
  61.4 0.0 all-to-all-done
  61.4 8.6 %collective-permute-start.1 = (bf16[448,2048]{1,0:T(8,128)(2,1)S(1)}, bf16[448,2048]{1,0:T(8,128)(2,1)}, u32[]{:S(2)}, u32[]{:S(2)}) collective-permute-start(bf16[448,2048]{1,0:T(8,128)(2,1)S(1)} %bitcast.19), channel_id=1, source_target_pairs={{0,1},{1,0},{2,3},{3,2},{4,5},{5,4},{6,7},{7,6},{8,9},{9,8},{10,11... | collective-permute-start | bytes 5505032 | tf_op jit(solution)/shard_map/ppermute | solution.py:395
  70.1 0.0 copy-start.10
  70.1 0.0 copy-start.18
  70.1 1.1 broadcast_in_dim.32
  71.2 3.5 %all-to-all-start.1 = ((bf16[4,512,256]{2,1,0:T(8,128)(2,1)}), bf16[4,512,256]{2,1,0:T(8,128)(2,1)S(1)}, u32[]{:S(2)}, u32[]{:S(2)}) async-start(bf16[4,512,256]{2,1,0:T(8,128)(2,1)} %broadcast_in_dim.32), calls=%async_computation.1 | async-start | bytes 2097152 | tf_op jit(solution)/shard_map/all_to_all | solution.py:399
  74.7 0.0 copy-done.18
  74.8 0.6 reduce-window.6
  75.3 0.2 slice_reduce_fusion
  75.5 0.2 reduce-window.9
  75.7 0.1 add_bitcast_fusion
  75.8 0.6 concatenate.3.running
  76.4 0.6 slice.38.tail
  77.0 12.9 %all-to-all-done.1 = bf16[4,512,256]{2,1,0:T(8,128)(2,1)S(1)} async-done(((bf16[4,512,256]{2,1,0:T(8,128)(2,1)}), bf16[4,512,256]{2,1,0:T(8,128)(2,1)S(1)}, u32[]{:S(2)}, u32[]{:S(2)}) %all-to-all-start.1) | async-done | bytes 1048608 | tf_op jit(solution)/shard_map/all_to_all | solution.py:399
  89.9 0.0 collective-permute-done.1.other
  89.9 1.0 copy-done.5
  90.9 4.7 %shard_map.147 = (bf16[768,128]{1,0:T(8,128)(2,1)}, bf16[768,128]{1,0:T(8,128)(2,1)}, bf16[16,160,128]{2,1,0:T(8,128)(2,1)}) custom-call(s32[1]{0:T(128)} %bitcast.1.core, bf16[448,2048]{1,0:T(8,128)(2,1)} %bitcast.20, bf16[448,2048]{1,0:T(8,128)(2,1)} %collective-permute-done.1.other, bf16[2048,256]{1,0:T(8,128)(2,1)} %bitcast.24, ...), custom_call_target="tpu_custom_call" | custom-call | tf_op jit(solution)/shard_map/pallas_call | solution.py:22
  95.6 3.9 %all-to-all-start.2 = ((bf16[16,160,128]{2,1,0:T(8,128)(2,1)}), bf16[16,160,128]{2,1,0:T(8,128)(2,1)S(1)}, u32[]{:S(2)}, u32[]{:S(2)}) async-start(bf16[16,160,128]{2,1,0:T(8,128)(2,1)} %get-tuple-element.31), calls=%async_computation.2 | async-start | bytes 1310720 | tf_op jit(solution)/shard_map/all_to_all | solution.py:480
  99.5 3.3 %collective-permute-start.5 = (bf16[512,256]{1,0:T(8,128)(2,1)S(1)}, bf16[512,256]{1,0:T(8,128)(2,1)S(1)}, u32[]{:S(2)}, u32[]{:S(2)}) collective-permute-start(bf16[512,256]{1,0:T(8,128)(2,1)S(1)} %get-tuple-element.39.p0), channel_id=1, source_target_pairs={{0,8},{8,16},{16,24},{24,0},{1,9},{9,17},{17,25},{25,1},{2,10},{10... | collective-permute-start | bytes 786440 | tf_op jit(solution)/shard_map/ppermute | solution.py:395
  102.8 0.0 copy-start.1
  102.8 3.1 %collective-permute-start.2 = (bf16[512,496]{1,0:T(8,128)(2,1)S(1)}, bf16[512,496]{1,0:T(8,128)(2,1)S(1)}, u32[]{:S(2)}, u32[]{:S(2)}) collective-permute-start(bf16[512,496]{1,0:T(8,128)(2,1)S(1)} %slice.30.p0), channel_id=1, source_target_pairs={{0,8},{8,16},{16,24},{24,0},{1,9},{9,17},{17,25},{25,1},{2,10},{10... | collective-permute-start | bytes 1523720 | tf_op jit(solution)/shard_map/ppermute | solution.py:395
  105.9 3.2 %collective-permute-start.3 = (bf16[512,496]{1,0:T(8,128)(2,1)S(1)}, bf16[512,496]{1,0:T(8,128)(2,1)S(1)}, u32[]{:S(2)}, u32[]{:S(2)}) collective-permute-start(bf16[512,496]{1,0:T(8,128)(2,1)S(1)} %slice.30.p0), channel_id=1, source_target_pairs={{0,16},{8,24},{16,0},{24,8},{1,17},{9,25},{17,1},{25,9},{2,18},{10... | collective-permute-start | bytes 1523720 | tf_op jit(solution)/shard_map/ppermute | solution.py:395
  109.2 3.9 %collective-permute-start.4 = (bf16[512,496]{1,0:T(8,128)(2,1)S(1)}, bf16[512,496]{1,0:T(8,128)(2,1)S(1)}, u32[]{:S(2)}, u32[]{:S(2)}) collective-permute-start(bf16[512,496]{1,0:T(8,128)(2,1)S(1)} %slice.30.p0), channel_id=1, source_target_pairs={{0,24},{8,0},{16,8},{24,16},{1,25},{9,1},{17,9},{25,17},{2,26},{10... | collective-permute-start | bytes 1523720 | tf_op jit(solution)/shard_map/ppermute | solution.py:395
  113.1 2.0 all-to-all-done.2.gathered
  115.0 0.9 copy-done.8
  115.9 2.0 shard_map.149
  117.8 6.4 %all-to-all-start.3 = ((bf16[4,144,128]{2,1,0:T(8,128)(2,1)}), bf16[4,144,128]{2,1,0:T(8,128)(2,1)S(1)}, u32[]{:S(2)}, u32[]{:S(2)}) async-start(bf16[4,144,128]{2,1,0:T(8,128)(2,1)} %get-tuple-element.32), calls=%async_computation.3 | async-start | bytes 294912 | tf_op jit(solution)/shard_map/all_to_all | solution.py:482
  124.2 3.9 %collective-permute-start.6 = (bf16[512,256]{1,0:T(8,128)(2,1)S(1)}, bf16[512,256]{1,0:T(8,128)(2,1)S(1)}, u32[]{:S(2)}, u32[]{:S(2)}) collective-permute-start(bf16[512,256]{1,0:T(8,128)(2,1)S(1)} %get-tuple-element.39.p0), channel_id=1, source_target_pairs={{0,16},{8,24},{16,0},{24,8},{1,17},{9,25},{17,1},{25,9},{2,18},{10... | collective-permute-start | bytes 786440 | tf_op jit(solution)/shard_map/ppermute | solution.py:395
  128.1 0.0 collective-permute-done.5.p1
  128.1 2.6 %collective-permute-start.7 = (bf16[512,256]{1,0:T(8,128)(2,1)S(1)}, bf16[512,256]{1,0:T(8,128)(2,1)S(1)}, u32[]{:S(2)}, u32[]{:S(2)}) collective-permute-start(bf16[512,256]{1,0:T(8,128)(2,1)S(1)} %get-tuple-element.39.p0), channel_id=1, source_target_pairs={{0,24},{8,0},{16,8},{24,16},{1,25},{9,1},{17,9},{25,17},{2,26},{10... | collective-permute-start | bytes 786440 | tf_op jit(solution)/shard_map/ppermute | solution.py:395
  130.8 0.1 copy.24
  130.9 0.7 reshape.27.start
  131.6 12.9 %collective-permute-done.6.p2 = bf16[512,256]{1,0:T(8,128)(2,1)S(1)} collective-permute-done((bf16[512,256]{1,0:T(8,128)(2,1)S(1)}, bf16[512,256]{1,0:T(8,128)(2,1)S(1)}, u32[]{:S(2)}, u32[]{:S(2)}) %collective-permute-start.6) | collective-permute-done | bytes 262176 | tf_op jit(solution)/shard_map/ppermute | solution.py:395
  144.5 1.3 collective-permute-done.7.p3
  145.8 0.7 copy-done.15
  146.5 5.6 %shard_map.150 = (f32[768,128]{1,0:T(8,128)}, f32[2,768]{1,0:T(2,128)}) custom-call(s32[1]{0:T(128)} %bitcast.1.core, s32[1]{0:T(128)} %bitcast.y, bf16[448,2048]{1,0:T(8,128)(2,1)} %bitcast.21, bf16[448,2048]{1,0:T(8,128)(2,1)} %collective-permute-done.1.other, bf16[512,256]{1,0:T(8,128)(2,1)} %copy-done.10, bf16[512,256]{1,0:T(8,128)(2,1)} %copy-done.13, ...), custom_call_target="tpu_custom_call" | custom-call | tf_op jit(solution)/shard_map/pallas_call | solution.py:22
  152.1 0.0 collective-permute-done.2.p1
  152.1 0.0 collective-permute-done.3.p2
  152.1 0.0 collective-permute-done.4.p3
  152.1 0.8 copy-done.2
  152.9 0.2 copy-done.3
  153.1 0.2 copy-done.4
  153.3 6.6 %shard_map.148 = (bf16[768,128]{1,0:T(8,128)(2,1)}, bf16[768,128]{1,0:T(8,128)(2,1)}, f32[768,128]{1,0:T(8,128)}) custom-call(s32[1]{0:T(128)} %bitcast.1.core, s32[1]{0:T(128)} %bitcast.y, bf16[448,2048]{1,0:T(8,128)(2,1)} %bitcast.22, bf16[448,2048]{1,0:T(8,128)(2,1)} %collective-permute-done.1.other, bf16[512,496]{1,0:T(8,128)(2,1)} %copy-done.1, ...), custom_call_target="tpu_custom_call" | custom-call | tf_op jit(solution)/shard_map/pallas_call | solution.py:22
  159.9 16.1 %all-gather.1.moments = f32[8,2,768]{2,1,0:T(2,128)} all-gather(f32[1,2,768]{2,1,0:T(2,128)S(1)} %bitcast.29), channel_id=2, replica_groups=mesh['zh'=4,'zl'=4,'y'=4,'x'=4,'c'=2] {'x','c'}, dimensions={0}, use_global_device_ids=true | all-gather | bytes 55296 | tf_op jit(solution)/shard_map/all_gather | solution.py:491
  176.0 0.0 all-to-all-done.3.gathered
  176.0 0.6 copy-done.11
  176.6 5.7 %shard_map.151 = (bf16[384,256]{1,0:T(8,128)(2,1)}, bf16[384,2048]{1,0:T(8,128)(2,1)}) custom-call(s32[1]{0:T(128)} %bitcast.1.core, s32[1]{0:T(128)} %bitcast.y, s32[1]{0:T(128)} %bitcast.2.position, bf16[768,128]{1,0:T(8,128)(2,1)} %get-tuple-element.28.queries, bf16[768,128]{1,0:T(8,128)(2,1)} %get-tuple-element.29.gates, ...), custom_call_target="tpu_custom_call" | custom-call | tf_op jit(solution)/shard_map/pallas_call | solution.py:22
  182.3 2.1 collective-permute-start.8
  184.4 3.4 %collective-permute-done.8.arrived = bf16[384,2048]{1,0:T(8,128)(2,1)S(1)} collective-permute-done((bf16[384,2048]{1,0:T(8,128)(2,1)}, bf16[384,2048]{1,0:T(8,128)(2,1)S(1)}, u32[]{:S(2)}, u32[]{:S(2)}) %collective-permute-start.8) | collective-permute-done | bytes 1572896 | tf_op jit(solution)/shard_map/ppermute | solution.py:395
  187.8 1.1 copy-done.9
  188.9 4.2 %shard_map.152 = bf16[384,2048]{1,0:T(8,128)(2,1)} custom-call(s32[1]{0:T(128)} %bitcast.y, bf16[384,256]{1,0:T(8,128)(2,1)} %get-tuple-element.37.mine, bf16[384,2048]{1,0:T(8,128)(2,1)} %copy-done.9, bf16[512,496]{1,0:T(8,128)(2,1)} %copy-done.1, bf16[512,496]{1,0:T(8,128)(2,1)} %copy-done.2, bf16[512,496]{1,0:T(8,128)(2,1)} %copy-done.3, ...), custom_call_target="tpu_custom_call" | custom-call | tf_op jit(solution)/shard_map/pallas_call | solution.py:22
  193.1 24.9 %all_to_all.25.parts = bf16[4,96,2048]{2,1,0:T(8,128)(2,1)} all-to-all(bf16[4,96,2048]{2,1,0:T(8,128)(2,1)} %bitcast.23), channel_id=1, replica_groups=mesh['zh'=4,'zl'=4,'y'=4,'x'=4,'c'=2] {'x'}, dimensions={0} | all-to-all | bytes 3145728 | tf_op jit(solution)/shard_map/all_to_all | solution.py:526
  218.0 2.9 %shard_map.153 = bf16[96,2048]{1,0:T(8,128)(2,1)} custom-call(bf16[4,96,2048]{2,1,0:T(8,128)(2,1)} %all_to_all.25.parts), custom_call_target="tpu_custom_call" | custom-call | tf_op jit(solution)/shard_map/pallas_call | solution.py:22
  (31 shorter events, 0.1 us)
Async XLA Ops:
  0.9 5.1 %collective-permute-start = (bf16[16,2048]{1,0:T(8,128)(2,1)S(1)}, bf16[16,2048]{1,0:T(8,128)(2,1)S(1)}, u32[]{:S(2)}, u32[]{:S(2)}) collective-permute-start(bf16[16,2048]{1,0:T(8,128)(2,1)S(1)} %slice_select_fusion), channel_id=1, source_target_pairs={{7,15},{15,23},{23,31},{31,39},{39,47},{47,55},{55,63},{63,71},{71... | collective-permute-start | bytes 196616 | tf_op jit(solution)/shard_map/ppermute | solution.py:428
  5.9 0.6 copy-start.17
  10.5 7.2 %copy-start.12 = (bf16[32,1024]{1,0:T(8,128)(2,1)S(1)}, bf16[32,1024]{1,0:T(8,128)(2,1)}, u32[]{:S(2)}) copy-start(bf16[32,1024]{1,0:T(8,128)(2,1)} %shard_map.145) | copy-start | bytes 196612
  10.5 50.9 %all-to-all-start = ((bf16[4,112,2048]{2,1,0:T(8,128)(2,1)}), bf16[4,112,2048]{2,1,0:T(8,128)(2,1)S(1)}, u32[]{:S(2)}, u32[]{:S(2)}) async-start(bf16[4,112,2048]{2,1,0:T(8,128)(2,1)} %shard_map.146), calls=%async_computation | async-start | bytes 3670016 | tf_op jit(solution)/shard_map/all_to_all | solution.py:453
  61.4 9.8 %copy-start.6 = (bf16[512,1008]{1,0:T(8,128)(2,1)}, bf16[512,1008]{1,0:T(8,128)(2,1)S(1)}, u32[]{:S(2)}) copy-start(bf16[512,1008]{1,0:T(8,128)(2,1)S(1)} %all_gather.13) | copy-start | bytes 3096580
  61.4 9.8 %copy-start = (bf16[4,112,2048]{2,1,0:T(8,128)(2,1)}, bf16[4,112,2048]{2,1,0:T(8,128)(2,1)S(1)}, u32[]{:S(2)}) copy-start(bf16[4,112,2048]{2,1,0:T(8,128)(2,1)S(1)} %all-to-all-done) | copy-start | bytes 5505028
  61.4 28.4 %collective-permute-start.1 = (bf16[448,2048]{1,0:T(8,128)(2,1)S(1)}, bf16[448,2048]{1,0:T(8,128)(2,1)}, u32[]{:S(2)}, u32[]{:S(2)}) collective-permute-start(bf16[448,2048]{1,0:T(8,128)(2,1)S(1)} %bitcast.19), channel_id=1, source_target_pairs={{0,1},{1,0},{2,3},{3,2},{4,5},{5,4},{6,7},{7,6},{8,9},{9,8},{10,11... | collective-permute-start | bytes 5505032 | tf_op jit(solution)/shard_map/ppermute | solution.py:395
  70.1 58.0 %copy-start.10 = (bf16[512,256]{1,0:T(8,128)(2,1)}, bf16[512,256]{1,0:T(8,128)(2,1)S(1)}, u32[]{:S(2)}) copy-start(bf16[512,256]{1,0:T(8,128)(2,1)S(1)} %get-tuple-element.39.p0) | copy-start | bytes 786436
  70.1 4.6 %copy-start.18 = (f32[2,768]{1,0:T(2,128)S(1)}, f32[2,768]{1,0:T(2,128)}, u32[]{:S(2)}) copy-start(f32[2,768]{1,0:T(2,128)} %param.25) | copy-start | bytes 18436
  71.2 18.7 %all-to-all-start.1 = ((bf16[4,512,256]{2,1,0:T(8,128)(2,1)}), bf16[4,512,256]{2,1,0:T(8,128)(2,1)S(1)}, u32[]{:S(2)}, u32[]{:S(2)}) async-start(bf16[4,512,256]{2,1,0:T(8,128)(2,1)} %broadcast_in_dim.32), calls=%async_computation.1 | async-start | bytes 2097152 | tf_op jit(solution)/shard_map/all_to_all | solution.py:399
  89.9 1.0 copy-start.5
  95.6 7.2 %copy-start.7 = (bf16[512,1008]{1,0:T(8,128)(2,1)S(1)}, bf16[512,1008]{1,0:T(8,128)(2,1)}, u32[]{:S(2)}) copy-start(bf16[512,1008]{1,0:T(8,128)(2,1)} %copy-done.6) | copy-start | bytes 3096580
  95.6 35.2 %copy-start.16 = (f32[2,2,64,64]{3,2,1,0:T(8,128)S(1)}, f32[2,2,64,64]{3,2,1,0:T(8,128)}, u32[]{:S(2)}) copy-start(f32[2,2,64,64]{3,2,1,0:T(8,128)} %param.26) | copy-start | bytes 196612
  95.6 19.4 %all-to-all-start.2 = ((bf16[16,160,128]{2,1,0:T(8,128)(2,1)}), bf16[16,160,128]{2,1,0:T(8,128)(2,1)S(1)}, u32[]{:S(2)}, u32[]{:S(2)}) async-start(bf16[16,160,128]{2,1,0:T(8,128)(2,1)} %get-tuple-element.31), calls=%async_computation.2 | async-start | bytes 1310720 | tf_op jit(solution)/shard_map/all_to_all | solution.py:480
  99.5 28.6 %collective-permute-start.5 = (bf16[512,256]{1,0:T(8,128)(2,1)S(1)}, bf16[512,256]{1,0:T(8,128)(2,1)S(1)}, u32[]{:S(2)}, u32[]{:S(2)}) collective-permute-start(bf16[512,256]{1,0:T(8,128)(2,1)S(1)} %get-tuple-element.39.p0), channel_id=1, source_target_pairs={{0,8},{8,16},{16,24},{24,0},{1,9},{9,17},{17,25},{25,1},{2,10},{10... | collective-permute-start | bytes 786440 | tf_op jit(solution)/shard_map/ppermute | solution.py:395
  102.8 49.2 %copy-start.1 = (bf16[512,496]{1,0:T(8,128)(2,1)}, bf16[512,496]{1,0:T(8,128)(2,1)S(1)}, u32[]{:S(2)}) copy-start(bf16[512,496]{1,0:T(8,128)(2,1)S(1)} %slice.30.p0) | copy-start | bytes 1523716
  102.8 49.2 %collective-permute-start.2 = (bf16[512,496]{1,0:T(8,128)(2,1)S(1)}, bf16[512,496]{1,0:T(8,128)(2,1)S(1)}, u32[]{:S(2)}, u32[]{:S(2)}) collective-permute-start(bf16[512,496]{1,0:T(8,128)(2,1)S(1)} %slice.30.p0), channel_id=1, source_target_pairs={{0,8},{8,16},{16,24},{24,0},{1,9},{9,17},{17,25},{25,1},{2,10},{10... | collective-permute-start | bytes 1523720 | tf_op jit(solution)/shard_map/ppermute | solution.py:395
  105.9 46.2 %collective-permute-start.3 = (bf16[512,496]{1,0:T(8,128)(2,1)S(1)}, bf16[512,496]{1,0:T(8,128)(2,1)S(1)}, u32[]{:S(2)}, u32[]{:S(2)}) collective-permute-start(bf16[512,496]{1,0:T(8,128)(2,1)S(1)} %slice.30.p0), channel_id=1, source_target_pairs={{0,16},{8,24},{16,0},{24,8},{1,17},{9,25},{17,1},{25,9},{2,18},{10... | collective-permute-start | bytes 1523720 | tf_op jit(solution)/shard_map/ppermute | solution.py:395
  109.2 42.9 %collective-permute-start.4 = (bf16[512,496]{1,0:T(8,128)(2,1)S(1)}, bf16[512,496]{1,0:T(8,128)(2,1)S(1)}, u32[]{:S(2)}, u32[]{:S(2)}) collective-permute-start(bf16[512,496]{1,0:T(8,128)(2,1)S(1)} %slice.30.p0), channel_id=1, source_target_pairs={{0,24},{8,0},{16,8},{24,16},{1,25},{9,1},{17,9},{25,17},{2,26},{10... | collective-permute-start | bytes 1523720 | tf_op jit(solution)/shard_map/ppermute | solution.py:395
  115.0 0.9 copy-start.8
  117.8 58.1 %all-to-all-start.3 = ((bf16[4,144,128]{2,1,0:T(8,128)(2,1)}), bf16[4,144,128]{2,1,0:T(8,128)(2,1)S(1)}, u32[]{:S(2)}, u32[]{:S(2)}) async-start(bf16[4,144,128]{2,1,0:T(8,128)(2,1)} %get-tuple-element.32), calls=%async_computation.3 | async-start | bytes 294912 | tf_op jit(solution)/shard_map/all_to_all | solution.py:482
  124.2 20.3 %collective-permute-start.6 = (bf16[512,256]{1,0:T(8,128)(2,1)S(1)}, bf16[512,256]{1,0:T(8,128)(2,1)S(1)}, u32[]{:S(2)}, u32[]{:S(2)}) collective-permute-start(bf16[512,256]{1,0:T(8,128)(2,1)S(1)} %get-tuple-element.39.p0), channel_id=1, source_target_pairs={{0,16},{8,24},{16,0},{24,8},{1,17},{9,25},{17,1},{25,9},{2,18},{10... | collective-permute-start | bytes 786440 | tf_op jit(solution)/shard_map/ppermute | solution.py:395
  128.1 17.6 %copy-start.13 = (bf16[512,256]{1,0:T(8,128)(2,1)}, bf16[512,256]{1,0:T(8,128)(2,1)S(1)}, u32[]{:S(2)}) copy-start(bf16[512,256]{1,0:T(8,128)(2,1)S(1)} %collective-permute-done.5.p1) | copy-start | bytes 786436
  128.1 17.6 %collective-permute-start.7 = (bf16[512,256]{1,0:T(8,128)(2,1)S(1)}, bf16[512,256]{1,0:T(8,128)(2,1)S(1)}, u32[]{:S(2)}, u32[]{:S(2)}) collective-permute-start(bf16[512,256]{1,0:T(8,128)(2,1)S(1)} %get-tuple-element.39.p0), channel_id=1, source_target_pairs={{0,24},{8,0},{16,8},{24,16},{1,25},{9,1},{17,9},{25,17},{2,26},{10... | collective-permute-start | bytes 786440 | tf_op jit(solution)/shard_map/ppermute | solution.py:395
  144.5 1.3 copy-start.14
  145.8 0.7 copy-start.15
  152.1 0.8 copy-start.2
  152.1 1.0 copy-start.3
  152.1 1.2 copy-start.4
  153.3 6.6 %copy-start.19 = (f32[2,768]{1,0:T(2,128)S(1)}, f32[2,768]{1,0:T(2,128)}, u32[]{:S(2)}) copy-start(f32[2,768]{1,0:T(2,128)} %get-tuple-element.35) | copy-start | bytes 18436
  176.0 0.6 copy-start.11
  182.3 5.5 %collective-permute-start.8 = (bf16[384,2048]{1,0:T(8,128)(2,1)}, bf16[384,2048]{1,0:T(8,128)(2,1)S(1)}, u32[]{:S(2)}, u32[]{:S(2)}) collective-permute-start(bf16[384,2048]{1,0:T(8,128)(2,1)} %get-tuple-element.38), channel_id=1, source_target_pairs={{0,1},{1,0},{2,3},{3,2},{4,5},{5,4},{6,7},{7,6},{8,9},{9,8},{10,11... | collective-permute-start | bytes 4718600 | tf_op jit(solution)/shard_map/ppermute | solution.py:395
  187.8 1.1 copy-start.9
where the time goes:
time: 222 us; the launch traced here: 221 us
  blocking collectives  84.7 us (38%)
  starting transfers between devices  52.3 us (24%)
  Pallas kernels  37.1 us (17%)
  waiting for transfers between devices  32.4 us (15%)
  local copies, waits for them, and re-layouts  12.4 us (6%)
    pallas_call x9, Pallas kernels, call(): pl.pallas_call(kernel, out_shape=out_shape, in_specs=[SMEM] * len(scalars...  37.1 us
    ppermute x8, starting transfers between devices, ring(): lax.ppermute(x, axis, [(i, (i + shift) % count) for i in range(count)])  30.6 us
    all_gather x1, blocking collectives, body(): rows = lax.all_gather(shard, 'zh', axis=0, tiled=True)  26.6 us
    all_to_all x1, blocking collectives, body(): parts = lax.all_to_all(joined.reshape(4, 96, 2048), 'x', 0, 0, tiled=True)  24.9 us
    ppermute x8, waiting for transfers between devices, ring(): lax.ppermute(x, axis, [(i, (i + shift) % count) for i in range(count)])  17.6 us
    all_gather x1, blocking collectives, body(): rows = lax.all_gather(rows[:, :1008], 'zl', axis=0, tiled=True)  17.1 us
    all_gather x1, blocking collectives, body(): moments = lax.all_gather(moments, ('x', 'c'))  16.1 us
    all_to_all x1, waiting for transfers between devices, copies(): lax.all_to_all(jnp.broadcast_to(x[None], (count, *x.shape)), axes, 0, 0,...  12.9 us
  transfers between devices with their start and end apart: 13, of which 5 were waited for; matrix products, arithmetic and copies ran while one was open for 3% of the time, Pallas kernels for 7%

commit v1 on v0

--- a/solution.py
+++ b/solution.py
@@ -1,3 +1,5 @@
+import functools
+
 import jax
 import jax.numpy as jnp
 from jax import lax
@@ -48,10 +50,9 @@
 
 
 def shard_kernel(k, v, bv, bg, q, s, oc, oh, out):
-    for i, part in enumerate((k, v, bv, bg, q, s)):
+    for i, part in enumerate((k, v, bv, bg, q, s, oc)):
         out[:, i * 128 : i * 128 + 128] = part[...]
-    for i, part in ((6, oc), (7, oh)):
-        out[:, i * 128 : i * 128 + 128] = jnp.transpose(part[...].astype(F32)).astype(BF16)
+    out[:, 896:1008] = oh[:, 0:112]
 
 
 def norm_kernel(tokens, edge, gain, out):
@@ -62,12 +63,12 @@
         inverse = lax.rsqrt(jnp.mean(x * x, axis=1, keepdims=True) + EPSILON)
         normed = x * inverse * gain[...]
 
-        def read(zl, zh):
+        def read(zh, zl):
             z = zh * 4 + zl
             return normed[:, z * 128 : z * 128 + 128]
 
-        def write(zl, y, made):
-            where = (y * 4 + zl) * 128
+        def write(zh, y, made):
+            where = (y * 4 + zh) * 128
             made = made.astype(BF16)
             for copy in range(4):
                 out[copy, to, where : where + 128] = made
@@ -79,28 +80,33 @@
         block(tokens, at, at)
         return carry
 
-    lax.fori_loop(0, 6, step, 0)
+    lax.fori_loop(0, 6, step, 0, unroll=2)
     block(edge, slice(0, 16), slice(96, 112))
 
 
-def last_kernel(parts, out):
+def last_kernel(y, parts_a, parts_b, out):
     rows = 16
+    group = lax.broadcasted_iota(jnp.int32, (rows, 128), 1) // 32
 
     def step(i, carry):
         at = pl.ds(pl.multiple_of(i * rows, rows), rows)
-        total = parts[0, at, :].astype(F32)
-        for k in range(1, 4):
-            total = total + parts[k, at, :].astype(F32)
-
-        def read(zl, y):
-            where = (y * 4 + zl) * 128
-            return total[:, where : where + 128]
-
-        def write(zl, zh, made):
-            where = (zh * 4 + zl) * 128
-            out[at, where : where + 128] = made.astype(BF16)
-
-        swap_groups(read, write, rows)
+        totals = []
+        for parts in (parts_a, parts_b):
+            total = parts[0, at, :].astype(F32)
+            for k in range(1, 4):
+                total = total + parts[k, at, :].astype(F32)
+            totals.append(total)
+        for zh in range(4):
+            for zl in range(4):
+                made = jnp.zeros((rows, 128), F32)
+                for d in range(4):
+                    source = (y[0] + 4 - d) % 4
+                    where = (d % 2) * 512 + zh * 128
+                    piece = totals[d // 2][:, where : where + 128]
+                    moved = pltpu.roll(piece, ((source + 4 - zl) % 4) * 32, 1)
+                    made = jnp.where(group == source, moved, made)
+                to = (zh * 4 + zl) * 128
+                out[at, to : to + 128] = made.astype(BF16)
         return carry
 
     lax.fori_loop(0, 6, step, 0)
@@ -147,7 +153,7 @@
         (slice(0, 64), jnp.where(second, ahead[64:, :], ahead[:64, :]).astype(BF16)),
         (slice(64, 128), jnp.where(second, back[64:, :], back[:64, :]).astype(BF16)),
         (slice(128, 144), log_rows(closing)),
-        (slice(144, 160), jnp.transpose(tail[...].astype(F32))[112:128, :].astype(BF16)),
+        (slice(144, 160), tail[...]),
     )
     for at, part in parts:
         for copy in range(16):
@@ -183,25 +189,27 @@
     return ahead, back
 
 
-def level_kernel(position, gathered, inside, message, spare):
+def level_kernel(position, gathered, inside, message):
     ahead, back = scan_states(gathered, 16, position[0])
     inside[0:64, :] = ahead[0]
     inside[64:128, :] = back[0]
     inside[128:136, :] = jnp.broadcast_to(ahead[1], (8, 128))
     inside[136:144, :] = jnp.broadcast_to(back[1], (8, 128))
-    parts = (
+    parts = [
         (slice(0, 64), ahead[2].astype(BF16)),
         (slice(64, 128), back[2].astype(BF16)),
         (slice(128, 144), log_rows(ahead[3])),
-    )
+    ]
+    group = lax.broadcasted_iota(jnp.int32, (16, 128), 1) // 32
+    for y in range(4):
+        made = gathered[y, 144:160, :].astype(F32)
+        for zl in range(1, 4):
+            moved = pltpu.roll(gathered[zl * 4 + y, 144:160, :].astype(F32), zl * 32, 1)
+            made = jnp.where(group == zl, moved, made)
+        parts.append((slice(144 + y * 16, 160 + y * 16), made.astype(BF16)))
     for at, part in parts:
         for copy in range(4):
             message[copy, at, :] = part
-
-    for y in range(4):
-        for zl in range(4):
-            where = y * 512 + zl * 128
-            spare[:, where : where + 128] = gathered[zl * 4 + y, 144:160, :]
 
 
 def column_block(position, shift):
@@ -246,8 +254,9 @@
         highest = lax.Precision.HIGHEST
         s1 = lax.dot_general(ones, total, NT, precision=highest, preferred_element_type=F32)
         s2 = lax.dot_general(ones, total * total, NT, precision=highest, preferred_element_type=F32)
-        moments[0:1, i * rows : (i + 1) * rows] = s1[0:1]
-        moments[1:2, i * rows : (i + 1) * rows] = s2[0:1]
+        for copy in range(8):
+            moments[copy, 0:1, i * rows : (i + 1) * rows] = s1[0:1]
+            moments[copy, 1:2, i * rows : (i + 1) * rows] = s2[0:1]
 
 
 def within_kernel(
@@ -288,17 +297,16 @@
         within[at, :] = total
 
 
-def out_rows(y, rows, pieces, spare, write):
-    for shift, piece in enumerate(pieces):
-        lanes = column_block(y, shift)
+def out_part(y, rows, pieces, shifts, spare):
+    parts = []
+    for piece, shift in zip(pieces, shifts):
         part = lax.dot_general(rows[:, :240], piece[:, 256:496], NT, preferred_element_type=F32)
-        part = part + jnp.dot(rows[:, 240:], spare[:, lanes], preferred_element_type=F32)
-        write(lanes, part)
-
-
-def mixers_kernel(
-    core,
-    y,
+        left = spare[:, column_block(y, shift)]
+        parts.append(part + jnp.dot(rows[:, 240:], left, preferred_element_type=F32))
+    return jnp.concatenate(parts, axis=1)
+
+
+def heads_kernel(
     position,
     queries,
     gates,
@@ -308,17 +316,8 @@
     inside,
     start,
     head_gain,
-    convolved,
-    moments,
-    channel_gain,
-    p0,
-    p1,
-    p2,
-    p3,
+    heads,
     spare,
-    mine,
-    sent,
-    rows_in,
 ):
     ahead, back = scan_states(gathered, 4, position[0])
     forward = inside[0:64, :] + jnp.exp(inside[128:129, :]) * (
@@ -337,10 +336,6 @@
     forward, backward = diagonal_blocks(forward), diagonal_blocks(backward)
     logs = by_lane(running[...])
     closing = logs[767:768, :]
-    sums = moments[0]
-    for k in range(1, 8):
-        sums = sums + moments[k]
-    sums = jnp.transpose(jnp.concatenate([sums, jnp.zeros((6, 768), F32)], axis=0)) / DC
     rows = 128
     half = lane_is_second(rows)
 
@@ -351,9 +346,6 @@
 
     for i in range(6):
         at = slice(i * rows, (i + 1) * rows)
-        average, squares = sums[at, 0:1], sums[at, 1:2]
-        scaled = (convolved[at, :] - average) * lax.rsqrt(squares - average * average + EPSILON)
-        rows_in[at, 0:128] = jax.nn.silu(scaled * channel_gain[...]).astype(BF16)
         q = queries[at, :]
         log = logs[at, :]
         retained = (
@@ -364,7 +356,41 @@
         centred = retained - head_mean(retained)
         normed = centred * lax.rsqrt(head_mean(centred * centred) + EPSILON)
         gate = jax.nn.silu(gates[at, :].astype(F32))
-        rows_in[at, 128:256] = (normed * head_gain[...] * gate).astype(BF16)
+        heads[at, :] = (normed * head_gain[...] * gate).astype(BF16)
+    for y in range(4):
+        for zh in range(4):
+            where = y * 512 + zh * 128
+            spare[:, where : where + 128] = gathered[zh, 144 + y * 16 : 160 + y * 16, :]
+
+
+def mixers_kernel(
+    core,
+    y,
+    heads,
+    convolved,
+    moments,
+    channel_gain,
+    p0,
+    p1,
+    p2,
+    p3,
+    spare,
+    mine,
+    sent_a,
+    sent_b,
+    rows_in,
+):
+    sums = moments[0]
+    for k in range(1, 8):
+        sums = sums + moments[k]
+    sums = jnp.transpose(jnp.concatenate([sums, jnp.zeros((6, 768), F32)], axis=0)) / DC
+    rows = 128
+    for i in range(6):
+        at = slice(i * rows, (i + 1) * rows)
+        average, squares = sums[at, 0:1], sums[at, 1:2]
+        scaled = (convolved[at, :] - average) * lax.rsqrt(squares - average * average + EPSILON)
+        rows_in[at, 0:128] = jax.nn.silu(scaled * channel_gain[...]).astype(BF16)
+        rows_in[at, 128:256] = heads[at, :]
 
     def half_of(which):
         return jnp.concatenate(
@@ -376,18 +402,14 @@
         )
 
     mine[...] = half_of(core[0])
-
-    def write(lanes, part):
-        sent[:, lanes] = part.astype(BF16)
-
-    out_rows(y[0], half_of(1 - core[0]), (p0, p1, p2, p3), spare, write)
-
-
-def join_kernel(y, mine, arrived, p0, p1, p2, p3, spare, out):
-    def write(lanes, part):
-        out[:, lanes] = (part + arrived[:, lanes].astype(F32)).astype(BF16)
-
-    out_rows(y[0], mine[...], (p0, p1, p2, p3), spare, write)
+    other = half_of(1 - core[0])
+    sent_a[...] = out_part(y[0], other, (p0, p1), (0, 1), spare).astype(BF16)
+    sent_b[...] = out_part(y[0], other, (p2, p3), (2, 3), spare).astype(BF16)
+
+
+def join_kernel(shifts, y, mine, arrived, p0, p1, spare, out):
+    own = out_part(y[0], mine[...], (p0, p1), shifts, spare)
+    out[...] = (own + arrived[...].astype(F32)).astype(BF16)
 
 
 def ring(x, axis, shift):
@@ -433,7 +455,7 @@
     )
     shard = call(
         shard_kernel,
-        shape((32, 1024), BF16),
+        shape((32, 1008), BF16),
         (),
         (
             key_weight,
@@ -442,8 +464,8 @@
             branch_gate,
             query_weight,
             swish_weight,
-            output_conv,
-            output_heads,
+            output_conv.T,
+            output_heads.T,
         ),
     )
     normed = call(
@@ -451,9 +473,7 @@
     )
     shard, normed = lax.optimization_barrier((shard, normed))
     own = lax.all_to_all(normed, "x", 0, 0, tiled=True).reshape(448, 2048)
-    rows = lax.all_gather(shard, "zh", axis=0, tiled=True)
-    tail = rows[:, 896:]
-    rows = lax.all_gather(rows[:, :1008], "zl", axis=0, tiled=True)
+    rows = lax.all_gather(shard, ("zh", "zl"), axis=0, tiled=True)
     own, rows = lax.optimization_barrier((own, rows))
     other = ring(own, "c", 1)
     state_weight = copies(rows[:, :256], "y", 4).reshape(2048, 256)
@@ -467,64 +487,66 @@
 
     half = shape((768, 128), BF16)
     full = shape((768, 128), F32)
+    tail = jnp.pad(output_heads[112:], ((0, 0), (0, 96)))
     keys, values, sent = call(
         states_kernel,
         (half, half, shape((16, 160, 128), BF16)),
         (core,),
         (own, other, state_weight, running, tail),
     )
-    inside, sent, spare = call(
+    gathered = lax.all_to_all(sent, ("zl", "y"), 0, 0, tiled=True)
+    inside, sent = call(
         level_kernel,
-        (shape((144, 128), F32), shape((4, 144, 128), BF16), shape((16, 2048), BF16)),
+        (shape((144, 128), F32), shape((4, 208, 128), BF16)),
         (low,),
-        (lax.all_to_all(sent, ("zl", "y"), 0, 0, tiled=True),),
+        (gathered,),
     )
     gathered = lax.all_to_all(sent, "zh", 0, 0, tiled=True)
-
     convolved, moments = call(
         conv_kernel,
-        (full, shape((2, 768), F32)),
+        (full, shape((8, 2, 768), F32)),
         (core, y),
         (own, other, *gate_pieces, kernel_taps),
         scratch=(pltpu.VMEM((800, 128), F32),),
     )
-    moments = lax.all_gather(moments, ("x", "c"))
+    moments = lax.all_to_all(moments, ("x", "c"), 0, 0, tiled=True)
     queries, gates, within = call(
         within_kernel,
         (half, half, full),
         (core, y),
         (own, other, *rest_pieces, keys, values, running),
     )
-    mine, sent = call(
+    heads, spare = call(
+        heads_kernel,
+        (half, shape((16, 2048), BF16)),
+        (high,),
+        (queries, gates, within, running, gathered, inside, start, head_gain[None]),
+    )
+    p0, p1, p2, p3 = rest_pieces
+    mine, sent_a, sent_b = call(
         mixers_kernel,
-        (shape((384, 256), BF16), shape((384, 2048), BF16)),
-        (core, y, high),
-        (
-            queries,
-            gates,
-            within,
-            running,
-            gathered,
-            inside,
-            start,
-            head_gain[None],
-            convolved,
-            moments,
-            channel_gain[None],
-            *rest_pieces,
-            spare,
-        ),
+        (shape((384, 256), BF16), shape((384, 1024), BF16), shape((384, 1024), BF16)),
+        (core, y),
+        (heads, convolved, moments, channel_gain[None], *rest_pieces, spare),
         scratch=(pltpu.VMEM((768, 256), BF16),),
     )
-    arrived = ring(sent, "c", 1)
-    joined = call(
-        join_kernel,
-        shape((384, 2048), BF16),
-        (y,),
-        (mine, arrived, *rest_pieces, spare),
-    )
-    parts = lax.all_to_all(joined.reshape(4, 96, 2048), "x", 0, 0, tiled=True)
-    return call(last_kernel, shape((96, 2048), BF16), (), (parts,))
+    arrived_a = ring(sent_a, "c", 1)
+    arrived_b = ring(sent_b, "c", 1)
+
+    def join(shifts, *arrays):
+        made = call(
+            functools.partial(join_kernel, shifts),
+            shape((384, 1024), BF16),
+            (y,),
+            (mine, *arrays, spare),
+        )
+        return made.reshape(4, 96, 1024)
+
+    joined_a = join((0, 1), arrived_a, p0, p1)
+    parts_a = lax.all_to_all(joined_a, "x", 0, 0, tiled=True)
+    joined_b = join((2, 3), arrived_b, p2, p3)
+    parts_b = lax.all_to_all(joined_b, "x", 0, 0, tiled=True)
+    return call(last_kernel, shape((96, 2048), BF16), (y,), (parts_a, parts_b))
 
 
 def solution(mesh):

time: 222 us -> 234 us (1.054)
  the two profiles are of different devices: /device:TPU:1 before, /device:TPU:40 now
where the time goes in v1:
time: 234 us; the launch traced here: 233 us
  waiting for transfers between devices  63.9 us (27%)
  starting transfers between devices  61.3 us (26%)
  blocking collectives  55.7 us (24%)
  Pallas kernels  40.9 us (17%)
  local copies, waits for them, and re-layouts  9.3 us (4%)
    pallas_call x11, Pallas kernels, call(): pl.pallas_call(kernel, out_shape=out_shape, in_specs=[SMEM] * len(scalars...  40.9 us
    all_gather x1, blocking collectives, body(): rows = lax.all_gather(shard, ('zh', 'zl'), axis=0, tiled=True)  39.7 us
    ppermute x9, starting transfers between devices, ring(): lax.ppermute(x, axis, [(i, (i + shift) % count) for i in range(count)])  25.9 us
    ppermute x9, waiting for transfers between devices, ring(): lax.ppermute(x, axis, [(i, (i + shift) % count) for i in range(count)])  24.4 us
    all_to_all x1, waiting for transfers between devices, body(): gathered = lax.all_to_all(sent, ('zl', 'y'), 0, 0, tiled=True)  16.1 us
    all_to_all x1, blocking collectives, body(): parts_a = lax.all_to_all(joined_a, 'x', 0, 0, tiled=True)  16 us
    all_to_all x1, waiting for transfers between devices, copies(): lax.all_to_all(jnp.broadcast_to(x[None], (count, *x.shape)), axes, 0, 0,...  12.3 us
    all_to_all x1, waiting for transfers between devices, body(): parts_b = lax.all_to_all(joined_b, 'x', 0, 0, tiled=True)  8.71 us
  transfers between devices with their start and end apart: 16, of which 7 were waited for; matrix products, arithmetic and copies ran while one was open for 2% of the time, Pallas kernels for 10%

profile of v1, /device:TPU:40, one launch (start us, length us, event | category | flops | bytes accessed | tf_op | source)
XLA Modules:
  0.0 233.0 jit_solution(10605965755683375742)
XLA Ops:
  0.0 0.9 slice_select_fusion
  0.9 2.4 %collective-permute-start = (bf16[16,2048]{1,0:T(8,128)(2,1)S(1)}, bf16[16,2048]{1,0:T(8,128)(2,1)S(1)}, u32[]{:S(2)}, u32[]{:S(2)}) collective-permute-start(bf16[16,2048]{1,0:T(8,128)(2,1)S(1)} %slice_select_fusion), channel_id=1, source_target_pairs={{7,15},{15,23},{23,31},{31,39},{39,47},{47,55},{55,63},{63,71},{71... | collective-permute-start | bytes 196616 | tf_op jit(solution)/shard_map/ppermute | solution.py:450
  3.2 1.5 shard_map.145
  4.7 2.3 %collective-permute-done.edge = bf16[16,2048]{1,0:T(8,128)(2,1)S(1)} collective-permute-done((bf16[16,2048]{1,0:T(8,128)(2,1)S(1)}, bf16[16,2048]{1,0:T(8,128)(2,1)S(1)}, u32[]{:S(2)}, u32[]{:S(2)}) %collective-permute-start) | collective-permute-done | bytes 65568 | tf_op jit(solution)/shard_map/ppermute | solution.py:450
  7.0 0.6 copy-done.17
  7.7 3.4 %shard_map.146 = bf16[4,112,2048]{2,1,0:T(8,128)(2,1)} custom-call(bf16[96,2048]{1,0:T(8,128)(2,1)} %tokens.1, bf16[16,2048]{1,0:T(8,128)(2,1)} %copy-done.17, f32[1,2048]{1,0:T(1,128)} %bitcast.29), custom_call_target="tpu_custom_call" | custom-call | tf_op jit(solution)/shard_map/pallas_call | solution.py:24
  11.1 3.7 %all-to-all-start = ((bf16[4,112,2048]{2,1,0:T(8,128)(2,1)}), bf16[4,112,2048]{2,1,0:T(8,128)(2,1)S(1)}, u32[]{:S(2)}, u32[]{:S(2)}) async-start(bf16[4,112,2048]{2,1,0:T(8,128)(2,1)} %shard_map.146), calls=%async_computation | async-start | bytes 3670016 | tf_op jit(solution)/shard_map/all_to_all | solution.py:475
  14.8 39.7 %all_gather.3 = bf16[512,1008]{1,0:T(8,128)(2,1)S(1)} all-gather(bf16[32,1008]{1,0:T(8,128)(2,1)S(1)} %copy-done.11), channel_id=1, replica_groups=mesh['zh'=4,'zl'=4,'y'=4,'x'=4,'c'=2] {'zh','zl'}, dimensions={0}, use_global_device_ids=true | all-gather | bytes 1096704 | tf_op jit(solution)/shard_map/all_gather | solution.py:476
  54.5 0.0 all-to-all-done
  54.5 1.9 collective-permute-start.1
  56.5 0.0 copy-start.7
  56.5 0.0 copy-start.18
  56.5 0.0 copy-start.19
  56.5 1.1 broadcast_in_dim.32
  57.6 7.1 %all-to-all-start.1 = ((bf16[4,512,256]{2,1,0:T(8,128)(2,1)}), bf16[4,512,256]{2,1,0:T(8,128)(2,1)}, u32[]{:S(2)}, u32[]{:S(2)}) async-start(bf16[4,512,256]{2,1,0:T(8,128)(2,1)} %broadcast_in_dim.32), calls=%async_computation.1 | async-start | bytes 2097152 | tf_op jit(solution)/shard_map/all_to_all | solution.py:421
  64.7 0.1 slice.30
  64.7 0.6 reduce-window.6
  65.3 0.2 slice_reduce_fusion
  65.5 0.2 reduce-window.9
  65.7 0.1 add_bitcast_fusion
  65.8 0.6 concatenate.3.running
  66.4 0.1 copy.20
  66.4 0.6 pad.5.tail
  67.0 12.3 %all-to-all-done.1 = bf16[4,512,256]{2,1,0:T(8,128)(2,1)} async-done(((bf16[4,512,256]{2,1,0:T(8,128)(2,1)}), bf16[4,512,256]{2,1,0:T(8,128)(2,1)}, u32[]{:S(2)}, u32[]{:S(2)}) %all-to-all-start.1) | async-done | bytes 1048608 | tf_op jit(solution)/shard_map/all_to_all | solution.py:421
  79.3 0.0 collective-permute-done.1.other
  79.3 4.7 %shard_map.147 = (bf16[768,128]{1,0:T(8,128)(2,1)}, bf16[768,128]{1,0:T(8,128)(2,1)}, bf16[16,160,128]{2,1,0:T(8,128)(2,1)}) custom-call(s32[1]{0:T(128)} %bitcast.1.core, bf16[448,2048]{1,0:T(8,128)(2,1)} %bitcast.21, bf16[448,2048]{1,0:T(8,128)(2,1)} %collective-permute-done.1.other, bf16[2048,256]{1,0:T(8,128)(2,1)} %bitcast.7.weight, ...), custom_call_target="tpu_custom_call" | custom-call | tf_op jit(solution)/shard_map/pallas_call | solution.py:24
  84.0 6.7 %all-to-all-start.2 = ((bf16[16,160,128]{2,1,0:T(8,128)(2,1)}), bf16[16,160,128]{2,1,0:T(8,128)(2,1)S(1)}, u32[]{:S(2)}, u32[]{:S(2)}) async-start(bf16[16,160,128]{2,1,0:T(8,128)(2,1)} %get-tuple-element.33), calls=%async_computation.2 | async-start | bytes 1310720 | tf_op jit(solution)/shard_map/all_to_all | solution.py:497
  90.8 16.1 %all-to-all-done.2.gathered = bf16[16,160,128]{2,1,0:T(8,128)(2,1)S(1)} async-done(((bf16[16,160,128]{2,1,0:T(8,128)(2,1)}), bf16[16,160,128]{2,1,0:T(8,128)(2,1)S(1)}, u32[]{:S(2)}, u32[]{:S(2)}) %all-to-all-start.2) | async-done | bytes 655392 | tf_op jit(solution)/shard_map/all_to_all | solution.py:497
  106.9 0.8 copy-done.6
  107.8 2.0 shard_map.149
  109.7 6.3 %all-to-all-start.3 = ((bf16[4,208,128]{2,1,0:T(8,128)(2,1)}), bf16[4,208,128]{2,1,0:T(8,128)(2,1)S(1)}, u32[]{:S(2)}, u32[]{:S(2)}) async-start(bf16[4,208,128]{2,1,0:T(8,128)(2,1)} %get-tuple-element.34), calls=%async_computation.3 | async-start | bytes 425984 | tf_op jit(solution)/shard_map/all_to_all | solution.py:504
  116.0 3.5 %collective-permute-start.5 = (bf16[512,256]{1,0:T(8,128)(2,1)S(1)}, bf16[512,256]{1,0:T(8,128)(2,1)S(1)}, u32[]{:S(2)}, u32[]{:S(2)}) collective-permute-start(bf16[512,256]{1,0:T(8,128)(2,1)S(1)} %get-tuple-element.43.p0), channel_id=1, source_target_pairs={{0,8},{8,16},{16,24},{24,0},{1,9},{9,17},{17,25},{25,1},{2,10},{10... | collective-permute-start | bytes 786440 | tf_op jit(solution)/shard_map/ppermute | solution.py:417
  119.6 2.8 %collective-permute-start.2 = (bf16[512,496]{1,0:T(8,128)(2,1)S(1)}, bf16[512,496]{1,0:T(8,128)(2,1)S(1)}, u32[]{:S(2)}, u32[]{:S(2)}) collective-permute-start(bf16[512,496]{1,0:T(8,128)(2,1)S(1)} %slice.26.p0), channel_id=1, source_target_pairs={{0,8},{8,16},{16,24},{24,0},{1,9},{9,17},{17,25},{25,1},{2,10},{10... | collective-permute-start | bytes 1523720 | tf_op jit(solution)/shard_map/ppermute | solution.py:417
  122.4 3.5 %collective-permute-start.3 = (bf16[512,496]{1,0:T(8,128)(2,1)S(1)}, bf16[512,496]{1,0:T(8,128)(2,1)S(1)}, u32[]{:S(2)}, u32[]{:S(2)}) collective-permute-start(bf16[512,496]{1,0:T(8,128)(2,1)S(1)} %slice.26.p0), channel_id=1, source_target_pairs={{0,16},{8,24},{16,0},{24,8},{1,17},{9,25},{17,1},{25,9},{2,18},{10... | collective-permute-start | bytes 1523720 | tf_op jit(solution)/shard_map/ppermute | solution.py:417
  125.9 4.3 %collective-permute-start.4 = (bf16[512,496]{1,0:T(8,128)(2,1)S(1)}, bf16[512,496]{1,0:T(8,128)(2,1)S(1)}, u32[]{:S(2)}, u32[]{:S(2)}) collective-permute-start(bf16[512,496]{1,0:T(8,128)(2,1)S(1)} %slice.26.p0), channel_id=1, source_target_pairs={{0,24},{8,0},{16,8},{24,16},{1,25},{9,1},{17,9},{25,17},{2,26},{10... | collective-permute-start | bytes 1523720 | tf_op jit(solution)/shard_map/ppermute | solution.py:417
  130.2 2.0 collective-permute-start.6
  132.2 0.0 collective-permute-done.5.p1
  132.3 3.5 %collective-permute-start.7 = (bf16[512,256]{1,0:T(8,128)(2,1)S(1)}, bf16[512,256]{1,0:T(8,128)(2,1)S(1)}, u32[]{:S(2)}, u32[]{:S(2)}) collective-permute-start(bf16[512,256]{1,0:T(8,128)(2,1)S(1)} %get-tuple-element.43.p0), channel_id=1, source_target_pairs={{0,24},{8,0},{16,8},{24,16},{1,25},{9,1},{17,9},{25,17},{2,26},{10... | collective-permute-start | bytes 786440 | tf_op jit(solution)/shard_map/ppermute | solution.py:417
  135.8 21.6 %collective-permute-done.6.p2 = bf16[512,256]{1,0:T(8,128)(2,1)S(1)} collective-permute-done((bf16[512,256]{1,0:T(8,128)(2,1)S(1)}, bf16[512,256]{1,0:T(8,128)(2,1)S(1)}, u32[]{:S(2)}, u32[]{:S(2)}) %collective-permute-start.6) | collective-permute-done | bytes 262176 | tf_op jit(solution)/shard_map/ppermute | solution.py:417
  157.4 2.7 %collective-permute-done.7.p3 = bf16[512,256]{1,0:T(8,128)(2,1)S(1)} collective-permute-done((bf16[512,256]{1,0:T(8,128)(2,1)S(1)}, bf16[512,256]{1,0:T(8,128)(2,1)S(1)}, u32[]{:S(2)}, u32[]{:S(2)}) %collective-permute-start.7) | collective-permute-done | bytes 262176 | tf_op jit(solution)/shard_map/ppermute | solution.py:417
  160.0 0.7 copy-done.14
  160.8 5.6 %shard_map.151 = (f32[768,128]{1,0:T(8,128)}, f32[8,2,768]{2,1,0:T(2,128)}) custom-call(s32[1]{0:T(128)} %bitcast.1.core, s32[1]{0:T(128)} %bitcast.y, bf16[448,2048]{1,0:T(8,128)(2,1)} %bitcast.22, bf16[448,2048]{1,0:T(8,128)(2,1)} %collective-permute-done.1.other, bf16[512,256]{1,0:T(8,128)(2,1)} %copy-done.7, bf16[512,256]{1,0:T(8,128)(2,1)} %copy-done.12, ...), custom_call_target="tpu_custom_call" | custom-call | tf_op jit(solution)/shard_map/pallas_call | solution.py:24
  166.4 0.0 all-to-all-done.3.gathered
  166.4 4.6 %all-to-all-start.4 = ((f32[8,2,768]{2,1,0:T(2,128)}), f32[8,2,768]{2,1,0:T(2,128)S(1)}, u32[]{:S(2)}, u32[]{:S(2)}) async-start(f32[8,2,768]{2,1,0:T(2,128)} %get-tuple-element.38), calls=%async_computation.4 | async-start | bytes 98304 | tf_op jit(solution)/shard_map/all_to_all | solution.py:512
  171.0 0.1 copy.19
  171.1 0.8 reshape.30.start
  171.9 0.8 copy-done.2
  172.7 0.2 copy-done.3
  172.9 0.2 copy-done.4
  173.0 6.6 %shard_map.148 = (bf16[768,128]{1,0:T(8,128)(2,1)}, bf16[768,128]{1,0:T(8,128)(2,1)}, f32[768,128]{1,0:T(8,128)}) custom-call(s32[1]{0:T(128)} %bitcast.1.core, s32[1]{0:T(128)} %bitcast.y, bf16[448,2048]{1,0:T(8,128)(2,1)} %bitcast.23, bf16[448,2048]{1,0:T(8,128)(2,1)} %collective-permute-done.1.other, bf16[512,496]{1,0:T(8,128)(2,1)} %copy-done.1, ...), custom_call_target="tpu_custom_call" | custom-call | tf_op jit(solution)/shard_map/pallas_call | solution.py:24
  179.6 3.3 %shard_map.150 = (bf16[768,128]{1,0:T(8,128)(2,1)}, bf16[16,2048]{1,0:T(8,128)(2,1)}) custom-call(s32[1]{0:T(128)} %bitcast.2.position, bf16[768,128]{1,0:T(8,128)(2,1)} %get-tuple-element.30.queries, bf16[768,128]{1,0:T(8,128)(2,1)} %get-tuple-element.31.gates, f32[768,128]{1,0:T(8,128)} %get-tuple-element.32.within, f32[8,768]{1,0:T(8,128)} %concatenate.3.running, ...), custom_call_target="tpu_custom_call" | custom-call | tf_op jit(solution)/shard_map/pallas_call | solution.py:24
  183.0 0.6 copy-done.15
  183.6 4.3 %shard_map.152 = (bf16[384,256]{1,0:T(8,128)(2,1)}, bf16[384,1024]{1,0:T(8,128)(2,1)}, bf16[384,1024]{1,0:T(8,128)(2,1)}) custom-call(s32[1]{0:T(128)} %bitcast.1.core, s32[1]{0:T(128)} %bitcast.y, bf16[768,128]{1,0:T(8,128)(2,1)} %get-tuple-element.36.heads, f32[768,128]{1,0:T(8,128)} %get-tuple-element.37.convolved, f32[8,2,768]{2,1,0:T(2,128)} %copy-done.15, ...), custom_call_target="tpu_custom_call" | custom-call | tf_op jit(solution)/shard_map/pallas_call | solution.py:24
  187.8 2.4 %collective-permute-start.9 = (bf16[384,1024]{1,0:T(8,128)(2,1)}, bf16[384,1024]{1,0:T(8,128)(2,1)S(1)}, u32[]{:S(2)}, u32[]{:S(2)}) collective-permute-start(bf16[384,1024]{1,0:T(8,128)(2,1)} %get-tuple-element.42), channel_id=1, source_target_pairs={{0,1},{1,0},{2,3},{3,2},{4,5},{5,4},{6,7},{7,6},{8,9},{9,8},{10,11... | collective-permute-start | bytes 2359304 | tf_op jit(solution)/shard_map/ppermute | solution.py:417
  190.2 1.9 collective-permute-start.8
  192.2 0.2 collective-permute-done.9.arrived
  192.3 0.9 copy-done.10
  193.2 3.0 %shard_map.154 = bf16[384,1024]{1,0:T(8,128)(2,1)} custom-call(s32[1]{0:T(128)} %bitcast.y, bf16[384,256]{1,0:T(8,128)(2,1)} %get-tuple-element.40.mine, bf16[384,1024]{1,0:T(8,128)(2,1)} %copy-done.10, bf16[512,496]{1,0:T(8,128)(2,1)} %copy-done.3, bf16[512,496]{1,0:T(8,128)(2,1)} %copy-done.4, bf16[16,2048]{1,0:T(8,128)(2,1)} %get-tuple-element.39.spare), custom_call_target="tpu_custom_call" | custom-call | tf_op jit(solution)/shard_map/pallas_call | solution.py:24
  196.2 4.7 %all-to-all-start.6 = ((bf16[4,96,1024]{2,1,0:T(8,128)(2,1)}), bf16[4,96,1024]{2,1,0:T(8,128)(2,1)S(1)}, u32[]{:S(2)}, u32[]{:S(2)}) async-start(bf16[4,96,1024]{2,1,0:T(8,128)(2,1)} %bitcast.24), calls=%async_computation.6 | async-start | bytes 1572864 | tf_op jit(solution)/shard_map/all_to_all | solution.py:548
  200.9 0.9 copy-done.9
  201.8 3.0 %shard_map.153 = bf16[384,1024]{1,0:T(8,128)(2,1)} custom-call(s32[1]{0:T(128)} %bitcast.y, bf16[384,256]{1,0:T(8,128)(2,1)} %get-tuple-element.40.mine, bf16[384,1024]{1,0:T(8,128)(2,1)} %copy-done.9, bf16[512,496]{1,0:T(8,128)(2,1)} %copy-done.1, bf16[512,496]{1,0:T(8,128)(2,1)} %copy-done.2, bf16[16,2048]{1,0:T(8,128)(2,1)} %get-tuple-element.39.spare), custom_call_target="tpu_custom_call" | custom-call | tf_op jit(solution)/shard_map/pallas_call | solution.py:24
  204.8 8.7 %all-to-all-done.6.parts_b = bf16[4,96,1024]{2,1,0:T(8,128)(2,1)S(1)} async-done(((bf16[4,96,1024]{2,1,0:T(8,128)(2,1)}), bf16[4,96,1024]{2,1,0:T(8,128)(2,1)S(1)}, u32[]{:S(2)}, u32[]{:S(2)}) %all-to-all-start.6) | async-done | bytes 786464 | tf_op jit(solution)/shard_map/all_to_all | solution.py:548
  213.5 16.0 %all_to_all.35.parts_a = bf16[4,96,1024]{2,1,0:T(8,128)(2,1)} all-to-all(bf16[4,96,1024]{2,1,0:T(8,128)(2,1)} %bitcast.25), channel_id=1, replica_groups=mesh['zh'=4,'zl'=4,'y'=4,'x'=4,'c'=2] {'x'}, dimensions={0} | all-to-all | bytes 1572864 | tf_op jit(solution)/shard_map/all_to_all | solution.py:546
  229.5 3.5 %shard_map.155 = bf16[96,2048]{1,0:T(8,128)(2,1)} custom-call(s32[1]{0:T(128)} %bitcast.y, bf16[4,96,1024]{2,1,0:T(8,128)(2,1)} %all_to_all.35.parts_a, bf16[4,96,1024]{2,1,0:T(8,128)(2,1)} %copy-done.5), custom_call_target="tpu_custom_call" | custom-call | tf_op jit(solution)/shard_map/pallas_call | solution.py:24
  (37 shorter events, 0.2 us)
Async XLA Ops:
  0.9 6.2 %collective-permute-start = (bf16[16,2048]{1,0:T(8,128)(2,1)S(1)}, bf16[16,2048]{1,0:T(8,128)(2,1)S(1)}, u32[]{:S(2)}, u32[]{:S(2)}) collective-permute-start(bf16[16,2048]{1,0:T(8,128)(2,1)S(1)} %slice_select_fusion), channel_id=1, source_target_pairs={{7,15},{15,23},{23,31},{31,39},{39,47},{47,55},{55,63},{63,71},{71... | collective-permute-start | bytes 196616 | tf_op jit(solution)/shard_map/ppermute | solution.py:450
  7.0 0.6 copy-start.17
  11.1 3.7 %copy-start.11 = (bf16[32,1008]{1,0:T(8,128)(2,1)S(1)}, bf16[32,1008]{1,0:T(8,128)(2,1)}, u32[]{:S(2)}) copy-start(bf16[32,1008]{1,0:T(8,128)(2,1)} %shard_map.145) | copy-start | bytes 193540
  11.1 43.5 %all-to-all-start = ((bf16[4,112,2048]{2,1,0:T(8,128)(2,1)}), bf16[4,112,2048]{2,1,0:T(8,128)(2,1)S(1)}, u32[]{:S(2)}, u32[]{:S(2)}) async-start(bf16[4,112,2048]{2,1,0:T(8,128)(2,1)} %shard_map.146), calls=%async_computation | async-start | bytes 3670016 | tf_op jit(solution)/shard_map/all_to_all | solution.py:475
  54.5 3.1 %copy-start = (bf16[4,112,2048]{2,1,0:T(8,128)(2,1)}, bf16[4,112,2048]{2,1,0:T(8,128)(2,1)S(1)}, u32[]{:S(2)}) copy-start(bf16[4,112,2048]{2,1,0:T(8,128)(2,1)S(1)} %all-to-all-done) | copy-start | bytes 5505028
  54.5 24.8 %collective-permute-start.1 = (bf16[448,2048]{1,0:T(8,128)(2,1)S(1)}, bf16[448,2048]{1,0:T(8,128)(2,1)}, u32[]{:S(2)}, u32[]{:S(2)}) collective-permute-start(bf16[448,2048]{1,0:T(8,128)(2,1)S(1)} %bitcast.20), channel_id=1, source_target_pairs={{0,1},{1,0},{2,3},{3,2},{4,5},{5,4},{6,7},{7,6},{8,9},{9,8},{10,11... | collective-permute-start | bytes 5505032 | tf_op jit(solution)/shard_map/ppermute | solution.py:417
  56.5 75.8 %copy-start.7 = (bf16[512,256]{1,0:T(8,128)(2,1)}, bf16[512,256]{1,0:T(8,128)(2,1)S(1)}, u32[]{:S(2)}) copy-start(bf16[512,256]{1,0:T(8,128)(2,1)S(1)} %get-tuple-element.43.p0) | copy-start | bytes 786436
  56.5 8.2 %copy-start.18 = (bf16[128,32]{0,1:T(8,128)(2,1)S(1)}, bf16[128,32]{0,1:T(8,128)(2,1)}, u32[]{:S(2)}) copy-start(bf16[128,32]{0,1:T(8,128)(2,1)} %param.29) | copy-start | bytes 24580
  56.5 8.2 %copy-start.19 = (f32[2,768]{1,0:T(2,128)S(1)}, f32[2,768]{1,0:T(2,128)}, u32[]{:S(2)}) copy-start(f32[2,768]{1,0:T(2,128)} %param.25) | copy-start | bytes 18436
  57.6 21.7 %all-to-all-start.1 = ((bf16[4,512,256]{2,1,0:T(8,128)(2,1)}), bf16[4,512,256]{2,1,0:T(8,128)(2,1)}, u32[]{:S(2)}, u32[]{:S(2)}) async-start(bf16[4,512,256]{2,1,0:T(8,128)(2,1)} %broadcast_in_dim.32), calls=%async_computation.1 | async-start | bytes 2097152 | tf_op jit(solution)/shard_map/all_to_all | solution.py:421
  84.0 22.9 %all-to-all-start.2 = ((bf16[16,160,128]{2,1,0:T(8,128)(2,1)}), bf16[16,160,128]{2,1,0:T(8,128)(2,1)S(1)}, u32[]{:S(2)}, u32[]{:S(2)}) async-start(bf16[16,160,128]{2,1,0:T(8,128)(2,1)} %get-tuple-element.33), calls=%async_computation.2 | async-start | bytes 1310720 | tf_op jit(solution)/shard_map/all_to_all | solution.py:497
  106.9 0.8 copy-start.6
  109.7 56.7 %all-to-all-start.3 = ((bf16[4,208,128]{2,1,0:T(8,128)(2,1)}), bf16[4,208,128]{2,1,0:T(8,128)(2,1)S(1)}, u32[]{:S(2)}, u32[]{:S(2)}) async-start(bf16[4,208,128]{2,1,0:T(8,128)(2,1)} %get-tuple-element.34), calls=%async_computation.3 | async-start | bytes 425984 | tf_op jit(solution)/shard_map/all_to_all | solution.py:504
  116.0 16.2 %collective-permute-start.5 = (bf16[512,256]{1,0:T(8,128)(2,1)S(1)}, bf16[512,256]{1,0:T(8,128)(2,1)S(1)}, u32[]{:S(2)}, u32[]{:S(2)}) collective-permute-start(bf16[512,256]{1,0:T(8,128)(2,1)S(1)} %get-tuple-element.43.p0), channel_id=1, source_target_pairs={{0,8},{8,16},{16,24},{24,0},{1,9},{9,17},{17,25},{25,1},{2,10},{10... | collective-permute-start | bytes 786440 | tf_op jit(solution)/shard_map/ppermute | solution.py:417
  119.6 46.8 %copy-start.1 = (bf16[512,496]{1,0:T(8,128)(2,1)}, bf16[512,496]{1,0:T(8,128)(2,1)S(1)}, u32[]{:S(2)}) copy-start(bf16[512,496]{1,0:T(8,128)(2,1)S(1)} %slice.26.p0) | copy-start | bytes 1523716
  119.6 52.3 %collective-permute-start.2 = (bf16[512,496]{1,0:T(8,128)(2,1)S(1)}, bf16[512,496]{1,0:T(8,128)(2,1)S(1)}, u32[]{:S(2)}, u32[]{:S(2)}) collective-permute-start(bf16[512,496]{1,0:T(8,128)(2,1)S(1)} %slice.26.p0), channel_id=1, source_target_pairs={{0,8},{8,16},{16,24},{24,0},{1,9},{9,17},{17,25},{25,1},{2,10},{10... | collective-permute-start | bytes 1523720 | tf_op jit(solution)/shard_map/ppermute | solution.py:417
  122.4 49.5 %collective-permute-start.3 = (bf16[512,496]{1,0:T(8,128)(2,1)S(1)}, bf16[512,496]{1,0:T(8,128)(2,1)S(1)}, u32[]{:S(2)}, u32[]{:S(2)}) collective-permute-start(bf16[512,496]{1,0:T(8,128)(2,1)S(1)} %slice.26.p0), channel_id=1, source_target_pairs={{0,16},{8,24},{16,0},{24,8},{1,17},{9,25},{17,1},{25,9},{2,18},{10... | collective-permute-start | bytes 1523720 | tf_op jit(solution)/shard_map/ppermute | solution.py:417
  125.9 46.0 %collective-permute-start.4 = (bf16[512,496]{1,0:T(8,128)(2,1)S(1)}, bf16[512,496]{1,0:T(8,128)(2,1)S(1)}, u32[]{:S(2)}, u32[]{:S(2)}) collective-permute-start(bf16[512,496]{1,0:T(8,128)(2,1)S(1)} %slice.26.p0), channel_id=1, source_target_pairs={{0,24},{8,0},{16,8},{24,16},{1,25},{9,1},{17,9},{25,17},{2,26},{10... | collective-permute-start | bytes 1523720 | tf_op jit(solution)/shard_map/ppermute | solution.py:417
  130.2 27.1 %collective-permute-start.6 = (bf16[512,256]{1,0:T(8,128)(2,1)S(1)}, bf16[512,256]{1,0:T(8,128)(2,1)S(1)}, u32[]{:S(2)}, u32[]{:S(2)}) collective-permute-start(bf16[512,256]{1,0:T(8,128)(2,1)S(1)} %get-tuple-element.43.p0), channel_id=1, source_target_pairs={{0,16},{8,24},{16,0},{24,8},{1,17},{9,25},{17,1},{25,9},{2,18},{10... | collective-permute-start | bytes 786440 | tf_op jit(solution)/shard_map/ppermute | solution.py:417
  132.3 27.8 %copy-start.12 = (bf16[512,256]{1,0:T(8,128)(2,1)}, bf16[512,256]{1,0:T(8,128)(2,1)S(1)}, u32[]{:S(2)}) copy-start(bf16[512,256]{1,0:T(8,128)(2,1)S(1)} %collective-permute-done.5.p1) | copy-start | bytes 786436
  132.3 27.8 %collective-permute-start.7 = (bf16[512,256]{1,0:T(8,128)(2,1)S(1)}, bf16[512,256]{1,0:T(8,128)(2,1)S(1)}, u32[]{:S(2)}, u32[]{:S(2)}) collective-permute-start(bf16[512,256]{1,0:T(8,128)(2,1)S(1)} %get-tuple-element.43.p0), channel_id=1, source_target_pairs={{0,24},{8,0},{16,8},{24,16},{1,25},{9,1},{17,9},{25,17},{2,26},{10... | collective-permute-start | bytes 786440 | tf_op jit(solution)/shard_map/ppermute | solution.py:417
  157.4 2.7 %copy-start.13 = (bf16[512,256]{1,0:T(8,128)(2,1)}, bf16[512,256]{1,0:T(8,128)(2,1)S(1)}, u32[]{:S(2)}) copy-start(bf16[512,256]{1,0:T(8,128)(2,1)S(1)} %collective-permute-done.6.p2) | copy-start | bytes 786436
  160.0 0.7 copy-start.14
  160.8 10.2 %copy-start.16 = (f32[2,2,64,64]{3,2,1,0:T(8,128)S(1)}, f32[2,2,64,64]{3,2,1,0:T(8,128)}, u32[]{:S(2)}) copy-start(f32[2,2,64,64]{3,2,1,0:T(8,128)} %param.26) | copy-start | bytes 196612
  166.4 13.2 %copy-start.8 = (bf16[4,208,128]{2,1,0:T(8,128)(2,1)}, bf16[4,208,128]{2,1,0:T(8,128)(2,1)S(1)}, u32[]{:S(2)}) copy-start(bf16[4,208,128]{2,1,0:T(8,128)(2,1)S(1)} %all-to-all-done.3.gathered) | copy-start | bytes 638980
  166.4 16.5 %all-to-all-start.4 = ((f32[8,2,768]{2,1,0:T(2,128)}), f32[8,2,768]{2,1,0:T(2,128)S(1)}, u32[]{:S(2)}, u32[]{:S(2)}) async-start(f32[8,2,768]{2,1,0:T(2,128)} %get-tuple-element.38), calls=%async_computation.4 | async-start | bytes 98304 | tf_op jit(solution)/shard_map/all_to_all | solution.py:512
  171.9 0.8 copy-start.2
  171.9 1.0 copy-start.3
  171.9 1.1 copy-start.4
  183.0 0.6 copy-start.15
  187.8 4.5 %collective-permute-start.9 = (bf16[384,1024]{1,0:T(8,128)(2,1)}, bf16[384,1024]{1,0:T(8,128)(2,1)S(1)}, u32[]{:S(2)}, u32[]{:S(2)}) collective-permute-start(bf16[384,1024]{1,0:T(8,128)(2,1)} %get-tuple-element.42), channel_id=1, source_target_pairs={{0,1},{1,0},{2,3},{3,2},{4,5},{5,4},{6,7},{7,6},{8,9},{9,8},{10,11... | collective-permute-start | bytes 2359304 | tf_op jit(solution)/shard_map/ppermute | solution.py:417
  190.2 10.7 %collective-permute-start.8 = (bf16[384,1024]{1,0:T(8,128)(2,1)}, bf16[384,1024]{1,0:T(8,128)(2,1)S(1)}, u32[]{:S(2)}, u32[]{:S(2)}) collective-permute-start(bf16[384,1024]{1,0:T(8,128)(2,1)} %get-tuple-element.41), channel_id=1, source_target_pairs={{0,1},{1,0},{2,3},{3,2},{4,5},{5,4},{6,7},{7,6},{8,9},{9,8},{10,11... | collective-permute-start | bytes 2359304 | tf_op jit(solution)/shard_map/ppermute | solution.py:417
  192.3 0.9 copy-start.10
  196.2 17.3 %all-to-all-start.6 = ((bf16[4,96,1024]{2,1,0:T(8,128)(2,1)}), bf16[4,96,1024]{2,1,0:T(8,128)(2,1)S(1)}, u32[]{:S(2)}, u32[]{:S(2)}) async-start(bf16[4,96,1024]{2,1,0:T(8,128)(2,1)} %bitcast.24), calls=%async_computation.6 | async-start | bytes 1572864 | tf_op jit(solution)/shard_map/all_to_all | solution.py:548
  200.9 0.9 copy-start.9
  213.5 16.0 %copy-start.5 = (bf16[4,96,1024]{2,1,0:T(8,128)(2,1)}, bf16[4,96,1024]{2,1,0:T(8,128)(2,1)S(1)}, u32[]{:S(2)}) copy-start(bf16[4,96,1024]{2,1,0:T(8,128)(2,1)S(1)} %all-to-all-done.6.parts_b) | copy-start | bytes 2359300

commit v2 on v1

--- a/solution.py
+++ b/solution.py
@@ -1,5 +1,3 @@
-import functools
-
 import jax
 import jax.numpy as jnp
 from jax import lax
@@ -25,9 +23,9 @@
         kernel,
         out_shape=out_shape,
         in_specs=[SMEM] * len(scalars) + [VMEM] * len(arrays),
-        out_specs=jax.tree.map(lambda _: VMEM, out_shape),
+        out_specs=[VMEM] * len(out_shape) if isinstance(out_shape, tuple) else VMEM,
         scratch_shapes=scratch,
-        compiler_params=pltpu.CompilerParams(vmem_limit_bytes=56 * 1024 * 1024),
+        compiler_params=pltpu.CompilerParams(vmem_limit_bytes=20 * 1024 * 1024),
     )(*scalars, *arrays)
 
 
@@ -84,32 +82,27 @@
     block(edge, slice(0, 16), slice(96, 112))
 
 
-def last_kernel(y, parts_a, parts_b, out):
+def last_kernel(parts, out):
     rows = 16
-    group = lax.broadcasted_iota(jnp.int32, (rows, 128), 1) // 32
 
     def step(i, carry):
         at = pl.ds(pl.multiple_of(i * rows, rows), rows)
-        totals = []
-        for parts in (parts_a, parts_b):
-            total = parts[0, at, :].astype(F32)
-            for k in range(1, 4):
-                total = total + parts[k, at, :].astype(F32)
-            totals.append(total)
-        for zh in range(4):
-            for zl in range(4):
-                made = jnp.zeros((rows, 128), F32)
-                for d in range(4):
-                    source = (y[0] + 4 - d) % 4
-                    where = (d % 2) * 512 + zh * 128
-                    piece = totals[d // 2][:, where : where + 128]
-                    moved = pltpu.roll(piece, ((source + 4 - zl) % 4) * 32, 1)
-                    made = jnp.where(group == source, moved, made)
-                to = (zh * 4 + zl) * 128
-                out[at, to : to + 128] = made.astype(BF16)
+        total = parts[0, at, :].astype(F32)
+        for k in range(1, 4):
+            total = total + parts[k, at, :].astype(F32)
+
+        def read(zh, y):
+            where = (y * 4 + zh) * 128
+            return total[:, where : where + 128]
+
+        def write(zh, zl, made):
+            where = (zh * 4 + zl) * 128
+            out[at, where : where + 128] = made.astype(BF16)
+
+        swap_groups(read, write, rows)
         return carry
 
-    lax.fori_loop(0, 6, step, 0)
+    lax.fori_loop(0, 6, step, 0, unroll=2)
 
 
 def lane_is_second(rows):
@@ -254,9 +247,8 @@
         highest = lax.Precision.HIGHEST
         s1 = lax.dot_general(ones, total, NT, precision=highest, preferred_element_type=F32)
         s2 = lax.dot_general(ones, total * total, NT, precision=highest, preferred_element_type=F32)
-        for copy in range(8):
-            moments[copy, 0:1, i * rows : (i + 1) * rows] = s1[0:1]
-            moments[copy, 1:2, i * rows : (i + 1) * rows] = s2[0:1]
+        moments[0:1, i * rows : (i + 1) * rows] = s1[0:1]
+        moments[1:2, i * rows : (i + 1) * rows] = s2[0:1]
 
 
 def within_kernel(
@@ -297,13 +289,12 @@
         within[at, :] = total
 
 
-def out_part(y, rows, pieces, shifts, spare):
-    parts = []
-    for piece, shift in zip(pieces, shifts):
+def out_rows(y, rows, pieces, spare, write):
+    for shift, piece in enumerate(pieces):
+        lanes = column_block(y, shift)
         part = lax.dot_general(rows[:, :240], piece[:, 256:496], NT, preferred_element_type=F32)
-        left = spare[:, column_block(y, shift)]
-        parts.append(part + jnp.dot(rows[:, 240:], left, preferred_element_type=F32))
-    return jnp.concatenate(parts, axis=1)
+        part = part + jnp.dot(rows[:, 240:], spare[:, lanes], preferred_element_type=F32)
+        write(lanes, part)
 
 
 def heads_kernel(
@@ -376,8 +367,7 @@
     p3,
     spare,
     mine,
-    sent_a,
-    sent_b,
+    sent,
     rows_in,
 ):
     sums = moments[0]
@@ -402,14 +392,18 @@
         )
 
     mine[...] = half_of(core[0])
-    other = half_of(1 - core[0])
-    sent_a[...] = out_part(y[0], other, (p0, p1), (0, 1), spare).astype(BF16)
-    sent_b[...] = out_part(y[0], other, (p2, p3), (2, 3), spare).astype(BF16)
-
-
-def join_kernel(shifts, y, mine, arrived, p0, p1, spare, out):
-    own = out_part(y[0], mine[...], (p0, p1), shifts, spare)
-    out[...] = (own + arrived[...].astype(F32)).astype(BF16)
+
+    def write(lanes, part):
+        sent[:, lanes] = part.astype(BF16)
+
+    out_rows(y[0], half_of(1 - core[0]), (p0, p1, p2, p3), spare, write)
+
+
+def join_kernel(y, mine, arrived, p0, p1, p2, p3, spare, out):
+    def write(lanes, part):
+        out[:, lanes] = (part + arrived[:, lanes].astype(F32)).astype(BF16)
+
+    out_rows(y[0], mine[...], (p0, p1, p2, p3), spare, write)
 
 
 def ring(x, axis, shift):
@@ -504,12 +498,12 @@
     gathered = lax.all_to_all(sent, "zh", 0, 0, tiled=True)
     convolved, moments = call(
         conv_kernel,
-        (full, shape((8, 2, 768), F32)),
+        (full, shape((2, 768), F32)),
         (core, y),
         (own, other, *gate_pieces, kernel_taps),
         scratch=(pltpu.VMEM((800, 128), F32),),
     )
-    moments = lax.all_to_all(moments, ("x", "c"), 0, 0, tiled=True)
+    moments = lax.all_gather(moments, ("x", "c"))
     queries, gates, within = call(
         within_kernel,
         (half, half, full),
@@ -522,31 +516,22 @@
         (high,),
         (queries, gates, within, running, gathered, inside, start, head_gain[None]),
     )
-    p0, p1, p2, p3 = rest_pieces
-    mine, sent_a, sent_b = call(
+    mine, sent = call(
         mixers_kernel,
-        (shape((384, 256), BF16), shape((384, 1024), BF16), shape((384, 1024), BF16)),
+        (shape((384, 256), BF16), shape((384, 2048), BF16)),
         (core, y),
         (heads, convolved, moments, channel_gain[None], *rest_pieces, spare),
         scratch=(pltpu.VMEM((768, 256), BF16),),
     )
-    arrived_a = ring(sent_a, "c", 1)
-    arrived_b = ring(sent_b, "c", 1)
-
-    def join(shifts, *arrays):
-        made = call(
-            functools.partial(join_kernel, shifts),
-            shape((384, 1024), BF16),
-            (y,),
-            (mine, *arrays, spare),
-        )
-        return made.reshape(4, 96, 1024)
-
-    joined_a = join((0, 1), arrived_a, p0, p1)
-    parts_a = lax.all_to_all(joined_a, "x", 0, 0, tiled=True)
-    joined_b = join((2, 3), arrived_b, p2, p3)
-    parts_b = lax.all_to_all(joined_b, "x", 0, 0, tiled=True)
-    return call(last_kernel, shape((96, 2048), BF16), (y,), (parts_a, parts_b))
+    arrived = ring(sent, "c", 1)
+    joined = call(
+        join_kernel,
+        shape((384, 2048), BF16),
+        (y,),
+        (mine, arrived, *rest_pieces, spare),
+    )
+    parts = lax.all_to_all(joined.reshape(4, 96, 2048), "x", 0, 0, tiled=True)
+    return call(last_kernel, shape((96, 2048), BF16), (), (parts,))
 
 
 def solution(mesh):

time: 234 us -> 234 us (level)
  blocking collectives: 55.7 us -> 78.3 us
  Pallas kernels: 40.9 us -> 23.3 us
  local copies, waits for them, and re-layouts: 9.3 us -> 24.9 us
  starting transfers between devices: 61.3 us -> 50.2 us
  waiting for transfers between devices: 63.9 us -> 53.8 us
    pallas_call x11 -> x10, Pallas kernels: 40.9 us -> 23.3 us  [call(): pl.pallas_call(kernel, out_shape=out_shape, in_specs=[SMEM] * len(scalars...]
    all_gather x0 -> x1, blocking collectives: none -> 13.5 us  [body(): moments = lax.all_gather(moments, ('x', 'c'))]
    unnamed x42 -> x68, local copies, waits for them, and re-layouts: 5.83 us -> 19.1 us
    all_to_all x2 -> x0, starting transfers between devices: 9.27 us -> none  [the longest x1 4.68 us: body(): parts_b = lax.all_to_all(joined_b, 'x', 0, 0, tiled=True)]
    all_to_all x1, blocking collectives: 16 us -> 24.9 us  [body(): parts = lax.all_to_all(joined.reshape(4, 96, 2048), 'x', 0, 0, tiled=True)]
    all_to_all x2 -> x0, waiting for transfers between devices: 8.71 us -> none  [the longest x1 8.71 us: body(): parts_b = lax.all_to_all(joined_b, 'x', 0, 0, tiled=True)]
    ppermute x9 -> x8, starting transfers between devices: 25.9 us -> 23.8 us  [ring(): lax.ppermute(x, axis, [(i, (i + shift) % count) for i in range(count)])]
    ppermute x9 -> x8, waiting for transfers between devices: 24.4 us -> 24 us  [ring(): lax.ppermute(x, axis, [(i, (i + shift) % count) for i in range(count)])]
  transfers between devices with their start and end apart: 16 -> 13, of which waited for: 7 -> 5; matrix products, arithmetic and copies ran while one was open for 2% -> 3% of each run, Pallas kernels for 10% -> 4%
where the time goes in v2:
time: 234 us; the launch traced here: 233 us
  blocking collectives  78.3 us (33%)
  waiting for transfers between devices  53.8 us (23%)
  starting transfers between devices  50.2 us (21%)
  local copies, waits for them, and re-layouts  24.9 us (11%)
  Pallas kernels  23.3 us (10%)
    all_gather x1, blocking collectives, body(): rows = lax.all_gather(shard, ('zh', 'zl'), axis=0, tiled=True)  40 us
    all_to_all x1, blocking collectives, body(): parts = lax.all_to_all(joined.reshape(4, 96, 2048), 'x', 0, 0, tiled=True)  24.9 us
    ppermute x8, waiting for transfers between devices, ring(): lax.ppermute(x, axis, [(i, (i + shift) % count) for i in range(count)])  24 us
    ppermute x8, starting transfers between devices, ring(): lax.ppermute(x, axis, [(i, (i + shift) % count) for i in range(count)])  23.8 us
    pallas_call x10, Pallas kernels, call(): pl.pallas_call(kernel, out_shape=out_shape, in_specs=[SMEM] * len(scalars...  23.3 us
    unnamed x68, local copies, waits for them, and re-layouts  19.1 us
    all_to_all x1, waiting for transfers between devices, body(): gathered = lax.all_to_all(sent, ('zl', 'y'), 0, 0, tiled=True)  16.4 us
    all_gather x1, blocking collectives, body(): moments = lax.all_gather(moments, ('x', 'c'))  13.5 us
  transfers between devices with their start and end apart: 13, of which 5 were waited for; matrix products, arithmetic and copies ran while one was open for 3% of the time, Pallas kernels for 4%

profile of v2, /device:TPU:40, one launch (start us, length us, event | category | flops | bytes accessed | tf_op | source)
XLA Modules:
  0.0 232.6 jit_solution(6205759735680963555)
XLA Ops:
  0.0 0.9 slice_select_fusion
  0.9 2.4 %collective-permute-start = (bf16[16,2048]{1,0:T(8,128)(2,1)S(1)}, bf16[16,2048]{1,0:T(8,128)(2,1)S(1)}, u32[]{:S(2)}, u32[]{:S(2)}) collective-permute-start(bf16[16,2048]{1,0:T(8,128)(2,1)S(1)} %slice_select_fusion), channel_id=1, source_target_pairs={{7,15},{15,23},{23,31},{31,39},{39,47},{47,55},{55,63},{63,71},{71... | collective-permute-start | bytes 196616 | tf_op jit(solution)/shard_map/ppermute | solution.py:444
  3.3 0.7 copy-done.18
  4.0 0.7 copy-done.22
  4.7 0.7 copy-done.23
  5.3 0.7 copy-done.24
  6.0 0.7 copy-done.25
  6.7 0.7 copy-done.26
  7.4 0.7 copy-done.27
  8.1 0.7 copy-done.28
  8.9 1.0 copy-done.1
  9.9 0.7 copy-done.21
  10.6 1.1 shard_map.146
  11.7 1.3 copy-done
  12.9 3.6 %all-to-all-start = ((bf16[4,112,2048]{2,1,0:T(8,128)(2,1)}), bf16[4,112,2048]{2,1,0:T(8,128)(2,1)S(1)}, u32[]{:S(2)}, u32[]{:S(2)}) async-start(bf16[4,112,2048]{2,1,0:T(8,128)(2,1)} %copy-done), calls=%async_computation | async-start | bytes 3670016 | tf_op jit(solution)/shard_map/all_to_all | solution.py:469
  16.5 40.0 %all_gather.9 = bf16[512,1008]{1,0:T(8,128)(2,1)S(1)} all-gather(bf16[32,1008]{1,0:T(8,128)(2,1)S(1)} %shard_map.145), channel_id=1, replica_groups=mesh['zh'=4,'zl'=4,'y'=4,'x'=4,'c'=2] {'zh','zl'}, dimensions={0}, use_global_device_ids=true | all-gather | bytes 1096704 | tf_op jit(solution)/shard_map/all_gather | solution.py:470
  56.5 1.9 collective-permute-start.1
  58.4 0.7 fusion
  59.2 1.0 broadcast_in_dim.32
  60.2 7.2 %all-to-all-start.1 = ((bf16[4,512,256]{2,1,0:T(8,128)(2,1)}), bf16[4,512,256]{2,1,0:T(8,128)(2,1)S(1)}, u32[]{:S(2)}, u32[]{:S(2)}) async-start(bf16[4,512,256]{2,1,0:T(8,128)(2,1)} %broadcast_in_dim.32), calls=%async_computation.1 | async-start | bytes 2097152 | tf_op jit(solution)/shard_map/all_to_all | solution.py:415
  67.5 0.6 reduce-window.6
  68.1 0.2 slice_reduce_fusion
  68.2 0.2 reduce-window.9
  68.5 0.1 copy.22
  68.6 13.4 %all-to-all-done.1 = bf16[4,512,256]{2,1,0:T(8,128)(2,1)S(1)} async-done(((bf16[4,512,256]{2,1,0:T(8,128)(2,1)}), bf16[4,512,256]{2,1,0:T(8,128)(2,1)S(1)}, u32[]{:S(2)}, u32[]{:S(2)}) %all-to-all-start.1) | async-done | bytes 1048608 | tf_op jit(solution)/shard_map/all_to_all | solution.py:415
  82.0 3.8 %shard_map.147 = (bf16[768,128]{1,0:T(8,128)(2,1)S(1)}, bf16[768,128]{1,0:T(8,128)(2,1)S(1)}, bf16[16,160,128]{2,1,0:T(8,128)(2,1)}) custom-call(s32[1]{0:T(128)} %bitcast.1.core, bf16[448,2048]{1,0:T(8,128)(2,1)S(1)} %bitcast.21, bf16[448,2048]{1,0:T(8,128)(2,1)} %collective-permute-done.1.other, bf16[2048,256]{1,0:T(8,128)(2,1)S(1)} %bitcast.25, ...), custom_call_target="tpu_custom_call" | custom-call | tf_op jit(solution)/shard_map/pallas_call | solution.py:22
  85.8 0.7 copy-done.8
  86.5 0.7 copy-done.10
  87.2 5.9 %all-to-all-start.2 = ((bf16[16,160,128]{2,1,0:T(8,128)(2,1)}), bf16[16,160,128]{2,1,0:T(8,128)(2,1)S(1)}, u32[]{:S(2)}, u32[]{:S(2)}) async-start(bf16[16,160,128]{2,1,0:T(8,128)(2,1)} %get-tuple-element.32), calls=%async_computation.2 | async-start | bytes 1310720 | tf_op jit(solution)/shard_map/all_to_all | solution.py:491
  93.1 16.4 %all-to-all-done.2.gathered = bf16[16,160,128]{2,1,0:T(8,128)(2,1)S(1)} async-done(((bf16[16,160,128]{2,1,0:T(8,128)(2,1)}), bf16[16,160,128]{2,1,0:T(8,128)(2,1)S(1)}, u32[]{:S(2)}, u32[]{:S(2)}) %all-to-all-start.2) | async-done | bytes 655392 | tf_op jit(solution)/shard_map/all_to_all | solution.py:491
  109.5 0.9 shard_map.149
  110.3 0.6 copy-done.16
  110.9 7.4 %all-to-all-start.3 = ((bf16[4,208,128]{2,1,0:T(8,128)(2,1)}), bf16[4,208,128]{2,1,0:T(8,128)(2,1)}, u32[]{:S(2)}, u32[]{:S(2)}) async-start(bf16[4,208,128]{2,1,0:T(8,128)(2,1)} %get-tuple-element.33), calls=%async_computation.3 | async-start | bytes 425984 | tf_op jit(solution)/shard_map/all_to_all | solution.py:498
  118.4 3.5 %collective-permute-start.5 = (bf16[512,256]{1,0:T(8,128)(2,1)}, bf16[512,256]{1,0:T(8,128)(2,1)S(1)}, u32[]{:S(2)}, u32[]{:S(2)}) collective-permute-start(bf16[512,256]{1,0:T(8,128)(2,1)} %get-tuple-element.41.p0), channel_id=1, source_target_pairs={{0,8},{8,16},{16,24},{24,0},{1,9},{9,17},{17,25},{25,1},{2,10},{10... | collective-permute-start | bytes 786440 | tf_op jit(solution)/shard_map/ppermute | solution.py:411
  121.9 1.1 slice.26.p0
  123.0 2.8 %collective-permute-start.2 = (bf16[512,496]{1,0:T(8,128)(2,1)S(1)}, bf16[512,496]{1,0:T(8,128)(2,1)S(1)}, u32[]{:S(2)}, u32[]{:S(2)}) collective-permute-start(bf16[512,496]{1,0:T(8,128)(2,1)S(1)} %slice.26.p0), channel_id=1, source_target_pairs={{0,8},{8,16},{16,24},{24,0},{1,9},{9,17},{17,25},{25,1},{2,10},{10... | collective-permute-start | bytes 1523720 | tf_op jit(solution)/shard_map/ppermute | solution.py:411
  125.8 3.5 %collective-permute-start.3 = (bf16[512,496]{1,0:T(8,128)(2,1)S(1)}, bf16[512,496]{1,0:T(8,128)(2,1)S(1)}, u32[]{:S(2)}, u32[]{:S(2)}) collective-permute-start(bf16[512,496]{1,0:T(8,128)(2,1)S(1)} %slice.26.p0), channel_id=1, source_target_pairs={{0,16},{8,24},{16,0},{24,8},{1,17},{9,25},{17,1},{25,9},{2,18},{10... | collective-permute-start | bytes 1523720 | tf_op jit(solution)/shard_map/ppermute | solution.py:411
  129.3 4.3 %collective-permute-start.4 = (bf16[512,496]{1,0:T(8,128)(2,1)S(1)}, bf16[512,496]{1,0:T(8,128)(2,1)}, u32[]{:S(2)}, u32[]{:S(2)}) collective-permute-start(bf16[512,496]{1,0:T(8,128)(2,1)S(1)} %slice.26.p0), channel_id=1, source_target_pairs={{0,24},{8,0},{16,8},{24,16},{1,25},{9,1},{17,9},{25,17},{2,26},{10... | collective-permute-start | bytes 1523720 | tf_op jit(solution)/shard_map/ppermute | solution.py:411
  133.6 2.0 collective-permute-start.6
  135.6 0.7 copy-done.6
  136.3 3.5 %collective-permute-start.7 = (bf16[512,256]{1,0:T(8,128)(2,1)}, bf16[512,256]{1,0:T(8,128)(2,1)}, u32[]{:S(2)}, u32[]{:S(2)}) collective-permute-start(bf16[512,256]{1,0:T(8,128)(2,1)} %get-tuple-element.41.p0), channel_id=1, source_target_pairs={{0,24},{8,0},{16,8},{24,16},{1,25},{9,1},{17,9},{25,17},{2,26},{10... | collective-permute-start | bytes 786440 | tf_op jit(solution)/shard_map/ppermute | solution.py:411
  139.8 1.7 copy.21
  141.5 1.0 reshape.27.start
  142.5 18.3 %collective-permute-done.6.p2 = bf16[512,256]{1,0:T(8,128)(2,1)} collective-permute-done((bf16[512,256]{1,0:T(8,128)(2,1)}, bf16[512,256]{1,0:T(8,128)(2,1)}, u32[]{:S(2)}, u32[]{:S(2)}) %collective-permute-start.6) | collective-permute-done | bytes 262176 | tf_op jit(solution)/shard_map/ppermute | solution.py:411
  160.8 2.7 %collective-permute-done.7.p3 = bf16[512,256]{1,0:T(8,128)(2,1)} collective-permute-done((bf16[512,256]{1,0:T(8,128)(2,1)}, bf16[512,256]{1,0:T(8,128)(2,1)}, u32[]{:S(2)}, u32[]{:S(2)}) %collective-permute-start.7) | collective-permute-done | bytes 262176 | tf_op jit(solution)/shard_map/ppermute | solution.py:411
  163.5 0.9 copy-done.7
  164.5 4.4 %shard_map.151 = (f32[768,128]{1,0:T(8,128)S(1)}, f32[2,768]{1,0:T(2,128)S(1)}) custom-call(s32[1]{0:T(128)} %bitcast.1.core, s32[1]{0:T(128)} %bitcast.y, bf16[448,2048]{1,0:T(8,128)(2,1)S(1)} %bitcast.22, bf16[448,2048]{1,0:T(8,128)(2,1)} %collective-permute-done.1.other, bf16[512,256]{1,0:T(8,128)(2,1)} %get-tuple-element.41.p0, ...), custom_call_target="tpu_custom_call" | custom-call | tf_op jit(solution)/shard_map/pallas_call | solution.py:22
  169.0 4.9 %shard_map.148 = (bf16[768,128]{1,0:T(8,128)(2,1)S(1)}, bf16[768,128]{1,0:T(8,128)(2,1)S(1)}, f32[768,128]{1,0:T(8,128)S(1)}) custom-call(s32[1]{0:T(128)} %bitcast.1.core, s32[1]{0:T(128)} %bitcast.y, bf16[448,2048]{1,0:T(8,128)(2,1)S(1)} %bitcast.23, bf16[448,2048]{1,0:T(8,128)(2,1)} %collective-permute-done.1.other, bf16[512,496]{1,0:T(8,128)(2,1)S(1)} %slice.26.p0, ...), custom_call_target="tpu_custom_call" | custom-call | tf_op jit(solution)/shard_map/pallas_call | solution.py:22
  173.9 0.7 copy-done.2
  174.6 0.7 copy-done.12
  175.3 0.7 copy-done.14
  175.9 13.5 %all-gather.1.moments = f32[8,2,768]{2,1,0:T(2,128)S(1)} all-gather(f32[1,2,768]{2,1,0:T(2,128)S(1)} %bitcast.29), channel_id=2, replica_groups=mesh['zh'=4,'zl'=4,'y'=4,'x'=4,'c'=2] {'x','c'}, dimensions={0}, use_global_device_ids=true | all-gather | bytes 55296 | tf_op jit(solution)/shard_map/all_gather | solution.py:506
  189.4 1.0 copy-done.3
  190.4 0.9 copy-done.13
  191.3 0.9 copy-done.15
  192.3 0.9 copy-done.17
  193.2 2.3 shard_map.150
  195.5 1.0 copy-done.5
  196.5 2.6 %shard_map.152 = (bf16[384,256]{1,0:T(8,128)(2,1)S(1)}, bf16[384,2048]{1,0:T(8,128)(2,1)S(1)}) custom-call(s32[1]{0:T(128)} %bitcast.1.core, s32[1]{0:T(128)} %bitcast.y, bf16[768,128]{1,0:T(8,128)(2,1)S(1)} %get-tuple-element.35.heads, f32[768,128]{1,0:T(8,128)S(1)} %copy-done.5, f32[8,2,768]{2,1,0:T(2,128)S(1)} %all-gather.1.moments, ...), custom_call_target="tpu_custom_call" | custom-call | tf_op jit(solution)/shard_map/pallas_call | solution.py:22
  199.0 2.2 collective-permute-start.8
  201.3 3.0 %collective-permute-done.8.arrived = bf16[384,2048]{1,0:T(8,128)(2,1)S(1)} collective-permute-done((bf16[384,2048]{1,0:T(8,128)(2,1)S(1)}, bf16[384,2048]{1,0:T(8,128)(2,1)S(1)}, u32[]{:S(2)}, u32[]{:S(2)}) %collective-permute-start.8) | collective-permute-done | bytes 1572896 | tf_op jit(solution)/shard_map/ppermute | solution.py:411
  204.4 2.1 shard_map.153
  206.4 24.9 %all_to_all.25.parts = bf16[4,96,2048]{2,1,0:T(8,128)(2,1)S(1)} all-to-all(bf16[4,96,2048]{2,1,0:T(8,128)(2,1)S(1)} %bitcast.24), channel_id=1, replica_groups=mesh['zh'=4,'zl'=4,'y'=4,'x'=4,'c'=2] {'x'}, dimensions={0} | all-to-all | bytes 3145728 | tf_op jit(solution)/shard_map/all_to_all | solution.py:533
  231.3 1.3 shard_map.154
  (57 shorter events, 0.3 us)
Async XLA Ops:
  0.9 8.0 %collective-permute-start = (bf16[16,2048]{1,0:T(8,128)(2,1)S(1)}, bf16[16,2048]{1,0:T(8,128)(2,1)S(1)}, u32[]{:S(2)}, u32[]{:S(2)}) collective-permute-start(bf16[16,2048]{1,0:T(8,128)(2,1)S(1)} %slice_select_fusion), channel_id=1, source_target_pairs={{7,15},{15,23},{23,31},{31,39},{39,47},{47,55},{55,63},{63,71},{71... | collective-permute-start | bytes 196616 | tf_op jit(solution)/shard_map/ppermute | solution.py:444
  3.2 0.7 copy-start.18
  4.0 0.7 copy-start.22
  4.6 0.7 copy-start.23
  5.3 0.7 copy-start.24
  6.0 0.7 copy-start.25
  6.7 0.7 copy-start.26
  7.4 0.7 copy-start.27
  8.1 0.7 copy-start.28
  8.9 1.0 copy-start.1
  9.9 0.7 copy-start.21
  11.6 1.3 copy-start
  12.9 43.6 %all-to-all-start = ((bf16[4,112,2048]{2,1,0:T(8,128)(2,1)}), bf16[4,112,2048]{2,1,0:T(8,128)(2,1)S(1)}, u32[]{:S(2)}, u32[]{:S(2)}) async-start(bf16[4,112,2048]{2,1,0:T(8,128)(2,1)} %copy-done), calls=%async_computation | async-start | bytes 3670016 | tf_op jit(solution)/shard_map/all_to_all | solution.py:469
  56.5 3.7 %copy-start.31 = (bf16[512,1008]{1,0:T(8,128)(2,1)}, bf16[512,1008]{1,0:T(8,128)(2,1)S(1)}, u32[]{:S(2)}) copy-start(bf16[512,1008]{1,0:T(8,128)(2,1)S(1)} %all_gather.9) | copy-start | bytes 3096580
  56.5 25.5 %collective-permute-start.1 = (bf16[448,2048]{1,0:T(8,128)(2,1)S(1)}, bf16[448,2048]{1,0:T(8,128)(2,1)}, u32[]{:S(2)}, u32[]{:S(2)}) collective-permute-start(bf16[448,2048]{1,0:T(8,128)(2,1)S(1)} %bitcast.20), channel_id=1, source_target_pairs={{0,1},{1,0},{2,3},{3,2},{4,5},{5,4},{6,7},{7,6},{8,9},{9,8},{10,11... | collective-permute-start | bytes 5505032 | tf_op jit(solution)/shard_map/ppermute | solution.py:411
  59.2 8.2 %copy-start.19 = (bf16[128,32]{0,1:T(8,128)(2,1)S(1)}, bf16[128,32]{0,1:T(8,128)(2,1)}, u32[]{:S(2)}) copy-start(bf16[128,32]{0,1:T(8,128)(2,1)} %param.29) | copy-start | bytes 24580
  59.2 8.3 %copy-start.32 = (f32[2,768]{1,0:T(2,128)S(1)}, f32[2,768]{1,0:T(2,128)}, u32[]{:S(2)}) copy-start(f32[2,768]{1,0:T(2,128)} %param.25) | copy-start | bytes 18436
  60.2 21.8 %all-to-all-start.1 = ((bf16[4,512,256]{2,1,0:T(8,128)(2,1)}), bf16[4,512,256]{2,1,0:T(8,128)(2,1)S(1)}, u32[]{:S(2)}, u32[]{:S(2)}) async-start(bf16[4,512,256]{2,1,0:T(8,128)(2,1)} %broadcast_in_dim.32), calls=%async_computation.1 | async-start | bytes 2097152 | tf_op jit(solution)/shard_map/all_to_all | solution.py:415
  85.8 0.7 copy-start.8
  86.5 0.7 copy-start.10
  87.2 22.3 %all-to-all-start.2 = ((bf16[16,160,128]{2,1,0:T(8,128)(2,1)}), bf16[16,160,128]{2,1,0:T(8,128)(2,1)S(1)}, u32[]{:S(2)}, u32[]{:S(2)}) async-start(bf16[16,160,128]{2,1,0:T(8,128)(2,1)} %get-tuple-element.32), calls=%async_computation.2 | async-start | bytes 1310720 | tf_op jit(solution)/shard_map/all_to_all | solution.py:491
  93.0 70.5 %copy-start.20 = (f32[31,128]{1,0:T(8,128)S(1)}, f32[31,128]{1,0:T(8,128)}, u32[]{:S(2)}) copy-start(f32[31,128]{1,0:T(8,128)} %taps.1) | copy-start | bytes 47620
  110.3 0.6 copy-start.16
  110.9 78.5 %all-to-all-start.3 = ((bf16[4,208,128]{2,1,0:T(8,128)(2,1)}), bf16[4,208,128]{2,1,0:T(8,128)(2,1)}, u32[]{:S(2)}, u32[]{:S(2)}) async-start(bf16[4,208,128]{2,1,0:T(8,128)(2,1)} %get-tuple-element.33), calls=%async_computation.3 | async-start | bytes 425984 | tf_op jit(solution)/shard_map/all_to_all | solution.py:498
  118.4 17.2 %collective-permute-start.5 = (bf16[512,256]{1,0:T(8,128)(2,1)}, bf16[512,256]{1,0:T(8,128)(2,1)S(1)}, u32[]{:S(2)}, u32[]{:S(2)}) collective-permute-start(bf16[512,256]{1,0:T(8,128)(2,1)} %get-tuple-element.41.p0), channel_id=1, source_target_pairs={{0,8},{8,16},{16,24},{24,0},{1,9},{9,17},{17,25},{25,1},{2,10},{10... | collective-permute-start | bytes 786440 | tf_op jit(solution)/shard_map/ppermute | solution.py:411
  123.0 45.9 %collective-permute-start.2 = (bf16[512,496]{1,0:T(8,128)(2,1)S(1)}, bf16[512,496]{1,0:T(8,128)(2,1)S(1)}, u32[]{:S(2)}, u32[]{:S(2)}) collective-permute-start(bf16[512,496]{1,0:T(8,128)(2,1)S(1)} %slice.26.p0), channel_id=1, source_target_pairs={{0,8},{8,16},{16,24},{24,0},{1,9},{9,17},{17,25},{25,1},{2,10},{10... | collective-permute-start | bytes 1523720 | tf_op jit(solution)/shard_map/ppermute | solution.py:411
  125.8 43.1 %collective-permute-start.3 = (bf16[512,496]{1,0:T(8,128)(2,1)S(1)}, bf16[512,496]{1,0:T(8,128)(2,1)S(1)}, u32[]{:S(2)}, u32[]{:S(2)}) collective-permute-start(bf16[512,496]{1,0:T(8,128)(2,1)S(1)} %slice.26.p0), channel_id=1, source_target_pairs={{0,16},{8,24},{16,0},{24,8},{1,17},{9,25},{17,1},{25,9},{2,18},{10... | collective-permute-start | bytes 1523720 | tf_op jit(solution)/shard_map/ppermute | solution.py:411
  129.3 39.6 %collective-permute-start.4 = (bf16[512,496]{1,0:T(8,128)(2,1)S(1)}, bf16[512,496]{1,0:T(8,128)(2,1)}, u32[]{:S(2)}, u32[]{:S(2)}) collective-permute-start(bf16[512,496]{1,0:T(8,128)(2,1)S(1)} %slice.26.p0), channel_id=1, source_target_pairs={{0,24},{8,0},{16,8},{24,16},{1,25},{9,1},{17,9},{25,17},{2,26},{10... | collective-permute-start | bytes 1523720 | tf_op jit(solution)/shard_map/ppermute | solution.py:411
  133.6 27.2 %collective-permute-start.6 = (bf16[512,256]{1,0:T(8,128)(2,1)}, bf16[512,256]{1,0:T(8,128)(2,1)}, u32[]{:S(2)}, u32[]{:S(2)}) collective-permute-start(bf16[512,256]{1,0:T(8,128)(2,1)} %get-tuple-element.41.p0), channel_id=1, source_target_pairs={{0,16},{8,24},{16,0},{24,8},{1,17},{9,25},{17,1},{25,9},{2,18},{10... | collective-permute-start | bytes 786440 | tf_op jit(solution)/shard_map/ppermute | solution.py:411
  135.6 0.7 copy-start.6
  136.3 27.2 %collective-permute-start.7 = (bf16[512,256]{1,0:T(8,128)(2,1)}, bf16[512,256]{1,0:T(8,128)(2,1)}, u32[]{:S(2)}, u32[]{:S(2)}) collective-permute-start(bf16[512,256]{1,0:T(8,128)(2,1)} %get-tuple-element.41.p0), channel_id=1, source_target_pairs={{0,24},{8,0},{16,8},{24,16},{1,25},{9,1},{17,9},{25,17},{2,26},{10... | collective-permute-start | bytes 786440 | tf_op jit(solution)/shard_map/ppermute | solution.py:411
  163.5 1.0 copy-start.7
  164.5 4.5 %copy-start.9 = (bf16[768,128]{1,0:T(8,128)(2,1)S(1)}, bf16[768,128]{1,0:T(8,128)(2,1)}, u32[]{:S(2)}) copy-start(bf16[768,128]{1,0:T(8,128)(2,1)} %copy-done.8) | copy-start | bytes 589828
  164.5 4.5 %copy-start.11 = (bf16[768,128]{1,0:T(8,128)(2,1)S(1)}, bf16[768,128]{1,0:T(8,128)(2,1)}, u32[]{:S(2)}) copy-start(bf16[768,128]{1,0:T(8,128)(2,1)} %copy-done.10) | copy-start | bytes 589828
  168.9 5.0 %copy-start.4 = (f32[768,128]{1,0:T(8,128)}, f32[768,128]{1,0:T(8,128)S(1)}, u32[]{:S(2)}) copy-start(f32[768,128]{1,0:T(8,128)S(1)} %get-tuple-element.36.convolved) | copy-start | bytes 1179652
  168.9 20.5 %copy-start.29 = (f32[128]{0:T(128)S(1)}, f32[128]{0:T(128)}, u32[]{:S(2)}) copy-start(f32[128]{0:T(128)} %param.27) | copy-start | bytes 1540
  169.0 26.5 %copy-start.30 = (f32[128]{0:T(128)S(1)}, f32[128]{0:T(128)}, u32[]{:S(2)}) copy-start(f32[128]{0:T(128)} %param.24) | copy-start | bytes 1540
  173.9 0.7 copy-start.2
  174.6 0.7 copy-start.12
  175.3 0.7 copy-start.14
  189.4 1.0 copy-start.3
  190.4 0.9 copy-start.13
  191.3 0.9 copy-start.15
  192.3 0.9 copy-start.17
  195.5 1.0 copy-start.5
  199.0 5.3 %collective-permute-start.8 = (bf16[384,2048]{1,0:T(8,128)(2,1)S(1)}, bf16[384,2048]{1,0:T(8,128)(2,1)S(1)}, u32[]{:S(2)}, u32[]{:S(2)}) collective-permute-start(bf16[384,2048]{1,0:T(8,128)(2,1)S(1)} %get-tuple-element.40), channel_id=1, source_target_pairs={{0,1},{1,0},{2,3},{3,2},{4,5},{5,4},{6,7},{7,6},{8,9},{9,8},{10,11... | collective-permute-start | bytes 4718600 | tf_op jit(solution)/shard_map/ppermute | solution.py:411

commit v3 on v2

--- a/solution.py
+++ b/solution.py
@@ -16,17 +16,42 @@
 TN = (((0,), (0,)), ((), ()))
 VMEM = pl.BlockSpec(memory_space=pltpu.VMEM)
 SMEM = pl.BlockSpec(memory_space=pltpu.SMEM)
-
-
-def call(kernel, out_shape, scalars, arrays, scratch=()):
+HBM = pl.BlockSpec(memory_space=pltpu.HBM)
+
+
+def call(kernel, out_shape, scalars, arrays, scratch=(), grant=20, far=(), out_far=()):
+    def specs(count, away):
+        return [HBM if i in away else VMEM for i in range(count)]
+
+    arrays = [
+        pltpu.with_memory_space_constraint(a, pltpu.HBM) if i in far else a
+        for i, a in enumerate(arrays)
+    ]
+    if isinstance(out_shape, tuple):
+        out_shape = tuple(
+            pltpu.HBM(s.shape, s.dtype) if i in out_far else s for i, s in enumerate(out_shape)
+        )
+    elif out_far:
+        out_shape = pltpu.HBM(out_shape.shape, out_shape.dtype)
+    outs = specs(len(out_shape), out_far) if isinstance(out_shape, tuple) else specs(1, out_far)[0]
     return pl.pallas_call(
         kernel,
         out_shape=out_shape,
-        in_specs=[SMEM] * len(scalars) + [VMEM] * len(arrays),
-        out_specs=[VMEM] * len(out_shape) if isinstance(out_shape, tuple) else VMEM,
+        in_specs=[SMEM] * len(scalars) + specs(len(arrays), far),
+        out_specs=outs,
         scratch_shapes=scratch,
-        compiler_params=pltpu.CompilerParams(vmem_limit_bytes=20 * 1024 * 1024),
+        compiler_params=pltpu.CompilerParams(vmem_limit_bytes=grant * 1024 * 1024),
     )(*scalars, *arrays)
+
+
+def start_copies(pairs, semaphores):
+    copies = [
+        pltpu.make_async_copy(source, target, semaphores.at[i])
+        for i, (source, target) in enumerate(pairs)
+    ]
+    for copy in copies:
+        copy.start()
+    return copies
 
 
 def shape(dims, dtype):
@@ -53,8 +78,10 @@
     out[:, 896:1008] = oh[:, 0:112]
 
 
-def norm_kernel(tokens, edge, gain, out):
+def norm_kernel(tokens_far, edge, gain_far, out_far, tokens, gain, out, semaphores):
     rows = 16
+    for copy in start_copies(((tokens_far, tokens), (gain_far, gain)), semaphores):
+        copy.wait()
 
     def block(source, at, to):
         x = source[at, :].astype(F32)
@@ -67,9 +94,7 @@
 
         def write(zh, y, made):
             where = (y * 4 + zh) * 128
-            made = made.astype(BF16)
-            for copy in range(4):
-                out[copy, to, where : where + 128] = made
+            out[to, where : where + 128] = made.astype(BF16)
 
         swap_groups(read, write, rows)
 
@@ -80,6 +105,8 @@
 
     lax.fori_loop(0, 6, step, 0, unroll=2)
     block(edge, slice(0, 16), slice(96, 112))
+    for copy in start_copies([(out, out_far.at[k]) for k in range(4)], semaphores):
+        copy.wait()
 
 
 def last_kernel(parts, out):
@@ -114,29 +141,28 @@
     return jnp.where(lane_is_second(turned.shape[0]), turned[:, 1:2], turned[:, 0:1])
 
 
-def put_rows(core, own, other, targets):
+def put_rows(core, own, other, target):
     for k in range(4):
         mine = pl.ds(pl.multiple_of(k * 192 + core * 96, 32), 96)
         theirs = pl.ds(pl.multiple_of(k * 192 + (1 - core) * 96, 32), 96)
         part = slice(k * 112, k * 112 + 96)
-        for n, target in enumerate(targets):
-            lanes = slice(n * 128, n * 128 + 128)
-            target[mine, :] = own[part, lanes].astype(BF16)
-            target[theirs, :] = other[part, lanes].astype(BF16)
-
-
-def states_kernel(core, own, other, weight, running, tail, keys, values, message):
+        target[mine, :] = own[part, :].astype(BF16)
+        target[theirs, :] = other[part, :].astype(BF16)
+
+
+def states_kernel(core, own, other, weight, running, tail, both_far, message, both, semaphores):
     w = weight[...]
     put_rows(
         core[0],
         jnp.dot(own[...], w, preferred_element_type=F32),
         jnp.dot(other[...], w, preferred_element_type=F32),
-        (keys, values),
-    )
+        both,
+    )
+    (kept,) = start_copies(((both, both_far),), semaphores)
     logs = by_lane(running[...])
     closing = logs[767:768, :]
-    k = keys[...].astype(F32) * 0.125
-    v = values[...]
+    k = both[:, 0:128].astype(F32) * 0.125
+    v = both[:, 128:256]
     second = lane_is_second(64)
     ahead = lax.dot_general(
         (k * jnp.exp(closing - logs)).astype(BF16), v, TN, preferred_element_type=F32
@@ -151,6 +177,7 @@
     for at, part in parts:
         for copy in range(16):
             message[copy, at, :] = part
+    kept.wait()
 
 
 def log_rows(log):
@@ -182,12 +209,8 @@
     return ahead, back
 
 
-def level_kernel(position, gathered, inside, message):
+def level_kernel(position, gathered, message_far, message, semaphores):
     ahead, back = scan_states(gathered, 16, position[0])
-    inside[0:64, :] = ahead[0]
-    inside[64:128, :] = back[0]
-    inside[128:136, :] = jnp.broadcast_to(ahead[1], (8, 128))
-    inside[136:144, :] = jnp.broadcast_to(back[1], (8, 128))
     parts = [
         (slice(0, 64), ahead[2].astype(BF16)),
         (slice(64, 128), back[2].astype(BF16)),
@@ -201,8 +224,9 @@
             made = jnp.where(group == zl, moved, made)
         parts.append((slice(144 + y * 16, 160 + y * 16), made.astype(BF16)))
     for at, part in parts:
-        for copy in range(4):
-            message[copy, at, :] = part
+        message[at, :] = part
+    for copy in start_copies([(message, message_far.at[k]) for k in range(4)], semaphores):
+        copy.wait()
 
 
 def column_block(position, shift):
@@ -219,7 +243,7 @@
     return total
 
 
-def conv_kernel(core, y, own, other, p0, p1, p2, p3, taps, convolved, moments, padded):
+def conv_kernel(core, y, own, other, p0, p1, p2, p3, taps, convolved_far, moments_far, padded, convolved, moments, semaphores):
     pieces = (p0, p1, p2, p3)
 
     def rows_of(rows):
@@ -249,138 +273,139 @@
         s2 = lax.dot_general(ones, total * total, NT, precision=highest, preferred_element_type=F32)
         moments[0:1, i * rows : (i + 1) * rows] = s1[0:1]
         moments[1:2, i * rows : (i + 1) * rows] = s2[0:1]
-
-
-def within_kernel(
-    core, y, own, other, p0, p1, p2, p3, keys, values, running, queries, gates, within
+    pairs = ((convolved, convolved_far), (moments, moments_far))
+    for copy in start_copies(pairs, semaphores):
+        copy.wait()
+
+
+def out_rows(y, rows, pieces, spare, write):
+    for shift, piece in enumerate(pieces):
+        lanes = column_block(y, shift)
+        part = lax.dot_general(rows[:, :240], piece[:, 256:496], NT, preferred_element_type=F32)
+        part = part + jnp.dot(rows[:, 240:], spare[:, lanes], preferred_element_type=F32)
+        write(lanes, part)
+
+
+def mixers_kernel(
+    core,
+    y,
+    low,
+    high,
+    own,
+    other,
+    p0,
+    p1,
+    p2,
+    p3,
+    inner,
+    outer,
+    both_far,
+    running_far,
+    start_far,
+    head_gain_far,
+    convolved_far,
+    moments_far,
+    channel_gain_far,
+    mine,
+    sent,
+    spare,
+    pair,
+    rows_in,
+    both,
+    running,
+    start,
+    head_gain,
+    convolved,
+    moments,
+    channel_gain,
+    semaphores,
 ):
     pieces = (p0, p1, p2, p3)
+    loads = start_copies(
+        (
+            (both_far, both),
+            (running_far, running),
+            (start_far, start),
+            (head_gain_far, head_gain),
+            (convolved_far, convolved),
+            (moments_far, moments),
+            (channel_gain_far, channel_gain),
+        ),
+        semaphores,
+    )
     put_rows(
         core[0],
         by_piece(y[0], own, pieces, slice(0, 256)),
         by_piece(y[0], other, pieces, slice(0, 256)),
-        (queries, gates),
-    )
+        pair,
+    )
+    for load in loads:
+        load.wait()
+    near = scan_states(inner, 16, low[0])
+    far = scan_states(outer, 4, high[0])
+    second = lane_is_second(64)
+
+    def entering(way):
+        begun = jnp.concatenate([start[way, 0], start[way, 1]], axis=1)
+        state = far[way][0] + jnp.exp(far[way][1]) * begun
+        state = near[way][0] + jnp.exp(near[way][1]) * state
+        return jnp.concatenate(
+            [jnp.where(second, 0.0, state), jnp.where(second, state, 0.0)], axis=0
+        ).astype(BF16)
+
+    forward, backward = entering(0), entering(1)
     logs = running[...]
     turned = jnp.transpose(logs)
-    k = (keys[...].astype(F32) * 0.125).astype(BF16)
-    v = values[...]
+    sums = moments[0]
+    for k in range(1, 8):
+        sums = sums + moments[k]
+    sums = jnp.transpose(jnp.concatenate([sums, jnp.zeros((6, 768), F32)], axis=0)) / DC
+    for yy in range(4):
+        for zh in range(4):
+            where = yy * 512 + zh * 128
+            spare[:, where : where + 128] = outer[zh, 144 + yy * 16 : 160 + yy * 16, :]
+
+    k = (both[:, 0:128].astype(F32) * 0.125).astype(BF16)
+    v = both[:, 128:256]
     rows = 128
     zero = jnp.zeros((), BF16)
+    half = lane_is_second(rows)
     masks = [lane_is_second(768) == bool(h) for h in range(2)]
     head_values = [jnp.where(mask, v, zero) for mask in masks]
+
+    def head_mean(x):
+        first = jnp.sum(jnp.where(half, 0.0, x), axis=1, keepdims=True)
+        last = jnp.sum(jnp.where(half, x, 0.0), axis=1, keepdims=True)
+        return jnp.where(half, last, first) / 64
+
     for i in range(6):
         at = slice(i * rows, (i + 1) * rows)
-        q = queries[at, :]
+        q = pair[at, 0:128]
         diagonal = lax.broadcasted_iota(jnp.int32, (rows, 768), 1) == (
             lax.broadcasted_iota(jnp.int32, (rows, 768), 0) + i * rows
         )
-        total = None
+        log = jnp.where(half, turned[at, 1:2], turned[at, 0:1])
+        closing = jnp.where(half[0:1], turned[767:768, 1:2], turned[767:768, 0:1])
+        retained = jnp.exp(log) * jnp.dot(q, forward, preferred_element_type=F32)
+        retained = retained + jnp.exp(closing - log) * jnp.dot(
+            q, backward, preferred_element_type=F32
+        )
         for h in range(2):
             scores = lax.dot_general(
                 jnp.where(masks[h][:rows], q, zero), k, NT, preferred_element_type=F32
             )
             distance = jnp.abs(turned[at, h : h + 1] - logs[h : h + 1, :])
             weights = jnp.exp(-distance) + jnp.where(diagonal, 1.0, 0.0)
-            part = jnp.dot(
+            retained = retained + jnp.dot(
                 (scores * weights).astype(BF16), head_values[h], preferred_element_type=F32
             )
-            total = part if total is None else total + part
-        within[at, :] = total
-
-
-def out_rows(y, rows, pieces, spare, write):
-    for shift, piece in enumerate(pieces):
-        lanes = column_block(y, shift)
-        part = lax.dot_general(rows[:, :240], piece[:, 256:496], NT, preferred_element_type=F32)
-        part = part + jnp.dot(rows[:, 240:], spare[:, lanes], preferred_element_type=F32)
-        write(lanes, part)
-
-
-def heads_kernel(
-    position,
-    queries,
-    gates,
-    within,
-    running,
-    gathered,
-    inside,
-    start,
-    head_gain,
-    heads,
-    spare,
-):
-    ahead, back = scan_states(gathered, 4, position[0])
-    forward = inside[0:64, :] + jnp.exp(inside[128:129, :]) * (
-        ahead[0] + jnp.exp(ahead[1]) * start[0:64, :]
-    )
-    backward = inside[64:128, :] + jnp.exp(inside[136:137, :]) * (
-        back[0] + jnp.exp(back[1]) * start[64:128, :]
-    )
-    second = lane_is_second(64)
-
-    def diagonal_blocks(state):
-        return jnp.concatenate(
-            [jnp.where(second, 0.0, state), jnp.where(second, state, 0.0)], axis=0
-        ).astype(BF16)
-
-    forward, backward = diagonal_blocks(forward), diagonal_blocks(backward)
-    logs = by_lane(running[...])
-    closing = logs[767:768, :]
-    rows = 128
-    half = lane_is_second(rows)
-
-    def head_mean(x):
-        low = jnp.sum(jnp.where(half, 0.0, x), axis=1, keepdims=True)
-        high = jnp.sum(jnp.where(half, x, 0.0), axis=1, keepdims=True)
-        return jnp.where(half, high, low) / 64
-
-    for i in range(6):
-        at = slice(i * rows, (i + 1) * rows)
-        q = queries[at, :]
-        log = logs[at, :]
-        retained = (
-            within[at, :]
-            + jnp.exp(log) * jnp.dot(q, forward, preferred_element_type=F32)
-            + jnp.exp(closing - log) * jnp.dot(q, backward, preferred_element_type=F32)
-        )
         centred = retained - head_mean(retained)
         normed = centred * lax.rsqrt(head_mean(centred * centred) + EPSILON)
-        gate = jax.nn.silu(gates[at, :].astype(F32))
-        heads[at, :] = (normed * head_gain[...] * gate).astype(BF16)
-    for y in range(4):
-        for zh in range(4):
-            where = y * 512 + zh * 128
-            spare[:, where : where + 128] = gathered[zh, 144 + y * 16 : 160 + y * 16, :]
-
-
-def mixers_kernel(
-    core,
-    y,
-    heads,
-    convolved,
-    moments,
-    channel_gain,
-    p0,
-    p1,
-    p2,
-    p3,
-    spare,
-    mine,
-    sent,
-    rows_in,
-):
-    sums = moments[0]
-    for k in range(1, 8):
-        sums = sums + moments[k]
-    sums = jnp.transpose(jnp.concatenate([sums, jnp.zeros((6, 768), F32)], axis=0)) / DC
-    rows = 128
-    for i in range(6):
-        at = slice(i * rows, (i + 1) * rows)
+        gate = jax.nn.silu(pair[at, 128:256].astype(F32))
+        rows_in[at, 128:256] = (normed * head_gain[...] * gate).astype(BF16)
         average, squares = sums[at, 0:1], sums[at, 1:2]
         scaled = (convolved[at, :] - average) * lax.rsqrt(squares - average * average + EPSILON)
         rows_in[at, 0:128] = jax.nn.silu(scaled * channel_gain[...]).astype(BF16)
-        rows_in[at, 128:256] = heads[at, :]
 
     def half_of(which):
         return jnp.concatenate(
@@ -396,7 +421,7 @@
     def write(lanes, part):
         sent[:, lanes] = part.astype(BF16)
 
-    out_rows(y[0], half_of(1 - core[0]), (p0, p1, p2, p3), spare, write)
+    out_rows(y[0], half_of(1 - core[0]), pieces, spare, write)
 
 
 def join_kernel(y, mine, arrived, p0, p1, p2, p3, spare, out):
@@ -461,9 +486,21 @@
             output_conv.T,
             output_heads.T,
         ),
+        grant=56,
     )
     normed = call(
-        norm_kernel, shape((4, 112, 2048), BF16), (), (tokens, edge, input_gain[None])
+        norm_kernel,
+        shape((4, 112, 2048), BF16),
+        (),
+        (tokens, edge, input_gain[None]),
+        scratch=(
+            pltpu.VMEM((96, 2048), BF16),
+            pltpu.VMEM((1, 2048), F32),
+            pltpu.VMEM((112, 2048), BF16),
+            pltpu.SemaphoreType.DMA((4,)),
+        ),
+        far=(0, 2),
+        out_far=(0,),
     )
     shard, normed = lax.optimization_barrier((shard, normed))
     own = lax.all_to_all(normed, "x", 0, 0, tiled=True).reshape(448, 2048)
@@ -477,59 +514,75 @@
 
     running = jnp.cumsum(decay_logs, axis=1)
     running = jnp.concatenate([running, jnp.zeros((6, 768), F32)], axis=0)
-    start = start_state.transpose(0, 2, 1, 3).reshape(128, 128)
-
-    half = shape((768, 128), BF16)
+
     full = shape((768, 128), F32)
     tail = jnp.pad(output_heads[112:], ((0, 0), (0, 96)))
-    keys, values, sent = call(
+    both, sent = call(
         states_kernel,
-        (half, half, shape((16, 160, 128), BF16)),
+        (shape((768, 256), BF16), shape((16, 160, 128), BF16)),
         (core,),
         (own, other, state_weight, running, tail),
-    )
-    gathered = lax.all_to_all(sent, ("zl", "y"), 0, 0, tiled=True)
-    inside, sent = call(
+        scratch=(pltpu.VMEM((768, 256), BF16), pltpu.SemaphoreType.DMA((1,))),
+        out_far=(0,),
+    )
+    inner = lax.all_to_all(sent, ("zl", "y"), 0, 0, tiled=True)
+    sent = call(
         level_kernel,
-        (shape((144, 128), F32), shape((4, 208, 128), BF16)),
+        shape((4, 208, 128), BF16),
         (low,),
-        (gathered,),
-    )
-    gathered = lax.all_to_all(sent, "zh", 0, 0, tiled=True)
+        (inner,),
+        scratch=(pltpu.VMEM((208, 128), BF16), pltpu.SemaphoreType.DMA((4,))),
+        out_far=(0,),
+    )
+    outer = lax.all_to_all(sent, "zh", 0, 0, tiled=True)
     convolved, moments = call(
         conv_kernel,
         (full, shape((2, 768), F32)),
         (core, y),
         (own, other, *gate_pieces, kernel_taps),
-        scratch=(pltpu.VMEM((800, 128), F32),),
+        scratch=(
+            pltpu.VMEM((800, 128), F32),
+            pltpu.VMEM((768, 128), F32),
+            pltpu.VMEM((2, 768), F32),
+            pltpu.SemaphoreType.DMA((2,)),
+        ),
+        out_far=(0, 1),
     )
     moments = lax.all_gather(moments, ("x", "c"))
-    queries, gates, within = call(
-        within_kernel,
-        (half, half, full),
-        (core, y),
-        (own, other, *rest_pieces, keys, values, running),
-    )
-    heads, spare = call(
-        heads_kernel,
-        (half, shape((16, 2048), BF16)),
-        (high,),
-        (queries, gates, within, running, gathered, inside, start, head_gain[None]),
-    )
-    mine, sent = call(
+    mine, sent, spare = call(
         mixers_kernel,
-        (shape((384, 256), BF16), shape((384, 2048), BF16)),
-        (core, y),
-        (heads, convolved, moments, channel_gain[None], *rest_pieces, spare),
-        scratch=(pltpu.VMEM((768, 256), BF16),),
+        (shape((384, 256), BF16), shape((384, 2048), BF16), shape((16, 2048), BF16)),
+        (core, y, low, high),
+        (
+            own,
+            other,
+            *rest_pieces,
+            inner,
+            outer,
+            both,
+            running,
+            start_state,
+            head_gain[None],
+            convolved,
+            moments,
+            channel_gain[None],
+        ),
+        scratch=(
+            pltpu.VMEM((768, 256), BF16),
+            pltpu.VMEM((768, 256), BF16),
+            pltpu.VMEM((768, 256), BF16),
+            pltpu.VMEM((8, 768), F32),
+            pltpu.VMEM((2, 2, 64, 64), F32),
+            pltpu.VMEM((1, 128), F32),
+            pltpu.VMEM((768, 128), F32),
+            pltpu.VMEM((8, 2, 768), F32),
+            pltpu.VMEM((1, 128), F32),
+            pltpu.SemaphoreType.DMA((7,)),
+        ),
+        far=(8, 9, 10, 11, 12, 13, 14),
     )
     arrived = ring(sent, "c", 1)
-    joined = call(
-        join_kernel,
-        shape((384, 2048), BF16),
-        (y,),
-        (mine, arrived, *rest_pieces, spare),
-    )
+    joined = call(join_kernel, shape((384, 2048), BF16), (y,), (mine, arrived, *rest_pieces, spare))
     parts = lax.all_to_all(joined.reshape(4, 96, 2048), "x", 0, 0, tiled=True)
     return call(last_kernel, shape((96, 2048), BF16), (), (parts,))
 

time: 234 us -> 224 us (0.957)
  the two profiles are of different devices: /device:TPU:40 before, /device:TPU:32 now
where the time goes in v3:
time: 224 us; the launch traced here: 223 us
  blocking collectives  80.3 us (36%)
  waiting for transfers between devices  59.3 us (26%)
  starting transfers between devices  49.9 us (22%)
  Pallas kernels  26.8 us (12%)
  local copies, waits for them, and re-layouts  4.86 us (2%)
    all_gather x1, blocking collectives, body(): rows = lax.all_gather(shard, ('zh', 'zl'), axis=0, tiled=True)  40.6 us
    ppermute x8, waiting for transfers between devices, ring(): lax.ppermute(x, axis, [(i, (i + shift) % count) for i in range(count)])  27 us
    pallas_call x8, Pallas kernels, call(): pl.pallas_call(kernel, out_shape=out_shape, in_specs=[SMEM] * len(scalars...  26.8 us
    all_to_all x1, blocking collectives, body(): parts = lax.all_to_all(joined.reshape(4, 96, 2048), 'x', 0, 0, tiled=True)  24.9 us
    ppermute x8, starting transfers between devices, ring(): lax.ppermute(x, axis, [(i, (i + shift) % count) for i in range(count)])  23.8 us
    all_to_all x1, waiting for transfers between devices, body(): inner = lax.all_to_all(sent, ('zl', 'y'), 0, 0, tiled=True)  17.3 us
    all_gather x1, blocking collectives, body(): moments = lax.all_gather(moments, ('x', 'c'))  14.7 us
    all_to_all x1, waiting for transfers between devices, copies(): lax.all_to_all(jnp.broadcast_to(x[None], (count, *x.shape)), axes, 0, 0,...  14.5 us
  transfers between devices with their start and end apart: 13, of which 6 were waited for; matrix products, arithmetic and copies ran while one was open for 2% of the time, Pallas kernels for 3%

profile of v3, /device:TPU:32, one launch (start us, length us, event | category | flops | bytes accessed | tf_op | source)
XLA Modules:
  0.0 223.1 jit_solution(9754059625087553832)
XLA Ops:
  0.0 0.9 slice_select_fusion
  0.9 4.5 %collective-permute-start = (bf16[16,2048]{1,0:T(8,128)(2,1)S(1)}, bf16[16,2048]{1,0:T(8,128)(2,1)S(1)}, u32[]{:S(2)}, u32[]{:S(2)}) collective-permute-start(bf16[16,2048]{1,0:T(8,128)(2,1)S(1)} %slice_select_fusion), channel_id=1, source_target_pairs={{7,15},{15,23},{23,31},{31,39},{39,47},{47,55},{55,63},{63,71},{71... | collective-permute-start | bytes 196616 | tf_op jit(solution)/shard_map/ppermute | solution.py:469
  5.4 1.5 shard_map.145
  6.8 0.4 collective-permute-done.edge
  7.2 3.4 %shard_map.146 = bf16[4,112,2048]{2,1,0:T(8,128)(2,1)} custom-call(bf16[96,2048]{1,0:T(8,128)(2,1)} %tokens_far.1, bf16[16,2048]{1,0:T(8,128)(2,1)S(1)} %collective-permute-done.edge, f32[1,2048]{1,0:T(1,128)} %bitcast.27), custom_call_target="tpu_custom_call" | custom-call | tf_op jit(solution)/shard_map/pallas_call | solution.py:37
  10.6 0.0 copy-start.5
  10.6 3.7 %all-to-all-start = ((bf16[4,112,2048]{2,1,0:T(8,128)(2,1)}), bf16[4,112,2048]{2,1,0:T(8,128)(2,1)S(1)}, u32[]{:S(2)}, u32[]{:S(2)}) async-start(bf16[4,112,2048]{2,1,0:T(8,128)(2,1)} %shard_map.146), calls=%async_computation | async-start | bytes 3670016 | tf_op jit(solution)/shard_map/all_to_all | solution.py:506
  14.4 0.0 copy-done.5
  14.4 40.6 %all_gather.9 = bf16[512,1008]{1,0:T(8,128)(2,1)S(1)} all-gather(bf16[32,1008]{1,0:T(8,128)(2,1)S(1)} %copy-done.5), channel_id=1, replica_groups=mesh['zh'=4,'zl'=4,'y'=4,'x'=4,'c'=2] {'zh','zl'}, dimensions={0}, use_global_device_ids=true | all-gather | bytes 1096704 | tf_op jit(solution)/shard_map/all_gather | solution.py:507
  55.0 0.0 copy-start.4
  55.0 0.0 all-to-all-done
  55.0 1.9 collective-permute-start.1
  57.0 0.7 fusion
  57.7 0.0 copy-start.6
  57.7 0.0 copy-start.7
  57.7 1.0 broadcast_in_dim.33
  58.7 0.0 copy-done.4
  58.7 5.5 %all-to-all-start.1 = ((bf16[4,512,256]{2,1,0:T(8,128)(2,1)}), bf16[4,512,256]{2,1,0:T(8,128)(2,1)S(1)}, u32[]{:S(2)}, u32[]{:S(2)}) async-start(bf16[4,512,256]{2,1,0:T(8,128)(2,1)} %broadcast_in_dim.33), calls=%async_computation.1 | async-start | bytes 2097152 | tf_op jit(solution)/shard_map/all_to_all | solution.py:440
  64.2 0.0 copy-done.6
  64.2 0.1 slice.30
  64.3 0.0 copy-done.7
  64.3 0.6 reduce-window.6
  64.9 0.2 slice_reduce_fusion
  65.0 0.2 reduce-window.9
  65.2 0.1 add_bitcast_fusion
  65.3 0.1 copy.19
  65.4 0.0 copy-start.2
  65.4 14.5 %all-to-all-done.1 = bf16[4,512,256]{2,1,0:T(8,128)(2,1)S(1)} async-done(((bf16[4,512,256]{2,1,0:T(8,128)(2,1)}), bf16[4,512,256]{2,1,0:T(8,128)(2,1)S(1)}, u32[]{:S(2)}, u32[]{:S(2)}) %all-to-all-start.1) | async-done | bytes 1048608 | tf_op jit(solution)/shard_map/all_to_all | solution.py:440
  80.0 0.0 collective-permute-done.1.other
  80.0 4.3 %shard_map.147 = (bf16[768,256]{1,0:T(8,128)(2,1)}, bf16[16,160,128]{2,1,0:T(8,128)(2,1)}) custom-call(s32[1]{0:T(128)} %bitcast.1.core, bf16[448,2048]{1,0:T(8,128)(2,1)S(1)} %bitcast.20, bf16[448,2048]{1,0:T(8,128)(2,1)} %collective-permute-done.1.other, bf16[2048,256]{1,0:T(8,128)(2,1)S(1)} %bitcast.24, f32[8,768]{1,0:T(8,128)S(1)} %concatenate.3.running.running_far, ...), custom_call_target="tpu_custom_call" | custom-call | tf_op jit(solution)/shard_map/pallas_call | solution.py:37
  84.2 0.0 copy-done.2
  84.2 0.0 copy-start.3
  84.3 6.1 %all-to-all-start.2 = ((bf16[16,160,128]{2,1,0:T(8,128)(2,1)}), bf16[16,160,128]{2,1,0:T(8,128)(2,1)S(1)}, u32[]{:S(2)}, u32[]{:S(2)}) async-start(bf16[16,160,128]{2,1,0:T(8,128)(2,1)} %get-tuple-element.20), calls=%async_computation.2 | async-start | bytes 1310720 | tf_op jit(solution)/shard_map/all_to_all | solution.py:528
  90.4 17.3 %all-to-all-done.2.gathered.inner = bf16[16,160,128]{2,1,0:T(8,128)(2,1)S(1)} async-done(((bf16[16,160,128]{2,1,0:T(8,128)(2,1)}), bf16[16,160,128]{2,1,0:T(8,128)(2,1)S(1)}, u32[]{:S(2)}, u32[]{:S(2)}) %all-to-all-start.2) | async-done | bytes 655392 | tf_op jit(solution)/shard_map/all_to_all | solution.py:528
  107.7 0.9 shard_map.148
  108.6 6.3 %all-to-all-start.3 = ((bf16[4,208,128]{2,1,0:T(8,128)(2,1)}), bf16[4,208,128]{2,1,0:T(8,128)(2,1)}, u32[]{:S(2)}, u32[]{:S(2)}) async-start(bf16[4,208,128]{2,1,0:T(8,128)(2,1)} %shard_map.148), calls=%async_computation.3 | async-start | bytes 425984 | tf_op jit(solution)/shard_map/all_to_all | solution.py:537
  114.9 3.2 %collective-permute-start.7 = (bf16[512,256]{1,0:T(8,128)(2,1)}, bf16[512,256]{1,0:T(8,128)(2,1)S(1)}, u32[]{:S(2)}, u32[]{:S(2)}) collective-permute-start(bf16[512,256]{1,0:T(8,128)(2,1)} %get-tuple-element.27.p0), channel_id=1, source_target_pairs={{0,24},{8,0},{16,8},{24,16},{1,25},{9,1},{17,9},{25,17},{2,26},{10... | collective-permute-start | bytes 786440 | tf_op jit(solution)/shard_map/ppermute | solution.py:436
  118.1 1.1 slice.26.p0
  119.2 3.1 %collective-permute-start.4 = (bf16[512,496]{1,0:T(8,128)(2,1)S(1)}, bf16[512,496]{1,0:T(8,128)(2,1)S(1)}, u32[]{:S(2)}, u32[]{:S(2)}) collective-permute-start(bf16[512,496]{1,0:T(8,128)(2,1)S(1)} %slice.26.p0), channel_id=1, source_target_pairs={{0,24},{8,0},{16,8},{24,16},{1,25},{9,1},{17,9},{25,17},{2,26},{10... | collective-permute-start | bytes 1523720 | tf_op jit(solution)/shard_map/ppermute | solution.py:436
  122.3 3.5 %collective-permute-start.3 = (bf16[512,496]{1,0:T(8,128)(2,1)S(1)}, bf16[512,496]{1,0:T(8,128)(2,1)}, u32[]{:S(2)}, u32[]{:S(2)}) collective-permute-start(bf16[512,496]{1,0:T(8,128)(2,1)S(1)} %slice.26.p0), channel_id=1, source_target_pairs={{0,16},{8,24},{16,0},{24,8},{1,17},{9,25},{17,1},{25,9},{2,18},{10... | collective-permute-start | bytes 1523720 | tf_op jit(solution)/shard_map/ppermute | solution.py:436
  125.8 1.9 collective-permute-start.2
  127.8 5.3 %collective-permute-start.6 = (bf16[512,256]{1,0:T(8,128)(2,1)}, bf16[512,256]{1,0:T(8,128)(2,1)}, u32[]{:S(2)}, u32[]{:S(2)}) collective-permute-start(bf16[512,256]{1,0:T(8,128)(2,1)} %get-tuple-element.27.p0), channel_id=1, source_target_pairs={{0,16},{8,24},{16,0},{24,8},{1,17},{9,25},{17,1},{25,9},{2,18},{10... | collective-permute-start | bytes 786440 | tf_op jit(solution)/shard_map/ppermute | solution.py:436
  133.0 0.0 collective-permute-done.7.p3
  133.0 0.0 copy-start
  133.0 0.7 copy-done
  133.7 2.6 %collective-permute-start.5 = (bf16[512,256]{1,0:T(8,128)(2,1)}, bf16[512,256]{1,0:T(8,128)(2,1)}, u32[]{:S(2)}, u32[]{:S(2)}) collective-permute-start(bf16[512,256]{1,0:T(8,128)(2,1)} %get-tuple-element.27.p0), channel_id=1, source_target_pairs={{0,8},{8,16},{16,24},{24,0},{1,9},{9,17},{17,25},{25,1},{2,10},{10... | collective-permute-start | bytes 786440 | tf_op jit(solution)/shard_map/ppermute | solution.py:436
  136.4 21.1 %collective-permute-done.6.p2 = bf16[512,256]{1,0:T(8,128)(2,1)} collective-permute-done((bf16[512,256]{1,0:T(8,128)(2,1)}, bf16[512,256]{1,0:T(8,128)(2,1)}, u32[]{:S(2)}, u32[]{:S(2)}) %collective-permute-start.6) | collective-permute-done | bytes 262176 | tf_op jit(solution)/shard_map/ppermute | solution.py:436
  157.5 2.9 %collective-permute-done.5.p1 = bf16[512,256]{1,0:T(8,128)(2,1)} collective-permute-done((bf16[512,256]{1,0:T(8,128)(2,1)}, bf16[512,256]{1,0:T(8,128)(2,1)}, u32[]{:S(2)}, u32[]{:S(2)}) %collective-permute-start.5) | collective-permute-done | bytes 262176 | tf_op jit(solution)/shard_map/ppermute | solution.py:436
  160.3 0.0 copy-done.3
  160.3 0.0 copy-start.1
  160.3 0.9 copy-done.1
  161.3 5.0 %shard_map.149 = (f32[768,128]{1,0:T(8,128)}, f32[2,768]{1,0:T(2,128)}) custom-call(s32[1]{0:T(128)} %bitcast.1.core, s32[1]{0:T(128)} %bitcast.y, bf16[448,2048]{1,0:T(8,128)(2,1)S(1)} %bitcast.21, bf16[448,2048]{1,0:T(8,128)(2,1)} %collective-permute-done.1.other, bf16[512,256]{1,0:T(8,128)(2,1)} %get-tuple-element.27.p0, ...), custom_call_target="tpu_custom_call" | custom-call | tf_op jit(solution)/shard_map/pallas_call | solution.py:37
  166.3 14.7 %all-gather.1.moments_far = f32[8,2,768]{2,1,0:T(2,128)} all-gather(f32[1,2,768]{2,1,0:T(2,128)} %bitcast.29), channel_id=2, replica_groups=mesh['zh'=4,'zl'=4,'y'=4,'x'=4,'c'=2] {'x','c'}, dimensions={0}, use_global_device_ids=true | all-gather | bytes 55296 | tf_op jit(solution)/shard_map/all_gather | solution.py:551
  180.9 0.0 collective-permute-done.4.p3
  180.9 0.0 collective-permute-done.3.p2
  180.9 0.0 collective-permute-done.2.p1
  181.0 0.0 all-to-all-done.3.outer
  181.0 8.4 %shard_map.150 = (bf16[384,256]{1,0:T(8,128)(2,1)S(1)}, bf16[384,2048]{1,0:T(8,128)(2,1)S(1)}, bf16[16,2048]{1,0:T(8,128)(2,1)S(1)}) custom-call(s32[1]{0:T(128)} %bitcast.1.core, s32[1]{0:T(128)} %bitcast.y, s32[1]{0:T(128)} %bitcast.2.position.low, s32[1]{0:T(128)} %bitcast.3.high, bf16[448,2048]{1,0:T(8,128)(2,1)S(1)} %bitcast.22, ...), custom_call_target="tpu_custom_call" | custom-call | tf_op jit(solution)/shard_map/pallas_call | solution.py:37
  189.4 2.3 %collective-permute-start.8 = (bf16[384,2048]{1,0:T(8,128)(2,1)S(1)}, bf16[384,2048]{1,0:T(8,128)(2,1)S(1)}, u32[]{:S(2)}, u32[]{:S(2)}) collective-permute-start(bf16[384,2048]{1,0:T(8,128)(2,1)S(1)} %get-tuple-element.25), channel_id=1, source_target_pairs={{0,1},{1,0},{2,3},{3,2},{4,5},{5,4},{6,7},{7,6},{8,9},{9,8},{10,11... | collective-permute-start | bytes 4718600 | tf_op jit(solution)/shard_map/ppermute | solution.py:436
  191.6 3.0 %collective-permute-done.8.arrived = bf16[384,2048]{1,0:T(8,128)(2,1)S(1)} collective-permute-done((bf16[384,2048]{1,0:T(8,128)(2,1)S(1)}, bf16[384,2048]{1,0:T(8,128)(2,1)S(1)}, u32[]{:S(2)}, u32[]{:S(2)}) %collective-permute-start.8) | collective-permute-done | bytes 1572896 | tf_op jit(solution)/shard_map/ppermute | solution.py:436
  194.7 2.2 shard_map.151
  196.9 24.9 %all_to_all.25.parts = bf16[4,96,2048]{2,1,0:T(8,128)(2,1)S(1)} all-to-all(bf16[4,96,2048]{2,1,0:T(8,128)(2,1)S(1)} %bitcast.23), channel_id=1, replica_groups=mesh['zh'=4,'zl'=4,'y'=4,'x'=4,'c'=2] {'x'}, dimensions={0} | all-to-all | bytes 3145728 | tf_op jit(solution)/shard_map/all_to_all | solution.py:586
  221.8 1.3 shard_map.152
  (4 shorter events, 0.0 us)
Async XLA Ops:
  0.9 6.4 %collective-permute-start = (bf16[16,2048]{1,0:T(8,128)(2,1)S(1)}, bf16[16,2048]{1,0:T(8,128)(2,1)S(1)}, u32[]{:S(2)}, u32[]{:S(2)}) collective-permute-start(bf16[16,2048]{1,0:T(8,128)(2,1)S(1)} %slice_select_fusion), channel_id=1, source_target_pairs={{7,15},{15,23},{23,31},{31,39},{39,47},{47,55},{55,63},{63,71},{71... | collective-permute-start | bytes 196616 | tf_op jit(solution)/shard_map/ppermute | solution.py:469
  10.6 3.8 %copy-start.5 = (bf16[32,1008]{1,0:T(8,128)(2,1)S(1)}, bf16[32,1008]{1,0:T(8,128)(2,1)}, u32[]{:S(2)}) copy-start(bf16[32,1008]{1,0:T(8,128)(2,1)} %shard_map.145) | copy-start | bytes 193540
  10.6 44.4 %all-to-all-start = ((bf16[4,112,2048]{2,1,0:T(8,128)(2,1)}), bf16[4,112,2048]{2,1,0:T(8,128)(2,1)S(1)}, u32[]{:S(2)}, u32[]{:S(2)}) async-start(bf16[4,112,2048]{2,1,0:T(8,128)(2,1)} %shard_map.146), calls=%async_computation | async-start | bytes 3670016 | tf_op jit(solution)/shard_map/all_to_all | solution.py:506
  55.0 3.7 %copy-start.4 = (bf16[512,1008]{1,0:T(8,128)(2,1)}, bf16[512,1008]{1,0:T(8,128)(2,1)S(1)}, u32[]{:S(2)}) copy-start(bf16[512,1008]{1,0:T(8,128)(2,1)S(1)} %all_gather.9) | copy-start | bytes 3096580
  55.0 24.9 %collective-permute-start.1 = (bf16[448,2048]{1,0:T(8,128)(2,1)S(1)}, bf16[448,2048]{1,0:T(8,128)(2,1)}, u32[]{:S(2)}, u32[]{:S(2)}) collective-permute-start(bf16[448,2048]{1,0:T(8,128)(2,1)S(1)} %bitcast.19), channel_id=1, source_target_pairs={{0,1},{1,0},{2,3},{3,2},{4,5},{5,4},{6,7},{7,6},{8,9},{9,8},{10,11... | collective-permute-start | bytes 5505032 | tf_op jit(solution)/shard_map/ppermute | solution.py:436
  57.7 6.5 %copy-start.6 = (bf16[128,32]{0,1:T(8,128)(2,1)S(1)}, bf16[128,32]{0,1:T(8,128)(2,1)}, u32[]{:S(2)}) copy-start(bf16[128,32]{0,1:T(8,128)(2,1)} %param.29) | copy-start | bytes 24580
  57.7 6.6 %copy-start.7 = (f32[2,768]{1,0:T(2,128)S(1)}, f32[2,768]{1,0:T(2,128)}, u32[]{:S(2)}) copy-start(f32[2,768]{1,0:T(2,128)} %param.25) | copy-start | bytes 18436
  58.7 21.2 %all-to-all-start.1 = ((bf16[4,512,256]{2,1,0:T(8,128)(2,1)}), bf16[4,512,256]{2,1,0:T(8,128)(2,1)S(1)}, u32[]{:S(2)}, u32[]{:S(2)}) async-start(bf16[4,512,256]{2,1,0:T(8,128)(2,1)} %broadcast_in_dim.33), calls=%async_computation.1 | async-start | bytes 2097152 | tf_op jit(solution)/shard_map/all_to_all | solution.py:440
  65.4 18.8 %copy-start.2 = (f32[8,768]{1,0:T(8,128)}, f32[8,768]{1,0:T(8,128)S(1)}, u32[]{:S(2)}) copy-start(f32[8,768]{1,0:T(8,128)S(1)} %concatenate.3.running.running_far) | copy-start | bytes 73732
  84.2 76.1 %copy-start.3 = (f32[31,128]{1,0:T(8,128)S(1)}, f32[31,128]{1,0:T(8,128)}, u32[]{:S(2)}) copy-start(f32[31,128]{1,0:T(8,128)} %taps.1) | copy-start | bytes 47620
  84.3 23.5 %all-to-all-start.2 = ((bf16[16,160,128]{2,1,0:T(8,128)(2,1)}), bf16[16,160,128]{2,1,0:T(8,128)(2,1)S(1)}, u32[]{:S(2)}, u32[]{:S(2)}) async-start(bf16[16,160,128]{2,1,0:T(8,128)(2,1)} %get-tuple-element.20), calls=%async_computation.2 | async-start | bytes 1310720 | tf_op jit(solution)/shard_map/all_to_all | solution.py:528
  108.6 72.3 %all-to-all-start.3 = ((bf16[4,208,128]{2,1,0:T(8,128)(2,1)}), bf16[4,208,128]{2,1,0:T(8,128)(2,1)}, u32[]{:S(2)}, u32[]{:S(2)}) async-start(bf16[4,208,128]{2,1,0:T(8,128)(2,1)} %shard_map.148), calls=%async_computation.3 | async-start | bytes 425984 | tf_op jit(solution)/shard_map/all_to_all | solution.py:537
  114.9 18.1 %collective-permute-start.7 = (bf16[512,256]{1,0:T(8,128)(2,1)}, bf16[512,256]{1,0:T(8,128)(2,1)S(1)}, u32[]{:S(2)}, u32[]{:S(2)}) collective-permute-start(bf16[512,256]{1,0:T(8,128)(2,1)} %get-tuple-element.27.p0), channel_id=1, source_target_pairs={{0,24},{8,0},{16,8},{24,16},{1,25},{9,1},{17,9},{25,17},{2,26},{10... | collective-permute-start | bytes 786440 | tf_op jit(solution)/shard_map/ppermute | solution.py:436
  119.2 61.7 %collective-permute-start.4 = (bf16[512,496]{1,0:T(8,128)(2,1)S(1)}, bf16[512,496]{1,0:T(8,128)(2,1)S(1)}, u32[]{:S(2)}, u32[]{:S(2)}) collective-permute-start(bf16[512,496]{1,0:T(8,128)(2,1)S(1)} %slice.26.p0), channel_id=1, source_target_pairs={{0,24},{8,0},{16,8},{24,16},{1,25},{9,1},{17,9},{25,17},{2,26},{10... | collective-permute-start | bytes 1523720 | tf_op jit(solution)/shard_map/ppermute | solution.py:436
  122.3 58.7 %collective-permute-start.3 = (bf16[512,496]{1,0:T(8,128)(2,1)S(1)}, bf16[512,496]{1,0:T(8,128)(2,1)}, u32[]{:S(2)}, u32[]{:S(2)}) collective-permute-start(bf16[512,496]{1,0:T(8,128)(2,1)S(1)} %slice.26.p0), channel_id=1, source_target_pairs={{0,16},{8,24},{16,0},{24,8},{1,17},{9,25},{17,1},{25,9},{2,18},{10... | collective-permute-start | bytes 1523720 | tf_op jit(solution)/shard_map/ppermute | solution.py:436
  125.8 55.1 %collective-permute-start.2 = (bf16[512,496]{1,0:T(8,128)(2,1)S(1)}, bf16[512,496]{1,0:T(8,128)(2,1)}, u32[]{:S(2)}, u32[]{:S(2)}) collective-permute-start(bf16[512,496]{1,0:T(8,128)(2,1)S(1)} %slice.26.p0), channel_id=1, source_target_pairs={{0,8},{8,16},{16,24},{24,0},{1,9},{9,17},{17,25},{25,1},{2,10},{10... | collective-permute-start | bytes 1523720 | tf_op jit(solution)/shard_map/ppermute | solution.py:436
  127.8 29.7 %collective-permute-start.6 = (bf16[512,256]{1,0:T(8,128)(2,1)}, bf16[512,256]{1,0:T(8,128)(2,1)}, u32[]{:S(2)}, u32[]{:S(2)}) collective-permute-start(bf16[512,256]{1,0:T(8,128)(2,1)} %get-tuple-element.27.p0), channel_id=1, source_target_pairs={{0,16},{8,24},{16,0},{24,8},{1,17},{9,25},{17,1},{25,9},{2,18},{10... | collective-permute-start | bytes 786440 | tf_op jit(solution)/shard_map/ppermute | solution.py:436
  133.0 0.7 copy-start
  133.7 26.6 %collective-permute-start.5 = (bf16[512,256]{1,0:T(8,128)(2,1)}, bf16[512,256]{1,0:T(8,128)(2,1)}, u32[]{:S(2)}, u32[]{:S(2)}) collective-permute-start(bf16[512,256]{1,0:T(8,128)(2,1)} %get-tuple-element.27.p0), channel_id=1, source_target_pairs={{0,8},{8,16},{16,24},{24,0},{1,9},{9,17},{17,25},{25,1},{2,10},{10... | collective-permute-start | bytes 786440 | tf_op jit(solution)/shard_map/ppermute | solution.py:436
  160.3 1.0 copy-start.1
  189.4 5.3 %collective-permute-start.8 = (bf16[384,2048]{1,0:T(8,128)(2,1)S(1)}, bf16[384,2048]{1,0:T(8,128)(2,1)S(1)}, u32[]{:S(2)}, u32[]{:S(2)}) collective-permute-start(bf16[384,2048]{1,0:T(8,128)(2,1)S(1)} %get-tuple-element.25), channel_id=1, source_target_pairs={{0,1},{1,0},{2,3},{3,2},{4,5},{5,4},{6,7},{7,6},{8,9},{9,8},{10,11... | collective-permute-start | bytes 4718600 | tf_op jit(solution)/shard_map/ppermute | solution.py:436

commit v4 on v3

--- a/solution.py
+++ b/solution.py
@@ -150,7 +150,7 @@
         target[theirs, :] = other[part, :].astype(BF16)
 
 
-def states_kernel(core, own, other, weight, running, tail, both_far, message, both, semaphores):
+def states_kernel(core, own, other, weight, running, tail, both_far, message_far, both, message, semaphores):
     w = weight[...]
     put_rows(
         core[0],
@@ -158,7 +158,8 @@
         jnp.dot(other[...], w, preferred_element_type=F32),
         both,
     )
-    (kept,) = start_copies(((both, both_far),), semaphores)
+    kept = pltpu.make_async_copy(both, both_far, semaphores.at[16])
+    kept.start()
     logs = by_lane(running[...])
     closing = logs[767:768, :]
     k = both[:, 0:128].astype(F32) * 0.125
@@ -175,8 +176,9 @@
         (slice(144, 160), tail[...]),
     )
     for at, part in parts:
-        for copy in range(16):
-            message[copy, at, :] = part
+        message[at, :] = part
+    for copy in start_copies([(message, message_far.at[k]) for k in range(16)], semaphores):
+        copy.wait()
     kept.wait()
 
 
@@ -231,6 +233,13 @@
 
 def column_block(position, shift):
     return pl.ds(pl.multiple_of(((position + 4 - shift) % 4) * 512, 512), 512)
+
+
+def split_kernel(rows_far, states_far, gate, rest, semaphores):
+    pairs = [(rows_far.at[:, 0:256], states_far.at[k]) for k in range(4)]
+    pairs += [(rows_far.at[:, 256:512], gate), (rows_far.at[:, 512:1008], rest)]
+    for copy in start_copies(pairs, semaphores):
+        copy.wait()
 
 
 def by_piece(y, rows, pieces, lanes):
@@ -278,6 +287,67 @@
         copy.wait()
 
 
+def within_kernel(
+    core,
+    y,
+    own,
+    other,
+    p0,
+    p1,
+    p2,
+    p3,
+    both_far,
+    running_far,
+    pair_far,
+    within_far,
+    pair,
+    within,
+    both,
+    running,
+    semaphores,
+):
+    loads = start_copies(((both_far, both), (running_far, running)), semaphores)
+    pieces = (p0, p1, p2, p3)
+    put_rows(
+        core[0],
+        by_piece(y[0], own, pieces, slice(0, 256)),
+        by_piece(y[0], other, pieces, slice(0, 256)),
+        pair,
+    )
+    for load in loads:
+        load.wait()
+    (kept,) = start_copies(((pair, pair_far),), semaphores)
+    logs = running[...]
+    turned = jnp.transpose(logs)
+    k = (both[:, 0:128].astype(F32) * 0.125).astype(BF16)
+    v = both[:, 128:256]
+    rows = 128
+    zero = jnp.zeros((), BF16)
+    masks = [lane_is_second(768) == bool(h) for h in range(2)]
+    head_values = [jnp.where(mask, v, zero) for mask in masks]
+    for i in range(6):
+        at = slice(i * rows, (i + 1) * rows)
+        q = pair[at, 0:128]
+        diagonal = lax.broadcasted_iota(jnp.int32, (rows, 768), 1) == (
+            lax.broadcasted_iota(jnp.int32, (rows, 768), 0) + i * rows
+        )
+        total = None
+        for h in range(2):
+            scores = lax.dot_general(
+                jnp.where(masks[h][:rows], q, zero), k, NT, preferred_element_type=F32
+            )
+            distance = jnp.abs(turned[at, h : h + 1] - logs[h : h + 1, :])
+            weights = jnp.exp(-distance) + jnp.where(diagonal, 1.0, 0.0)
+            part = jnp.dot(
+                (scores * weights).astype(BF16), head_values[h], preferred_element_type=F32
+            )
+            total = part if total is None else total + part
+        within[at, :] = total
+    kept.wait()
+    (kept,) = start_copies(((within, within_far),), semaphores)
+    kept.wait()
+
+
 def out_rows(y, rows, pieces, spare, write):
     for shift, piece in enumerate(pieces):
         lanes = column_block(y, shift)
@@ -291,27 +361,29 @@
     y,
     low,
     high,
-    own,
-    other,
     p0,
     p1,
     p2,
     p3,
     inner,
     outer,
-    both_far,
+    pair_far,
+    within_far,
     running_far,
     start_far,
     head_gain_far,
     convolved_far,
-    moments_far,
+    moments_0,
+    moments_1,
+    moments_2,
+    moments_3,
     channel_gain_far,
     mine,
     sent,
     spare,
+    rows_in,
     pair,
-    rows_in,
-    both,
+    within,
     running,
     start,
     head_gain,
@@ -323,27 +395,29 @@
     pieces = (p0, p1, p2, p3)
     loads = start_copies(
         (
-            (both_far, both),
+            (start_far, start),
             (running_far, running),
-            (start_far, start),
+            (moments_0, moments.at[0]),
+            (moments_1, moments.at[1]),
+            (moments_2, moments.at[2]),
+            (moments_3, moments.at[3]),
+            (pair_far, pair),
             (head_gain_far, head_gain),
+            (within_far, within),
             (convolved_far, convolved),
-            (moments_far, moments),
             (channel_gain_far, channel_gain),
         ),
         semaphores,
     )
-    put_rows(
-        core[0],
-        by_piece(y[0], own, pieces, slice(0, 256)),
-        by_piece(y[0], other, pieces, slice(0, 256)),
-        pair,
-    )
-    for load in loads:
-        load.wait()
     near = scan_states(inner, 16, low[0])
     far = scan_states(outer, 4, high[0])
     second = lane_is_second(64)
+    for yy in range(4):
+        for zh in range(4):
+            where = yy * 512 + zh * 128
+            spare[:, where : where + 128] = outer[zh, 144 + yy * 16 : 160 + yy * 16, :]
+    for load in loads:
+        load.wait()
 
     def entering(way):
         begun = jnp.concatenate([start[way, 0], start[way, 1]], axis=1)
@@ -354,24 +428,11 @@
         ).astype(BF16)
 
     forward, backward = entering(0), entering(1)
-    logs = running[...]
-    turned = jnp.transpose(logs)
-    sums = moments[0]
-    for k in range(1, 8):
-        sums = sums + moments[k]
+    turned = jnp.transpose(running[...])
+    sums = moments[0] + moments[1] + (moments[2] + moments[3])
     sums = jnp.transpose(jnp.concatenate([sums, jnp.zeros((6, 768), F32)], axis=0)) / DC
-    for yy in range(4):
-        for zh in range(4):
-            where = yy * 512 + zh * 128
-            spare[:, where : where + 128] = outer[zh, 144 + yy * 16 : 160 + yy * 16, :]
-
-    k = (both[:, 0:128].astype(F32) * 0.125).astype(BF16)
-    v = both[:, 128:256]
     rows = 128
-    zero = jnp.zeros((), BF16)
     half = lane_is_second(rows)
-    masks = [lane_is_second(768) == bool(h) for h in range(2)]
-    head_values = [jnp.where(mask, v, zero) for mask in masks]
 
     def head_mean(x):
         first = jnp.sum(jnp.where(half, 0.0, x), axis=1, keepdims=True)
@@ -381,24 +442,14 @@
     for i in range(6):
         at = slice(i * rows, (i + 1) * rows)
         q = pair[at, 0:128]
-        diagonal = lax.broadcasted_iota(jnp.int32, (rows, 768), 1) == (
-            lax.broadcasted_iota(jnp.int32, (rows, 768), 0) + i * rows
-        )
         log = jnp.where(half, turned[at, 1:2], turned[at, 0:1])
         closing = jnp.where(half[0:1], turned[767:768, 1:2], turned[767:768, 0:1])
-        retained = jnp.exp(log) * jnp.dot(q, forward, preferred_element_type=F32)
+        retained = within[at, :] + jnp.exp(log) * jnp.dot(
+            q, forward, preferred_element_type=F32
+        )
         retained = retained + jnp.exp(closing - log) * jnp.dot(
             q, backward, preferred_element_type=F32
         )
-        for h in range(2):
-            scores = lax.dot_general(
-                jnp.where(masks[h][:rows], q, zero), k, NT, preferred_element_type=F32
-            )
-            distance = jnp.abs(turned[at, h : h + 1] - logs[h : h + 1, :])
-            weights = jnp.exp(-distance) + jnp.where(diagonal, 1.0, 0.0)
-            retained = retained + jnp.dot(
-                (scores * weights).astype(BF16), head_values[h], preferred_element_type=F32
-            )
         centred = retained - head_mean(retained)
         normed = centred * lax.rsqrt(head_mean(centred * centred) + EPSILON)
         gate = jax.nn.silu(pair[at, 128:256].astype(F32))
@@ -434,12 +485,6 @@
 def ring(x, axis, shift):
     count = lax.axis_size(axis)
     return lax.ppermute(x, axis, [(i, (i + shift) % count) for i in range(count)])
-
-
-def copies(x, axes, count):
-    return lax.all_to_all(
-        jnp.broadcast_to(x[None], (count, *x.shape)), axes, 0, 0, tiled=True
-    )
 
 
 def body(
@@ -507,8 +552,20 @@
     rows = lax.all_gather(shard, ("zh", "zl"), axis=0, tiled=True)
     own, rows = lax.optimization_barrier((own, rows))
     other = ring(own, "c", 1)
-    state_weight = copies(rows[:, :256], "y", 4).reshape(2048, 256)
-    gate_piece, rest_piece = rows[:, 256:512], rows[:, 512:]
+    state_piece, gate_piece, rest_piece = call(
+        split_kernel,
+        (
+            shape((4, 512, 256), BF16),
+            shape((512, 256), BF16),
+            shape((512, 496), BF16),
+        ),
+        (),
+        (rows,),
+        scratch=(pltpu.SemaphoreType.DMA((6,)),),
+        far=(0,),
+        out_far=(0,),
+    )
+    state_weight = lax.all_to_all(state_piece, "y", 0, 0, tiled=True).reshape(2048, 256)
     gate_pieces = (gate_piece,) + tuple(ring(gate_piece, "y", d) for d in (1, 2, 3))
     rest_pieces = (rest_piece,) + tuple(ring(rest_piece, "y", d) for d in (1, 2, 3))
 
@@ -522,8 +579,12 @@
         (shape((768, 256), BF16), shape((16, 160, 128), BF16)),
         (core,),
         (own, other, state_weight, running, tail),
-        scratch=(pltpu.VMEM((768, 256), BF16), pltpu.SemaphoreType.DMA((1,))),
-        out_far=(0,),
+        scratch=(
+            pltpu.VMEM((768, 256), BF16),
+            pltpu.VMEM((160, 128), BF16),
+            pltpu.SemaphoreType.DMA((17,)),
+        ),
+        out_far=(0, 1),
     )
     inner = lax.all_to_all(sent, ("zl", "y"), 0, 0, tiled=True)
     sent = call(
@@ -548,38 +609,54 @@
         ),
         out_far=(0, 1),
     )
-    moments = lax.all_gather(moments, ("x", "c"))
+    partner = ring(moments, "c", 1)
+    moments = moments + partner
+    moments = (moments,) + tuple(ring(moments, "x", d) for d in (1, 2, 3))
+    pair, within = call(
+        within_kernel,
+        (shape((768, 256), BF16), full),
+        (core, y),
+        (own, other, *rest_pieces, both, running),
+        scratch=(
+            pltpu.VMEM((768, 256), BF16),
+            pltpu.VMEM((768, 128), F32),
+            pltpu.VMEM((768, 256), BF16),
+            pltpu.VMEM((8, 768), F32),
+            pltpu.SemaphoreType.DMA((2,)),
+        ),
+        far=(6, 7),
+        out_far=(0, 1),
+    )
     mine, sent, spare = call(
         mixers_kernel,
         (shape((384, 256), BF16), shape((384, 2048), BF16), shape((16, 2048), BF16)),
         (core, y, low, high),
         (
-            own,
-            other,
             *rest_pieces,
             inner,
             outer,
-            both,
+            pair,
+            within,
             running,
             start_state,
             head_gain[None],
             convolved,
-            moments,
+            *moments,
             channel_gain[None],
         ),
         scratch=(
             pltpu.VMEM((768, 256), BF16),
             pltpu.VMEM((768, 256), BF16),
-            pltpu.VMEM((768, 256), BF16),
+            pltpu.VMEM((768, 128), F32),
             pltpu.VMEM((8, 768), F32),
             pltpu.VMEM((2, 2, 64, 64), F32),
             pltpu.VMEM((1, 128), F32),
             pltpu.VMEM((768, 128), F32),
-            pltpu.VMEM((8, 2, 768), F32),
+            pltpu.VMEM((4, 2, 768), F32),
             pltpu.VMEM((1, 128), F32),
-            pltpu.SemaphoreType.DMA((7,)),
-        ),
-        far=(8, 9, 10, 11, 12, 13, 14),
+            pltpu.SemaphoreType.DMA((11,)),
+        ),
+        far=tuple(range(6, 17)),
     )
     arrived = ring(sent, "c", 1)
     joined = call(join_kernel, shape((384, 2048), BF16), (y,), (mine, arrived, *rest_pieces, spare))

time: 224 us -> 258 us (1.15)
  the two profiles are of different devices: /device:TPU:32 before, /device:TPU:40 now
where the time goes in v4:
time: 258 us; the launch traced here: 257 us
  blocking collectives  66.4 us (26%)
  Pallas kernels  63.4 us (25%)
  starting transfers between devices  62.9 us (24%)
  waiting for transfers between devices  60.9 us (24%)
    pallas_call x10, Pallas kernels, call(): pl.pallas_call(kernel, out_shape=out_shape, in_specs=[SMEM] * len(scalars...  63.4 us
    all_gather x1, blocking collectives, body(): rows = lax.all_gather(shard, ('zh', 'zl'), axis=0, tiled=True)  41.9 us
    ppermute x12, starting transfers between devices, ring(): lax.ppermute(x, axis, [(i, (i + shift) % count) for i in range(count)])  36.6 us
    ppermute x12, waiting for transfers between devices, ring(): lax.ppermute(x, axis, [(i, (i + shift) % count) for i in range(count)])  29 us
    all_to_all x1, blocking collectives, body(): parts = lax.all_to_all(joined.reshape(4, 96, 2048), 'x', 0, 0, tiled=True)  24.5 us
    all_to_all x1, waiting for transfers between devices, body(): inner = lax.all_to_all(sent, ('zl', 'y'), 0, 0, tiled=True)  16.1 us
    all_to_all x1, waiting for transfers between devices, body(): lax.all_to_all(state_piece, 'y', 0, 0, tiled=True).reshape(2048, 256)  13.5 us
    all_to_all x1, starting transfers between devices, body(): lax.all_to_all(state_piece, 'y', 0, 0, tiled=True).reshape(2048, 256)  7.39 us
  transfers between devices with their start and end apart: 17, of which 7 were waited for; matrix products, arithmetic and copies ran while one was open for 1% of the time, Pallas kernels for 18%

profile of v4, /device:TPU:40, one launch (start us, length us, event | category | flops | bytes accessed | tf_op | source)
XLA Modules:
  0.0 257.2 jit_solution(5113730799425623461)
XLA Ops:
  0.0 0.9 slice_select_fusion
  0.9 2.4 collective-permute-start
  3.2 1.5 shard_map.145
  4.7 2.3 collective-permute-done.edge
  7.0 3.4 %shard_map.146 = bf16[4,112,2048]{2,1,0:T(8,128)(2,1)} custom-call(bf16[96,2048]{1,0:T(8,128)(2,1)} %tokens_far.1, bf16[16,2048]{1,0:T(8,128)(2,1)S(1)} %collective-permute-done.edge, f32[1,2048]{1,0:T(1,128)} %bitcast.25), custom_call_target="tpu_custom_call" | custom-call | tf_op jit(solution)/shard_map/pallas_call | solution.py:37
  10.4 0.0 copy-start.2
  10.4 3.7 %all-to-all-start = ((bf16[4,112,2048]{2,1,0:T(8,128)(2,1)}), bf16[4,112,2048]{2,1,0:T(8,128)(2,1)S(1)}, u32[]{:S(2)}, u32[]{:S(2)}) async-start(bf16[4,112,2048]{2,1,0:T(8,128)(2,1)} %shard_map.146), calls=%async_computation | async-start | bytes 3670016 | tf_op jit(solution)/shard_map/all_to_all | solution.py:551
  14.2 0.0 copy-done.2
  14.2 41.9 %all_gather.3.rows_far = bf16[512,1008]{1,0:T(8,128)(2,1)} all-gather(bf16[32,1008]{1,0:T(8,128)(2,1)S(1)} %copy-done.2), channel_id=1, replica_groups=mesh['zh'=4,'zl'=4,'y'=4,'x'=4,'c'=2] {'zh','zl'}, dimensions={0}, use_global_device_ids=true | all-gather | bytes 1096704 | tf_op jit(solution)/shard_map/all_gather | solution.py:552
  56.1 0.0 all-to-all-done
  56.1 2.1 collective-permute-start.4
  58.2 33.6 %shard_map.147 = (bf16[4,512,256]{2,1,0:T(8,128)(2,1)}, bf16[512,256]{1,0:T(8,128)(2,1)}, bf16[512,496]{1,0:T(8,128)(2,1)S(1)}) custom-call(bf16[512,1008]{1,0:T(8,128)(2,1)} %all_gather.3.rows_far), custom_call_target="tpu_custom_call" | custom-call | tf_op jit(solution)/shard_map/pallas_call | solution.py:37
  91.8 7.4 %all-to-all-start.1 = ((bf16[4,512,256]{2,1,0:T(8,128)(2,1)}), bf16[4,512,256]{2,1,0:T(8,128)(2,1)}, u32[]{:S(2)}, u32[]{:S(2)}) async-start(bf16[4,512,256]{2,1,0:T(8,128)(2,1)} %get-tuple-element.26), calls=%async_computation.1 | async-start | bytes 2097152 | tf_op jit(solution)/shard_map/all_to_all | solution.py:568
  99.2 0.0 copy-done.3
  99.2 0.1 slice.19
  99.3 0.0 copy-done.6
  99.3 0.6 reduce-window.6
  99.9 0.2 slice_reduce_fusion
  100.0 0.2 reduce-window.9
  100.2 0.1 add_bitcast_fusion
  100.3 0.0 copy-start
  100.3 0.1 copy.18
  100.4 13.5 %all-to-all-done.1 = bf16[4,512,256]{2,1,0:T(8,128)(2,1)} async-done(((bf16[4,512,256]{2,1,0:T(8,128)(2,1)}), bf16[4,512,256]{2,1,0:T(8,128)(2,1)}, u32[]{:S(2)}, u32[]{:S(2)}) %all-to-all-start.1) | async-done | bytes 1048608 | tf_op jit(solution)/shard_map/all_to_all | solution.py:568
  113.9 0.0 collective-permute-done.4.other
  113.9 4.2 %shard_map.148 = (bf16[768,256]{1,0:T(8,128)(2,1)}, bf16[16,160,128]{2,1,0:T(8,128)(2,1)}) custom-call(s32[1]{0:T(128)} %bitcast.1.core, bf16[448,2048]{1,0:T(8,128)(2,1)S(1)} %bitcast.19, bf16[448,2048]{1,0:T(8,128)(2,1)} %collective-permute-done.4.other, bf16[2048,256]{1,0:T(8,128)(2,1)} %bitcast.8.weight, f32[8,768]{1,0:T(8,128)S(1)} %concatenate.3.running.running_far, ...), custom_call_target="tpu_custom_call" | custom-call | tf_op jit(solution)/shard_map/pallas_call | solution.py:37
  118.1 0.0 copy-done
  118.2 0.0 copy-start.1
  118.2 5.7 %all-to-all-start.2 = ((bf16[16,160,128]{2,1,0:T(8,128)(2,1)}), bf16[16,160,128]{2,1,0:T(8,128)(2,1)S(1)}, u32[]{:S(2)}, u32[]{:S(2)}) async-start(bf16[16,160,128]{2,1,0:T(8,128)(2,1)} %get-tuple-element.27), calls=%async_computation.2 | async-start | bytes 1310720 | tf_op jit(solution)/shard_map/all_to_all | solution.py:589
  123.9 16.1 %all-to-all-done.2.gathered.inner = bf16[16,160,128]{2,1,0:T(8,128)(2,1)S(1)} async-done(((bf16[16,160,128]{2,1,0:T(8,128)(2,1)}), bf16[16,160,128]{2,1,0:T(8,128)(2,1)S(1)}, u32[]{:S(2)}, u32[]{:S(2)}) %all-to-all-start.2) | async-done | bytes 655392 | tf_op jit(solution)/shard_map/all_to_all | solution.py:589
  140.0 0.9 shard_map.149
  140.9 7.1 %all-to-all-start.3 = ((bf16[4,208,128]{2,1,0:T(8,128)(2,1)}), bf16[4,208,128]{2,1,0:T(8,128)(2,1)}, u32[]{:S(2)}, u32[]{:S(2)}) async-start(bf16[4,208,128]{2,1,0:T(8,128)(2,1)} %shard_map.149), calls=%async_computation.3 | async-start | bytes 425984 | tf_op jit(solution)/shard_map/all_to_all | solution.py:598
  147.9 3.5 %collective-permute-start.5 = (bf16[512,256]{1,0:T(8,128)(2,1)}, bf16[512,256]{1,0:T(8,128)(2,1)S(1)}, u32[]{:S(2)}, u32[]{:S(2)}) collective-permute-start(bf16[512,256]{1,0:T(8,128)(2,1)} %get-tuple-element.31.p0), channel_id=1, source_target_pairs={{0,8},{8,16},{16,24},{24,0},{1,9},{9,17},{17,25},{25,1},{2,10},{10... | collective-permute-start | bytes 786440 | tf_op jit(solution)/shard_map/ppermute | solution.py:487
  151.5 2.8 %collective-permute-start.1 = (bf16[512,496]{1,0:T(8,128)(2,1)S(1)}, bf16[512,496]{1,0:T(8,128)(2,1)S(1)}, u32[]{:S(2)}, u32[]{:S(2)}) collective-permute-start(bf16[512,496]{1,0:T(8,128)(2,1)S(1)} %get-tuple-element.24.p0), channel_id=1, source_target_pairs={{0,8},{8,16},{16,24},{24,0},{1,9},{9,17},{17,25},{25,1},{2,10},{10... | collective-permute-start | bytes 1523720 | tf_op jit(solution)/shard_map/ppermute | solution.py:487
  154.2 3.5 %collective-permute-start.2 = (bf16[512,496]{1,0:T(8,128)(2,1)S(1)}, bf16[512,496]{1,0:T(8,128)(2,1)}, u32[]{:S(2)}, u32[]{:S(2)}) collective-permute-start(bf16[512,496]{1,0:T(8,128)(2,1)S(1)} %get-tuple-element.24.p0), channel_id=1, source_target_pairs={{0,16},{8,24},{16,0},{24,8},{1,17},{9,25},{17,1},{25,9},{2,18},{10... | collective-permute-start | bytes 1523720 | tf_op jit(solution)/shard_map/ppermute | solution.py:487
  157.8 4.3 %collective-permute-start.3 = (bf16[512,496]{1,0:T(8,128)(2,1)S(1)}, bf16[512,496]{1,0:T(8,128)(2,1)}, u32[]{:S(2)}, u32[]{:S(2)}) collective-permute-start(bf16[512,496]{1,0:T(8,128)(2,1)S(1)} %get-tuple-element.24.p0), channel_id=1, source_target_pairs={{0,24},{8,0},{16,8},{24,16},{1,25},{9,1},{17,9},{25,17},{2,26},{10... | collective-permute-start | bytes 1523720 | tf_op jit(solution)/shard_map/ppermute | solution.py:487
  162.1 2.0 collective-permute-start.6
  164.1 0.0 collective-permute-done.5.p1
  164.1 3.5 %collective-permute-start.7 = (bf16[512,256]{1,0:T(8,128)(2,1)}, bf16[512,256]{1,0:T(8,128)(2,1)S(1)}, u32[]{:S(2)}, u32[]{:S(2)}) collective-permute-start(bf16[512,256]{1,0:T(8,128)(2,1)} %get-tuple-element.31.p0), channel_id=1, source_target_pairs={{0,24},{8,0},{16,8},{24,16},{1,25},{9,1},{17,9},{25,17},{2,26},{10... | collective-permute-start | bytes 786440 | tf_op jit(solution)/shard_map/ppermute | solution.py:487
  167.6 21.6 %collective-permute-done.6.p2 = bf16[512,256]{1,0:T(8,128)(2,1)S(1)} collective-permute-done((bf16[512,256]{1,0:T(8,128)(2,1)}, bf16[512,256]{1,0:T(8,128)(2,1)S(1)}, u32[]{:S(2)}, u32[]{:S(2)}) %collective-permute-start.6) | collective-permute-done | bytes 262176 | tf_op jit(solution)/shard_map/ppermute | solution.py:487
  189.2 2.7 %collective-permute-done.7.p3 = bf16[512,256]{1,0:T(8,128)(2,1)S(1)} collective-permute-done((bf16[512,256]{1,0:T(8,128)(2,1)}, bf16[512,256]{1,0:T(8,128)(2,1)S(1)}, u32[]{:S(2)}, u32[]{:S(2)}) %collective-permute-start.7) | collective-permute-done | bytes 262176 | tf_op jit(solution)/shard_map/ppermute | solution.py:487
  191.9 4.8 %shard_map.151 = (f32[768,128]{1,0:T(8,128)}, f32[2,768]{1,0:T(2,128)}) custom-call(s32[1]{0:T(128)} %bitcast.1.core, s32[1]{0:T(128)} %bitcast.y, bf16[448,2048]{1,0:T(8,128)(2,1)S(1)} %bitcast.20, bf16[448,2048]{1,0:T(8,128)(2,1)} %collective-permute-done.4.other, bf16[512,256]{1,0:T(8,128)(2,1)} %get-tuple-element.31.p0, ...), custom_call_target="tpu_custom_call" | custom-call | tf_op jit(solution)/shard_map/pallas_call | solution.py:37
  196.7 1.9 collective-permute-start.8
  198.6 1.3 collective-permute-done.8
  200.0 0.7 add.15.moments_0
  200.7 5.2 %collective-permute-start.10 = (f32[2,768]{1,0:T(2,128)S(1)}, f32[2,768]{1,0:T(2,128)S(1)}, u32[]{:S(2)}, u32[]{:S(2)}) collective-permute-start(f32[2,768]{1,0:T(2,128)S(1)} %add.15.moments_0), channel_id=1, source_target_pairs={{0,4},{2,6},{4,0},{6,2},{1,5},{3,7},{5,1},{7,3},{8,12},{10,14},{12... | collective-permute-start | bytes 18440 | tf_op jit(solution)/shard_map/ppermute | solution.py:487
  205.9 3.1 %collective-permute-start.11 = (f32[2,768]{1,0:T(2,128)S(1)}, f32[2,768]{1,0:T(2,128)}, u32[]{:S(2)}, u32[]{:S(2)}) collective-permute-start(f32[2,768]{1,0:T(2,128)S(1)} %add.15.moments_0), channel_id=1, source_target_pairs={{0,6},{2,0},{4,2},{6,4},{1,7},{3,1},{5,3},{7,5},{8,14},{10,8},{12,... | collective-permute-start | bytes 18440 | tf_op jit(solution)/shard_map/ppermute | solution.py:487
  209.0 0.0 collective-permute-done.1.p1
  209.0 2.8 %collective-permute-start.9 = (f32[2,768]{1,0:T(2,128)S(1)}, f32[2,768]{1,0:T(2,128)}, u32[]{:S(2)}, u32[]{:S(2)}) collective-permute-start(f32[2,768]{1,0:T(2,128)S(1)} %add.15.moments_0), channel_id=1, source_target_pairs={{0,2},{2,4},{4,6},{6,0},{1,3},{3,5},{5,7},{7,1},{8,10},{10,12},{12... | collective-permute-start | bytes 18440 | tf_op jit(solution)/shard_map/ppermute | solution.py:487
  211.8 0.0 collective-permute-done.2.p2
  211.8 0.0 collective-permute-done.3.p3
  211.8 6.0 %shard_map.150 = (bf16[768,256]{1,0:T(8,128)(2,1)}, f32[768,128]{1,0:T(8,128)}) custom-call(s32[1]{0:T(128)} %bitcast.1.core, s32[1]{0:T(128)} %bitcast.y, bf16[448,2048]{1,0:T(8,128)(2,1)S(1)} %bitcast.21, bf16[448,2048]{1,0:T(8,128)(2,1)} %collective-permute-done.4.other, bf16[512,496]{1,0:T(8,128)(2,1)S(1)} %get-tuple-element.24.p0, ...), custom_call_target="tpu_custom_call" | custom-call | tf_op jit(solution)/shard_map/pallas_call | solution.py:37
  217.8 0.0 copy-done.4
  217.8 0.0 collective-permute-done.10.moments_2
  217.8 0.0 copy-start.5
  217.8 0.0 collective-permute-done.11.moments_3
  217.8 0.0 collective-permute-done.9.moments_1
  217.8 0.0 all-to-all-done.3.outer
  217.8 0.6 copy-done.5
  218.4 5.5 %shard_map.152 = (bf16[384,256]{1,0:T(8,128)(2,1)S(1)}, bf16[384,2048]{1,0:T(8,128)(2,1)S(1)}, bf16[16,2048]{1,0:T(8,128)(2,1)S(1)}) custom-call(s32[1]{0:T(128)} %bitcast.1.core, s32[1]{0:T(128)} %bitcast.y, s32[1]{0:T(128)} %bitcast.2.position.low, s32[1]{0:T(128)} %bitcast.3.high, bf16[512,496]{1,0:T(8,128)(2,1)S(1)} %get-tuple-element.24.p0, ...), custom_call_target="tpu_custom_call" | custom-call | tf_op jit(solution)/shard_map/pallas_call | solution.py:37
  223.9 1.9 collective-permute-start.12
  225.9 3.4 %collective-permute-done.12.arrived = bf16[384,2048]{1,0:T(8,128)(2,1)S(1)} collective-permute-done((bf16[384,2048]{1,0:T(8,128)(2,1)S(1)}, bf16[384,2048]{1,0:T(8,128)(2,1)S(1)}, u32[]{:S(2)}, u32[]{:S(2)}) %collective-permute-start.12) | collective-permute-done | bytes 1572896 | tf_op jit(solution)/shard_map/ppermute | solution.py:487
  229.3 2.2 shard_map.153
  231.5 24.5 %all_to_all.25.parts = bf16[4,96,2048]{2,1,0:T(8,128)(2,1)S(1)} all-to-all(bf16[4,96,2048]{2,1,0:T(8,128)(2,1)S(1)} %bitcast.22), channel_id=1, replica_groups=mesh['zh'=4,'zl'=4,'y'=4,'x'=4,'c'=2] {'x'}, dimensions={0} | all-to-all | bytes 3145728 | tf_op jit(solution)/shard_map/all_to_all | solution.py:663
  255.9 1.3 shard_map.154
  (8 shorter events, 0.0 us)
Async XLA Ops:
  0.9 6.2 %collective-permute-start = (bf16[16,2048]{1,0:T(8,128)(2,1)S(1)}, bf16[16,2048]{1,0:T(8,128)(2,1)S(1)}, u32[]{:S(2)}, u32[]{:S(2)}) collective-permute-start(bf16[16,2048]{1,0:T(8,128)(2,1)S(1)} %slice_select_fusion), channel_id=1, source_target_pairs={{7,15},{15,23},{23,31},{31,39},{39,47},{47,55},{55,63},{63,71},{71... | collective-permute-start | bytes 196616 | tf_op jit(solution)/shard_map/ppermute | solution.py:514
  10.4 3.8 %copy-start.2 = (bf16[32,1008]{1,0:T(8,128)(2,1)S(1)}, bf16[32,1008]{1,0:T(8,128)(2,1)}, u32[]{:S(2)}) copy-start(bf16[32,1008]{1,0:T(8,128)(2,1)} %shard_map.145) | copy-start | bytes 193540
  10.4 45.7 %all-to-all-start = ((bf16[4,112,2048]{2,1,0:T(8,128)(2,1)}), bf16[4,112,2048]{2,1,0:T(8,128)(2,1)S(1)}, u32[]{:S(2)}, u32[]{:S(2)}) async-start(bf16[4,112,2048]{2,1,0:T(8,128)(2,1)} %shard_map.146), calls=%async_computation | async-start | bytes 3670016 | tf_op jit(solution)/shard_map/all_to_all | solution.py:551
  56.1 43.1 %copy-start.3 = (bf16[128,32]{0,1:T(8,128)(2,1)S(1)}, bf16[128,32]{0,1:T(8,128)(2,1)}, u32[]{:S(2)}) copy-start(bf16[128,32]{0,1:T(8,128)(2,1)} %param.29) | copy-start | bytes 24580
  56.1 43.2 %copy-start.6 = (f32[2,768]{1,0:T(2,128)S(1)}, f32[2,768]{1,0:T(2,128)}, u32[]{:S(2)}) copy-start(f32[2,768]{1,0:T(2,128)} %param.25) | copy-start | bytes 18436
  56.1 57.8 %collective-permute-start.4 = (bf16[448,2048]{1,0:T(8,128)(2,1)S(1)}, bf16[448,2048]{1,0:T(8,128)(2,1)}, u32[]{:S(2)}, u32[]{:S(2)}) collective-permute-start(bf16[448,2048]{1,0:T(8,128)(2,1)S(1)} %bitcast.18), channel_id=1, source_target_pairs={{0,1},{1,0},{2,3},{3,2},{4,5},{5,4},{6,7},{7,6},{8,9},{9,8},{10,11... | collective-permute-start | bytes 5505032 | tf_op jit(solution)/shard_map/ppermute | solution.py:487
  91.8 22.1 %all-to-all-start.1 = ((bf16[4,512,256]{2,1,0:T(8,128)(2,1)}), bf16[4,512,256]{2,1,0:T(8,128)(2,1)}, u32[]{:S(2)}, u32[]{:S(2)}) async-start(bf16[4,512,256]{2,1,0:T(8,128)(2,1)} %get-tuple-element.26), calls=%async_computation.1 | async-start | bytes 2097152 | tf_op jit(solution)/shard_map/all_to_all | solution.py:568
  100.3 17.8 %copy-start = (f32[8,768]{1,0:T(8,128)}, f32[8,768]{1,0:T(8,128)S(1)}, u32[]{:S(2)}) copy-start(f32[8,768]{1,0:T(8,128)S(1)} %concatenate.3.running.running_far) | copy-start | bytes 73732
  118.2 73.7 %copy-start.1 = (f32[31,128]{1,0:T(8,128)S(1)}, f32[31,128]{1,0:T(8,128)}, u32[]{:S(2)}) copy-start(f32[31,128]{1,0:T(8,128)} %taps.1) | copy-start | bytes 47620
  118.2 21.8 %all-to-all-start.2 = ((bf16[16,160,128]{2,1,0:T(8,128)(2,1)}), bf16[16,160,128]{2,1,0:T(8,128)(2,1)S(1)}, u32[]{:S(2)}, u32[]{:S(2)}) async-start(bf16[16,160,128]{2,1,0:T(8,128)(2,1)} %get-tuple-element.27), calls=%async_computation.2 | async-start | bytes 1310720 | tf_op jit(solution)/shard_map/all_to_all | solution.py:589
  140.9 77.0 %all-to-all-start.3 = ((bf16[4,208,128]{2,1,0:T(8,128)(2,1)}), bf16[4,208,128]{2,1,0:T(8,128)(2,1)}, u32[]{:S(2)}, u32[]{:S(2)}) async-start(bf16[4,208,128]{2,1,0:T(8,128)(2,1)} %shard_map.149), calls=%async_computation.3 | async-start | bytes 425984 | tf_op jit(solution)/shard_map/all_to_all | solution.py:598
  147.9 16.1 %collective-permute-start.5 = (bf16[512,256]{1,0:T(8,128)(2,1)}, bf16[512,256]{1,0:T(8,128)(2,1)S(1)}, u32[]{:S(2)}, u32[]{:S(2)}) collective-permute-start(bf16[512,256]{1,0:T(8,128)(2,1)} %get-tuple-element.31.p0), channel_id=1, source_target_pairs={{0,8},{8,16},{16,24},{24,0},{1,9},{9,17},{17,25},{25,1},{2,10},{10... | collective-permute-start | bytes 786440 | tf_op jit(solution)/shard_map/ppermute | solution.py:487
  151.5 57.5 %collective-permute-start.1 = (bf16[512,496]{1,0:T(8,128)(2,1)S(1)}, bf16[512,496]{1,0:T(8,128)(2,1)S(1)}, u32[]{:S(2)}, u32[]{:S(2)}) collective-permute-start(bf16[512,496]{1,0:T(8,128)(2,1)S(1)} %get-tuple-element.24.p0), channel_id=1, source_target_pairs={{0,8},{8,16},{16,24},{24,0},{1,9},{9,17},{17,25},{25,1},{2,10},{10... | collective-permute-start | bytes 1523720 | tf_op jit(solution)/shard_map/ppermute | solution.py:487
  154.2 57.5 %collective-permute-start.2 = (bf16[512,496]{1,0:T(8,128)(2,1)S(1)}, bf16[512,496]{1,0:T(8,128)(2,1)}, u32[]{:S(2)}, u32[]{:S(2)}) collective-permute-start(bf16[512,496]{1,0:T(8,128)(2,1)S(1)} %get-tuple-element.24.p0), channel_id=1, source_target_pairs={{0,16},{8,24},{16,0},{24,8},{1,17},{9,25},{17,1},{25,9},{2,18},{10... | collective-permute-start | bytes 1523720 | tf_op jit(solution)/shard_map/ppermute | solution.py:487
  157.8 54.0 %collective-permute-start.3 = (bf16[512,496]{1,0:T(8,128)(2,1)S(1)}, bf16[512,496]{1,0:T(8,128)(2,1)}, u32[]{:S(2)}, u32[]{:S(2)}) collective-permute-start(bf16[512,496]{1,0:T(8,128)(2,1)S(1)} %get-tuple-element.24.p0), channel_id=1, source_target_pairs={{0,24},{8,0},{16,8},{24,16},{1,25},{9,1},{17,9},{25,17},{2,26},{10... | collective-permute-start | bytes 1523720 | tf_op jit(solution)/shard_map/ppermute | solution.py:487
  162.1 27.1 %collective-permute-start.6 = (bf16[512,256]{1,0:T(8,128)(2,1)}, bf16[512,256]{1,0:T(8,128)(2,1)S(1)}, u32[]{:S(2)}, u32[]{:S(2)}) collective-permute-start(bf16[512,256]{1,0:T(8,128)(2,1)} %get-tuple-element.31.p0), channel_id=1, source_target_pairs={{0,16},{8,24},{16,0},{24,8},{1,17},{9,25},{17,1},{25,9},{2,18},{10... | collective-permute-start | bytes 786440 | tf_op jit(solution)/shard_map/ppermute | solution.py:487
  164.1 27.8 %collective-permute-start.7 = (bf16[512,256]{1,0:T(8,128)(2,1)}, bf16[512,256]{1,0:T(8,128)(2,1)S(1)}, u32[]{:S(2)}, u32[]{:S(2)}) collective-permute-start(bf16[512,256]{1,0:T(8,128)(2,1)} %get-tuple-element.31.p0), channel_id=1, source_target_pairs={{0,24},{8,0},{16,8},{24,16},{1,25},{9,1},{17,9},{25,17},{2,26},{10... | collective-permute-start | bytes 786440 | tf_op jit(solution)/shard_map/ppermute | solution.py:487
  196.7 3.3 %collective-permute-start.8 = (f32[2,768]{1,0:T(2,128)}, f32[2,768]{1,0:T(2,128)S(1)}, u32[]{:S(2)}, u32[]{:S(2)}) collective-permute-start(f32[2,768]{1,0:T(2,128)} %get-tuple-element.33), channel_id=1, source_target_pairs={{0,1},{1,0},{2,3},{3,2},{4,5},{5,4},{6,7},{7,6},{8,9},{9,8},{10,11... | collective-permute-start | bytes 18440 | tf_op jit(solution)/shard_map/ppermute | solution.py:487
  200.7 17.1 %copy-start.4 = (f32[2,768]{1,0:T(2,128)}, f32[2,768]{1,0:T(2,128)S(1)}, u32[]{:S(2)}) copy-start(f32[2,768]{1,0:T(2,128)S(1)} %add.15.moments_0) | copy-start | bytes 18436
  200.7 17.1 %collective-permute-start.10 = (f32[2,768]{1,0:T(2,128)S(1)}, f32[2,768]{1,0:T(2,128)S(1)}, u32[]{:S(2)}, u32[]{:S(2)}) collective-permute-start(f32[2,768]{1,0:T(2,128)S(1)} %add.15.moments_0), channel_id=1, source_target_pairs={{0,4},{2,6},{4,0},{6,2},{1,5},{3,7},{5,1},{7,3},{8,12},{10,14},{12... | collective-permute-start | bytes 18440 | tf_op jit(solution)/shard_map/ppermute | solution.py:487
  205.9 11.9 %collective-permute-start.11 = (f32[2,768]{1,0:T(2,128)S(1)}, f32[2,768]{1,0:T(2,128)}, u32[]{:S(2)}, u32[]{:S(2)}) collective-permute-start(f32[2,768]{1,0:T(2,128)S(1)} %add.15.moments_0), channel_id=1, source_target_pairs={{0,6},{2,0},{4,2},{6,4},{1,7},{3,1},{5,3},{7,5},{8,14},{10,8},{12,... | collective-permute-start | bytes 18440 | tf_op jit(solution)/shard_map/ppermute | solution.py:487
  209.0 8.8 %collective-permute-start.9 = (f32[2,768]{1,0:T(2,128)S(1)}, f32[2,768]{1,0:T(2,128)}, u32[]{:S(2)}, u32[]{:S(2)}) collective-permute-start(f32[2,768]{1,0:T(2,128)S(1)} %add.15.moments_0), channel_id=1, source_target_pairs={{0,2},{2,4},{4,6},{6,0},{1,3},{3,5},{5,7},{7,1},{8,10},{10,12},{12... | collective-permute-start | bytes 18440 | tf_op jit(solution)/shard_map/ppermute | solution.py:487
  217.8 0.6 copy-start.5
  223.9 5.3 %collective-permute-start.12 = (bf16[384,2048]{1,0:T(8,128)(2,1)S(1)}, bf16[384,2048]{1,0:T(8,128)(2,1)S(1)}, u32[]{:S(2)}, u32[]{:S(2)}) collective-permute-start(bf16[384,2048]{1,0:T(8,128)(2,1)S(1)} %get-tuple-element.35), channel_id=1, source_target_pairs={{0,1},{1,0},{2,3},{3,2},{4,5},{5,4},{6,7},{7,6},{8,9},{9,8},{10,11... | collective-permute-start | bytes 4718600 | tf_op jit(solution)/shard_map/ppermute | solution.py:487

commit v5 on v3

--- a/solution.py
+++ b/solution.py
@@ -19,7 +19,7 @@
 HBM = pl.BlockSpec(memory_space=pltpu.HBM)
 
 
-def call(kernel, out_shape, scalars, arrays, scratch=(), grant=20, far=(), out_far=()):
+def call(kernel, out_shape, scalars, arrays, scratch=(), grant=20, far=(), out_far=(), aliases={}):
     def specs(count, away):
         return [HBM if i in away else VMEM for i in range(count)]
 
@@ -41,6 +41,7 @@
         out_specs=outs,
         scratch_shapes=scratch,
         compiler_params=pltpu.CompilerParams(vmem_limit_bytes=grant * 1024 * 1024),
+        input_output_aliases=aliases,
     )(*scalars, *arrays)
 
 
@@ -78,34 +79,42 @@
     out[:, 896:1008] = oh[:, 0:112]
 
 
-def norm_kernel(tokens_far, edge, gain_far, out_far, tokens, gain, out, semaphores):
+def normed_rows(source, at, gain, out, to):
     rows = 16
+    x = source[at, :].astype(F32)
+    inverse = lax.rsqrt(jnp.mean(x * x, axis=1, keepdims=True) + EPSILON)
+    normed = x * inverse * gain[...]
+
+    def read(zh, zl):
+        z = zh * 4 + zl
+        return normed[:, z * 128 : z * 128 + 128]
+
+    def write(zh, y, made):
+        where = (y * 4 + zh) * 128
+        out[to, where : where + 128] = made.astype(BF16)
+
+    swap_groups(read, write, rows)
+
+
+def norm_kernel(tokens_far, gain_far, out_far, tokens, gain, out, semaphores):
     for copy in start_copies(((tokens_far, tokens), (gain_far, gain)), semaphores):
         copy.wait()
 
-    def block(source, at, to):
-        x = source[at, :].astype(F32)
-        inverse = lax.rsqrt(jnp.mean(x * x, axis=1, keepdims=True) + EPSILON)
-        normed = x * inverse * gain[...]
-
-        def read(zh, zl):
-            z = zh * 4 + zl
-            return normed[:, z * 128 : z * 128 + 128]
-
-        def write(zh, y, made):
-            where = (y * 4 + zh) * 128
-            out[to, where : where + 128] = made.astype(BF16)
-
-        swap_groups(read, write, rows)
-
     def step(i, carry):
-        at = pl.ds(pl.multiple_of(i * rows, rows), rows)
-        block(tokens, at, at)
+        at = pl.ds(pl.multiple_of(i * 16, 16), 16)
+        normed_rows(tokens, at, gain, out, at)
         return carry
 
     lax.fori_loop(0, 6, step, 0, unroll=2)
-    block(edge, slice(0, 16), slice(96, 112))
-    for copy in start_copies([(out, out_far.at[k]) for k in range(4)], semaphores):
+    pairs = [(out, out_far.at[k, 0:96, :]) for k in range(4)]
+    for copy in start_copies(pairs, semaphores):
+        copy.wait()
+
+
+def edge_kernel(edge, gain, given_far, out_far, out, semaphores):
+    normed_rows(edge, slice(0, 16), gain, out, slice(0, 16))
+    pairs = [(out, out_far.at[k, 96:112, :]) for k in range(4)]
+    for copy in start_copies(pairs, semaphores):
         copy.wait()
 
 
@@ -381,9 +390,6 @@
     for i in range(6):
         at = slice(i * rows, (i + 1) * rows)
         q = pair[at, 0:128]
-        diagonal = lax.broadcasted_iota(jnp.int32, (rows, 768), 1) == (
-            lax.broadcasted_iota(jnp.int32, (rows, 768), 0) + i * rows
-        )
         log = jnp.where(half, turned[at, 1:2], turned[at, 0:1])
         closing = jnp.where(half[0:1], turned[767:768, 1:2], turned[767:768, 0:1])
         retained = jnp.exp(log) * jnp.dot(q, forward, preferred_element_type=F32)
@@ -395,10 +401,12 @@
                 jnp.where(masks[h][:rows], q, zero), k, NT, preferred_element_type=F32
             )
             distance = jnp.abs(turned[at, h : h + 1] - logs[h : h + 1, :])
-            weights = jnp.exp(-distance) + jnp.where(diagonal, 1.0, 0.0)
+            weights = jnp.exp(-distance)
             retained = retained + jnp.dot(
                 (scores * weights).astype(BF16), head_values[h], preferred_element_type=F32
             )
+        same = q.astype(F32) * k[at, :].astype(F32)
+        retained = retained + 64 * head_mean(same) * v[at, :].astype(F32)
         centred = retained - head_mean(retained)
         normed = centred * lax.rsqrt(head_mean(centred * centred) + EPSILON)
         gate = jax.nn.silu(pair[at, 128:256].astype(F32))
@@ -488,19 +496,33 @@
         ),
         grant=56,
     )
+    running = jnp.cumsum(decay_logs, axis=1)
+    running = jnp.concatenate([running, jnp.zeros((6, 768), F32)], axis=0)
+    tail = jnp.pad(output_heads[112:], ((0, 0), (0, 96)))
     normed = call(
         norm_kernel,
         shape((4, 112, 2048), BF16),
         (),
-        (tokens, edge, input_gain[None]),
+        (tokens, input_gain[None]),
         scratch=(
             pltpu.VMEM((96, 2048), BF16),
             pltpu.VMEM((1, 2048), F32),
-            pltpu.VMEM((112, 2048), BF16),
+            pltpu.VMEM((96, 2048), BF16),
             pltpu.SemaphoreType.DMA((4,)),
         ),
-        far=(0, 2),
+        far=(0, 1),
         out_far=(0,),
+    )
+    edge, normed, running, tail = lax.optimization_barrier((edge, normed, running, tail))
+    normed = call(
+        edge_kernel,
+        shape((4, 112, 2048), BF16),
+        (),
+        (edge, input_gain[None], normed),
+        scratch=(pltpu.VMEM((16, 2048), BF16), pltpu.SemaphoreType.DMA((4,))),
+        far=(2,),
+        out_far=(0,),
+        aliases={2: 0},
     )
     shard, normed = lax.optimization_barrier((shard, normed))
     own = lax.all_to_all(normed, "x", 0, 0, tiled=True).reshape(448, 2048)
@@ -512,11 +534,7 @@
     gate_pieces = (gate_piece,) + tuple(ring(gate_piece, "y", d) for d in (1, 2, 3))
     rest_pieces = (rest_piece,) + tuple(ring(rest_piece, "y", d) for d in (1, 2, 3))
 
-    running = jnp.cumsum(decay_logs, axis=1)
-    running = jnp.concatenate([running, jnp.zeros((6, 768), F32)], axis=0)
-
     full = shape((768, 128), F32)
-    tail = jnp.pad(output_heads[112:], ((0, 0), (0, 96)))
     both, sent = call(
         states_kernel,
         (shape((768, 256), BF16), shape((16, 160, 128), BF16)),

time: 224 us -> 224 us (level)
  blocking collectives: 80.3 us -> 99.1 us
  waiting for transfers between devices: 59.3 us -> 44.3 us
  starting transfers between devices: 49.9 us -> 44.4 us
  local copies, waits for them, and re-layouts: 4.86 us -> 8.31 us
    all_to_all x0 -> x1, blocking collectives: none -> 18.5 us  [copies(): lax.all_to_all(jnp.broadcast_to(x[None], (count, *x.shape)), axes, 0, 0,...]
    all_to_all x1 -> x0, waiting for transfers between devices: 14.5 us -> none  [copies(): lax.all_to_all(jnp.broadcast_to(x[None], (count, *x.shape)), axes, 0, 0,...]
    all_to_all x1 -> x0, starting transfers between devices: 5.47 us -> none  [copies(): lax.all_to_all(jnp.broadcast_to(x[None], (count, *x.shape)), axes, 0, 0,...]
    unnamed x18 -> x22, local copies, waits for them, and re-layouts: 1.76 us -> 4.75 us
    pallas_call x8 -> x9, Pallas kernels: 26.8 us -> 24.9 us  [call(): pl.pallas_call(kernel, out_shape=out_shape, in_specs=[SMEM] * len(scalars...]
  transfers between devices with their start and end apart: 13 -> 12, of which waited for: 6 -> 4; matrix products, arithmetic and copies ran while one was open for 2% -> 2% of each run, Pallas kernels for 3% -> 4%
where the time goes in v5:
time: 224 us; the launch traced here: 223 us
  blocking collectives  99.1 us (44%)
  starting transfers between devices  44.4 us (20%)
  waiting for transfers between devices  44.3 us (20%)
  Pallas kernels  24.9 us (11%)
  local copies, waits for them, and re-layouts  8.31 us (4%)
    all_gather x1, blocking collectives, body(): rows = lax.all_gather(shard, ('zh', 'zl'), axis=0, tiled=True)  41.1 us
    ppermute x8, waiting for transfers between devices, ring(): lax.ppermute(x, axis, [(i, (i + shift) % count) for i in range(count)])  27 us
    pallas_call x9, Pallas kernels, call(): pl.pallas_call(kernel, out_shape=out_shape, in_specs=[SMEM] * len(scalars...  24.9 us
    all_to_all x1, blocking collectives, body(): parts = lax.all_to_all(joined.reshape(4, 96, 2048), 'x', 0, 0, tiled=True)  24.8 us
    ppermute x8, starting transfers between devices, ring(): lax.ppermute(x, axis, [(i, (i + shift) % count) for i in range(count)])  23.8 us
    all_to_all x1, blocking collectives, copies(): lax.all_to_all(jnp.broadcast_to(x[None], (count, *x.shape)), axes, 0, 0,...  18.5 us
    all_to_all x1, waiting for transfers between devices, body(): inner = lax.all_to_all(sent, ('zl', 'y'), 0, 0, tiled=True)  17.3 us
    all_gather x1, blocking collectives, body(): moments = lax.all_gather(moments, ('x', 'c'))  14.7 us
  transfers between devices with their start and end apart: 12, of which 4 were waited for; matrix products, arithmetic and copies ran while one was open for 2% of the time, Pallas kernels for 4%

profile of v5, /device:TPU:32, one launch (start us, length us, event | category | flops | bytes accessed | tf_op | source)
XLA Modules:
  0.0 223.0 jit_solution(12729926177079902180)
XLA Ops:
  0.0 0.0 copy-start.6
  0.0 0.9 slice_select_fusion
  0.9 4.5 %collective-permute-start = (bf16[16,2048]{1,0:T(8,128)(2,1)S(1)}, bf16[16,2048]{1,0:T(8,128)(2,1)S(1)}, u32[]{:S(2)}, u32[]{:S(2)}) collective-permute-start(bf16[16,2048]{1,0:T(8,128)(2,1)S(1)} %slice_select_fusion), channel_id=1, source_target_pairs={{7,15},{15,23},{23,31},{31,39},{39,47},{47,55},{55,63},{63,71},{71... | collective-permute-start | bytes 196616 | tf_op jit(solution)/shard_map/ppermute | solution.py:477
  5.4 0.7 reshape.20
  6.1 0.6 reduce-window.6
  6.6 0.2 slice_reduce_fusion
  6.8 0.2 reduce-window.9
  7.0 0.1 add_bitcast_fusion
  7.1 0.8 slice.28
  7.8 0.1 copy.20
  7.9 0.0 copy-start.5
  7.9 3.1 %shard_map.146.given_far = bf16[4,112,2048]{2,1,0:T(8,128)(2,1)} custom-call(bf16[96,2048]{1,0:T(8,128)(2,1)} %tokens_far.1, f32[1,2048]{1,0:T(1,128)} %bitcast.25), custom_call_target="tpu_custom_call" | custom-call | tf_op jit(solution)/shard_map/pallas_call | solution.py:37
  11.0 1.5 shard_map.145
  12.5 0.0 collective-permute-done.edge
  12.5 0.0 copy-done.6
  12.5 1.0 shard_map.147
  13.5 0.0 copy-start.9
  13.5 3.7 %all-to-all-start = ((bf16[4,112,2048]{2,1,0:T(8,128)(2,1)}), bf16[4,112,2048]{2,1,0:T(8,128)(2,1)S(1)}, u32[]{:S(2)}, u32[]{:S(2)}) async-start(bf16[4,112,2048]{2,1,0:T(8,128)(2,1)} %shard_map.147), calls=%async_computation | async-start | bytes 3670016 | tf_op jit(solution)/shard_map/all_to_all | solution.py:528
  17.2 0.0 copy-done.9
  17.3 41.1 %all_gather.9 = bf16[512,1008]{1,0:T(8,128)(2,1)S(1)} all-gather(bf16[32,1008]{1,0:T(8,128)(2,1)S(1)} %copy-done.9), channel_id=1, replica_groups=mesh['zh'=4,'zl'=4,'y'=4,'x'=4,'c'=2] {'zh','zl'}, dimensions={0}, use_global_device_ids=true | all-gather | bytes 1096704 | tf_op jit(solution)/shard_map/all_gather | solution.py:529
  58.4 0.0 all-to-all-done
  58.4 1.9 collective-permute-start.1
  60.3 0.8 fusion
  61.1 0.1 broadcast_in_dim.34
  61.1 18.5 %all_to_all.25 = bf16[4,512,256]{2,1,0:T(8,128)(2,1)S(1)} all-to-all(bf16[4,512,256]{2,1,0:T(8,128)(2,1)S(1)} %broadcast_in_dim.34), channel_id=1, replica_groups=mesh['zh'=4,'zl'=4,'y'=4,'x'=4,'c'=2] {'y'}, dimensions={0} | all-to-all | bytes 2097152 | tf_op jit(solution)/shard_map/all_to_all | solution.py:448
  79.6 0.0 copy-done.8
  79.6 0.0 collective-permute-done.1.other
  79.6 0.0 copy-done.5
  79.6 2.8 %shard_map.148 = (bf16[768,256]{1,0:T(8,128)(2,1)}, bf16[16,160,128]{2,1,0:T(8,128)(2,1)}) custom-call(s32[1]{0:T(128)} %bitcast.1.core, bf16[448,2048]{1,0:T(8,128)(2,1)S(1)} %bitcast.20, bf16[448,2048]{1,0:T(8,128)(2,1)S(1)} %collective-permute-done.1.other, bf16[2048,256]{1,0:T(8,128)(2,1)S(1)} %bitcast.24, f32[8,768]{1,0:T(8,128)S(1)} %concatenate.3.running.running_far, ...), custom_call_target="tpu_custom_call" | custom-call | tf_op jit(solution)/shard_map/pallas_call | solution.py:37
  82.4 0.0 copy-done
  82.4 0.0 copy-start.7
  82.4 5.0 %all-to-all-start.2 = ((bf16[16,160,128]{2,1,0:T(8,128)(2,1)}), bf16[16,160,128]{2,1,0:T(8,128)(2,1)S(1)}, u32[]{:S(2)}, u32[]{:S(2)}) async-start(bf16[16,160,128]{2,1,0:T(8,128)(2,1)} %get-tuple-element.28), calls=%async_computation.2 | async-start | bytes 1310720 | tf_op jit(solution)/shard_map/all_to_all | solution.py:546
  87.4 17.3 %all-to-all-done.2.gathered.inner = bf16[16,160,128]{2,1,0:T(8,128)(2,1)S(1)} async-done(((bf16[16,160,128]{2,1,0:T(8,128)(2,1)}), bf16[16,160,128]{2,1,0:T(8,128)(2,1)S(1)}, u32[]{:S(2)}, u32[]{:S(2)}) %all-to-all-start.2) | async-done | bytes 655392 | tf_op jit(solution)/shard_map/all_to_all | solution.py:546
  104.7 0.9 shard_map.149
  105.6 7.5 %all-to-all-start.3 = ((bf16[4,208,128]{2,1,0:T(8,128)(2,1)}), bf16[4,208,128]{2,1,0:T(8,128)(2,1)}, u32[]{:S(2)}, u32[]{:S(2)}) async-start(bf16[4,208,128]{2,1,0:T(8,128)(2,1)} %shard_map.149), calls=%async_computation.3 | async-start | bytes 425984 | tf_op jit(solution)/shard_map/all_to_all | solution.py:555
  113.1 3.2 %collective-permute-start.7 = (bf16[512,256]{1,0:T(8,128)(2,1)}, bf16[512,256]{1,0:T(8,128)(2,1)S(1)}, u32[]{:S(2)}, u32[]{:S(2)}) collective-permute-start(bf16[512,256]{1,0:T(8,128)(2,1)} %get-tuple-element.35.p0), channel_id=1, source_target_pairs={{0,24},{8,0},{16,8},{24,16},{1,25},{9,1},{17,9},{25,17},{2,26},{10... | collective-permute-start | bytes 786440 | tf_op jit(solution)/shard_map/ppermute | solution.py:444
  116.3 1.1 slice.29.p0
  117.3 3.1 %collective-permute-start.4 = (bf16[512,496]{1,0:T(8,128)(2,1)S(1)}, bf16[512,496]{1,0:T(8,128)(2,1)S(1)}, u32[]{:S(2)}, u32[]{:S(2)}) collective-permute-start(bf16[512,496]{1,0:T(8,128)(2,1)S(1)} %slice.29.p0), channel_id=1, source_target_pairs={{0,24},{8,0},{16,8},{24,16},{1,25},{9,1},{17,9},{25,17},{2,26},{10... | collective-permute-start | bytes 1523720 | tf_op jit(solution)/shard_map/ppermute | solution.py:444
  120.4 3.5 %collective-permute-start.3 = (bf16[512,496]{1,0:T(8,128)(2,1)S(1)}, bf16[512,496]{1,0:T(8,128)(2,1)}, u32[]{:S(2)}, u32[]{:S(2)}) collective-permute-start(bf16[512,496]{1,0:T(8,128)(2,1)S(1)} %slice.29.p0), channel_id=1, source_target_pairs={{0,16},{8,24},{16,0},{24,8},{1,17},{9,25},{17,1},{25,9},{2,18},{10... | collective-permute-start | bytes 1523720 | tf_op jit(solution)/shard_map/ppermute | solution.py:444
  124.0 1.9 collective-permute-start.2
  125.9 5.3 %collective-permute-start.6 = (bf16[512,256]{1,0:T(8,128)(2,1)}, bf16[512,256]{1,0:T(8,128)(2,1)}, u32[]{:S(2)}, u32[]{:S(2)}) collective-permute-start(bf16[512,256]{1,0:T(8,128)(2,1)} %get-tuple-element.35.p0), channel_id=1, source_target_pairs={{0,16},{8,24},{16,0},{24,8},{1,17},{9,25},{17,1},{25,9},{2,18},{10... | collective-permute-start | bytes 786440 | tf_op jit(solution)/shard_map/ppermute | solution.py:444
  131.2 0.0 collective-permute-done.7.p3
  131.2 0.0 copy-start.3
  131.2 0.7 copy-done.3
  131.9 2.6 %collective-permute-start.5 = (bf16[512,256]{1,0:T(8,128)(2,1)}, bf16[512,256]{1,0:T(8,128)(2,1)}, u32[]{:S(2)}, u32[]{:S(2)}) collective-permute-start(bf16[512,256]{1,0:T(8,128)(2,1)} %get-tuple-element.35.p0), channel_id=1, source_target_pairs={{0,8},{8,16},{16,24},{24,0},{1,9},{9,17},{17,25},{25,1},{2,10},{10... | collective-permute-start | bytes 786440 | tf_op jit(solution)/shard_map/ppermute | solution.py:444
  134.5 21.1 %collective-permute-done.6.p2 = bf16[512,256]{1,0:T(8,128)(2,1)} collective-permute-done((bf16[512,256]{1,0:T(8,128)(2,1)}, bf16[512,256]{1,0:T(8,128)(2,1)}, u32[]{:S(2)}, u32[]{:S(2)}) %collective-permute-start.6) | collective-permute-done | bytes 262176 | tf_op jit(solution)/shard_map/ppermute | solution.py:444
  155.6 2.9 %collective-permute-done.5.p1 = bf16[512,256]{1,0:T(8,128)(2,1)} collective-permute-done((bf16[512,256]{1,0:T(8,128)(2,1)}, bf16[512,256]{1,0:T(8,128)(2,1)}, u32[]{:S(2)}, u32[]{:S(2)}) %collective-permute-start.5) | collective-permute-done | bytes 262176 | tf_op jit(solution)/shard_map/ppermute | solution.py:444
  158.5 0.0 copy-done.7
  158.5 1.5 copy-done.1
  160.0 0.9 copy-done.4
  160.9 4.4 %shard_map.150 = (f32[768,128]{1,0:T(8,128)}, f32[2,768]{1,0:T(2,128)}) custom-call(s32[1]{0:T(128)} %bitcast.1.core, s32[1]{0:T(128)} %bitcast.y, bf16[448,2048]{1,0:T(8,128)(2,1)S(1)} %bitcast.21, bf16[448,2048]{1,0:T(8,128)(2,1)S(1)} %copy-done.1, bf16[512,256]{1,0:T(8,128)(2,1)} %get-tuple-element.35.p0, bf16[512,256]{1,0:T(8,128)(2,1)} %collective-permute-done.5.p1, ...), custom_call_target="tpu_custom_call" | custom-call | tf_op jit(solution)/shard_map/pallas_call | solution.py:37
  165.3 14.7 %all-gather.1.moments_far = f32[8,2,768]{2,1,0:T(2,128)} all-gather(f32[1,2,768]{2,1,0:T(2,128)} %bitcast.30), channel_id=2, replica_groups=mesh['zh'=4,'zl'=4,'y'=4,'x'=4,'c'=2] {'x','c'}, dimensions={0}, use_global_device_ids=true | all-gather | bytes 55296 | tf_op jit(solution)/shard_map/all_gather | solution.py:569
  180.0 0.0 collective-permute-done.4.p3
  180.0 0.0 collective-permute-done.3.p2
  180.0 0.0 collective-permute-done.2.p1
  180.0 0.0 all-to-all-done.3.outer
  180.0 0.0 copy-start.2
  180.1 1.5 copy-done.2
  181.5 7.8 %shard_map.151 = (bf16[384,256]{1,0:T(8,128)(2,1)S(1)}, bf16[384,2048]{1,0:T(8,128)(2,1)S(1)}, bf16[16,2048]{1,0:T(8,128)(2,1)S(1)}) custom-call(s32[1]{0:T(128)} %bitcast.1.core, s32[1]{0:T(128)} %bitcast.y, s32[1]{0:T(128)} %bitcast.2.position.low, s32[1]{0:T(128)} %bitcast.3.high, bf16[448,2048]{1,0:T(8,128)(2,1)S(1)} %bitcast.22, ...), custom_call_target="tpu_custom_call" | custom-call | tf_op jit(solution)/shard_map/pallas_call | solution.py:37
  189.4 2.3 %collective-permute-start.8 = (bf16[384,2048]{1,0:T(8,128)(2,1)S(1)}, bf16[384,2048]{1,0:T(8,128)(2,1)S(1)}, u32[]{:S(2)}, u32[]{:S(2)}) collective-permute-start(bf16[384,2048]{1,0:T(8,128)(2,1)S(1)} %get-tuple-element.33), channel_id=1, source_target_pairs={{0,1},{1,0},{2,3},{3,2},{4,5},{5,4},{6,7},{7,6},{8,9},{9,8},{10,11... | collective-permute-start | bytes 4718600 | tf_op jit(solution)/shard_map/ppermute | solution.py:444
  191.7 3.0 %collective-permute-done.8.arrived = bf16[384,2048]{1,0:T(8,128)(2,1)S(1)} collective-permute-done((bf16[384,2048]{1,0:T(8,128)(2,1)S(1)}, bf16[384,2048]{1,0:T(8,128)(2,1)S(1)}, u32[]{:S(2)}, u32[]{:S(2)}) %collective-permute-start.8) | collective-permute-done | bytes 1572896 | tf_op jit(solution)/shard_map/ppermute | solution.py:444
  194.7 2.2 shard_map.152
  196.9 24.8 %all_to_all.26.parts = bf16[4,96,2048]{2,1,0:T(8,128)(2,1)S(1)} all-to-all(bf16[4,96,2048]{2,1,0:T(8,128)(2,1)S(1)} %bitcast.23), channel_id=1, replica_groups=mesh['zh'=4,'zl'=4,'y'=4,'x'=4,'c'=2] {'x'}, dimensions={0} | all-to-all | bytes 3145728 | tf_op jit(solution)/shard_map/all_to_all | solution.py:604
  221.8 1.3 shard_map.153
  (7 shorter events, 0.0 us)
Async XLA Ops:
  0.0 12.5 %copy-start.6 = (f32[2048]{0:T(1024)S(1)}, f32[2048]{0:T(1024)}, u32[]{:S(2)}) copy-start(f32[2048]{0:T(1024)} %param.16) | copy-start | bytes 24580
  0.9 11.6 %collective-permute-start = (bf16[16,2048]{1,0:T(8,128)(2,1)S(1)}, bf16[16,2048]{1,0:T(8,128)(2,1)S(1)}, u32[]{:S(2)}, u32[]{:S(2)}) collective-permute-start(bf16[16,2048]{1,0:T(8,128)(2,1)S(1)} %slice_select_fusion), channel_id=1, source_target_pairs={{7,15},{15,23},{23,31},{31,39},{39,47},{47,55},{55,63},{63,71},{71... | collective-permute-start | bytes 196616 | tf_op jit(solution)/shard_map/ppermute | solution.py:477
  7.9 71.7 %copy-start.5 = (f32[8,768]{1,0:T(8,128)}, f32[8,768]{1,0:T(8,128)S(1)}, u32[]{:S(2)}) copy-start(f32[8,768]{1,0:T(8,128)S(1)} %concatenate.3.running.running_far) | copy-start | bytes 73732
  13.5 3.8 %copy-start.9 = (bf16[32,1008]{1,0:T(8,128)(2,1)S(1)}, bf16[32,1008]{1,0:T(8,128)(2,1)}, u32[]{:S(2)}) copy-start(bf16[32,1008]{1,0:T(8,128)(2,1)} %shard_map.145) | copy-start | bytes 193540
  13.5 44.9 %all-to-all-start = ((bf16[4,112,2048]{2,1,0:T(8,128)(2,1)}), bf16[4,112,2048]{2,1,0:T(8,128)(2,1)S(1)}, u32[]{:S(2)}, u32[]{:S(2)}) async-start(bf16[4,112,2048]{2,1,0:T(8,128)(2,1)} %shard_map.147), calls=%async_computation | async-start | bytes 3670016 | tf_op jit(solution)/shard_map/all_to_all | solution.py:528
  58.4 21.2 %copy-start.8 = (bf16[512,1008]{1,0:T(8,128)(2,1)}, bf16[512,1008]{1,0:T(8,128)(2,1)S(1)}, u32[]{:S(2)}) copy-start(bf16[512,1008]{1,0:T(8,128)(2,1)S(1)} %all_gather.9) | copy-start | bytes 3096580
  58.4 21.2 %collective-permute-start.1 = (bf16[448,2048]{1,0:T(8,128)(2,1)S(1)}, bf16[448,2048]{1,0:T(8,128)(2,1)S(1)}, u32[]{:S(2)}, u32[]{:S(2)}) collective-permute-start(bf16[448,2048]{1,0:T(8,128)(2,1)S(1)} %bitcast.19), channel_id=1, source_target_pairs={{0,1},{1,0},{2,3},{3,2},{4,5},{5,4},{6,7},{7,6},{8,9},{9,8},{10,11... | collective-permute-start | bytes 5505032 | tf_op jit(solution)/shard_map/ppermute | solution.py:444
  79.6 2.8 %copy-start = (bf16[448,2048]{1,0:T(8,128)(2,1)}, bf16[448,2048]{1,0:T(8,128)(2,1)S(1)}, u32[]{:S(2)}) copy-start(bf16[448,2048]{1,0:T(8,128)(2,1)S(1)} %collective-permute-done.1.other) | copy-start | bytes 5505028
  82.4 76.1 %copy-start.7 = (f32[31,128]{1,0:T(8,128)S(1)}, f32[31,128]{1,0:T(8,128)}, u32[]{:S(2)}) copy-start(f32[31,128]{1,0:T(8,128)} %taps.1) | copy-start | bytes 47620
  82.4 22.3 %all-to-all-start.2 = ((bf16[16,160,128]{2,1,0:T(8,128)(2,1)}), bf16[16,160,128]{2,1,0:T(8,128)(2,1)S(1)}, u32[]{:S(2)}, u32[]{:S(2)}) async-start(bf16[16,160,128]{2,1,0:T(8,128)(2,1)} %get-tuple-element.28), calls=%async_computation.2 | async-start | bytes 1310720 | tf_op jit(solution)/shard_map/all_to_all | solution.py:546
  105.6 74.4 %all-to-all-start.3 = ((bf16[4,208,128]{2,1,0:T(8,128)(2,1)}), bf16[4,208,128]{2,1,0:T(8,128)(2,1)}, u32[]{:S(2)}, u32[]{:S(2)}) async-start(bf16[4,208,128]{2,1,0:T(8,128)(2,1)} %shard_map.149), calls=%async_computation.3 | async-start | bytes 425984 | tf_op jit(solution)/shard_map/all_to_all | solution.py:555
  113.1 18.1 %collective-permute-start.7 = (bf16[512,256]{1,0:T(8,128)(2,1)}, bf16[512,256]{1,0:T(8,128)(2,1)S(1)}, u32[]{:S(2)}, u32[]{:S(2)}) collective-permute-start(bf16[512,256]{1,0:T(8,128)(2,1)} %get-tuple-element.35.p0), channel_id=1, source_target_pairs={{0,24},{8,0},{16,8},{24,16},{1,25},{9,1},{17,9},{25,17},{2,26},{10... | collective-permute-start | bytes 786440 | tf_op jit(solution)/shard_map/ppermute | solution.py:444
  117.3 62.7 %collective-permute-start.4 = (bf16[512,496]{1,0:T(8,128)(2,1)S(1)}, bf16[512,496]{1,0:T(8,128)(2,1)S(1)}, u32[]{:S(2)}, u32[]{:S(2)}) collective-permute-start(bf16[512,496]{1,0:T(8,128)(2,1)S(1)} %slice.29.p0), channel_id=1, source_target_pairs={{0,24},{8,0},{16,8},{24,16},{1,25},{9,1},{17,9},{25,17},{2,26},{10... | collective-permute-start | bytes 1523720 | tf_op jit(solution)/shard_map/ppermute | solution.py:444
  120.4 59.6 %collective-permute-start.3 = (bf16[512,496]{1,0:T(8,128)(2,1)S(1)}, bf16[512,496]{1,0:T(8,128)(2,1)}, u32[]{:S(2)}, u32[]{:S(2)}) collective-permute-start(bf16[512,496]{1,0:T(8,128)(2,1)S(1)} %slice.29.p0), channel_id=1, source_target_pairs={{0,16},{8,24},{16,0},{24,8},{1,17},{9,25},{17,1},{25,9},{2,18},{10... | collective-permute-start | bytes 1523720 | tf_op jit(solution)/shard_map/ppermute | solution.py:444
  124.0 56.1 %collective-permute-start.2 = (bf16[512,496]{1,0:T(8,128)(2,1)S(1)}, bf16[512,496]{1,0:T(8,128)(2,1)}, u32[]{:S(2)}, u32[]{:S(2)}) collective-permute-start(bf16[512,496]{1,0:T(8,128)(2,1)S(1)} %slice.29.p0), channel_id=1, source_target_pairs={{0,8},{8,16},{16,24},{24,0},{1,9},{9,17},{17,25},{25,1},{2,10},{10... | collective-permute-start | bytes 1523720 | tf_op jit(solution)/shard_map/ppermute | solution.py:444
  125.9 29.7 %collective-permute-start.6 = (bf16[512,256]{1,0:T(8,128)(2,1)}, bf16[512,256]{1,0:T(8,128)(2,1)}, u32[]{:S(2)}, u32[]{:S(2)}) collective-permute-start(bf16[512,256]{1,0:T(8,128)(2,1)} %get-tuple-element.35.p0), channel_id=1, source_target_pairs={{0,16},{8,24},{16,0},{24,8},{1,17},{9,25},{17,1},{25,9},{2,18},{10... | collective-permute-start | bytes 786440 | tf_op jit(solution)/shard_map/ppermute | solution.py:444
  131.2 0.7 copy-start.3
  131.9 26.6 %collective-permute-start.5 = (bf16[512,256]{1,0:T(8,128)(2,1)}, bf16[512,256]{1,0:T(8,128)(2,1)}, u32[]{:S(2)}, u32[]{:S(2)}) collective-permute-start(bf16[512,256]{1,0:T(8,128)(2,1)} %get-tuple-element.35.p0), channel_id=1, source_target_pairs={{0,8},{8,16},{16,24},{24,0},{1,9},{9,17},{17,25},{25,1},{2,10},{10... | collective-permute-start | bytes 786440 | tf_op jit(solution)/shard_map/ppermute | solution.py:444
  158.5 1.5 copy-start.1
  160.0 0.9 copy-start.4
  180.0 1.5 copy-start.2
  189.4 5.3 %collective-permute-start.8 = (bf16[384,2048]{1,0:T(8,128)(2,1)S(1)}, bf16[384,2048]{1,0:T(8,128)(2,1)S(1)}, u32[]{:S(2)}, u32[]{:S(2)}) collective-permute-start(bf16[384,2048]{1,0:T(8,128)(2,1)S(1)} %get-tuple-element.33), channel_id=1, source_target_pairs={{0,1},{1,0},{2,3},{3,2},{4,5},{5,4},{6,7},{7,6},{8,9},{9,8},{10,11... | collective-permute-start | bytes 4718600 | tf_op jit(solution)/shard_map/ppermute | solution.py:444

commit v6 on v5

--- a/solution.py
+++ b/solution.py
@@ -159,14 +159,14 @@
         target[theirs, :] = other[part, :].astype(BF16)
 
 
-def states_kernel(core, own, other, weight, running, tail, both_far, message, both, semaphores):
+def states_kernel(
+    core, own, other_far, weight, running, tail, both_far, message, both, other, semaphores
+):
+    (load,) = start_copies(((other_far, other),), semaphores)
     w = weight[...]
-    put_rows(
-        core[0],
-        jnp.dot(own[...], w, preferred_element_type=F32),
-        jnp.dot(other[...], w, preferred_element_type=F32),
-        both,
-    )
+    first = jnp.dot(own[...], w, preferred_element_type=F32)
+    load.wait()
+    put_rows(core[0], first, jnp.dot(other[...], w, preferred_element_type=F32), both)
     (kept,) = start_copies(((both, both_far),), semaphores)
     logs = by_lane(running[...])
     closing = logs[767:768, :]
@@ -252,14 +252,34 @@
     return total
 
 
-def conv_kernel(core, y, own, other, p0, p1, p2, p3, taps, convolved_far, moments_far, padded, convolved, moments, semaphores):
+def conv_kernel(
+    core,
+    y,
+    own,
+    other_far,
+    p0,
+    p1,
+    p2,
+    p3,
+    taps,
+    convolved_far,
+    moments_far,
+    padded,
+    convolved,
+    moments,
+    other,
+    semaphores,
+):
+    (load,) = start_copies(((other_far, other),), semaphores)
     pieces = (p0, p1, p2, p3)
 
     def rows_of(rows):
         both = by_piece(y[0], rows, pieces, slice(0, 256))
         return (both[:, :128] * jax.nn.sigmoid(both[:, 128:])).astype(BF16).astype(F32)
 
-    first, second = rows_of(own), rows_of(other)
+    first = rows_of(own)
+    load.wait()
+    second = rows_of(other)
     for k in range(4):
         mine = pl.ds(pl.multiple_of(16 + k * 192 + core[0] * 96, 16), 96)
         theirs = pl.ds(pl.multiple_of(16 + k * 192 + (1 - core[0]) * 96, 16), 96)
@@ -301,7 +321,7 @@
     low,
     high,
     own,
-    other,
+    other_far,
     p0,
     p1,
     p2,
@@ -327,11 +347,13 @@
     convolved,
     moments,
     channel_gain,
+    other,
     semaphores,
 ):
     pieces = (p0, p1, p2, p3)
     loads = start_copies(
         (
+            (other_far, other),
             (both_far, both),
             (running_far, running),
             (start_far, start),
@@ -342,14 +364,10 @@
         ),
         semaphores,
     )
-    put_rows(
-        core[0],
-        by_piece(y[0], own, pieces, slice(0, 256)),
-        by_piece(y[0], other, pieces, slice(0, 256)),
-        pair,
-    )
+    first = by_piece(y[0], own, pieces, slice(0, 256))
     for load in loads:
         load.wait()
+    put_rows(core[0], first, by_piece(y[0], other, pieces, slice(0, 256)), pair)
     near = scan_states(inner, 16, low[0])
     far = scan_states(outer, 4, high[0])
     second = lane_is_second(64)
@@ -540,7 +558,12 @@
         (shape((768, 256), BF16), shape((16, 160, 128), BF16)),
         (core,),
         (own, other, state_weight, running, tail),
-        scratch=(pltpu.VMEM((768, 256), BF16), pltpu.SemaphoreType.DMA((1,))),
+        scratch=(
+            pltpu.VMEM((768, 256), BF16),
+            pltpu.VMEM((448, 2048), BF16),
+            pltpu.SemaphoreType.DMA((1,)),
+        ),
+        far=(1,),
         out_far=(0,),
     )
     inner = lax.all_to_all(sent, ("zl", "y"), 0, 0, tiled=True)
@@ -562,8 +585,10 @@
             pltpu.VMEM((800, 128), F32),
             pltpu.VMEM((768, 128), F32),
             pltpu.VMEM((2, 768), F32),
+            pltpu.VMEM((448, 2048), BF16),
             pltpu.SemaphoreType.DMA((2,)),
         ),
+        far=(1,),
         out_far=(0, 1),
     )
     moments = lax.all_gather(moments, ("x", "c"))
@@ -595,9 +620,10 @@
             pltpu.VMEM((768, 128), F32),
             pltpu.VMEM((8, 2, 768), F32),
             pltpu.VMEM((1, 128), F32),
-            pltpu.SemaphoreType.DMA((7,)),
+            pltpu.VMEM((448, 2048), BF16),
+            pltpu.SemaphoreType.DMA((8,)),
         ),
-        far=(8, 9, 10, 11, 12, 13, 14),
+        far=(1, 8, 9, 10, 11, 12, 13, 14),
     )
     arrived = ring(sent, "c", 1)
     joined = call(join_kernel, shape((384, 2048), BF16), (y,), (mine, arrived, *rest_pieces, spare))

time: 224 us -> 229 us (1.022)
  Pallas kernels: 24.9 us -> 30.9 us
    pallas_call x9, Pallas kernels: 24.9 us -> 30.9 us  [call(): pl.pallas_call(kernel, out_shape=out_shape, in_specs=[SMEM] * len(scalars...]
    unnamed x22 -> x18, local copies, waits for them, and re-layouts: 4.75 us -> 3 us
  transfers between devices with their start and end apart: 12 -> 12, of which waited for: 4 -> 4; matrix products, arithmetic and copies ran while one was open for 2% -> 2% of each run, Pallas kernels for 4% -> 5%
where the time goes in v6:
time: 229 us; the launch traced here: 227 us
  blocking collectives  99.3 us (43%)
  starting transfers between devices  44.4 us (19%)
  waiting for transfers between devices  44.4 us (19%)
  Pallas kernels  30.9 us (13%)
  local copies, waits for them, and re-layouts  6.54 us (3%)
    all_gather x1, blocking collectives, body(): rows = lax.all_gather(shard, ('zh', 'zl'), axis=0, tiled=True)  41.1 us
    pallas_call x9, Pallas kernels, call(): pl.pallas_call(kernel, out_shape=out_shape, in_specs=[SMEM] * len(scalars...  30.9 us
    ppermute x8, waiting for transfers between devices, ring(): lax.ppermute(x, axis, [(i, (i + shift) % count) for i in range(count)])  27 us
    all_to_all x1, blocking collectives, body(): parts = lax.all_to_all(joined.reshape(4, 96, 2048), 'x', 0, 0, tiled=True)  24.9 us
    ppermute x8, starting transfers between devices, ring(): lax.ppermute(x, axis, [(i, (i + shift) % count) for i in range(count)])  23.8 us
    all_to_all x1, blocking collectives, copies(): lax.all_to_all(jnp.broadcast_to(x[None], (count, *x.shape)), axes, 0, 0,...  18.5 us
    all_to_all x1, waiting for transfers between devices, body(): inner = lax.all_to_all(sent, ('zl', 'y'), 0, 0, tiled=True)  17.3 us
    all_gather x1, blocking collectives, body(): moments = lax.all_gather(moments, ('x', 'c'))  14.8 us
  transfers between devices with their start and end apart: 12, of which 4 were waited for; matrix products, arithmetic and copies ran while one was open for 2% of the time, Pallas kernels for 5%

profile of v6, /device:TPU:32, one launch (start us, length us, event | category | flops | bytes accessed | tf_op | source)
XLA Modules:
  0.0 227.4 jit_solution(1293622956279433341)
XLA Ops:
  0.0 0.0 copy-start.3
  0.0 0.9 slice_select_fusion
  0.9 4.5 %collective-permute-start = (bf16[16,2048]{1,0:T(8,128)(2,1)S(1)}, bf16[16,2048]{1,0:T(8,128)(2,1)S(1)}, u32[]{:S(2)}, u32[]{:S(2)}) collective-permute-start(bf16[16,2048]{1,0:T(8,128)(2,1)S(1)} %slice_select_fusion), channel_id=1, source_target_pairs={{7,15},{15,23},{23,31},{31,39},{39,47},{47,55},{55,63},{63,71},{71... | collective-permute-start | bytes 196616 | tf_op jit(solution)/shard_map/ppermute | solution.py:495
  5.4 0.7 reshape.20
  6.1 0.6 reduce-window.6
  6.6 0.2 slice_reduce_fusion
  6.8 0.2 reduce-window.9
  7.0 0.1 add_bitcast_fusion
  7.1 0.8 slice.28
  7.8 0.1 copy.20
  7.9 0.0 copy-start.2
  7.9 3.1 %shard_map.146.given_far = bf16[4,112,2048]{2,1,0:T(8,128)(2,1)} custom-call(bf16[96,2048]{1,0:T(8,128)(2,1)} %tokens_far.1, f32[1,2048]{1,0:T(1,128)} %bitcast.25), custom_call_target="tpu_custom_call" | custom-call | tf_op jit(solution)/shard_map/pallas_call | solution.py:37
  11.0 1.5 shard_map.145
  12.5 0.0 collective-permute-done.edge
  12.5 0.0 copy-done.3
  12.5 1.0 shard_map.147
  13.5 0.0 copy-start.7
  13.5 3.7 %all-to-all-start = ((bf16[4,112,2048]{2,1,0:T(8,128)(2,1)}), bf16[4,112,2048]{2,1,0:T(8,128)(2,1)S(1)}, u32[]{:S(2)}, u32[]{:S(2)}) async-start(bf16[4,112,2048]{2,1,0:T(8,128)(2,1)} %shard_map.147), calls=%async_computation | async-start | bytes 3670016 | tf_op jit(solution)/shard_map/all_to_all | solution.py:546
  17.3 0.0 copy-done.7
  17.3 41.1 %all_gather.9 = bf16[512,1008]{1,0:T(8,128)(2,1)S(1)} all-gather(bf16[32,1008]{1,0:T(8,128)(2,1)S(1)} %copy-done.7), channel_id=1, replica_groups=mesh['zh'=4,'zl'=4,'y'=4,'x'=4,'c'=2] {'zh','zl'}, dimensions={0}, use_global_device_ids=true | all-gather | bytes 1096704 | tf_op jit(solution)/shard_map/all_gather | solution.py:547
  58.4 0.0 copy-start.6
  58.4 0.0 all-to-all-done
  58.4 1.9 collective-permute-start.1
  60.3 0.7 fusion
  61.1 0.1 broadcast_in_dim.34
  61.1 18.5 %all_to_all.25 = bf16[4,512,256]{2,1,0:T(8,128)(2,1)S(1)} all-to-all(bf16[4,512,256]{2,1,0:T(8,128)(2,1)S(1)} %broadcast_in_dim.34), channel_id=1, replica_groups=mesh['zh'=4,'zl'=4,'y'=4,'x'=4,'c'=2] {'y'}, dimensions={0} | all-to-all | bytes 2097152 | tf_op jit(solution)/shard_map/all_to_all | solution.py:466
  79.6 0.0 copy-done.6
  79.6 0.0 collective-permute-done.1.other_far
  79.6 0.0 copy-start.5
  79.6 0.0 copy-done.2
  79.6 1.2 copy-done.5
  80.8 5.2 %shard_map.148 = (bf16[768,256]{1,0:T(8,128)(2,1)}, bf16[16,160,128]{2,1,0:T(8,128)(2,1)}) custom-call(s32[1]{0:T(128)} %bitcast.1.core, bf16[448,2048]{1,0:T(8,128)(2,1)S(1)} %bitcast.20, bf16[448,2048]{1,0:T(8,128)(2,1)} %copy-done.5, bf16[2048,256]{1,0:T(8,128)(2,1)S(1)} %bitcast.24, f32[8,768]{1,0:T(8,128)S(1)} %concatenate.3.running.running_far, ...), custom_call_target="tpu_custom_call" | custom-call | tf_op jit(solution)/shard_map/pallas_call | solution.py:37
  86.0 0.0 copy-start.4
  86.0 5.0 %all-to-all-start.2 = ((bf16[16,160,128]{2,1,0:T(8,128)(2,1)}), bf16[16,160,128]{2,1,0:T(8,128)(2,1)S(1)}, u32[]{:S(2)}, u32[]{:S(2)}) async-start(bf16[16,160,128]{2,1,0:T(8,128)(2,1)} %get-tuple-element.28), calls=%async_computation.2 | async-start | bytes 1310720 | tf_op jit(solution)/shard_map/all_to_all | solution.py:569
  91.0 17.3 %all-to-all-done.2.gathered.inner = bf16[16,160,128]{2,1,0:T(8,128)(2,1)S(1)} async-done(((bf16[16,160,128]{2,1,0:T(8,128)(2,1)}), bf16[16,160,128]{2,1,0:T(8,128)(2,1)S(1)}, u32[]{:S(2)}, u32[]{:S(2)}) %all-to-all-start.2) | async-done | bytes 655392 | tf_op jit(solution)/shard_map/all_to_all | solution.py:569
  108.3 0.9 shard_map.149
  109.2 7.4 %all-to-all-start.3 = ((bf16[4,208,128]{2,1,0:T(8,128)(2,1)}), bf16[4,208,128]{2,1,0:T(8,128)(2,1)}, u32[]{:S(2)}, u32[]{:S(2)}) async-start(bf16[4,208,128]{2,1,0:T(8,128)(2,1)} %shard_map.149), calls=%async_computation.3 | async-start | bytes 425984 | tf_op jit(solution)/shard_map/all_to_all | solution.py:578
  116.7 3.2 %collective-permute-start.7 = (bf16[512,256]{1,0:T(8,128)(2,1)}, bf16[512,256]{1,0:T(8,128)(2,1)S(1)}, u32[]{:S(2)}, u32[]{:S(2)}) collective-permute-start(bf16[512,256]{1,0:T(8,128)(2,1)} %get-tuple-element.35.p0), channel_id=1, source_target_pairs={{0,24},{8,0},{16,8},{24,16},{1,25},{9,1},{17,9},{25,17},{2,26},{10... | collective-permute-start | bytes 786440 | tf_op jit(solution)/shard_map/ppermute | solution.py:462
  119.9 1.1 slice.29.p0
  120.9 3.1 %collective-permute-start.4 = (bf16[512,496]{1,0:T(8,128)(2,1)S(1)}, bf16[512,496]{1,0:T(8,128)(2,1)S(1)}, u32[]{:S(2)}, u32[]{:S(2)}) collective-permute-start(bf16[512,496]{1,0:T(8,128)(2,1)S(1)} %slice.29.p0), channel_id=1, source_target_pairs={{0,24},{8,0},{16,8},{24,16},{1,25},{9,1},{17,9},{25,17},{2,26},{10... | collective-permute-start | bytes 1523720 | tf_op jit(solution)/shard_map/ppermute | solution.py:462
  124.0 3.5 %collective-permute-start.3 = (bf16[512,496]{1,0:T(8,128)(2,1)S(1)}, bf16[512,496]{1,0:T(8,128)(2,1)}, u32[]{:S(2)}, u32[]{:S(2)}) collective-permute-start(bf16[512,496]{1,0:T(8,128)(2,1)S(1)} %slice.29.p0), channel_id=1, source_target_pairs={{0,16},{8,24},{16,0},{24,8},{1,17},{9,25},{17,1},{25,9},{2,18},{10... | collective-permute-start | bytes 1523720 | tf_op jit(solution)/shard_map/ppermute | solution.py:462
  127.6 1.9 collective-permute-start.2
  129.5 5.3 %collective-permute-start.6 = (bf16[512,256]{1,0:T(8,128)(2,1)}, bf16[512,256]{1,0:T(8,128)(2,1)}, u32[]{:S(2)}, u32[]{:S(2)}) collective-permute-start(bf16[512,256]{1,0:T(8,128)(2,1)} %get-tuple-element.35.p0), channel_id=1, source_target_pairs={{0,16},{8,24},{16,0},{24,8},{1,17},{9,25},{17,1},{25,9},{2,18},{10... | collective-permute-start | bytes 786440 | tf_op jit(solution)/shard_map/ppermute | solution.py:462
  134.8 0.0 collective-permute-done.7.p3
  134.8 0.0 copy-start
  134.8 0.7 copy-done
  135.5 2.6 %collective-permute-start.5 = (bf16[512,256]{1,0:T(8,128)(2,1)}, bf16[512,256]{1,0:T(8,128)(2,1)}, u32[]{:S(2)}, u32[]{:S(2)}) collective-permute-start(bf16[512,256]{1,0:T(8,128)(2,1)} %get-tuple-element.35.p0), channel_id=1, source_target_pairs={{0,8},{8,16},{16,24},{24,0},{1,9},{9,17},{17,25},{25,1},{2,10},{10... | collective-permute-start | bytes 786440 | tf_op jit(solution)/shard_map/ppermute | solution.py:462
  138.1 21.1 %collective-permute-done.6.p2 = bf16[512,256]{1,0:T(8,128)(2,1)} collective-permute-done((bf16[512,256]{1,0:T(8,128)(2,1)}, bf16[512,256]{1,0:T(8,128)(2,1)}, u32[]{:S(2)}, u32[]{:S(2)}) %collective-permute-start.6) | collective-permute-done | bytes 262176 | tf_op jit(solution)/shard_map/ppermute | solution.py:462
  159.2 2.9 %collective-permute-done.5.p1 = bf16[512,256]{1,0:T(8,128)(2,1)} collective-permute-done((bf16[512,256]{1,0:T(8,128)(2,1)}, bf16[512,256]{1,0:T(8,128)(2,1)}, u32[]{:S(2)}, u32[]{:S(2)}) %collective-permute-start.5) | collective-permute-done | bytes 262176 | tf_op jit(solution)/shard_map/ppermute | solution.py:462
  162.1 0.0 copy-done.4
  162.1 0.0 copy-start.1
  162.1 0.9 copy-done.1
  163.0 6.7 %shard_map.150 = (f32[768,128]{1,0:T(8,128)}, f32[2,768]{1,0:T(2,128)}) custom-call(s32[1]{0:T(128)} %bitcast.1.core, s32[1]{0:T(128)} %bitcast.y, bf16[448,2048]{1,0:T(8,128)(2,1)S(1)} %bitcast.21, bf16[448,2048]{1,0:T(8,128)(2,1)} %copy-done.5, bf16[512,256]{1,0:T(8,128)(2,1)} %get-tuple-element.35.p0, bf16[512,256]{1,0:T(8,128)(2,1)} %collective-permute-done.5.p1, ...), custom_call_target="tpu_custom_call" | custom-call | tf_op jit(solution)/shard_map/pallas_call | solution.py:37
  169.8 14.8 %all-gather.1.moments_far = f32[8,2,768]{2,1,0:T(2,128)} all-gather(f32[1,2,768]{2,1,0:T(2,128)} %bitcast.30), channel_id=2, replica_groups=mesh['zh'=4,'zl'=4,'y'=4,'x'=4,'c'=2] {'x','c'}, dimensions={0}, use_global_device_ids=true | all-gather | bytes 55296 | tf_op jit(solution)/shard_map/all_gather | solution.py:594
  184.6 0.0 collective-permute-done.4.p3
  184.6 0.0 collective-permute-done.3.p2
  184.6 0.0 collective-permute-done.2.p1
  184.6 0.0 all-to-all-done.3.outer
  184.6 9.1 %shard_map.151 = (bf16[384,256]{1,0:T(8,128)(2,1)S(1)}, bf16[384,2048]{1,0:T(8,128)(2,1)S(1)}, bf16[16,2048]{1,0:T(8,128)(2,1)S(1)}) custom-call(s32[1]{0:T(128)} %bitcast.1.core, s32[1]{0:T(128)} %bitcast.y, s32[1]{0:T(128)} %bitcast.2.position.low, s32[1]{0:T(128)} %bitcast.3.high, bf16[448,2048]{1,0:T(8,128)(2,1)S(1)} %bitcast.22, ...), custom_call_target="tpu_custom_call" | custom-call | tf_op jit(solution)/shard_map/pallas_call | solution.py:37
  193.7 2.3 collective-permute-start.8
  196.0 3.0 %collective-permute-done.8.arrived = bf16[384,2048]{1,0:T(8,128)(2,1)S(1)} collective-permute-done((bf16[384,2048]{1,0:T(8,128)(2,1)S(1)}, bf16[384,2048]{1,0:T(8,128)(2,1)S(1)}, u32[]{:S(2)}, u32[]{:S(2)}) %collective-permute-start.8) | collective-permute-done | bytes 1572896 | tf_op jit(solution)/shard_map/ppermute | solution.py:462
  199.0 2.2 shard_map.152
  201.2 24.9 %all_to_all.26.parts = bf16[4,96,2048]{2,1,0:T(8,128)(2,1)S(1)} all-to-all(bf16[4,96,2048]{2,1,0:T(8,128)(2,1)S(1)} %bitcast.23), channel_id=1, replica_groups=mesh['zh'=4,'zl'=4,'y'=4,'x'=4,'c'=2] {'x'}, dimensions={0} | all-to-all | bytes 3145728 | tf_op jit(solution)/shard_map/all_to_all | solution.py:630
  226.2 1.3 shard_map.153
  (3 shorter events, 0.0 us)
Async XLA Ops:
  0.0 12.5 %copy-start.3 = (f32[2048]{0:T(1024)S(1)}, f32[2048]{0:T(1024)}, u32[]{:S(2)}) copy-start(f32[2048]{0:T(1024)} %param.16) | copy-start | bytes 24580
  0.9 11.6 %collective-permute-start = (bf16[16,2048]{1,0:T(8,128)(2,1)S(1)}, bf16[16,2048]{1,0:T(8,128)(2,1)S(1)}, u32[]{:S(2)}, u32[]{:S(2)}) collective-permute-start(bf16[16,2048]{1,0:T(8,128)(2,1)S(1)} %slice_select_fusion), channel_id=1, source_target_pairs={{7,15},{15,23},{23,31},{31,39},{39,47},{47,55},{55,63},{63,71},{71... | collective-permute-start | bytes 196616 | tf_op jit(solution)/shard_map/ppermute | solution.py:495
  7.9 71.7 %copy-start.2 = (f32[8,768]{1,0:T(8,128)}, f32[8,768]{1,0:T(8,128)S(1)}, u32[]{:S(2)}) copy-start(f32[8,768]{1,0:T(8,128)S(1)} %concatenate.3.running.running_far) | copy-start | bytes 73732
  13.5 3.8 %copy-start.7 = (bf16[32,1008]{1,0:T(8,128)(2,1)S(1)}, bf16[32,1008]{1,0:T(8,128)(2,1)}, u32[]{:S(2)}) copy-start(bf16[32,1008]{1,0:T(8,128)(2,1)} %shard_map.145) | copy-start | bytes 193540
  13.5 44.9 %all-to-all-start = ((bf16[4,112,2048]{2,1,0:T(8,128)(2,1)}), bf16[4,112,2048]{2,1,0:T(8,128)(2,1)S(1)}, u32[]{:S(2)}, u32[]{:S(2)}) async-start(bf16[4,112,2048]{2,1,0:T(8,128)(2,1)} %shard_map.147), calls=%async_computation | async-start | bytes 3670016 | tf_op jit(solution)/shard_map/all_to_all | solution.py:546
  58.4 21.2 %copy-start.6 = (bf16[512,1008]{1,0:T(8,128)(2,1)}, bf16[512,1008]{1,0:T(8,128)(2,1)S(1)}, u32[]{:S(2)}) copy-start(bf16[512,1008]{1,0:T(8,128)(2,1)S(1)} %all_gather.9) | copy-start | bytes 3096580
  58.4 21.2 %collective-permute-start.1 = (bf16[448,2048]{1,0:T(8,128)(2,1)S(1)}, bf16[448,2048]{1,0:T(8,128)(2,1)S(1)}, u32[]{:S(2)}, u32[]{:S(2)}) collective-permute-start(bf16[448,2048]{1,0:T(8,128)(2,1)S(1)} %bitcast.19), channel_id=1, source_target_pairs={{0,1},{1,0},{2,3},{3,2},{4,5},{5,4},{6,7},{7,6},{8,9},{9,8},{10,11... | collective-permute-start | bytes 5505032 | tf_op jit(solution)/shard_map/ppermute | solution.py:462
  79.6 1.3 copy-start.5
  86.0 76.1 %copy-start.4 = (f32[31,128]{1,0:T(8,128)S(1)}, f32[31,128]{1,0:T(8,128)}, u32[]{:S(2)}) copy-start(f32[31,128]{1,0:T(8,128)} %taps.1) | copy-start | bytes 47620
  86.0 22.3 %all-to-all-start.2 = ((bf16[16,160,128]{2,1,0:T(8,128)(2,1)}), bf16[16,160,128]{2,1,0:T(8,128)(2,1)S(1)}, u32[]{:S(2)}, u32[]{:S(2)}) async-start(bf16[16,160,128]{2,1,0:T(8,128)(2,1)} %get-tuple-element.28), calls=%async_computation.2 | async-start | bytes 1310720 | tf_op jit(solution)/shard_map/all_to_all | solution.py:569
  109.2 75.4 %all-to-all-start.3 = ((bf16[4,208,128]{2,1,0:T(8,128)(2,1)}), bf16[4,208,128]{2,1,0:T(8,128)(2,1)}, u32[]{:S(2)}, u32[]{:S(2)}) async-start(bf16[4,208,128]{2,1,0:T(8,128)(2,1)} %shard_map.149), calls=%async_computation.3 | async-start | bytes 425984 | tf_op jit(solution)/shard_map/all_to_all | solution.py:578
  116.7 18.1 %collective-permute-start.7 = (bf16[512,256]{1,0:T(8,128)(2,1)}, bf16[512,256]{1,0:T(8,128)(2,1)S(1)}, u32[]{:S(2)}, u32[]{:S(2)}) collective-permute-start(bf16[512,256]{1,0:T(8,128)(2,1)} %get-tuple-element.35.p0), channel_id=1, source_target_pairs={{0,24},{8,0},{16,8},{24,16},{1,25},{9,1},{17,9},{25,17},{2,26},{10... | collective-permute-start | bytes 786440 | tf_op jit(solution)/shard_map/ppermute | solution.py:462
  120.9 63.6 %collective-permute-start.4 = (bf16[512,496]{1,0:T(8,128)(2,1)S(1)}, bf16[512,496]{1,0:T(8,128)(2,1)S(1)}, u32[]{:S(2)}, u32[]{:S(2)}) collective-permute-start(bf16[512,496]{1,0:T(8,128)(2,1)S(1)} %slice.29.p0), channel_id=1, source_target_pairs={{0,24},{8,0},{16,8},{24,16},{1,25},{9,1},{17,9},{25,17},{2,26},{10... | collective-permute-start | bytes 1523720 | tf_op jit(solution)/shard_map/ppermute | solution.py:462
  124.0 60.6 %collective-permute-start.3 = (bf16[512,496]{1,0:T(8,128)(2,1)S(1)}, bf16[512,496]{1,0:T(8,128)(2,1)}, u32[]{:S(2)}, u32[]{:S(2)}) collective-permute-start(bf16[512,496]{1,0:T(8,128)(2,1)S(1)} %slice.29.p0), channel_id=1, source_target_pairs={{0,16},{8,24},{16,0},{24,8},{1,17},{9,25},{17,1},{25,9},{2,18},{10... | collective-permute-start | bytes 1523720 | tf_op jit(solution)/shard_map/ppermute | solution.py:462
  127.6 57.0 %collective-permute-start.2 = (bf16[512,496]{1,0:T(8,128)(2,1)S(1)}, bf16[512,496]{1,0:T(8,128)(2,1)}, u32[]{:S(2)}, u32[]{:S(2)}) collective-permute-start(bf16[512,496]{1,0:T(8,128)(2,1)S(1)} %slice.29.p0), channel_id=1, source_target_pairs={{0,8},{8,16},{16,24},{24,0},{1,9},{9,17},{17,25},{25,1},{2,10},{10... | collective-permute-start | bytes 1523720 | tf_op jit(solution)/shard_map/ppermute | solution.py:462
  129.5 29.7 %collective-permute-start.6 = (bf16[512,256]{1,0:T(8,128)(2,1)}, bf16[512,256]{1,0:T(8,128)(2,1)}, u32[]{:S(2)}, u32[]{:S(2)}) collective-permute-start(bf16[512,256]{1,0:T(8,128)(2,1)} %get-tuple-element.35.p0), channel_id=1, source_target_pairs={{0,16},{8,24},{16,0},{24,8},{1,17},{9,25},{17,1},{25,9},{2,18},{10... | collective-permute-start | bytes 786440 | tf_op jit(solution)/shard_map/ppermute | solution.py:462
  134.8 0.7 copy-start
  135.5 26.6 %collective-permute-start.5 = (bf16[512,256]{1,0:T(8,128)(2,1)}, bf16[512,256]{1,0:T(8,128)(2,1)}, u32[]{:S(2)}, u32[]{:S(2)}) collective-permute-start(bf16[512,256]{1,0:T(8,128)(2,1)} %get-tuple-element.35.p0), channel_id=1, source_target_pairs={{0,8},{8,16},{16,24},{24,0},{1,9},{9,17},{17,25},{25,1},{2,10},{10... | collective-permute-start | bytes 786440 | tf_op jit(solution)/shard_map/ppermute | solution.py:462
  162.1 1.0 copy-start.1
  193.7 5.3 %collective-permute-start.8 = (bf16[384,2048]{1,0:T(8,128)(2,1)S(1)}, bf16[384,2048]{1,0:T(8,128)(2,1)S(1)}, u32[]{:S(2)}, u32[]{:S(2)}) collective-permute-start(bf16[384,2048]{1,0:T(8,128)(2,1)S(1)} %get-tuple-element.33), channel_id=1, source_target_pairs={{0,1},{1,0},{2,3},{3,2},{4,5},{5,4},{6,7},{7,6},{8,9},{9,8},{10,11... | collective-permute-start | bytes 4718600 | tf_op jit(solution)/shard_map/ppermute | solution.py:462

commit v7 on v5

--- a/solution.py
+++ b/solution.py
@@ -159,7 +159,31 @@
         target[theirs, :] = other[part, :].astype(BF16)
 
 
-def states_kernel(core, own, other, weight, running, tail, both_far, message, both, semaphores):
+def summed(x):
+    lane = lax.broadcasted_iota(jnp.int32, x.shape, 1)
+    shift = 1
+    while shift < x.shape[1]:
+        x = x + jnp.where(lane >= shift, pltpu.roll(x, shift, 1), 0.0)
+        shift *= 2
+    return x
+
+
+def states_kernel(
+    core,
+    own,
+    other,
+    weight,
+    decay,
+    tail,
+    both_far,
+    message_far,
+    running_far,
+    both,
+    running,
+    message,
+    semaphores,
+):
+    running[...] = summed(jnp.concatenate([decay[...], jnp.zeros((6, 768), F32)], axis=0))
     w = weight[...]
     put_rows(
         core[0],
@@ -167,7 +191,9 @@
         jnp.dot(other[...], w, preferred_element_type=F32),
         both,
     )
-    (kept,) = start_copies(((both, both_far),), semaphores)
+    kept = start_copies(
+        ((both, both_far), (running, running_far)), semaphores.at[pl.ds(16, 2)]
+    )
     logs = by_lane(running[...])
     closing = logs[767:768, :]
     k = both[:, 0:128].astype(F32) * 0.125
@@ -184,9 +210,10 @@
         (slice(144, 160), tail[...]),
     )
     for at, part in parts:
-        for copy in range(16):
-            message[copy, at, :] = part
-    kept.wait()
+        message[at, :] = part
+    kept += start_copies([(message, message_far.at[k]) for k in range(16)], semaphores)
+    for copy in kept:
+        copy.wait()
 
 
 def log_rows(log):
@@ -287,12 +314,10 @@
         copy.wait()
 
 
-def out_rows(y, rows, pieces, spare, write):
-    for shift, piece in enumerate(pieces):
-        lanes = column_block(y, shift)
-        part = lax.dot_general(rows[:, :240], piece[:, 256:496], NT, preferred_element_type=F32)
-        part = part + jnp.dot(rows[:, 240:], spare[:, lanes], preferred_element_type=F32)
-        write(lanes, part)
+def out_rows(y, rows, weight, write):
+    for shift in range(4):
+        part = lax.dot_general(rows, weight[shift], NT, preferred_element_type=F32)
+        write(column_block(y, shift), part)
 
 
 def mixers_kernel(
@@ -317,6 +342,7 @@
     channel_gain_far,
     mine,
     sent,
+    weight,
     spare,
     pair,
     rows_in,
@@ -373,14 +399,16 @@
         for zh in range(4):
             where = yy * 512 + zh * 128
             spare[:, where : where + 128] = outer[zh, 144 + yy * 16 : 160 + yy * 16, :]
+    for shift, piece in enumerate(pieces):
+        last = jnp.transpose(spare[:, column_block(y[0], shift)].astype(F32)).astype(BF16)
+        weight[shift, :, 0:240] = piece[:, 256:496]
+        weight[shift, :, 240:256] = last
 
     k = (both[:, 0:128].astype(F32) * 0.125).astype(BF16)
     v = both[:, 128:256]
     rows = 128
     zero = jnp.zeros((), BF16)
     half = lane_is_second(rows)
-    masks = [lane_is_second(768) == bool(h) for h in range(2)]
-    head_values = [jnp.where(mask, v, zero) for mask in masks]
 
     def head_mean(x):
         first = jnp.sum(jnp.where(half, 0.0, x), axis=1, keepdims=True)
@@ -396,15 +424,17 @@
         retained = retained + jnp.exp(closing - log) * jnp.dot(
             q, backward, preferred_element_type=F32
         )
+        stacked = jnp.concatenate(
+            [jnp.where(half, zero, q), jnp.where(half, q, zero)], axis=0
+        )
+        scores = lax.dot_general(stacked, k, NT, preferred_element_type=F32)
+        parts = []
         for h in range(2):
-            scores = lax.dot_general(
-                jnp.where(masks[h][:rows], q, zero), k, NT, preferred_element_type=F32
-            )
             distance = jnp.abs(turned[at, h : h + 1] - logs[h : h + 1, :])
-            weights = jnp.exp(-distance)
-            retained = retained + jnp.dot(
-                (scores * weights).astype(BF16), head_values[h], preferred_element_type=F32
-            )
+            part = scores[h * rows : (h + 1) * rows, :] * jnp.exp(-distance)
+            parts.append(part.astype(BF16))
+        mixed = jnp.dot(jnp.concatenate(parts, axis=0), v, preferred_element_type=F32)
+        retained = retained + jnp.where(half, mixed[rows:, :], mixed[:rows, :])
         same = q.astype(F32) * k[at, :].astype(F32)
         retained = retained + 64 * head_mean(same) * v[at, :].astype(F32)
         centred = retained - head_mean(retained)
@@ -429,14 +459,14 @@
     def write(lanes, part):
         sent[:, lanes] = part.astype(BF16)
 
-    out_rows(y[0], half_of(1 - core[0]), pieces, spare, write)
-
-
-def join_kernel(y, mine, arrived, p0, p1, p2, p3, spare, out):
+    out_rows(y[0], half_of(1 - core[0]), weight, write)
+
+
+def join_kernel(y, mine, arrived, weight, out):
     def write(lanes, part):
         out[:, lanes] = (part + arrived[:, lanes].astype(F32)).astype(BF16)
 
-    out_rows(y[0], mine[...], (p0, p1, p2, p3), spare, write)
+    out_rows(y[0], mine[...], weight, write)
 
 
 def ring(x, axis, shift):
@@ -496,8 +526,6 @@
         ),
         grant=56,
     )
-    running = jnp.cumsum(decay_logs, axis=1)
-    running = jnp.concatenate([running, jnp.zeros((6, 768), F32)], axis=0)
     tail = jnp.pad(output_heads[112:], ((0, 0), (0, 96)))
     normed = call(
         norm_kernel,
@@ -513,7 +541,7 @@
         far=(0, 1),
         out_far=(0,),
     )
-    edge, normed, running, tail = lax.optimization_barrier((edge, normed, running, tail))
+    edge, normed = lax.optimization_barrier((edge, normed))
     normed = call(
         edge_kernel,
         shape((4, 112, 2048), BF16),
@@ -535,13 +563,18 @@
     rest_pieces = (rest_piece,) + tuple(ring(rest_piece, "y", d) for d in (1, 2, 3))
 
     full = shape((768, 128), F32)
-    both, sent = call(
+    both, sent, running = call(
         states_kernel,
-        (shape((768, 256), BF16), shape((16, 160, 128), BF16)),
+        (shape((768, 256), BF16), shape((16, 160, 128), BF16), shape((8, 768), F32)),
         (core,),
-        (own, other, state_weight, running, tail),
-        scratch=(pltpu.VMEM((768, 256), BF16), pltpu.SemaphoreType.DMA((1,))),
-        out_far=(0,),
+        (own, other, state_weight, decay_logs, tail),
+        scratch=(
+            pltpu.VMEM((768, 256), BF16),
+            pltpu.VMEM((8, 768), F32),
+            pltpu.VMEM((160, 128), BF16),
+            pltpu.SemaphoreType.DMA((18,)),
+        ),
+        out_far=(0, 1, 2),
     )
     inner = lax.all_to_all(sent, ("zl", "y"), 0, 0, tiled=True)
     sent = call(
@@ -567,9 +600,9 @@
         out_far=(0, 1),
     )
     moments = lax.all_gather(moments, ("x", "c"))
-    mine, sent, spare = call(
+    mine, sent, weight = call(
         mixers_kernel,
-        (shape((384, 256), BF16), shape((384, 2048), BF16), shape((16, 2048), BF16)),
+        (shape((384, 256), BF16), shape((384, 2048), BF16), shape((4, 512, 256), BF16)),
         (core, y, low, high),
         (
             own,
@@ -586,6 +619,7 @@
             channel_gain[None],
         ),
         scratch=(
+            pltpu.VMEM((16, 2048), BF16),
             pltpu.VMEM((768, 256), BF16),
             pltpu.VMEM((768, 256), BF16),
             pltpu.VMEM((768, 256), BF16),
@@ -600,7 +634,7 @@
         far=(8, 9, 10, 11, 12, 13, 14),
     )
     arrived = ring(sent, "c", 1)
-    joined = call(join_kernel, shape((384, 2048), BF16), (y,), (mine, arrived, *rest_pieces, spare))
+    joined = call(join_kernel, shape((384, 2048), BF16), (y,), (mine, arrived, weight))
     parts = lax.all_to_all(joined.reshape(4, 96, 2048), "x", 0, 0, tiled=True)
     return call(last_kernel, shape((96, 2048), BF16), (), (parts,))
 

time: 224 us -> 220 us (0.982)
  blocking collectives: 99.1 us -> 80.1 us
  waiting for transfers between devices: 44.3 us -> 60.4 us
  local copies, waits for them, and re-layouts: 8.31 us -> 4.05 us
  starting transfers between devices: 44.4 us -> 47.9 us
    all_to_all x1 -> x0, blocking collectives: 18.5 us -> none  [copies(): lax.all_to_all(jnp.broadcast_to(x[None], (count, *x.shape)), axes, 0, 0,...]
    all_to_all x0 -> x1, waiting for transfers between devices: none -> 15.8 us  [copies(): lax.all_to_all(jnp.broadcast_to(x[None], (count, *x.shape)), axes, 0, 0,...]
    all_to_all x0 -> x1, starting transfers between devices: none -> 3.51 us  [copies(): lax.all_to_all(jnp.broadcast_to(x[None], (count, *x.shape)), axes, 0, 0,...]
    unnamed x22 -> x17, local copies, waits for them, and re-layouts: 4.75 us -> 1.78 us
  transfers between devices with their start and end apart: 12 -> 13, of which waited for: 4 -> 5; matrix products, arithmetic and copies ran while one was open for 2% -> 1% of each run, Pallas kernels for 4% -> 4%
where the time goes in v7:
time: 220 us; the launch traced here: 219 us
  blocking collectives  80.1 us (36%)
  waiting for transfers between devices  60.4 us (27%)
  starting transfers between devices  47.9 us (22%)
  Pallas kernels  25.3 us (12%)
  local copies, waits for them, and re-layouts  4.05 us (2%)
    all_gather x1, blocking collectives, body(): rows = lax.all_gather(shard, ('zh', 'zl'), axis=0, tiled=True)  41.1 us
    ppermute x8, waiting for transfers between devices, ring(): lax.ppermute(x, axis, [(i, (i + shift) % count) for i in range(count)])  27 us
    pallas_call x9, Pallas kernels, call(): pl.pallas_call(kernel, out_shape=out_shape, in_specs=[SMEM] * len(scalars...  25.3 us
    all_to_all x1, blocking collectives, body(): parts = lax.all_to_all(joined.reshape(4, 96, 2048), 'x', 0, 0, tiled=True)  24.1 us
    ppermute x8, starting transfers between devices, ring(): lax.ppermute(x, axis, [(i, (i + shift) % count) for i in range(count)])  23.8 us
    all_to_all x1, waiting for transfers between devices, body(): inner = lax.all_to_all(sent, ('zl', 'y'), 0, 0, tiled=True)  17.6 us
    all_to_all x1, waiting for transfers between devices, copies(): lax.all_to_all(jnp.broadcast_to(x[None], (count, *x.shape)), axes, 0, 0,...  15.8 us
    all_gather x1, blocking collectives, body(): moments = lax.all_gather(moments, ('x', 'c'))  14.9 us
  transfers between devices with their start and end apart: 13, of which 5 were waited for; matrix products, arithmetic and copies ran while one was open for 1% of the time, Pallas kernels for 4%

profile of v7, /device:TPU:32, one launch (start us, length us, event | category | flops | bytes accessed | tf_op | source)
XLA Modules:
  0.0 218.9 jit_solution(4310347834211762885)
XLA Ops:
  0.0 0.0 copy-start.2
  0.0 0.9 slice_select_fusion
  0.9 4.5 %collective-permute-start = (bf16[16,2048]{1,0:T(8,128)(2,1)S(1)}, bf16[16,2048]{1,0:T(8,128)(2,1)S(1)}, u32[]{:S(2)}, u32[]{:S(2)}) collective-permute-start(bf16[16,2048]{1,0:T(8,128)(2,1)S(1)} %slice_select_fusion), channel_id=1, source_target_pairs={{7,15},{15,23},{23,31},{31,39},{39,47},{47,55},{55,63},{63,71},{71... | collective-permute-start | bytes 196616 | tf_op jit(solution)/shard_map/ppermute | solution.py:507
  5.4 3.0 %shard_map.146.given_far = bf16[4,112,2048]{2,1,0:T(8,128)(2,1)} custom-call(bf16[96,2048]{1,0:T(8,128)(2,1)} %tokens_far.1, f32[1,2048]{1,0:T(1,128)} %bitcast.19), custom_call_target="tpu_custom_call" | custom-call | tf_op jit(solution)/shard_map/pallas_call | solution.py:37
  8.4 1.5 shard_map.145
  9.9 0.0 collective-permute-done.edge
  9.9 0.0 copy-done.2
  9.9 1.0 shard_map.147
  10.9 0.0 copy-start.6
  10.9 3.7 %all-to-all-start = ((bf16[4,112,2048]{2,1,0:T(8,128)(2,1)}), bf16[4,112,2048]{2,1,0:T(8,128)(2,1)S(1)}, u32[]{:S(2)}, u32[]{:S(2)}) async-start(bf16[4,112,2048]{2,1,0:T(8,128)(2,1)} %shard_map.147), calls=%async_computation | async-start | bytes 3670016 | tf_op jit(solution)/shard_map/all_to_all | solution.py:556
  14.6 0.0 copy-done.6
  14.6 41.1 %all_gather.9 = bf16[512,1008]{1,0:T(8,128)(2,1)S(1)} all-gather(bf16[32,1008]{1,0:T(8,128)(2,1)S(1)} %copy-done.6), channel_id=1, replica_groups=mesh['zh'=4,'zl'=4,'y'=4,'x'=4,'c'=2] {'zh','zl'}, dimensions={0}, use_global_device_ids=true | all-gather | bytes 1096704 | tf_op jit(solution)/shard_map/all_gather | solution.py:557
  55.8 0.0 copy-start.5
  55.8 0.0 all-to-all-done
  55.8 1.9 collective-permute-start.1
  57.7 0.0 copy-done.5
  57.7 0.0 copy-start.7
  57.7 0.0 copy-start.4
  57.8 1.1 broadcast_in_dim.33
  58.8 3.5 %all-to-all-start.1 = ((bf16[4,512,256]{2,1,0:T(8,128)(2,1)}), bf16[4,512,256]{2,1,0:T(8,128)(2,1)S(1)}, u32[]{:S(2)}, u32[]{:S(2)}) async-start(bf16[4,512,256]{2,1,0:T(8,128)(2,1)} %broadcast_in_dim.33), calls=%async_computation.1 | async-start | bytes 2097152 | tf_op jit(solution)/shard_map/all_to_all | solution.py:478
  62.3 0.0 copy-done.7
  62.4 0.1 slice.22
  62.4 0.1 copy.19
  62.5 15.8 %all-to-all-done.1 = bf16[4,512,256]{2,1,0:T(8,128)(2,1)S(1)} async-done(((bf16[4,512,256]{2,1,0:T(8,128)(2,1)}), bf16[4,512,256]{2,1,0:T(8,128)(2,1)S(1)}, u32[]{:S(2)}, u32[]{:S(2)}) %all-to-all-start.1) | async-done | bytes 1048608 | tf_op jit(solution)/shard_map/all_to_all | solution.py:478
  78.4 0.0 collective-permute-done.1.other
  78.4 0.0 copy-done.4
  78.4 4.0 %shard_map.148 = (bf16[768,256]{1,0:T(8,128)(2,1)}, bf16[16,160,128]{2,1,0:T(8,128)(2,1)}, f32[8,768]{1,0:T(8,128)}) custom-call(s32[1]{0:T(128)} %bitcast.1.core, bf16[448,2048]{1,0:T(8,128)(2,1)S(1)} %bitcast.14, bf16[448,2048]{1,0:T(8,128)(2,1)} %collective-permute-done.1.other, bf16[2048,256]{1,0:T(8,128)(2,1)S(1)} %bitcast.18, f32[2,768]{1,0:T(2,128)S(1)} %copy-done.4, ...), custom_call_target="tpu_custom_call" | custom-call | tf_op jit(solution)/shard_map/pallas_call | solution.py:37
  82.4 0.0 copy-start.3
  82.4 5.0 %all-to-all-start.2 = ((bf16[16,160,128]{2,1,0:T(8,128)(2,1)}), bf16[16,160,128]{2,1,0:T(8,128)(2,1)S(1)}, u32[]{:S(2)}, u32[]{:S(2)}) async-start(bf16[16,160,128]{2,1,0:T(8,128)(2,1)} %get-tuple-element.25), calls=%async_computation.2 | async-start | bytes 1310720 | tf_op jit(solution)/shard_map/all_to_all | solution.py:579
  87.4 17.6 %all-to-all-done.2.gathered.inner = bf16[16,160,128]{2,1,0:T(8,128)(2,1)S(1)} async-done(((bf16[16,160,128]{2,1,0:T(8,128)(2,1)}), bf16[16,160,128]{2,1,0:T(8,128)(2,1)S(1)}, u32[]{:S(2)}, u32[]{:S(2)}) %all-to-all-start.2) | async-done | bytes 655392 | tf_op jit(solution)/shard_map/all_to_all | solution.py:579
  105.0 0.9 shard_map.149
  105.9 7.5 %all-to-all-start.3 = ((bf16[4,208,128]{2,1,0:T(8,128)(2,1)}), bf16[4,208,128]{2,1,0:T(8,128)(2,1)S(1)}, u32[]{:S(2)}, u32[]{:S(2)}) async-start(bf16[4,208,128]{2,1,0:T(8,128)(2,1)} %shard_map.149), calls=%async_computation.3 | async-start | bytes 425984 | tf_op jit(solution)/shard_map/all_to_all | solution.py:588
  113.3 3.2 %collective-permute-start.7 = (bf16[512,256]{1,0:T(8,128)(2,1)S(1)}, bf16[512,256]{1,0:T(8,128)(2,1)S(1)}, u32[]{:S(2)}, u32[]{:S(2)}) collective-permute-start(bf16[512,256]{1,0:T(8,128)(2,1)S(1)} %get-tuple-element.33.p0), channel_id=1, source_target_pairs={{0,24},{8,0},{16,8},{24,16},{1,25},{9,1},{17,9},{25,17},{2,26},{10... | collective-permute-start | bytes 786440 | tf_op jit(solution)/shard_map/ppermute | solution.py:474
  116.5 1.1 slice.20.p0
  117.6 3.1 %collective-permute-start.4 = (bf16[512,496]{1,0:T(8,128)(2,1)S(1)}, bf16[512,496]{1,0:T(8,128)(2,1)}, u32[]{:S(2)}, u32[]{:S(2)}) collective-permute-start(bf16[512,496]{1,0:T(8,128)(2,1)S(1)} %slice.20.p0), channel_id=1, source_target_pairs={{0,24},{8,0},{16,8},{24,16},{1,25},{9,1},{17,9},{25,17},{2,26},{10... | collective-permute-start | bytes 1523720 | tf_op jit(solution)/shard_map/ppermute | solution.py:474
  120.7 3.5 %collective-permute-start.3 = (bf16[512,496]{1,0:T(8,128)(2,1)S(1)}, bf16[512,496]{1,0:T(8,128)(2,1)}, u32[]{:S(2)}, u32[]{:S(2)}) collective-permute-start(bf16[512,496]{1,0:T(8,128)(2,1)S(1)} %slice.20.p0), channel_id=1, source_target_pairs={{0,16},{8,24},{16,0},{24,8},{1,17},{9,25},{17,1},{25,9},{2,18},{10... | collective-permute-start | bytes 1523720 | tf_op jit(solution)/shard_map/ppermute | solution.py:474
  124.2 1.9 collective-permute-start.2
  126.2 5.3 %collective-permute-start.6 = (bf16[512,256]{1,0:T(8,128)(2,1)S(1)}, bf16[512,256]{1,0:T(8,128)(2,1)}, u32[]{:S(2)}, u32[]{:S(2)}) collective-permute-start(bf16[512,256]{1,0:T(8,128)(2,1)S(1)} %get-tuple-element.33.p0), channel_id=1, source_target_pairs={{0,16},{8,24},{16,0},{24,8},{1,17},{9,25},{17,1},{25,9},{2,18},{10... | collective-permute-start | bytes 786440 | tf_op jit(solution)/shard_map/ppermute | solution.py:474
  131.4 0.0 collective-permute-done.7.p3
  131.4 0.0 copy-start
  131.4 0.7 copy-done
  132.2 2.6 %collective-permute-start.5 = (bf16[512,256]{1,0:T(8,128)(2,1)S(1)}, bf16[512,256]{1,0:T(8,128)(2,1)}, u32[]{:S(2)}, u32[]{:S(2)}) collective-permute-start(bf16[512,256]{1,0:T(8,128)(2,1)S(1)} %get-tuple-element.33.p0), channel_id=1, source_target_pairs={{0,8},{8,16},{16,24},{24,0},{1,9},{9,17},{17,25},{25,1},{2,10},{10... | collective-permute-start | bytes 786440 | tf_op jit(solution)/shard_map/ppermute | solution.py:474
  134.8 21.1 %collective-permute-done.6.p2 = bf16[512,256]{1,0:T(8,128)(2,1)} collective-permute-done((bf16[512,256]{1,0:T(8,128)(2,1)S(1)}, bf16[512,256]{1,0:T(8,128)(2,1)}, u32[]{:S(2)}, u32[]{:S(2)}) %collective-permute-start.6) | collective-permute-done | bytes 262176 | tf_op jit(solution)/shard_map/ppermute | solution.py:474
  155.9 2.9 %collective-permute-done.5.p1 = bf16[512,256]{1,0:T(8,128)(2,1)} collective-permute-done((bf16[512,256]{1,0:T(8,128)(2,1)S(1)}, bf16[512,256]{1,0:T(8,128)(2,1)}, u32[]{:S(2)}, u32[]{:S(2)}) %collective-permute-start.5) | collective-permute-done | bytes 262176 | tf_op jit(solution)/shard_map/ppermute | solution.py:474
  158.7 0.0 copy-done.3
  158.7 0.0 copy-start.1
  158.7 0.9 copy-done.1
  159.7 4.9 %shard_map.150 = (f32[768,128]{1,0:T(8,128)}, f32[2,768]{1,0:T(2,128)}) custom-call(s32[1]{0:T(128)} %bitcast.1.core, s32[1]{0:T(128)} %bitcast.y, bf16[448,2048]{1,0:T(8,128)(2,1)S(1)} %bitcast.15, bf16[448,2048]{1,0:T(8,128)(2,1)} %collective-permute-done.1.other, bf16[512,256]{1,0:T(8,128)(2,1)S(1)} %get-tuple-element.33.p0, ...), custom_call_target="tpu_custom_call" | custom-call | tf_op jit(solution)/shard_map/pallas_call | solution.py:37
  164.6 14.9 %all-gather.1.moments_far = f32[8,2,768]{2,1,0:T(2,128)} all-gather(f32[1,2,768]{2,1,0:T(2,128)} %bitcast.23), channel_id=2, replica_groups=mesh['zh'=4,'zl'=4,'y'=4,'x'=4,'c'=2] {'x','c'}, dimensions={0}, use_global_device_ids=true | all-gather | bytes 55296 | tf_op jit(solution)/shard_map/all_gather | solution.py:602
  179.5 0.0 collective-permute-done.4.p3
  179.5 0.0 collective-permute-done.3.p2
  179.5 0.0 collective-permute-done.2.p1
  179.5 0.0 all-to-all-done.3.outer
  179.5 8.1 %shard_map.151 = (bf16[384,256]{1,0:T(8,128)(2,1)S(1)}, bf16[384,2048]{1,0:T(8,128)(2,1)S(1)}, bf16[4,512,256]{2,1,0:T(8,128)(2,1)S(1)}) custom-call(s32[1]{0:T(128)} %bitcast.1.core, s32[1]{0:T(128)} %bitcast.y, s32[1]{0:T(128)} %bitcast.2.position.low, s32[1]{0:T(128)} %bitcast.3.high, bf16[448,2048]{1,0:T(8,128)(2,1)S(1)} %bitcast.16, ...), custom_call_target="tpu_custom_call" | custom-call | tf_op jit(solution)/shard_map/pallas_call | solution.py:37
  187.6 2.3 %collective-permute-start.8 = (bf16[384,2048]{1,0:T(8,128)(2,1)S(1)}, bf16[384,2048]{1,0:T(8,128)(2,1)S(1)}, u32[]{:S(2)}, u32[]{:S(2)}) collective-permute-start(bf16[384,2048]{1,0:T(8,128)(2,1)S(1)} %get-tuple-element.31), channel_id=1, source_target_pairs={{0,1},{1,0},{2,3},{3,2},{4,5},{5,4},{6,7},{7,6},{8,9},{9,8},{10,11... | collective-permute-start | bytes 4718600 | tf_op jit(solution)/shard_map/ppermute | solution.py:474
  189.9 3.0 %collective-permute-done.8.arrived = bf16[384,2048]{1,0:T(8,128)(2,1)S(1)} collective-permute-done((bf16[384,2048]{1,0:T(8,128)(2,1)S(1)}, bf16[384,2048]{1,0:T(8,128)(2,1)S(1)}, u32[]{:S(2)}, u32[]{:S(2)}) %collective-permute-start.8) | collective-permute-done | bytes 1572896 | tf_op jit(solution)/shard_map/ppermute | solution.py:474
  192.9 0.6 shard_map.152
  193.5 24.1 %all_to_all.25.parts = bf16[4,96,2048]{2,1,0:T(8,128)(2,1)S(1)} all-to-all(bf16[4,96,2048]{2,1,0:T(8,128)(2,1)S(1)} %bitcast.17), channel_id=1, replica_groups=mesh['zh'=4,'zl'=4,'y'=4,'x'=4,'c'=2] {'x'}, dimensions={0} | all-to-all | bytes 3145728 | tf_op jit(solution)/shard_map/all_to_all | solution.py:638
  217.6 1.3 shard_map.153
  (2 shorter events, 0.0 us)
Async XLA Ops:
  0.0 9.9 %copy-start.2 = (f32[2048]{0:T(1024)S(1)}, f32[2048]{0:T(1024)}, u32[]{:S(2)}) copy-start(f32[2048]{0:T(1024)} %param.16) | copy-start | bytes 24580
  0.9 9.0 %collective-permute-start = (bf16[16,2048]{1,0:T(8,128)(2,1)S(1)}, bf16[16,2048]{1,0:T(8,128)(2,1)S(1)}, u32[]{:S(2)}, u32[]{:S(2)}) collective-permute-start(bf16[16,2048]{1,0:T(8,128)(2,1)S(1)} %slice_select_fusion), channel_id=1, source_target_pairs={{7,15},{15,23},{23,31},{31,39},{39,47},{47,55},{55,63},{63,71},{71... | collective-permute-start | bytes 196616 | tf_op jit(solution)/shard_map/ppermute | solution.py:507
  10.9 3.8 %copy-start.6 = (bf16[32,1008]{1,0:T(8,128)(2,1)S(1)}, bf16[32,1008]{1,0:T(8,128)(2,1)}, u32[]{:S(2)}) copy-start(bf16[32,1008]{1,0:T(8,128)(2,1)} %shard_map.145) | copy-start | bytes 193540
  10.9 44.9 %all-to-all-start = ((bf16[4,112,2048]{2,1,0:T(8,128)(2,1)}), bf16[4,112,2048]{2,1,0:T(8,128)(2,1)S(1)}, u32[]{:S(2)}, u32[]{:S(2)}) async-start(bf16[4,112,2048]{2,1,0:T(8,128)(2,1)} %shard_map.147), calls=%async_computation | async-start | bytes 3670016 | tf_op jit(solution)/shard_map/all_to_all | solution.py:556
  55.8 1.9 copy-start.5
  55.8 22.6 %collective-permute-start.1 = (bf16[448,2048]{1,0:T(8,128)(2,1)S(1)}, bf16[448,2048]{1,0:T(8,128)(2,1)}, u32[]{:S(2)}, u32[]{:S(2)}) collective-permute-start(bf16[448,2048]{1,0:T(8,128)(2,1)S(1)} %bitcast.13), channel_id=1, source_target_pairs={{0,1},{1,0},{2,3},{3,2},{4,5},{5,4},{6,7},{7,6},{8,9},{9,8},{10,11... | collective-permute-start | bytes 5505032 | tf_op jit(solution)/shard_map/ppermute | solution.py:474
  57.7 4.6 %copy-start.7 = (bf16[128,32]{0,1:T(8,128)(2,1)S(1)}, bf16[128,32]{0,1:T(8,128)(2,1)}, u32[]{:S(2)}) copy-start(bf16[128,32]{0,1:T(8,128)(2,1)} %param.29) | copy-start | bytes 24580
  57.7 20.6 %copy-start.4 = (f32[2,768]{1,0:T(2,128)S(1)}, f32[2,768]{1,0:T(2,128)}, u32[]{:S(2)}) copy-start(f32[2,768]{1,0:T(2,128)} %decay.1) | copy-start | bytes 18436
  58.8 19.5 %all-to-all-start.1 = ((bf16[4,512,256]{2,1,0:T(8,128)(2,1)}), bf16[4,512,256]{2,1,0:T(8,128)(2,1)S(1)}, u32[]{:S(2)}, u32[]{:S(2)}) async-start(bf16[4,512,256]{2,1,0:T(8,128)(2,1)} %broadcast_in_dim.33), calls=%async_computation.1 | async-start | bytes 2097152 | tf_op jit(solution)/shard_map/all_to_all | solution.py:478
  82.4 76.3 %copy-start.3 = (f32[31,128]{1,0:T(8,128)S(1)}, f32[31,128]{1,0:T(8,128)}, u32[]{:S(2)}) copy-start(f32[31,128]{1,0:T(8,128)} %taps.1) | copy-start | bytes 47620
  82.4 22.6 %all-to-all-start.2 = ((bf16[16,160,128]{2,1,0:T(8,128)(2,1)}), bf16[16,160,128]{2,1,0:T(8,128)(2,1)S(1)}, u32[]{:S(2)}, u32[]{:S(2)}) async-start(bf16[16,160,128]{2,1,0:T(8,128)(2,1)} %get-tuple-element.25), calls=%async_computation.2 | async-start | bytes 1310720 | tf_op jit(solution)/shard_map/all_to_all | solution.py:579
  105.9 73.6 %all-to-all-start.3 = ((bf16[4,208,128]{2,1,0:T(8,128)(2,1)}), bf16[4,208,128]{2,1,0:T(8,128)(2,1)S(1)}, u32[]{:S(2)}, u32[]{:S(2)}) async-start(bf16[4,208,128]{2,1,0:T(8,128)(2,1)} %shard_map.149), calls=%async_computation.3 | async-start | bytes 425984 | tf_op jit(solution)/shard_map/all_to_all | solution.py:588
  113.3 18.1 %collective-permute-start.7 = (bf16[512,256]{1,0:T(8,128)(2,1)S(1)}, bf16[512,256]{1,0:T(8,128)(2,1)S(1)}, u32[]{:S(2)}, u32[]{:S(2)}) collective-permute-start(bf16[512,256]{1,0:T(8,128)(2,1)S(1)} %get-tuple-element.33.p0), channel_id=1, source_target_pairs={{0,24},{8,0},{16,8},{24,16},{1,25},{9,1},{17,9},{25,17},{2,26},{10... | collective-permute-start | bytes 786440 | tf_op jit(solution)/shard_map/ppermute | solution.py:474
  117.6 61.9 %collective-permute-start.4 = (bf16[512,496]{1,0:T(8,128)(2,1)S(1)}, bf16[512,496]{1,0:T(8,128)(2,1)}, u32[]{:S(2)}, u32[]{:S(2)}) collective-permute-start(bf16[512,496]{1,0:T(8,128)(2,1)S(1)} %slice.20.p0), channel_id=1, source_target_pairs={{0,24},{8,0},{16,8},{24,16},{1,25},{9,1},{17,9},{25,17},{2,26},{10... | collective-permute-start | bytes 1523720 | tf_op jit(solution)/shard_map/ppermute | solution.py:474
  120.7 58.8 %collective-permute-start.3 = (bf16[512,496]{1,0:T(8,128)(2,1)S(1)}, bf16[512,496]{1,0:T(8,128)(2,1)}, u32[]{:S(2)}, u32[]{:S(2)}) collective-permute-start(bf16[512,496]{1,0:T(8,128)(2,1)S(1)} %slice.20.p0), channel_id=1, source_target_pairs={{0,16},{8,24},{16,0},{24,8},{1,17},{9,25},{17,1},{25,9},{2,18},{10... | collective-permute-start | bytes 1523720 | tf_op jit(solution)/shard_map/ppermute | solution.py:474
  124.2 55.3 %collective-permute-start.2 = (bf16[512,496]{1,0:T(8,128)(2,1)S(1)}, bf16[512,496]{1,0:T(8,128)(2,1)}, u32[]{:S(2)}, u32[]{:S(2)}) collective-permute-start(bf16[512,496]{1,0:T(8,128)(2,1)S(1)} %slice.20.p0), channel_id=1, source_target_pairs={{0,8},{8,16},{16,24},{24,0},{1,9},{9,17},{17,25},{25,1},{2,10},{10... | collective-permute-start | bytes 1523720 | tf_op jit(solution)/shard_map/ppermute | solution.py:474
  126.2 29.7 %collective-permute-start.6 = (bf16[512,256]{1,0:T(8,128)(2,1)S(1)}, bf16[512,256]{1,0:T(8,128)(2,1)}, u32[]{:S(2)}, u32[]{:S(2)}) collective-permute-start(bf16[512,256]{1,0:T(8,128)(2,1)S(1)} %get-tuple-element.33.p0), channel_id=1, source_target_pairs={{0,16},{8,24},{16,0},{24,8},{1,17},{9,25},{17,1},{25,9},{2,18},{10... | collective-permute-start | bytes 786440 | tf_op jit(solution)/shard_map/ppermute | solution.py:474
  131.4 0.7 copy-start
  132.2 26.6 %collective-permute-start.5 = (bf16[512,256]{1,0:T(8,128)(2,1)S(1)}, bf16[512,256]{1,0:T(8,128)(2,1)}, u32[]{:S(2)}, u32[]{:S(2)}) collective-permute-start(bf16[512,256]{1,0:T(8,128)(2,1)S(1)} %get-tuple-element.33.p0), channel_id=1, source_target_pairs={{0,8},{8,16},{16,24},{24,0},{1,9},{9,17},{17,25},{25,1},{2,10},{10... | collective-permute-start | bytes 786440 | tf_op jit(solution)/shard_map/ppermute | solution.py:474
  158.7 1.0 copy-start.1
  187.6 5.3 %collective-permute-start.8 = (bf16[384,2048]{1,0:T(8,128)(2,1)S(1)}, bf16[384,2048]{1,0:T(8,128)(2,1)S(1)}, u32[]{:S(2)}, u32[]{:S(2)}) collective-permute-start(bf16[384,2048]{1,0:T(8,128)(2,1)S(1)} %get-tuple-element.31), channel_id=1, source_target_pairs={{0,1},{1,0},{2,3},{3,2},{4,5},{5,4},{6,7},{7,6},{8,9},{9,8},{10,11... | collective-permute-start | bytes 4718600 | tf_op jit(solution)/shard_map/ppermute | solution.py:474

commit v8 on v7

--- a/solution.py
+++ b/solution.py
@@ -73,12 +73,6 @@
             write(outer, inner, made)
 
 
-def shard_kernel(k, v, bv, bg, q, s, oc, oh, out):
-    for i, part in enumerate((k, v, bv, bg, q, s, oc)):
-        out[:, i * 128 : i * 128 + 128] = part[...]
-    out[:, 896:1008] = oh[:, 0:112]
-
-
 def normed_rows(source, at, gain, out, to):
     rows = 16
     x = source[at, :].astype(F32)
@@ -96,22 +90,37 @@
     swap_groups(read, write, rows)
 
 
-def norm_kernel(tokens_far, gain_far, out_far, tokens, gain, out, semaphores):
-    for copy in start_copies(((tokens_far, tokens), (gain_far, gain)), semaphores):
-        copy.wait()
-
-    def step(i, carry):
-        at = pl.ds(pl.multiple_of(i * 16, 16), 16)
-        normed_rows(tokens, at, gain, out, at)
-        return carry
-
-    lax.fori_loop(0, 6, step, 0, unroll=2)
-    pairs = [(out, out_far.at[k, 0:96, :]) for k in range(4)]
-    for copy in start_copies(pairs, semaphores):
-        copy.wait()
-
-
-def edge_kernel(edge, gain, given_far, out_far, out, semaphores):
+def norm_kernel(*refs):
+    tokens_far, gain_far, *weights_far = refs[:10]
+    out_far, shard, tokens, gain, out, weights, semaphores = refs[10:]
+
+    def piece(ref, i):
+        return ref.at[pl.ds(i * 32, 32), :]
+
+    pairs = [(gain_far, gain)] + [(piece(tokens_far, i), piece(tokens, i)) for i in range(3)]
+    pairs += [(part, weights.at[i]) for i, part in enumerate(weights_far)]
+    loads = start_copies(pairs, semaphores)
+    loads[0].wait()
+    stores = []
+    for i in range(3):
+        loads[1 + i].wait()
+        for part in range(2):
+            at = slice(i * 32 + part * 16, i * 32 + part * 16 + 16)
+            normed_rows(tokens, at, gain, out, at)
+        pairs = [(piece(out, i), out_far.at[k, pl.ds(i * 32, 32), :]) for k in range(4)]
+        stores += start_copies(pairs, semaphores.at[pl.ds(12 + 4 * i, 4)])
+    for load in loads[4:]:
+        load.wait()
+    for i in range(7):
+        shard[:, i * 128 : i * 128 + 128] = weights[i]
+    shard[:, 896:1008] = weights[7, :, 0:112]
+    for store in stores:
+        store.wait()
+
+
+def edge_kernel(edge, gain_far, given_far, out_far, gain, out, semaphores):
+    (load,) = start_copies(((gain_far, gain),), semaphores)
+    load.wait()
     normed_rows(edge, slice(0, 16), gain, out, slice(0, 16))
     pairs = [(out, out_far.at[k, 96:112, :]) for k in range(4)]
     for copy in start_copies(pairs, semaphores):
@@ -409,6 +418,9 @@
     rows = 128
     zero = jnp.zeros((), BF16)
     half = lane_is_second(rows)
+    diagonal = lax.broadcasted_iota(jnp.int32, (rows, rows), 0) == (
+        lax.broadcasted_iota(jnp.int32, (rows, rows), 1)
+    )
 
     def head_mean(x):
         first = jnp.sum(jnp.where(half, 0.0, x), axis=1, keepdims=True)
@@ -431,12 +443,14 @@
         parts = []
         for h in range(2):
             distance = jnp.abs(turned[at, h : h + 1] - logs[h : h + 1, :])
-            part = scores[h * rows : (h + 1) * rows, :] * jnp.exp(-distance)
+            head_scores = scores[h * rows : (h + 1) * rows, :]
+            part = head_scores * jnp.exp(-distance)
+            twice = part[:, at] + jnp.where(diagonal, head_scores[:, at], 0.0)
+            sides = [part[:, : at.start], twice, part[:, at.stop :]]
+            part = jnp.concatenate([side for side in sides if side.shape[1]], axis=1)
             parts.append(part.astype(BF16))
         mixed = jnp.dot(jnp.concatenate(parts, axis=0), v, preferred_element_type=F32)
         retained = retained + jnp.where(half, mixed[rows:, :], mixed[:rows, :])
-        same = q.astype(F32) * k[at, :].astype(F32)
-        retained = retained + 64 * head_mean(same) * v[at, :].astype(F32)
         centred = retained - head_mean(retained)
         normed = centred * lax.rsqrt(head_mean(centred * centred) + EPSILON)
         gate = jax.nn.silu(pair[at, 128:256].astype(F32))
@@ -510,35 +524,30 @@
         [(i * 8 + 7, i * 8 + 15) for i in range(count - 1)]
         + [(i * 8 + 8, i * 8) for i in range(count - 1)],
     )
-    shard = call(
-        shard_kernel,
-        shape((32, 1008), BF16),
+    tail = jnp.pad(output_heads[112:], ((0, 0), (0, 96)))
+    weights = (
+        key_weight,
+        value_weight,
+        branch_value,
+        branch_gate,
+        query_weight,
+        swish_weight,
+        output_conv.T,
+        output_heads.T,
+    )
+    normed, shard = call(
+        norm_kernel,
+        (shape((4, 112, 2048), BF16), shape((32, 1008), BF16)),
         (),
-        (
-            key_weight,
-            value_weight,
-            branch_value,
-            branch_gate,
-            query_weight,
-            swish_weight,
-            output_conv.T,
-            output_heads.T,
-        ),
-        grant=56,
-    )
-    tail = jnp.pad(output_heads[112:], ((0, 0), (0, 96)))
-    normed = call(
-        norm_kernel,
-        shape((4, 112, 2048), BF16),
-        (),
-        (tokens, input_gain[None]),
+        (tokens, input_gain[None], *weights),
         scratch=(
             pltpu.VMEM((96, 2048), BF16),
             pltpu.VMEM((1, 2048), F32),
             pltpu.VMEM((96, 2048), BF16),
-            pltpu.SemaphoreType.DMA((4,)),
+            pltpu.VMEM((8, 32, 128), BF16),
+            pltpu.SemaphoreType.DMA((24,)),
         ),
-        far=(0, 1),
+        far=tuple(range(10)),
         out_far=(0,),
     )
     edge, normed = lax.optimization_barrier((edge, normed))
@@ -547,8 +556,12 @@
         shape((4, 112, 2048), BF16),
         (),
         (edge, input_gain[None], normed),
-        scratch=(pltpu.VMEM((16, 2048), BF16), pltpu.SemaphoreType.DMA((4,))),
-        far=(2,),
+        scratch=(
+            pltpu.VMEM((1, 2048), F32),
+            pltpu.VMEM((16, 2048), BF16),
+            pltpu.SemaphoreType.DMA((4,)),
+        ),
+        far=(1, 2),
         out_far=(0,),
         aliases={2: 0},
     )

time: 220 us -> 219 us (level)
    pallas_call x9 -> x8, Pallas kernels: 25.3 us -> 23.8 us  [call(): pl.pallas_call(kernel, out_shape=out_shape, in_specs=[SMEM] * len(scalars...]
where the time goes in v8:
time: 219 us; the launch traced here: 218 us
  blocking collectives  80.5 us (37%)
  waiting for transfers between devices  60 us (27%)
  starting transfers between devices  49 us (22%)
  Pallas kernels  23.8 us (11%)
  local copies, waits for them, and re-layouts  4.02 us (2%)
    all_gather x1, blocking collectives, body(): rows = lax.all_gather(shard, ('zh', 'zl'), axis=0, tiled=True)  40.9 us
    ppermute x8, waiting for transfers between devices, ring(): lax.ppermute(x, axis, [(i, (i + shift) % count) for i in range(count)])  27 us
    all_to_all x1, blocking collectives, body(): parts = lax.all_to_all(joined.reshape(4, 96, 2048), 'x', 0, 0, tiled=True)  25.2 us
    ppermute x8, starting transfers between devices, ring(): lax.ppermute(x, axis, [(i, (i + shift) % count) for i in range(count)])  23.8 us
    pallas_call x8, Pallas kernels, call(): pl.pallas_call(kernel, out_shape=out_shape, in_specs=[SMEM] * len(scalars...  23.8 us
    all_to_all x1, waiting for transfers between devices, body(): inner = lax.all_to_all(sent, ('zl', 'y'), 0, 0, tiled=True)  17.4 us
    all_to_all x1, waiting for transfers between devices, copies(): lax.all_to_all(jnp.broadcast_to(x[None], (count, *x.shape)), axes, 0, 0,...  15.6 us
    all_gather x1, blocking collectives, body(): moments = lax.all_gather(moments, ('x', 'c'))  14.4 us
  transfers between devices with their start and end apart: 13, of which 5 were waited for; matrix products, arithmetic and copies ran while one was open for 1% of the time, Pallas kernels for 4%

profile of v8, /device:TPU:32, one launch (start us, length us, event | category | flops | bytes accessed | tf_op | source)
XLA Modules:
  0.0 218.3 jit_solution(2661899867834065092)
XLA Ops:
  0.0 0.9 slice_select_fusion
  0.9 4.5 %collective-permute-start = (bf16[16,2048]{1,0:T(8,128)(2,1)S(1)}, bf16[16,2048]{1,0:T(8,128)(2,1)S(1)}, u32[]{:S(2)}, u32[]{:S(2)}) collective-permute-start(bf16[16,2048]{1,0:T(8,128)(2,1)S(1)} %slice_select_fusion), channel_id=1, source_target_pairs={{7,15},{15,23},{23,31},{31,39},{39,47},{47,55},{55,63},{63,71},{71... | collective-permute-start | bytes 196616 | tf_op jit(solution)/shard_map/ppermute | solution.py:521
  5.4 2.8 %shard_map.145 = (bf16[4,112,2048]{2,1,0:T(8,128)(2,1)}, bf16[32,1008]{1,0:T(8,128)(2,1)S(1)}) custom-call(bf16[96,2048]{1,0:T(8,128)(2,1)} %refs_0_.1, f32[1,2048]{1,0:T(1,128)} %bitcast.19, bf16[32,128]{1,0:T(8,128)(2,1)} %refs_2_.1, bf16[32,128]{1,0:T(8,128)(2,1)} %refs_3_.1, bf16[32,128]{1,0:T(8,128)(2,1)} %refs_4_.1, bf16[32,128]{1,0:T(8,128)(2,1)} %refs_5_.1, ...), custom_call_target="tpu_custom_call" | custom-call | tf_op jit(solution)/shard_map/pallas_call | solution.py:37
  8.1 0.0 collective-permute-done.edge
  8.2 1.7 shard_map.146
  9.8 3.6 %all-to-all-start = ((bf16[4,112,2048]{2,1,0:T(8,128)(2,1)}), bf16[4,112,2048]{2,1,0:T(8,128)(2,1)S(1)}, u32[]{:S(2)}, u32[]{:S(2)}) async-start(bf16[4,112,2048]{2,1,0:T(8,128)(2,1)} %shard_map.146), calls=%async_computation | async-start | bytes 3670016 | tf_op jit(solution)/shard_map/all_to_all | solution.py:569
  13.4 40.9 %all_gather.9 = bf16[512,1008]{1,0:T(8,128)(2,1)S(1)} all-gather(bf16[32,1008]{1,0:T(8,128)(2,1)S(1)} %get-tuple-element.26), channel_id=1, replica_groups=mesh['zh'=4,'zl'=4,'y'=4,'x'=4,'c'=2] {'zh','zl'}, dimensions={0}, use_global_device_ids=true | all-gather | bytes 1096704 | tf_op jit(solution)/shard_map/all_gather | solution.py:570
  54.3 0.0 copy-start.4
  54.3 0.0 all-to-all-done
  54.3 1.9 collective-permute-start.1
  56.2 0.0 copy-done.4
  56.3 0.0 copy-start.5
  56.3 0.0 copy-start.3
  56.3 1.1 broadcast_in_dim.33
  57.4 4.2 %all-to-all-start.1 = ((bf16[4,512,256]{2,1,0:T(8,128)(2,1)}), bf16[4,512,256]{2,1,0:T(8,128)(2,1)S(1)}, u32[]{:S(2)}, u32[]{:S(2)}) async-start(bf16[4,512,256]{2,1,0:T(8,128)(2,1)} %broadcast_in_dim.33), calls=%async_computation.1 | async-start | bytes 2097152 | tf_op jit(solution)/shard_map/all_to_all | solution.py:492
  61.5 0.0 copy-done.5
  61.6 0.1 slice.22
  61.6 0.1 copy.19
  61.7 15.6 %all-to-all-done.1 = bf16[4,512,256]{2,1,0:T(8,128)(2,1)S(1)} async-done(((bf16[4,512,256]{2,1,0:T(8,128)(2,1)}), bf16[4,512,256]{2,1,0:T(8,128)(2,1)S(1)}, u32[]{:S(2)}, u32[]{:S(2)}) %all-to-all-start.1) | async-done | bytes 1048608 | tf_op jit(solution)/shard_map/all_to_all | solution.py:492
  77.3 0.0 collective-permute-done.1.other
  77.3 0.0 copy-done.3
  77.3 4.0 %shard_map.147 = (bf16[768,256]{1,0:T(8,128)(2,1)}, bf16[16,160,128]{2,1,0:T(8,128)(2,1)}, f32[8,768]{1,0:T(8,128)}) custom-call(s32[1]{0:T(128)} %bitcast.1.core, bf16[448,2048]{1,0:T(8,128)(2,1)S(1)} %bitcast.14, bf16[448,2048]{1,0:T(8,128)(2,1)} %collective-permute-done.1.other, bf16[2048,256]{1,0:T(8,128)(2,1)S(1)} %bitcast.18, f32[2,768]{1,0:T(2,128)S(1)} %copy-done.3, ...), custom_call_target="tpu_custom_call" | custom-call | tf_op jit(solution)/shard_map/pallas_call | solution.py:37
  81.3 0.0 copy-start.2
  81.3 6.1 %all-to-all-start.2 = ((bf16[16,160,128]{2,1,0:T(8,128)(2,1)}), bf16[16,160,128]{2,1,0:T(8,128)(2,1)S(1)}, u32[]{:S(2)}, u32[]{:S(2)}) async-start(bf16[16,160,128]{2,1,0:T(8,128)(2,1)} %get-tuple-element.29), calls=%async_computation.2 | async-start | bytes 1310720 | tf_op jit(solution)/shard_map/all_to_all | solution.py:592
  87.4 17.4 %all-to-all-done.2.gathered.inner = bf16[16,160,128]{2,1,0:T(8,128)(2,1)S(1)} async-done(((bf16[16,160,128]{2,1,0:T(8,128)(2,1)}), bf16[16,160,128]{2,1,0:T(8,128)(2,1)S(1)}, u32[]{:S(2)}, u32[]{:S(2)}) %all-to-all-start.2) | async-done | bytes 655392 | tf_op jit(solution)/shard_map/all_to_all | solution.py:592
  104.8 0.9 shard_map.148
  105.7 6.9 %all-to-all-start.3 = ((bf16[4,208,128]{2,1,0:T(8,128)(2,1)}), bf16[4,208,128]{2,1,0:T(8,128)(2,1)S(1)}, u32[]{:S(2)}, u32[]{:S(2)}) async-start(bf16[4,208,128]{2,1,0:T(8,128)(2,1)} %shard_map.148), calls=%async_computation.3 | async-start | bytes 425984 | tf_op jit(solution)/shard_map/all_to_all | solution.py:601
  112.6 3.2 %collective-permute-start.7 = (bf16[512,256]{1,0:T(8,128)(2,1)S(1)}, bf16[512,256]{1,0:T(8,128)(2,1)S(1)}, u32[]{:S(2)}, u32[]{:S(2)}) collective-permute-start(bf16[512,256]{1,0:T(8,128)(2,1)S(1)} %get-tuple-element.37.p0), channel_id=1, source_target_pairs={{0,24},{8,0},{16,8},{24,16},{1,25},{9,1},{17,9},{25,17},{2,26},{10... | collective-permute-start | bytes 786440 | tf_op jit(solution)/shard_map/ppermute | solution.py:488
  115.7 1.1 slice.20.p0
  116.8 3.1 %collective-permute-start.4 = (bf16[512,496]{1,0:T(8,128)(2,1)S(1)}, bf16[512,496]{1,0:T(8,128)(2,1)}, u32[]{:S(2)}, u32[]{:S(2)}) collective-permute-start(bf16[512,496]{1,0:T(8,128)(2,1)S(1)} %slice.20.p0), channel_id=1, source_target_pairs={{0,24},{8,0},{16,8},{24,16},{1,25},{9,1},{17,9},{25,17},{2,26},{10... | collective-permute-start | bytes 1523720 | tf_op jit(solution)/shard_map/ppermute | solution.py:488
  119.9 3.5 %collective-permute-start.3 = (bf16[512,496]{1,0:T(8,128)(2,1)S(1)}, bf16[512,496]{1,0:T(8,128)(2,1)}, u32[]{:S(2)}, u32[]{:S(2)}) collective-permute-start(bf16[512,496]{1,0:T(8,128)(2,1)S(1)} %slice.20.p0), channel_id=1, source_target_pairs={{0,16},{8,24},{16,0},{24,8},{1,17},{9,25},{17,1},{25,9},{2,18},{10... | collective-permute-start | bytes 1523720 | tf_op jit(solution)/shard_map/ppermute | solution.py:488
  123.5 1.9 collective-permute-start.2
  125.4 5.3 %collective-permute-start.6 = (bf16[512,256]{1,0:T(8,128)(2,1)S(1)}, bf16[512,256]{1,0:T(8,128)(2,1)}, u32[]{:S(2)}, u32[]{:S(2)}) collective-permute-start(bf16[512,256]{1,0:T(8,128)(2,1)S(1)} %get-tuple-element.37.p0), channel_id=1, source_target_pairs={{0,16},{8,24},{16,0},{24,8},{1,17},{9,25},{17,1},{25,9},{2,18},{10... | collective-permute-start | bytes 786440 | tf_op jit(solution)/shard_map/ppermute | solution.py:488
  130.7 0.0 collective-permute-done.7.p3
  130.7 0.0 copy-start
  130.7 0.7 copy-done
  131.4 2.6 %collective-permute-start.5 = (bf16[512,256]{1,0:T(8,128)(2,1)S(1)}, bf16[512,256]{1,0:T(8,128)(2,1)}, u32[]{:S(2)}, u32[]{:S(2)}) collective-permute-start(bf16[512,256]{1,0:T(8,128)(2,1)S(1)} %get-tuple-element.37.p0), channel_id=1, source_target_pairs={{0,8},{8,16},{16,24},{24,0},{1,9},{9,17},{17,25},{25,1},{2,10},{10... | collective-permute-start | bytes 786440 | tf_op jit(solution)/shard_map/ppermute | solution.py:488
  134.0 21.1 %collective-permute-done.6.p2 = bf16[512,256]{1,0:T(8,128)(2,1)} collective-permute-done((bf16[512,256]{1,0:T(8,128)(2,1)S(1)}, bf16[512,256]{1,0:T(8,128)(2,1)}, u32[]{:S(2)}, u32[]{:S(2)}) %collective-permute-start.6) | collective-permute-done | bytes 262176 | tf_op jit(solution)/shard_map/ppermute | solution.py:488
  155.1 2.9 %collective-permute-done.5.p1 = bf16[512,256]{1,0:T(8,128)(2,1)} collective-permute-done((bf16[512,256]{1,0:T(8,128)(2,1)S(1)}, bf16[512,256]{1,0:T(8,128)(2,1)}, u32[]{:S(2)}, u32[]{:S(2)}) %collective-permute-start.5) | collective-permute-done | bytes 262176 | tf_op jit(solution)/shard_map/ppermute | solution.py:488
  158.0 0.0 copy-done.2
  158.0 0.0 copy-start.1
  158.0 0.9 copy-done.1
  158.9 4.9 %shard_map.149 = (f32[768,128]{1,0:T(8,128)}, f32[2,768]{1,0:T(2,128)}) custom-call(s32[1]{0:T(128)} %bitcast.1.core, s32[1]{0:T(128)} %bitcast.y, bf16[448,2048]{1,0:T(8,128)(2,1)S(1)} %bitcast.15, bf16[448,2048]{1,0:T(8,128)(2,1)} %collective-permute-done.1.other, bf16[512,256]{1,0:T(8,128)(2,1)S(1)} %get-tuple-element.37.p0, ...), custom_call_target="tpu_custom_call" | custom-call | tf_op jit(solution)/shard_map/pallas_call | solution.py:37
  163.8 14.4 %all-gather.1.moments_far = f32[8,2,768]{2,1,0:T(2,128)} all-gather(f32[1,2,768]{2,1,0:T(2,128)} %bitcast.23), channel_id=2, replica_groups=mesh['zh'=4,'zl'=4,'y'=4,'x'=4,'c'=2] {'x','c'}, dimensions={0}, use_global_device_ids=true | all-gather | bytes 55296 | tf_op jit(solution)/shard_map/all_gather | solution.py:615
  178.2 0.0 collective-permute-done.4.p3
  178.2 0.0 collective-permute-done.3.p2
  178.2 0.0 collective-permute-done.2.p1
  178.2 0.0 all-to-all-done.3.outer
  178.3 7.7 %shard_map.150 = (bf16[384,256]{1,0:T(8,128)(2,1)S(1)}, bf16[384,2048]{1,0:T(8,128)(2,1)S(1)}, bf16[4,512,256]{2,1,0:T(8,128)(2,1)S(1)}) custom-call(s32[1]{0:T(128)} %bitcast.1.core, s32[1]{0:T(128)} %bitcast.y, s32[1]{0:T(128)} %bitcast.2.position.low, s32[1]{0:T(128)} %bitcast.3.high, bf16[448,2048]{1,0:T(8,128)(2,1)S(1)} %bitcast.16, ...), custom_call_target="tpu_custom_call" | custom-call | tf_op jit(solution)/shard_map/pallas_call | solution.py:37
  185.9 2.3 %collective-permute-start.8 = (bf16[384,2048]{1,0:T(8,128)(2,1)S(1)}, bf16[384,2048]{1,0:T(8,128)(2,1)S(1)}, u32[]{:S(2)}, u32[]{:S(2)}) collective-permute-start(bf16[384,2048]{1,0:T(8,128)(2,1)S(1)} %get-tuple-element.35), channel_id=1, source_target_pairs={{0,1},{1,0},{2,3},{3,2},{4,5},{5,4},{6,7},{7,6},{8,9},{9,8},{10,11... | collective-permute-start | bytes 4718600 | tf_op jit(solution)/shard_map/ppermute | solution.py:488
  188.2 3.0 %collective-permute-done.8.arrived = bf16[384,2048]{1,0:T(8,128)(2,1)S(1)} collective-permute-done((bf16[384,2048]{1,0:T(8,128)(2,1)S(1)}, bf16[384,2048]{1,0:T(8,128)(2,1)S(1)}, u32[]{:S(2)}, u32[]{:S(2)}) %collective-permute-start.8) | collective-permute-done | bytes 1572896 | tf_op jit(solution)/shard_map/ppermute | solution.py:488
  191.2 0.6 shard_map.151
  191.9 25.2 %all_to_all.25.parts = bf16[4,96,2048]{2,1,0:T(8,128)(2,1)S(1)} all-to-all(bf16[4,96,2048]{2,1,0:T(8,128)(2,1)S(1)} %bitcast.17), channel_id=1, replica_groups=mesh['zh'=4,'zl'=4,'y'=4,'x'=4,'c'=2] {'x'}, dimensions={0} | all-to-all | bytes 3145728 | tf_op jit(solution)/shard_map/all_to_all | solution.py:651
  217.1 1.3 shard_map.152
  (2 shorter events, 0.0 us)
Async XLA Ops:
  0.9 7.3 %collective-permute-start = (bf16[16,2048]{1,0:T(8,128)(2,1)S(1)}, bf16[16,2048]{1,0:T(8,128)(2,1)S(1)}, u32[]{:S(2)}, u32[]{:S(2)}) collective-permute-start(bf16[16,2048]{1,0:T(8,128)(2,1)S(1)} %slice_select_fusion), channel_id=1, source_target_pairs={{7,15},{15,23},{23,31},{31,39},{39,47},{47,55},{55,63},{63,71},{71... | collective-permute-start | bytes 196616 | tf_op jit(solution)/shard_map/ppermute | solution.py:521
  9.8 44.5 %all-to-all-start = ((bf16[4,112,2048]{2,1,0:T(8,128)(2,1)}), bf16[4,112,2048]{2,1,0:T(8,128)(2,1)S(1)}, u32[]{:S(2)}, u32[]{:S(2)}) async-start(bf16[4,112,2048]{2,1,0:T(8,128)(2,1)} %shard_map.146), calls=%async_computation | async-start | bytes 3670016 | tf_op jit(solution)/shard_map/all_to_all | solution.py:569
  54.3 1.9 copy-start.4
  54.3 23.0 %collective-permute-start.1 = (bf16[448,2048]{1,0:T(8,128)(2,1)S(1)}, bf16[448,2048]{1,0:T(8,128)(2,1)}, u32[]{:S(2)}, u32[]{:S(2)}) collective-permute-start(bf16[448,2048]{1,0:T(8,128)(2,1)S(1)} %bitcast.13), channel_id=1, source_target_pairs={{0,1},{1,0},{2,3},{3,2},{4,5},{5,4},{6,7},{7,6},{8,9},{9,8},{10,11... | collective-permute-start | bytes 5505032 | tf_op jit(solution)/shard_map/ppermute | solution.py:488
  56.3 5.3 %copy-start.5 = (bf16[128,32]{0,1:T(8,128)(2,1)S(1)}, bf16[128,32]{0,1:T(8,128)(2,1)}, u32[]{:S(2)}) copy-start(bf16[128,32]{0,1:T(8,128)(2,1)} %param.29) | copy-start | bytes 24580
  56.3 21.0 %copy-start.3 = (f32[2,768]{1,0:T(2,128)S(1)}, f32[2,768]{1,0:T(2,128)}, u32[]{:S(2)}) copy-start(f32[2,768]{1,0:T(2,128)} %decay.1) | copy-start | bytes 18436
  57.4 19.9 %all-to-all-start.1 = ((bf16[4,512,256]{2,1,0:T(8,128)(2,1)}), bf16[4,512,256]{2,1,0:T(8,128)(2,1)S(1)}, u32[]{:S(2)}, u32[]{:S(2)}) async-start(bf16[4,512,256]{2,1,0:T(8,128)(2,1)} %broadcast_in_dim.33), calls=%async_computation.1 | async-start | bytes 2097152 | tf_op jit(solution)/shard_map/all_to_all | solution.py:492
  81.3 76.6 %copy-start.2 = (f32[31,128]{1,0:T(8,128)S(1)}, f32[31,128]{1,0:T(8,128)}, u32[]{:S(2)}) copy-start(f32[31,128]{1,0:T(8,128)} %taps.1) | copy-start | bytes 47620
  81.3 23.4 %all-to-all-start.2 = ((bf16[16,160,128]{2,1,0:T(8,128)(2,1)}), bf16[16,160,128]{2,1,0:T(8,128)(2,1)S(1)}, u32[]{:S(2)}, u32[]{:S(2)}) async-start(bf16[16,160,128]{2,1,0:T(8,128)(2,1)} %get-tuple-element.29), calls=%async_computation.2 | async-start | bytes 1310720 | tf_op jit(solution)/shard_map/all_to_all | solution.py:592
  105.7 72.6 %all-to-all-start.3 = ((bf16[4,208,128]{2,1,0:T(8,128)(2,1)}), bf16[4,208,128]{2,1,0:T(8,128)(2,1)S(1)}, u32[]{:S(2)}, u32[]{:S(2)}) async-start(bf16[4,208,128]{2,1,0:T(8,128)(2,1)} %shard_map.148), calls=%async_computation.3 | async-start | bytes 425984 | tf_op jit(solution)/shard_map/all_to_all | solution.py:601
  112.6 18.1 %collective-permute-start.7 = (bf16[512,256]{1,0:T(8,128)(2,1)S(1)}, bf16[512,256]{1,0:T(8,128)(2,1)S(1)}, u32[]{:S(2)}, u32[]{:S(2)}) collective-permute-start(bf16[512,256]{1,0:T(8,128)(2,1)S(1)} %get-tuple-element.37.p0), channel_id=1, source_target_pairs={{0,24},{8,0},{16,8},{24,16},{1,25},{9,1},{17,9},{25,17},{2,26},{10... | collective-permute-start | bytes 786440 | tf_op jit(solution)/shard_map/ppermute | solution.py:488
  116.8 61.4 %collective-permute-start.4 = (bf16[512,496]{1,0:T(8,128)(2,1)S(1)}, bf16[512,496]{1,0:T(8,128)(2,1)}, u32[]{:S(2)}, u32[]{:S(2)}) collective-permute-start(bf16[512,496]{1,0:T(8,128)(2,1)S(1)} %slice.20.p0), channel_id=1, source_target_pairs={{0,24},{8,0},{16,8},{24,16},{1,25},{9,1},{17,9},{25,17},{2,26},{10... | collective-permute-start | bytes 1523720 | tf_op jit(solution)/shard_map/ppermute | solution.py:488
  119.9 58.3 %collective-permute-start.3 = (bf16[512,496]{1,0:T(8,128)(2,1)S(1)}, bf16[512,496]{1,0:T(8,128)(2,1)}, u32[]{:S(2)}, u32[]{:S(2)}) collective-permute-start(bf16[512,496]{1,0:T(8,128)(2,1)S(1)} %slice.20.p0), channel_id=1, source_target_pairs={{0,16},{8,24},{16,0},{24,8},{1,17},{9,25},{17,1},{25,9},{2,18},{10... | collective-permute-start | bytes 1523720 | tf_op jit(solution)/shard_map/ppermute | solution.py:488
  123.5 54.8 %collective-permute-start.2 = (bf16[512,496]{1,0:T(8,128)(2,1)S(1)}, bf16[512,496]{1,0:T(8,128)(2,1)}, u32[]{:S(2)}, u32[]{:S(2)}) collective-permute-start(bf16[512,496]{1,0:T(8,128)(2,1)S(1)} %slice.20.p0), channel_id=1, source_target_pairs={{0,8},{8,16},{16,24},{24,0},{1,9},{9,17},{17,25},{25,1},{2,10},{10... | collective-permute-start | bytes 1523720 | tf_op jit(solution)/shard_map/ppermute | solution.py:488
  125.4 29.7 %collective-permute-start.6 = (bf16[512,256]{1,0:T(8,128)(2,1)S(1)}, bf16[512,256]{1,0:T(8,128)(2,1)}, u32[]{:S(2)}, u32[]{:S(2)}) collective-permute-start(bf16[512,256]{1,0:T(8,128)(2,1)S(1)} %get-tuple-element.37.p0), channel_id=1, source_target_pairs={{0,16},{8,24},{16,0},{24,8},{1,17},{9,25},{17,1},{25,9},{2,18},{10... | collective-permute-start | bytes 786440 | tf_op jit(solution)/shard_map/ppermute | solution.py:488
  130.7 0.7 copy-start
  131.4 26.6 %collective-permute-start.5 = (bf16[512,256]{1,0:T(8,128)(2,1)S(1)}, bf16[512,256]{1,0:T(8,128)(2,1)}, u32[]{:S(2)}, u32[]{:S(2)}) collective-permute-start(bf16[512,256]{1,0:T(8,128)(2,1)S(1)} %get-tuple-element.37.p0), channel_id=1, source_target_pairs={{0,8},{8,16},{16,24},{24,0},{1,9},{9,17},{17,25},{25,1},{2,10},{10... | collective-permute-start | bytes 786440 | tf_op jit(solution)/shard_map/ppermute | solution.py:488
  158.0 1.0 copy-start.1
  185.9 5.3 %collective-permute-start.8 = (bf16[384,2048]{1,0:T(8,128)(2,1)S(1)}, bf16[384,2048]{1,0:T(8,128)(2,1)S(1)}, u32[]{:S(2)}, u32[]{:S(2)}) collective-permute-start(bf16[384,2048]{1,0:T(8,128)(2,1)S(1)} %get-tuple-element.35), channel_id=1, source_target_pairs={{0,1},{1,0},{2,3},{3,2},{4,5},{5,4},{6,7},{7,6},{8,9},{9,8},{10,11... | collective-permute-start | bytes 4718600 | tf_op jit(solution)/shard_map/ppermute | solution.py:488

commit v9 on v7

--- a/solution.py
+++ b/solution.py
@@ -409,6 +409,9 @@
     rows = 128
     zero = jnp.zeros((), BF16)
     half = lane_is_second(rows)
+    diagonal = lax.broadcasted_iota(jnp.int32, (rows, rows), 0) == (
+        lax.broadcasted_iota(jnp.int32, (rows, rows), 1)
+    )
 
     def head_mean(x):
         first = jnp.sum(jnp.where(half, 0.0, x), axis=1, keepdims=True)
@@ -431,12 +434,14 @@
         parts = []
         for h in range(2):
             distance = jnp.abs(turned[at, h : h + 1] - logs[h : h + 1, :])
-            part = scores[h * rows : (h + 1) * rows, :] * jnp.exp(-distance)
+            head_scores = scores[h * rows : (h + 1) * rows, :]
+            part = head_scores * jnp.exp(-distance)
+            twice = part[:, at] + jnp.where(diagonal, head_scores[:, at], 0.0)
+            sides = [part[:, : at.start], twice, part[:, at.stop :]]
+            part = jnp.concatenate([side for side in sides if side.shape[1]], axis=1)
             parts.append(part.astype(BF16))
         mixed = jnp.dot(jnp.concatenate(parts, axis=0), v, preferred_element_type=F32)
         retained = retained + jnp.where(half, mixed[rows:, :], mixed[:rows, :])
-        same = q.astype(F32) * k[at, :].astype(F32)
-        retained = retained + 64 * head_mean(same) * v[at, :].astype(F32)
         centred = retained - head_mean(retained)
         normed = centred * lax.rsqrt(head_mean(centred * centred) + EPSILON)
         gate = jax.nn.silu(pair[at, 128:256].astype(F32))

time: 220 us -> 220 us (level)
  no operation moved by 1% of the time
where the time goes in v9:
time: 220 us; the launch traced here: 218 us
  blocking collectives  80.1 us (36%)
  waiting for transfers between devices  60.4 us (27%)
  starting transfers between devices  47.9 us (22%)
  Pallas kernels  24.8 us (11%)
  local copies, waits for them, and re-layouts  4.05 us (2%)
    all_gather x1, blocking collectives, body(): rows = lax.all_gather(shard, ('zh', 'zl'), axis=0, tiled=True)  41.1 us
    ppermute x8, waiting for transfers between devices, ring(): lax.ppermute(x, axis, [(i, (i + shift) % count) for i in range(count)])  27 us
    pallas_call x9, Pallas kernels, call(): pl.pallas_call(kernel, out_shape=out_shape, in_specs=[SMEM] * len(scalars...  24.8 us
    all_to_all x1, blocking collectives, body(): parts = lax.all_to_all(joined.reshape(4, 96, 2048), 'x', 0, 0, tiled=True)  24.1 us
    ppermute x8, starting transfers between devices, ring(): lax.ppermute(x, axis, [(i, (i + shift) % count) for i in range(count)])  23.8 us
    all_to_all x1, waiting for transfers between devices, body(): inner = lax.all_to_all(sent, ('zl', 'y'), 0, 0, tiled=True)  17.6 us
    all_to_all x1, waiting for transfers between devices, copies(): lax.all_to_all(jnp.broadcast_to(x[None], (count, *x.shape)), axes, 0, 0,...  15.8 us
    all_gather x1, blocking collectives, body(): moments = lax.all_gather(moments, ('x', 'c'))  14.9 us
  transfers between devices with their start and end apart: 13, of which 5 were waited for; matrix products, arithmetic and copies ran while one was open for 1% of the time, Pallas kernels for 4%

profile of v9, /device:TPU:32, one launch (start us, length us, event | category | flops | bytes accessed | tf_op | source)
XLA Modules:
  0.0 218.5 jit_solution(1683637786644491796)
XLA Ops:
  0.0 0.0 copy-start.2
  0.0 0.9 slice_select_fusion
  0.9 4.5 %collective-permute-start = (bf16[16,2048]{1,0:T(8,128)(2,1)S(1)}, bf16[16,2048]{1,0:T(8,128)(2,1)S(1)}, u32[]{:S(2)}, u32[]{:S(2)}) collective-permute-start(bf16[16,2048]{1,0:T(8,128)(2,1)S(1)} %slice_select_fusion), channel_id=1, source_target_pairs={{7,15},{15,23},{23,31},{31,39},{39,47},{47,55},{55,63},{63,71},{71... | collective-permute-start | bytes 196616 | tf_op jit(solution)/shard_map/ppermute | solution.py:512
  5.4 3.0 %shard_map.146.given_far = bf16[4,112,2048]{2,1,0:T(8,128)(2,1)} custom-call(bf16[96,2048]{1,0:T(8,128)(2,1)} %tokens_far.1, f32[1,2048]{1,0:T(1,128)} %bitcast.19), custom_call_target="tpu_custom_call" | custom-call | tf_op jit(solution)/shard_map/pallas_call | solution.py:37
  8.4 1.5 shard_map.145
  9.9 0.0 collective-permute-done.edge
  9.9 0.0 copy-done.2
  9.9 1.0 shard_map.147
  10.9 0.0 copy-start.6
  10.9 3.7 %all-to-all-start = ((bf16[4,112,2048]{2,1,0:T(8,128)(2,1)}), bf16[4,112,2048]{2,1,0:T(8,128)(2,1)S(1)}, u32[]{:S(2)}, u32[]{:S(2)}) async-start(bf16[4,112,2048]{2,1,0:T(8,128)(2,1)} %shard_map.147), calls=%async_computation | async-start | bytes 3670016 | tf_op jit(solution)/shard_map/all_to_all | solution.py:561
  14.6 0.0 copy-done.6
  14.6 41.1 %all_gather.9 = bf16[512,1008]{1,0:T(8,128)(2,1)S(1)} all-gather(bf16[32,1008]{1,0:T(8,128)(2,1)S(1)} %copy-done.6), channel_id=1, replica_groups=mesh['zh'=4,'zl'=4,'y'=4,'x'=4,'c'=2] {'zh','zl'}, dimensions={0}, use_global_device_ids=true | all-gather | bytes 1096704 | tf_op jit(solution)/shard_map/all_gather | solution.py:562
  55.8 0.0 copy-start.5
  55.8 0.0 all-to-all-done
  55.8 1.9 collective-permute-start.1
  57.7 0.0 copy-done.5
  57.7 0.0 copy-start.7
  57.7 0.0 copy-start.4
  57.8 1.1 broadcast_in_dim.33
  58.8 3.5 %all-to-all-start.1 = ((bf16[4,512,256]{2,1,0:T(8,128)(2,1)}), bf16[4,512,256]{2,1,0:T(8,128)(2,1)S(1)}, u32[]{:S(2)}, u32[]{:S(2)}) async-start(bf16[4,512,256]{2,1,0:T(8,128)(2,1)} %broadcast_in_dim.33), calls=%async_computation.1 | async-start | bytes 2097152 | tf_op jit(solution)/shard_map/all_to_all | solution.py:483
  62.3 0.0 copy-done.7
  62.4 0.1 slice.22
  62.4 0.1 copy.19
  62.5 15.8 %all-to-all-done.1 = bf16[4,512,256]{2,1,0:T(8,128)(2,1)S(1)} async-done(((bf16[4,512,256]{2,1,0:T(8,128)(2,1)}), bf16[4,512,256]{2,1,0:T(8,128)(2,1)S(1)}, u32[]{:S(2)}, u32[]{:S(2)}) %all-to-all-start.1) | async-done | bytes 1048608 | tf_op jit(solution)/shard_map/all_to_all | solution.py:483
  78.4 0.0 collective-permute-done.1.other
  78.4 0.0 copy-done.4
  78.4 4.0 %shard_map.148 = (bf16[768,256]{1,0:T(8,128)(2,1)}, bf16[16,160,128]{2,1,0:T(8,128)(2,1)}, f32[8,768]{1,0:T(8,128)}) custom-call(s32[1]{0:T(128)} %bitcast.1.core, bf16[448,2048]{1,0:T(8,128)(2,1)S(1)} %bitcast.14, bf16[448,2048]{1,0:T(8,128)(2,1)} %collective-permute-done.1.other, bf16[2048,256]{1,0:T(8,128)(2,1)S(1)} %bitcast.18, f32[2,768]{1,0:T(2,128)S(1)} %copy-done.4, ...), custom_call_target="tpu_custom_call" | custom-call | tf_op jit(solution)/shard_map/pallas_call | solution.py:37
  82.4 0.0 copy-start.3
  82.4 5.0 %all-to-all-start.2 = ((bf16[16,160,128]{2,1,0:T(8,128)(2,1)}), bf16[16,160,128]{2,1,0:T(8,128)(2,1)S(1)}, u32[]{:S(2)}, u32[]{:S(2)}) async-start(bf16[16,160,128]{2,1,0:T(8,128)(2,1)} %get-tuple-element.25), calls=%async_computation.2 | async-start | bytes 1310720 | tf_op jit(solution)/shard_map/all_to_all | solution.py:584
  87.4 17.6 %all-to-all-done.2.gathered.inner = bf16[16,160,128]{2,1,0:T(8,128)(2,1)S(1)} async-done(((bf16[16,160,128]{2,1,0:T(8,128)(2,1)}), bf16[16,160,128]{2,1,0:T(8,128)(2,1)S(1)}, u32[]{:S(2)}, u32[]{:S(2)}) %all-to-all-start.2) | async-done | bytes 655392 | tf_op jit(solution)/shard_map/all_to_all | solution.py:584
  105.0 0.9 shard_map.149
  105.9 7.5 %all-to-all-start.3 = ((bf16[4,208,128]{2,1,0:T(8,128)(2,1)}), bf16[4,208,128]{2,1,0:T(8,128)(2,1)S(1)}, u32[]{:S(2)}, u32[]{:S(2)}) async-start(bf16[4,208,128]{2,1,0:T(8,128)(2,1)} %shard_map.149), calls=%async_computation.3 | async-start | bytes 425984 | tf_op jit(solution)/shard_map/all_to_all | solution.py:593
  113.3 3.2 %collective-permute-start.7 = (bf16[512,256]{1,0:T(8,128)(2,1)S(1)}, bf16[512,256]{1,0:T(8,128)(2,1)S(1)}, u32[]{:S(2)}, u32[]{:S(2)}) collective-permute-start(bf16[512,256]{1,0:T(8,128)(2,1)S(1)} %get-tuple-element.33.p0), channel_id=1, source_target_pairs={{0,24},{8,0},{16,8},{24,16},{1,25},{9,1},{17,9},{25,17},{2,26},{10... | collective-permute-start | bytes 786440 | tf_op jit(solution)/shard_map/ppermute | solution.py:479
  116.5 1.1 slice.20.p0
  117.6 3.1 %collective-permute-start.4 = (bf16[512,496]{1,0:T(8,128)(2,1)S(1)}, bf16[512,496]{1,0:T(8,128)(2,1)}, u32[]{:S(2)}, u32[]{:S(2)}) collective-permute-start(bf16[512,496]{1,0:T(8,128)(2,1)S(1)} %slice.20.p0), channel_id=1, source_target_pairs={{0,24},{8,0},{16,8},{24,16},{1,25},{9,1},{17,9},{25,17},{2,26},{10... | collective-permute-start | bytes 1523720 | tf_op jit(solution)/shard_map/ppermute | solution.py:479
  120.7 3.5 %collective-permute-start.3 = (bf16[512,496]{1,0:T(8,128)(2,1)S(1)}, bf16[512,496]{1,0:T(8,128)(2,1)}, u32[]{:S(2)}, u32[]{:S(2)}) collective-permute-start(bf16[512,496]{1,0:T(8,128)(2,1)S(1)} %slice.20.p0), channel_id=1, source_target_pairs={{0,16},{8,24},{16,0},{24,8},{1,17},{9,25},{17,1},{25,9},{2,18},{10... | collective-permute-start | bytes 1523720 | tf_op jit(solution)/shard_map/ppermute | solution.py:479
  124.2 1.9 collective-permute-start.2
  126.2 5.3 %collective-permute-start.6 = (bf16[512,256]{1,0:T(8,128)(2,1)S(1)}, bf16[512,256]{1,0:T(8,128)(2,1)}, u32[]{:S(2)}, u32[]{:S(2)}) collective-permute-start(bf16[512,256]{1,0:T(8,128)(2,1)S(1)} %get-tuple-element.33.p0), channel_id=1, source_target_pairs={{0,16},{8,24},{16,0},{24,8},{1,17},{9,25},{17,1},{25,9},{2,18},{10... | collective-permute-start | bytes 786440 | tf_op jit(solution)/shard_map/ppermute | solution.py:479
  131.4 0.0 collective-permute-done.7.p3
  131.4 0.0 copy-start
  131.4 0.7 copy-done
  132.2 2.6 %collective-permute-start.5 = (bf16[512,256]{1,0:T(8,128)(2,1)S(1)}, bf16[512,256]{1,0:T(8,128)(2,1)}, u32[]{:S(2)}, u32[]{:S(2)}) collective-permute-start(bf16[512,256]{1,0:T(8,128)(2,1)S(1)} %get-tuple-element.33.p0), channel_id=1, source_target_pairs={{0,8},{8,16},{16,24},{24,0},{1,9},{9,17},{17,25},{25,1},{2,10},{10... | collective-permute-start | bytes 786440 | tf_op jit(solution)/shard_map/ppermute | solution.py:479
  134.8 21.1 %collective-permute-done.6.p2 = bf16[512,256]{1,0:T(8,128)(2,1)} collective-permute-done((bf16[512,256]{1,0:T(8,128)(2,1)S(1)}, bf16[512,256]{1,0:T(8,128)(2,1)}, u32[]{:S(2)}, u32[]{:S(2)}) %collective-permute-start.6) | collective-permute-done | bytes 262176 | tf_op jit(solution)/shard_map/ppermute | solution.py:479
  155.9 2.9 %collective-permute-done.5.p1 = bf16[512,256]{1,0:T(8,128)(2,1)} collective-permute-done((bf16[512,256]{1,0:T(8,128)(2,1)S(1)}, bf16[512,256]{1,0:T(8,128)(2,1)}, u32[]{:S(2)}, u32[]{:S(2)}) %collective-permute-start.5) | collective-permute-done | bytes 262176 | tf_op jit(solution)/shard_map/ppermute | solution.py:479
  158.7 0.0 copy-done.3
  158.7 0.0 copy-start.1
  158.7 0.9 copy-done.1
  159.7 4.9 %shard_map.150 = (f32[768,128]{1,0:T(8,128)}, f32[2,768]{1,0:T(2,128)}) custom-call(s32[1]{0:T(128)} %bitcast.1.core, s32[1]{0:T(128)} %bitcast.y, bf16[448,2048]{1,0:T(8,128)(2,1)S(1)} %bitcast.15, bf16[448,2048]{1,0:T(8,128)(2,1)} %collective-permute-done.1.other, bf16[512,256]{1,0:T(8,128)(2,1)S(1)} %get-tuple-element.33.p0, ...), custom_call_target="tpu_custom_call" | custom-call | tf_op jit(solution)/shard_map/pallas_call | solution.py:37
  164.6 14.9 %all-gather.1.moments_far = f32[8,2,768]{2,1,0:T(2,128)} all-gather(f32[1,2,768]{2,1,0:T(2,128)} %bitcast.23), channel_id=2, replica_groups=mesh['zh'=4,'zl'=4,'y'=4,'x'=4,'c'=2] {'x','c'}, dimensions={0}, use_global_device_ids=true | all-gather | bytes 55296 | tf_op jit(solution)/shard_map/all_gather | solution.py:607
  179.5 0.0 collective-permute-done.4.p3
  179.5 0.0 collective-permute-done.3.p2
  179.5 0.0 collective-permute-done.2.p1
  179.5 0.0 all-to-all-done.3.outer
  179.5 7.7 %shard_map.151 = (bf16[384,256]{1,0:T(8,128)(2,1)S(1)}, bf16[384,2048]{1,0:T(8,128)(2,1)S(1)}, bf16[4,512,256]{2,1,0:T(8,128)(2,1)S(1)}) custom-call(s32[1]{0:T(128)} %bitcast.1.core, s32[1]{0:T(128)} %bitcast.y, s32[1]{0:T(128)} %bitcast.2.position.low, s32[1]{0:T(128)} %bitcast.3.high, bf16[448,2048]{1,0:T(8,128)(2,1)S(1)} %bitcast.16, ...), custom_call_target="tpu_custom_call" | custom-call | tf_op jit(solution)/shard_map/pallas_call | solution.py:37
  187.2 2.3 %collective-permute-start.8 = (bf16[384,2048]{1,0:T(8,128)(2,1)S(1)}, bf16[384,2048]{1,0:T(8,128)(2,1)S(1)}, u32[]{:S(2)}, u32[]{:S(2)}) collective-permute-start(bf16[384,2048]{1,0:T(8,128)(2,1)S(1)} %get-tuple-element.31), channel_id=1, source_target_pairs={{0,1},{1,0},{2,3},{3,2},{4,5},{5,4},{6,7},{7,6},{8,9},{9,8},{10,11... | collective-permute-start | bytes 4718600 | tf_op jit(solution)/shard_map/ppermute | solution.py:479
  189.4 3.0 %collective-permute-done.8.arrived = bf16[384,2048]{1,0:T(8,128)(2,1)S(1)} collective-permute-done((bf16[384,2048]{1,0:T(8,128)(2,1)S(1)}, bf16[384,2048]{1,0:T(8,128)(2,1)S(1)}, u32[]{:S(2)}, u32[]{:S(2)}) %collective-permute-start.8) | collective-permute-done | bytes 1572896 | tf_op jit(solution)/shard_map/ppermute | solution.py:479
  192.5 0.6 shard_map.152
  193.1 24.1 %all_to_all.25.parts = bf16[4,96,2048]{2,1,0:T(8,128)(2,1)S(1)} all-to-all(bf16[4,96,2048]{2,1,0:T(8,128)(2,1)S(1)} %bitcast.17), channel_id=1, replica_groups=mesh['zh'=4,'zl'=4,'y'=4,'x'=4,'c'=2] {'x'}, dimensions={0} | all-to-all | bytes 3145728 | tf_op jit(solution)/shard_map/all_to_all | solution.py:643
  217.2 1.3 shard_map.153
  (2 shorter events, 0.0 us)
Async XLA Ops:
  0.0 9.9 %copy-start.2 = (f32[2048]{0:T(1024)S(1)}, f32[2048]{0:T(1024)}, u32[]{:S(2)}) copy-start(f32[2048]{0:T(1024)} %param.16) | copy-start | bytes 24580
  0.9 9.0 %collective-permute-start = (bf16[16,2048]{1,0:T(8,128)(2,1)S(1)}, bf16[16,2048]{1,0:T(8,128)(2,1)S(1)}, u32[]{:S(2)}, u32[]{:S(2)}) collective-permute-start(bf16[16,2048]{1,0:T(8,128)(2,1)S(1)} %slice_select_fusion), channel_id=1, source_target_pairs={{7,15},{15,23},{23,31},{31,39},{39,47},{47,55},{55,63},{63,71},{71... | collective-permute-start | bytes 196616 | tf_op jit(solution)/shard_map/ppermute | solution.py:512
  10.9 3.8 %copy-start.6 = (bf16[32,1008]{1,0:T(8,128)(2,1)S(1)}, bf16[32,1008]{1,0:T(8,128)(2,1)}, u32[]{:S(2)}) copy-start(bf16[32,1008]{1,0:T(8,128)(2,1)} %shard_map.145) | copy-start | bytes 193540
  10.9 44.9 %all-to-all-start = ((bf16[4,112,2048]{2,1,0:T(8,128)(2,1)}), bf16[4,112,2048]{2,1,0:T(8,128)(2,1)S(1)}, u32[]{:S(2)}, u32[]{:S(2)}) async-start(bf16[4,112,2048]{2,1,0:T(8,128)(2,1)} %shard_map.147), calls=%async_computation | async-start | bytes 3670016 | tf_op jit(solution)/shard_map/all_to_all | solution.py:561
  55.8 1.9 copy-start.5
  55.8 22.6 %collective-permute-start.1 = (bf16[448,2048]{1,0:T(8,128)(2,1)S(1)}, bf16[448,2048]{1,0:T(8,128)(2,1)}, u32[]{:S(2)}, u32[]{:S(2)}) collective-permute-start(bf16[448,2048]{1,0:T(8,128)(2,1)S(1)} %bitcast.13), channel_id=1, source_target_pairs={{0,1},{1,0},{2,3},{3,2},{4,5},{5,4},{6,7},{7,6},{8,9},{9,8},{10,11... | collective-permute-start | bytes 5505032 | tf_op jit(solution)/shard_map/ppermute | solution.py:479
  57.7 4.6 %copy-start.7 = (bf16[128,32]{0,1:T(8,128)(2,1)S(1)}, bf16[128,32]{0,1:T(8,128)(2,1)}, u32[]{:S(2)}) copy-start(bf16[128,32]{0,1:T(8,128)(2,1)} %param.29) | copy-start | bytes 24580
  57.7 20.6 %copy-start.4 = (f32[2,768]{1,0:T(2,128)S(1)}, f32[2,768]{1,0:T(2,128)}, u32[]{:S(2)}) copy-start(f32[2,768]{1,0:T(2,128)} %decay.1) | copy-start | bytes 18436
  58.8 19.5 %all-to-all-start.1 = ((bf16[4,512,256]{2,1,0:T(8,128)(2,1)}), bf16[4,512,256]{2,1,0:T(8,128)(2,1)S(1)}, u32[]{:S(2)}, u32[]{:S(2)}) async-start(bf16[4,512,256]{2,1,0:T(8,128)(2,1)} %broadcast_in_dim.33), calls=%async_computation.1 | async-start | bytes 2097152 | tf_op jit(solution)/shard_map/all_to_all | solution.py:483
  82.4 76.3 %copy-start.3 = (f32[31,128]{1,0:T(8,128)S(1)}, f32[31,128]{1,0:T(8,128)}, u32[]{:S(2)}) copy-start(f32[31,128]{1,0:T(8,128)} %taps.1) | copy-start | bytes 47620
  82.4 22.6 %all-to-all-start.2 = ((bf16[16,160,128]{2,1,0:T(8,128)(2,1)}), bf16[16,160,128]{2,1,0:T(8,128)(2,1)S(1)}, u32[]{:S(2)}, u32[]{:S(2)}) async-start(bf16[16,160,128]{2,1,0:T(8,128)(2,1)} %get-tuple-element.25), calls=%async_computation.2 | async-start | bytes 1310720 | tf_op jit(solution)/shard_map/all_to_all | solution.py:584
  105.9 73.6 %all-to-all-start.3 = ((bf16[4,208,128]{2,1,0:T(8,128)(2,1)}), bf16[4,208,128]{2,1,0:T(8,128)(2,1)S(1)}, u32[]{:S(2)}, u32[]{:S(2)}) async-start(bf16[4,208,128]{2,1,0:T(8,128)(2,1)} %shard_map.149), calls=%async_computation.3 | async-start | bytes 425984 | tf_op jit(solution)/shard_map/all_to_all | solution.py:593
  113.3 18.1 %collective-permute-start.7 = (bf16[512,256]{1,0:T(8,128)(2,1)S(1)}, bf16[512,256]{1,0:T(8,128)(2,1)S(1)}, u32[]{:S(2)}, u32[]{:S(2)}) collective-permute-start(bf16[512,256]{1,0:T(8,128)(2,1)S(1)} %get-tuple-element.33.p0), channel_id=1, source_target_pairs={{0,24},{8,0},{16,8},{24,16},{1,25},{9,1},{17,9},{25,17},{2,26},{10... | collective-permute-start | bytes 786440 | tf_op jit(solution)/shard_map/ppermute | solution.py:479
  117.6 61.9 %collective-permute-start.4 = (bf16[512,496]{1,0:T(8,128)(2,1)S(1)}, bf16[512,496]{1,0:T(8,128)(2,1)}, u32[]{:S(2)}, u32[]{:S(2)}) collective-permute-start(bf16[512,496]{1,0:T(8,128)(2,1)S(1)} %slice.20.p0), channel_id=1, source_target_pairs={{0,24},{8,0},{16,8},{24,16},{1,25},{9,1},{17,9},{25,17},{2,26},{10... | collective-permute-start | bytes 1523720 | tf_op jit(solution)/shard_map/ppermute | solution.py:479
  120.7 58.8 %collective-permute-start.3 = (bf16[512,496]{1,0:T(8,128)(2,1)S(1)}, bf16[512,496]{1,0:T(8,128)(2,1)}, u32[]{:S(2)}, u32[]{:S(2)}) collective-permute-start(bf16[512,496]{1,0:T(8,128)(2,1)S(1)} %slice.20.p0), channel_id=1, source_target_pairs={{0,16},{8,24},{16,0},{24,8},{1,17},{9,25},{17,1},{25,9},{2,18},{10... | collective-permute-start | bytes 1523720 | tf_op jit(solution)/shard_map/ppermute | solution.py:479
  124.2 55.3 %collective-permute-start.2 = (bf16[512,496]{1,0:T(8,128)(2,1)S(1)}, bf16[512,496]{1,0:T(8,128)(2,1)}, u32[]{:S(2)}, u32[]{:S(2)}) collective-permute-start(bf16[512,496]{1,0:T(8,128)(2,1)S(1)} %slice.20.p0), channel_id=1, source_target_pairs={{0,8},{8,16},{16,24},{24,0},{1,9},{9,17},{17,25},{25,1},{2,10},{10... | collective-permute-start | bytes 1523720 | tf_op jit(solution)/shard_map/ppermute | solution.py:479
  126.2 29.7 %collective-permute-start.6 = (bf16[512,256]{1,0:T(8,128)(2,1)S(1)}, bf16[512,256]{1,0:T(8,128)(2,1)}, u32[]{:S(2)}, u32[]{:S(2)}) collective-permute-start(bf16[512,256]{1,0:T(8,128)(2,1)S(1)} %get-tuple-element.33.p0), channel_id=1, source_target_pairs={{0,16},{8,24},{16,0},{24,8},{1,17},{9,25},{17,1},{25,9},{2,18},{10... | collective-permute-start | bytes 786440 | tf_op jit(solution)/shard_map/ppermute | solution.py:479
  131.4 0.7 copy-start
  132.2 26.6 %collective-permute-start.5 = (bf16[512,256]{1,0:T(8,128)(2,1)S(1)}, bf16[512,256]{1,0:T(8,128)(2,1)}, u32[]{:S(2)}, u32[]{:S(2)}) collective-permute-start(bf16[512,256]{1,0:T(8,128)(2,1)S(1)} %get-tuple-element.33.p0), channel_id=1, source_target_pairs={{0,8},{8,16},{16,24},{24,0},{1,9},{9,17},{17,25},{25,1},{2,10},{10... | collective-permute-start | bytes 786440 | tf_op jit(solution)/shard_map/ppermute | solution.py:479
  158.7 1.0 copy-start.1
  187.2 5.3 %collective-permute-start.8 = (bf16[384,2048]{1,0:T(8,128)(2,1)S(1)}, bf16[384,2048]{1,0:T(8,128)(2,1)S(1)}, u32[]{:S(2)}, u32[]{:S(2)}) collective-permute-start(bf16[384,2048]{1,0:T(8,128)(2,1)S(1)} %get-tuple-element.31), channel_id=1, source_target_pairs={{0,1},{1,0},{2,3},{3,2},{4,5},{5,4},{6,7},{7,6},{8,9},{9,8},{10,11... | collective-permute-start | bytes 4718600 | tf_op jit(solution)/shard_map/ppermute | solution.py:479

commit v10 on v9

--- a/solution.py
+++ b/solution.py
@@ -295,8 +295,8 @@
     is_second = jnp.full((16, 128), core[0], jnp.int32) == 1
     padded[0:16, :] = jnp.where(is_second, first[432:448, :], second[432:448, :])
     padded[784:800, :] = jnp.where(is_second, second[96:112, :], first[96:112, :])
-    ones = jnp.ones((8, 128), F32)
     rows = 128
+    first_lane = lax.broadcasted_iota(jnp.int32, (rows, 128), 1) == 0
     for i in range(6):
         total = None
         for j in range(31):
@@ -304,11 +304,11 @@
             term = taps[j : j + 1, :] * padded[start : start + rows, :]
             total = term if total is None else total + term
         convolved[i * rows : (i + 1) * rows, :] = total
-        highest = lax.Precision.HIGHEST
-        s1 = lax.dot_general(ones, total, NT, precision=highest, preferred_element_type=F32)
-        s2 = lax.dot_general(ones, total * total, NT, precision=highest, preferred_element_type=F32)
-        moments[0:1, i * rows : (i + 1) * rows] = s1[0:1]
-        moments[1:2, i * rows : (i + 1) * rows] = s2[0:1]
+        s1 = jnp.sum(total, axis=1, keepdims=True)
+        s2 = jnp.sum(total * total, axis=1, keepdims=True)
+        turned = jnp.transpose(jnp.where(first_lane, s1, s2))
+        moments[0:1, i * rows : (i + 1) * rows] = turned[0:1]
+        moments[1:2, i * rows : (i + 1) * rows] = turned[1:2]
     pairs = ((convolved, convolved_far), (moments, moments_far))
     for copy in start_copies(pairs, semaphores):
         copy.wait()

time: 220 us -> 219 us (level)
  no operation moved by 1% of the time
where the time goes in v10:
time: 219 us; the launch traced here: 218 us
  blocking collectives  80.1 us (37%)
  waiting for transfers between devices  60.4 us (28%)
  starting transfers between devices  47.9 us (22%)
  Pallas kernels  24.4 us (11%)
  local copies, waits for them, and re-layouts  4.05 us (2%)
    all_gather x1, blocking collectives, body(): rows = lax.all_gather(shard, ('zh', 'zl'), axis=0, tiled=True)  41.1 us
    ppermute x8, waiting for transfers between devices, ring(): lax.ppermute(x, axis, [(i, (i + shift) % count) for i in range(count)])  27 us
    pallas_call x9, Pallas kernels, call(): pl.pallas_call(kernel, out_shape=out_shape, in_specs=[SMEM] * len(scalars...  24.4 us
    all_to_all x1, blocking collectives, body(): parts = lax.all_to_all(joined.reshape(4, 96, 2048), 'x', 0, 0, tiled=True)  24.1 us
    ppermute x8, starting transfers between devices, ring(): lax.ppermute(x, axis, [(i, (i + shift) % count) for i in range(count)])  23.8 us
    all_to_all x1, waiting for transfers between devices, body(): inner = lax.all_to_all(sent, ('zl', 'y'), 0, 0, tiled=True)  17.6 us
    all_to_all x1, waiting for transfers between devices, copies(): lax.all_to_all(jnp.broadcast_to(x[None], (count, *x.shape)), axes, 0, 0,...  15.8 us
    all_gather x1, blocking collectives, body(): moments = lax.all_gather(moments, ('x', 'c'))  14.9 us
  transfers between devices with their start and end apart: 13, of which 5 were waited for; matrix products, arithmetic and copies ran while one was open for 1% of the time, Pallas kernels for 4%

profile of v10, /device:TPU:32, one launch (start us, length us, event | category | flops | bytes accessed | tf_op | source)
XLA Modules:
  0.0 218.1 jit_solution(12810015633718074097)
XLA Ops:
  0.0 0.0 copy-start.2
  0.0 0.9 slice_select_fusion
  0.9 4.5 %collective-permute-start = (bf16[16,2048]{1,0:T(8,128)(2,1)S(1)}, bf16[16,2048]{1,0:T(8,128)(2,1)S(1)}, u32[]{:S(2)}, u32[]{:S(2)}) collective-permute-start(bf16[16,2048]{1,0:T(8,128)(2,1)S(1)} %slice_select_fusion), channel_id=1, source_target_pairs={{7,15},{15,23},{23,31},{31,39},{39,47},{47,55},{55,63},{63,71},{71... | collective-permute-start | bytes 196616 | tf_op jit(solution)/shard_map/ppermute | solution.py:512
  5.4 3.0 %shard_map.146.given_far = bf16[4,112,2048]{2,1,0:T(8,128)(2,1)} custom-call(bf16[96,2048]{1,0:T(8,128)(2,1)} %tokens_far.1, f32[1,2048]{1,0:T(1,128)} %bitcast.19), custom_call_target="tpu_custom_call" | custom-call | tf_op jit(solution)/shard_map/pallas_call | solution.py:37
  8.4 1.5 shard_map.145
  9.9 0.0 collective-permute-done.edge
  9.9 0.0 copy-done.2
  9.9 1.0 shard_map.147
  10.9 0.0 copy-start.6
  10.9 3.7 %all-to-all-start = ((bf16[4,112,2048]{2,1,0:T(8,128)(2,1)}), bf16[4,112,2048]{2,1,0:T(8,128)(2,1)S(1)}, u32[]{:S(2)}, u32[]{:S(2)}) async-start(bf16[4,112,2048]{2,1,0:T(8,128)(2,1)} %shard_map.147), calls=%async_computation | async-start | bytes 3670016 | tf_op jit(solution)/shard_map/all_to_all | solution.py:561
  14.6 0.0 copy-done.6
  14.6 41.1 %all_gather.9 = bf16[512,1008]{1,0:T(8,128)(2,1)S(1)} all-gather(bf16[32,1008]{1,0:T(8,128)(2,1)S(1)} %copy-done.6), channel_id=1, replica_groups=mesh['zh'=4,'zl'=4,'y'=4,'x'=4,'c'=2] {'zh','zl'}, dimensions={0}, use_global_device_ids=true | all-gather | bytes 1096704 | tf_op jit(solution)/shard_map/all_gather | solution.py:562
  55.8 0.0 copy-start.5
  55.8 0.0 all-to-all-done
  55.8 1.9 collective-permute-start.1
  57.7 0.0 copy-done.5
  57.7 0.0 copy-start.7
  57.7 0.0 copy-start.4
  57.8 1.1 broadcast_in_dim.33
  58.8 3.5 %all-to-all-start.1 = ((bf16[4,512,256]{2,1,0:T(8,128)(2,1)}), bf16[4,512,256]{2,1,0:T(8,128)(2,1)S(1)}, u32[]{:S(2)}, u32[]{:S(2)}) async-start(bf16[4,512,256]{2,1,0:T(8,128)(2,1)} %broadcast_in_dim.33), calls=%async_computation.1 | async-start | bytes 2097152 | tf_op jit(solution)/shard_map/all_to_all | solution.py:483
  62.3 0.0 copy-done.7
  62.4 0.1 slice.22
  62.4 0.1 copy.19
  62.5 15.8 %all-to-all-done.1 = bf16[4,512,256]{2,1,0:T(8,128)(2,1)S(1)} async-done(((bf16[4,512,256]{2,1,0:T(8,128)(2,1)}), bf16[4,512,256]{2,1,0:T(8,128)(2,1)S(1)}, u32[]{:S(2)}, u32[]{:S(2)}) %all-to-all-start.1) | async-done | bytes 1048608 | tf_op jit(solution)/shard_map/all_to_all | solution.py:483
  78.4 0.0 collective-permute-done.1.other
  78.4 0.0 copy-done.4
  78.4 4.0 %shard_map.148 = (bf16[768,256]{1,0:T(8,128)(2,1)}, bf16[16,160,128]{2,1,0:T(8,128)(2,1)}, f32[8,768]{1,0:T(8,128)}) custom-call(s32[1]{0:T(128)} %bitcast.1.core, bf16[448,2048]{1,0:T(8,128)(2,1)S(1)} %bitcast.14, bf16[448,2048]{1,0:T(8,128)(2,1)} %collective-permute-done.1.other, bf16[2048,256]{1,0:T(8,128)(2,1)S(1)} %bitcast.18, f32[2,768]{1,0:T(2,128)S(1)} %copy-done.4, ...), custom_call_target="tpu_custom_call" | custom-call | tf_op jit(solution)/shard_map/pallas_call | solution.py:37
  82.4 0.0 copy-start.3
  82.4 5.0 %all-to-all-start.2 = ((bf16[16,160,128]{2,1,0:T(8,128)(2,1)}), bf16[16,160,128]{2,1,0:T(8,128)(2,1)S(1)}, u32[]{:S(2)}, u32[]{:S(2)}) async-start(bf16[16,160,128]{2,1,0:T(8,128)(2,1)} %get-tuple-element.25), calls=%async_computation.2 | async-start | bytes 1310720 | tf_op jit(solution)/shard_map/all_to_all | solution.py:584
  87.4 17.6 %all-to-all-done.2.gathered.inner = bf16[16,160,128]{2,1,0:T(8,128)(2,1)S(1)} async-done(((bf16[16,160,128]{2,1,0:T(8,128)(2,1)}), bf16[16,160,128]{2,1,0:T(8,128)(2,1)S(1)}, u32[]{:S(2)}, u32[]{:S(2)}) %all-to-all-start.2) | async-done | bytes 655392 | tf_op jit(solution)/shard_map/all_to_all | solution.py:584
  105.0 0.9 shard_map.149
  105.9 7.5 %all-to-all-start.3 = ((bf16[4,208,128]{2,1,0:T(8,128)(2,1)}), bf16[4,208,128]{2,1,0:T(8,128)(2,1)S(1)}, u32[]{:S(2)}, u32[]{:S(2)}) async-start(bf16[4,208,128]{2,1,0:T(8,128)(2,1)} %shard_map.149), calls=%async_computation.3 | async-start | bytes 425984 | tf_op jit(solution)/shard_map/all_to_all | solution.py:593
  113.3 3.2 %collective-permute-start.7 = (bf16[512,256]{1,0:T(8,128)(2,1)S(1)}, bf16[512,256]{1,0:T(8,128)(2,1)S(1)}, u32[]{:S(2)}, u32[]{:S(2)}) collective-permute-start(bf16[512,256]{1,0:T(8,128)(2,1)S(1)} %get-tuple-element.33.p0), channel_id=1, source_target_pairs={{0,24},{8,0},{16,8},{24,16},{1,25},{9,1},{17,9},{25,17},{2,26},{10... | collective-permute-start | bytes 786440 | tf_op jit(solution)/shard_map/ppermute | solution.py:479
  116.5 1.1 slice.20.p0
  117.6 3.1 %collective-permute-start.4 = (bf16[512,496]{1,0:T(8,128)(2,1)S(1)}, bf16[512,496]{1,0:T(8,128)(2,1)}, u32[]{:S(2)}, u32[]{:S(2)}) collective-permute-start(bf16[512,496]{1,0:T(8,128)(2,1)S(1)} %slice.20.p0), channel_id=1, source_target_pairs={{0,24},{8,0},{16,8},{24,16},{1,25},{9,1},{17,9},{25,17},{2,26},{10... | collective-permute-start | bytes 1523720 | tf_op jit(solution)/shard_map/ppermute | solution.py:479
  120.7 3.5 %collective-permute-start.3 = (bf16[512,496]{1,0:T(8,128)(2,1)S(1)}, bf16[512,496]{1,0:T(8,128)(2,1)}, u32[]{:S(2)}, u32[]{:S(2)}) collective-permute-start(bf16[512,496]{1,0:T(8,128)(2,1)S(1)} %slice.20.p0), channel_id=1, source_target_pairs={{0,16},{8,24},{16,0},{24,8},{1,17},{9,25},{17,1},{25,9},{2,18},{10... | collective-permute-start | bytes 1523720 | tf_op jit(solution)/shard_map/ppermute | solution.py:479
  124.2 1.9 collective-permute-start.2
  126.2 5.3 %collective-permute-start.6 = (bf16[512,256]{1,0:T(8,128)(2,1)S(1)}, bf16[512,256]{1,0:T(8,128)(2,1)}, u32[]{:S(2)}, u32[]{:S(2)}) collective-permute-start(bf16[512,256]{1,0:T(8,128)(2,1)S(1)} %get-tuple-element.33.p0), channel_id=1, source_target_pairs={{0,16},{8,24},{16,0},{24,8},{1,17},{9,25},{17,1},{25,9},{2,18},{10... | collective-permute-start | bytes 786440 | tf_op jit(solution)/shard_map/ppermute | solution.py:479
  131.4 0.0 collective-permute-done.7.p3
  131.4 0.0 copy-start
  131.4 0.7 copy-done
  132.2 2.6 %collective-permute-start.5 = (bf16[512,256]{1,0:T(8,128)(2,1)S(1)}, bf16[512,256]{1,0:T(8,128)(2,1)}, u32[]{:S(2)}, u32[]{:S(2)}) collective-permute-start(bf16[512,256]{1,0:T(8,128)(2,1)S(1)} %get-tuple-element.33.p0), channel_id=1, source_target_pairs={{0,8},{8,16},{16,24},{24,0},{1,9},{9,17},{17,25},{25,1},{2,10},{10... | collective-permute-start | bytes 786440 | tf_op jit(solution)/shard_map/ppermute | solution.py:479
  134.8 21.1 %collective-permute-done.6.p2 = bf16[512,256]{1,0:T(8,128)(2,1)} collective-permute-done((bf16[512,256]{1,0:T(8,128)(2,1)S(1)}, bf16[512,256]{1,0:T(8,128)(2,1)}, u32[]{:S(2)}, u32[]{:S(2)}) %collective-permute-start.6) | collective-permute-done | bytes 262176 | tf_op jit(solution)/shard_map/ppermute | solution.py:479
  155.9 2.9 %collective-permute-done.5.p1 = bf16[512,256]{1,0:T(8,128)(2,1)} collective-permute-done((bf16[512,256]{1,0:T(8,128)(2,1)S(1)}, bf16[512,256]{1,0:T(8,128)(2,1)}, u32[]{:S(2)}, u32[]{:S(2)}) %collective-permute-start.5) | collective-permute-done | bytes 262176 | tf_op jit(solution)/shard_map/ppermute | solution.py:479
  158.7 0.0 copy-done.3
  158.7 0.0 copy-start.1
  158.7 0.9 copy-done.1
  159.7 4.5 %shard_map.150 = (f32[768,128]{1,0:T(8,128)}, f32[2,768]{1,0:T(2,128)}) custom-call(s32[1]{0:T(128)} %bitcast.1.core, s32[1]{0:T(128)} %bitcast.y, bf16[448,2048]{1,0:T(8,128)(2,1)S(1)} %bitcast.15, bf16[448,2048]{1,0:T(8,128)(2,1)} %collective-permute-done.1.other, bf16[512,256]{1,0:T(8,128)(2,1)S(1)} %get-tuple-element.33.p0, ...), custom_call_target="tpu_custom_call" | custom-call | tf_op jit(solution)/shard_map/pallas_call | solution.py:37
  164.2 14.9 %all-gather.1.moments_far = f32[8,2,768]{2,1,0:T(2,128)} all-gather(f32[1,2,768]{2,1,0:T(2,128)} %bitcast.23), channel_id=2, replica_groups=mesh['zh'=4,'zl'=4,'y'=4,'x'=4,'c'=2] {'x','c'}, dimensions={0}, use_global_device_ids=true | all-gather | bytes 55296 | tf_op jit(solution)/shard_map/all_gather | solution.py:607
  179.1 0.0 collective-permute-done.4.p3
  179.1 0.0 collective-permute-done.3.p2
  179.1 0.0 collective-permute-done.2.p1
  179.1 0.0 all-to-all-done.3.outer
  179.1 7.7 %shard_map.151 = (bf16[384,256]{1,0:T(8,128)(2,1)S(1)}, bf16[384,2048]{1,0:T(8,128)(2,1)S(1)}, bf16[4,512,256]{2,1,0:T(8,128)(2,1)S(1)}) custom-call(s32[1]{0:T(128)} %bitcast.1.core, s32[1]{0:T(128)} %bitcast.y, s32[1]{0:T(128)} %bitcast.2.position.low, s32[1]{0:T(128)} %bitcast.3.high, bf16[448,2048]{1,0:T(8,128)(2,1)S(1)} %bitcast.16, ...), custom_call_target="tpu_custom_call" | custom-call | tf_op jit(solution)/shard_map/pallas_call | solution.py:37
  186.8 2.3 %collective-permute-start.8 = (bf16[384,2048]{1,0:T(8,128)(2,1)S(1)}, bf16[384,2048]{1,0:T(8,128)(2,1)S(1)}, u32[]{:S(2)}, u32[]{:S(2)}) collective-permute-start(bf16[384,2048]{1,0:T(8,128)(2,1)S(1)} %get-tuple-element.31), channel_id=1, source_target_pairs={{0,1},{1,0},{2,3},{3,2},{4,5},{5,4},{6,7},{7,6},{8,9},{9,8},{10,11... | collective-permute-start | bytes 4718600 | tf_op jit(solution)/shard_map/ppermute | solution.py:479
  189.0 3.0 %collective-permute-done.8.arrived = bf16[384,2048]{1,0:T(8,128)(2,1)S(1)} collective-permute-done((bf16[384,2048]{1,0:T(8,128)(2,1)S(1)}, bf16[384,2048]{1,0:T(8,128)(2,1)S(1)}, u32[]{:S(2)}, u32[]{:S(2)}) %collective-permute-start.8) | collective-permute-done | bytes 1572896 | tf_op jit(solution)/shard_map/ppermute | solution.py:479
  192.1 0.6 shard_map.152
  192.7 24.1 %all_to_all.25.parts = bf16[4,96,2048]{2,1,0:T(8,128)(2,1)S(1)} all-to-all(bf16[4,96,2048]{2,1,0:T(8,128)(2,1)S(1)} %bitcast.17), channel_id=1, replica_groups=mesh['zh'=4,'zl'=4,'y'=4,'x'=4,'c'=2] {'x'}, dimensions={0} | all-to-all | bytes 3145728 | tf_op jit(solution)/shard_map/all_to_all | solution.py:643
  216.8 1.3 shard_map.153
  (2 shorter events, 0.0 us)
Async XLA Ops:
  0.0 9.9 %copy-start.2 = (f32[2048]{0:T(1024)S(1)}, f32[2048]{0:T(1024)}, u32[]{:S(2)}) copy-start(f32[2048]{0:T(1024)} %param.16) | copy-start | bytes 24580
  0.9 9.0 %collective-permute-start = (bf16[16,2048]{1,0:T(8,128)(2,1)S(1)}, bf16[16,2048]{1,0:T(8,128)(2,1)S(1)}, u32[]{:S(2)}, u32[]{:S(2)}) collective-permute-start(bf16[16,2048]{1,0:T(8,128)(2,1)S(1)} %slice_select_fusion), channel_id=1, source_target_pairs={{7,15},{15,23},{23,31},{31,39},{39,47},{47,55},{55,63},{63,71},{71... | collective-permute-start | bytes 196616 | tf_op jit(solution)/shard_map/ppermute | solution.py:512
  10.9 3.8 %copy-start.6 = (bf16[32,1008]{1,0:T(8,128)(2,1)S(1)}, bf16[32,1008]{1,0:T(8,128)(2,1)}, u32[]{:S(2)}) copy-start(bf16[32,1008]{1,0:T(8,128)(2,1)} %shard_map.145) | copy-start | bytes 193540
  10.9 44.9 %all-to-all-start = ((bf16[4,112,2048]{2,1,0:T(8,128)(2,1)}), bf16[4,112,2048]{2,1,0:T(8,128)(2,1)S(1)}, u32[]{:S(2)}, u32[]{:S(2)}) async-start(bf16[4,112,2048]{2,1,0:T(8,128)(2,1)} %shard_map.147), calls=%async_computation | async-start | bytes 3670016 | tf_op jit(solution)/shard_map/all_to_all | solution.py:561
  55.8 1.9 copy-start.5
  55.8 22.6 %collective-permute-start.1 = (bf16[448,2048]{1,0:T(8,128)(2,1)S(1)}, bf16[448,2048]{1,0:T(8,128)(2,1)}, u32[]{:S(2)}, u32[]{:S(2)}) collective-permute-start(bf16[448,2048]{1,0:T(8,128)(2,1)S(1)} %bitcast.13), channel_id=1, source_target_pairs={{0,1},{1,0},{2,3},{3,2},{4,5},{5,4},{6,7},{7,6},{8,9},{9,8},{10,11... | collective-permute-start | bytes 5505032 | tf_op jit(solution)/shard_map/ppermute | solution.py:479
  57.7 4.6 %copy-start.7 = (bf16[128,32]{0,1:T(8,128)(2,1)S(1)}, bf16[128,32]{0,1:T(8,128)(2,1)}, u32[]{:S(2)}) copy-start(bf16[128,32]{0,1:T(8,128)(2,1)} %param.29) | copy-start | bytes 24580
  57.7 20.6 %copy-start.4 = (f32[2,768]{1,0:T(2,128)S(1)}, f32[2,768]{1,0:T(2,128)}, u32[]{:S(2)}) copy-start(f32[2,768]{1,0:T(2,128)} %decay.1) | copy-start | bytes 18436
  58.8 19.5 %all-to-all-start.1 = ((bf16[4,512,256]{2,1,0:T(8,128)(2,1)}), bf16[4,512,256]{2,1,0:T(8,128)(2,1)S(1)}, u32[]{:S(2)}, u32[]{:S(2)}) async-start(bf16[4,512,256]{2,1,0:T(8,128)(2,1)} %broadcast_in_dim.33), calls=%async_computation.1 | async-start | bytes 2097152 | tf_op jit(solution)/shard_map/all_to_all | solution.py:483
  82.4 76.3 %copy-start.3 = (f32[31,128]{1,0:T(8,128)S(1)}, f32[31,128]{1,0:T(8,128)}, u32[]{:S(2)}) copy-start(f32[31,128]{1,0:T(8,128)} %taps.1) | copy-start | bytes 47620
  82.4 22.6 %all-to-all-start.2 = ((bf16[16,160,128]{2,1,0:T(8,128)(2,1)}), bf16[16,160,128]{2,1,0:T(8,128)(2,1)S(1)}, u32[]{:S(2)}, u32[]{:S(2)}) async-start(bf16[16,160,128]{2,1,0:T(8,128)(2,1)} %get-tuple-element.25), calls=%async_computation.2 | async-start | bytes 1310720 | tf_op jit(solution)/shard_map/all_to_all | solution.py:584
  105.9 73.2 %all-to-all-start.3 = ((bf16[4,208,128]{2,1,0:T(8,128)(2,1)}), bf16[4,208,128]{2,1,0:T(8,128)(2,1)S(1)}, u32[]{:S(2)}, u32[]{:S(2)}) async-start(bf16[4,208,128]{2,1,0:T(8,128)(2,1)} %shard_map.149), calls=%async_computation.3 | async-start | bytes 425984 | tf_op jit(solution)/shard_map/all_to_all | solution.py:593
  113.3 18.1 %collective-permute-start.7 = (bf16[512,256]{1,0:T(8,128)(2,1)S(1)}, bf16[512,256]{1,0:T(8,128)(2,1)S(1)}, u32[]{:S(2)}, u32[]{:S(2)}) collective-permute-start(bf16[512,256]{1,0:T(8,128)(2,1)S(1)} %get-tuple-element.33.p0), channel_id=1, source_target_pairs={{0,24},{8,0},{16,8},{24,16},{1,25},{9,1},{17,9},{25,17},{2,26},{10... | collective-permute-start | bytes 786440 | tf_op jit(solution)/shard_map/ppermute | solution.py:479
  117.6 61.5 %collective-permute-start.4 = (bf16[512,496]{1,0:T(8,128)(2,1)S(1)}, bf16[512,496]{1,0:T(8,128)(2,1)}, u32[]{:S(2)}, u32[]{:S(2)}) collective-permute-start(bf16[512,496]{1,0:T(8,128)(2,1)S(1)} %slice.20.p0), channel_id=1, source_target_pairs={{0,24},{8,0},{16,8},{24,16},{1,25},{9,1},{17,9},{25,17},{2,26},{10... | collective-permute-start | bytes 1523720 | tf_op jit(solution)/shard_map/ppermute | solution.py:479
  120.7 58.4 %collective-permute-start.3 = (bf16[512,496]{1,0:T(8,128)(2,1)S(1)}, bf16[512,496]{1,0:T(8,128)(2,1)}, u32[]{:S(2)}, u32[]{:S(2)}) collective-permute-start(bf16[512,496]{1,0:T(8,128)(2,1)S(1)} %slice.20.p0), channel_id=1, source_target_pairs={{0,16},{8,24},{16,0},{24,8},{1,17},{9,25},{17,1},{25,9},{2,18},{10... | collective-permute-start | bytes 1523720 | tf_op jit(solution)/shard_map/ppermute | solution.py:479
  124.2 54.8 %collective-permute-start.2 = (bf16[512,496]{1,0:T(8,128)(2,1)S(1)}, bf16[512,496]{1,0:T(8,128)(2,1)}, u32[]{:S(2)}, u32[]{:S(2)}) collective-permute-start(bf16[512,496]{1,0:T(8,128)(2,1)S(1)} %slice.20.p0), channel_id=1, source_target_pairs={{0,8},{8,16},{16,24},{24,0},{1,9},{9,17},{17,25},{25,1},{2,10},{10... | collective-permute-start | bytes 1523720 | tf_op jit(solution)/shard_map/ppermute | solution.py:479
  126.2 29.7 %collective-permute-start.6 = (bf16[512,256]{1,0:T(8,128)(2,1)S(1)}, bf16[512,256]{1,0:T(8,128)(2,1)}, u32[]{:S(2)}, u32[]{:S(2)}) collective-permute-start(bf16[512,256]{1,0:T(8,128)(2,1)S(1)} %get-tuple-element.33.p0), channel_id=1, source_target_pairs={{0,16},{8,24},{16,0},{24,8},{1,17},{9,25},{17,1},{25,9},{2,18},{10... | collective-permute-start | bytes 786440 | tf_op jit(solution)/shard_map/ppermute | solution.py:479
  131.4 0.7 copy-start
  132.2 26.6 %collective-permute-start.5 = (bf16[512,256]{1,0:T(8,128)(2,1)S(1)}, bf16[512,256]{1,0:T(8,128)(2,1)}, u32[]{:S(2)}, u32[]{:S(2)}) collective-permute-start(bf16[512,256]{1,0:T(8,128)(2,1)S(1)} %get-tuple-element.33.p0), channel_id=1, source_target_pairs={{0,8},{8,16},{16,24},{24,0},{1,9},{9,17},{17,25},{25,1},{2,10},{10... | collective-permute-start | bytes 786440 | tf_op jit(solution)/shard_map/ppermute | solution.py:479
  158.7 1.0 copy-start.1
  186.8 5.3 %collective-permute-start.8 = (bf16[384,2048]{1,0:T(8,128)(2,1)S(1)}, bf16[384,2048]{1,0:T(8,128)(2,1)S(1)}, u32[]{:S(2)}, u32[]{:S(2)}) collective-permute-start(bf16[384,2048]{1,0:T(8,128)(2,1)S(1)} %get-tuple-element.31), channel_id=1, source_target_pairs={{0,1},{1,0},{2,3},{3,2},{4,5},{5,4},{6,7},{7,6},{8,9},{9,8},{10,11... | collective-permute-start | bytes 4718600 | tf_op jit(solution)/shard_map/ppermute | solution.py:479
